TPU v7x, 512 devices: a 4x2x32 block of a 4x8x32 slice. The times are simulated.
512 devices in a mesh: grp: 2 (over y), fs: 32 (over z), tp: 8 (over x, core).
Axes of the slice: x: 4, y: 2, z: 32, core: 2. Of those that a mesh axis runs over, the one named last changes fastest.
The devices are a block of a 4x8x32 slice.
Arguments:
- tokens: bfloat16 [8192, 2048], P(('grp', 'fs'), 'tp'), parts along dimension 0, may hold values from -340 to 340
- routes: int32 [8192, 2], P(('grp', 'fs')), parts along dimension 0, may hold values from 0 to 7, all different within a row; in each aligned block of 128 rows (0 to 127, 128 to 255, ...) at most 40 rows name the same one
- route_weights: float32 [8192, 2], P(('grp', 'fs')), parts along dimension 0, may hold values from 0.2 to 1
- norm_gain: float32 [2048], P('fs'), may hold values from 0.1 to 1.9
- gate_weight: float32 [8, 2048, 4096], P(None, 'fs', 'tp'), may hold values from -0.125 to 0.125
- up_weight: float32 [8, 2048, 4096], P(None, 'fs', 'tp'), may hold values from -0.125 to 0.125
- down_weight: float32 [8, 2048, 4096], P(None, 'fs', 'tp'), may hold values from -0.09375 to 0.09375
Outputs:
- gate_out: bfloat16 [32, 4096, 1024], P('fs', 'grp', 'tp'), parts along dimension 1
- up_out: bfloat16 [32, 4096, 1024], P('fs', 'grp', 'tp'), parts along dimension 1
- down_out: bfloat16 [32, 4096, 1024], P('fs', 'grp', 'tp'), parts along dimension 1
- mixed_out: bfloat16 [8192, 2048], P(('grp', 'fs'), 'tp'), parts along dimension 0
There are 2 independent parts, one for each index of `grp`. A program takes and returns all parts, laid end to end along the dimension named above; an argument that names none is the same for every part. Nothing has to cross between parts.
Inputs may be any that keep to these rules, and one draw needn't show every extreme that they name: `routes`: each row names 2 different experts; in each aligned block of 128 rows no expert is named by more than 40 rows, and in some block one expert is named by exactly 40 rows.
All inputs are finite; a program needn't handle non-finite values.
Results may differ from a plain program's by a relative error of at most 0.015.
Values may be sent and summed in bfloat16 or wider, within the bound.
No kernel may reach another device: no remote copies, remote signals or barrier semaphores. Data moves between devices by JAX's collectives and lax.ppermute only.
A program may use at most 64 MiB of HBM per device.

v0:
```python
import jax
import jax.numpy as jnp
from jax import lax
from jax.sharding import Mesh
from jax.sharding import PartitionSpec as P

TP = ("tp_0", "tp_1")


epsilon = 1e-06


def side_by_side(arrays, axis, split_dim, concat_dim, along):
    widths = [a.shape[along] for a in arrays]
    both = jnp.concatenate(arrays, axis=along)
    out = lax.all_to_all(both, axis, split_axis=split_dim, concat_axis=concat_dim, tiled=True)
    return tuple(jnp.split(out, [sum(widths[:k]) for k in range(1, len(widths))], axis=along))


def sent_to_all(shard, axis):
    copies = jnp.broadcast_to(shard, (lax.axis_size(axis), *shard.shape))
    return lax.all_to_all(copies, axis, split_axis=0, concat_axis=0, tiled=True)


def over_copies(shard, axis):
    return sent_to_all(shard, axis).sum(axis=0)


def cut_rows(length, count):
    hop = length // count
    if hop >= 8:
        hop -= hop % 8
    return [hop * k for k in range(1, count)]


def gather_in_order(shard, axes, turns):
    pieces = shard
    for k in turns:
        pieces = lax.all_gather(pieces, axes[k])
    done = turns[::-1]
    back = [done.index(k) for k in range(len(axes))]
    pieces = pieces.transpose(*back, *range(len(axes), pieces.ndim))
    return pieces.reshape(-1, *shard.shape)


def laid_out(pieces, dim):
    lengths = list(pieces.shape[1:])
    lengths[dim] *= pieces.shape[0]
    return jnp.moveaxis(pieces, 0, dim).reshape(lengths)


def spread_gather(shard, axes, dim):
    numbers = list(range(len(axes)))[::-1]
    split_at = shard.shape.index(max(shard.shape[:-1] or shard.shape))
    edges = [0, *cut_rows(shard.shape[split_at], len(axes)), shard.shape[split_at]]
    gathered = []
    for k, (start, end) in enumerate(zip(edges, edges[1:])):
        if end > start:
            section = lax.slice_in_dim(shard, start, end, axis=split_at)
            gathered.append(gather_in_order(section, axes, numbers[k:] + numbers[:k]))
    return laid_out(jnp.concatenate(gathered, axis=split_at + 1), dim)


def expert_slots(routes, experts, capacity):
    row_count = routes.shape[0] * routes.shape[1]
    flat_routes = routes.reshape(row_count)
    onehot = (flat_routes[:, None] == jnp.arange(experts, dtype=jnp.int32)[None, :]).astype(
        jnp.int32
    )
    earlier = jnp.cumsum(onehot, axis=0) - onehot
    position = jnp.sum(earlier * onehot, axis=1)
    return (flat_routes * capacity + position).reshape(routes.shape)


def dispatch(normed, slots, experts, capacity, copies, local_count):
    col_width = normed.shape[1]
    slot_ids = jnp.arange(experts * capacity, dtype=jnp.int32)
    select = jnp.any(slot_ids[:, None, None] == slots[None, :, :], axis=2).astype(jnp.bfloat16)
    packed = jnp.dot(select, normed, preferred_element_type=jnp.float32).astype(jnp.bfloat16)
    packed = jnp.broadcast_to(
        packed.reshape(experts, 1, capacity, col_width), (experts, copies, capacity, col_width)
    )
    return packed.reshape(experts * copies // local_count, local_count, capacity, col_width)


def combine(returned, slots, route_weights, experts, copies):
    capacity, col_width = (returned.shape[2], returned.shape[3])
    summed_up = jnp.sum(
        returned.reshape(experts, copies, capacity, col_width), axis=1, dtype=jnp.float32
    )
    selected = summed_up.reshape(experts * capacity, col_width)[slots]
    return jnp.sum(route_weights[:, :, None] * selected, axis=1)


def on_device(tokens, routes, route_weights, norm_gain, gate_weight, up_weight, down_weight):
    fs_count = lax.axis_size("fs")
    tp_count = lax.axis_size(TP)
    experts = gate_weight.shape[0]
    copies = max(1, fs_count // experts)
    local_count = max(1, experts // fs_count)
    capacity = tokens.shape[0] * 5 // 16
    block_width = gate_weight.shape[2] // copies

    def pieces(matrix):
        localized = matrix.reshape(experts, matrix.shape[1], copies, block_width)
        return jnp.transpose(localized, (0, 2, 1, 3)).reshape(
            experts * copies, matrix.shape[1], block_width
        )

    gain_row = norm_gain[None, :, None]
    gate_new, up_new, down_new = side_by_side(
        (
            pieces((gain_row * gate_weight).astype(jnp.bfloat16)),
            pieces((gain_row * up_weight).astype(jnp.bfloat16)),
            pieces(down_weight.astype(jnp.bfloat16)),
        ),
        "fs",
        0,
        1,
        2,
    )
    slots = expert_slots(routes, experts, capacity)
    narrow = tokens.astype(jnp.float32)
    squares = over_copies(jnp.sum(narrow * narrow, axis=1), TP)
    row_scale = lax.rsqrt(squares[:, None] / (narrow.shape[1] * tp_count) + epsilon)
    normed = (narrow * row_scale).astype(jnp.bfloat16)
    outgoing = dispatch(normed, slots, experts, capacity, copies, local_count)
    piece_cols = spread_gather(
        lax.all_to_all(outgoing, "fs", split_axis=0, concat_axis=0, tiled=True), TP, 3
    )
    gate_sums = jnp.einsum(
        "slck,lkf->slcf", piece_cols, gate_new, preferred_element_type=jnp.float32
    )
    up_sums = jnp.einsum("slck,lkf->slcf", piece_cols, up_new, preferred_element_type=jnp.float32)
    hidden = (jax.nn.silu(gate_sums) * up_sums).astype(jnp.bfloat16)
    partial_value = jnp.einsum(
        "slcf,ldf->slcd", hidden, down_new, preferred_element_type=jnp.float32
    ).astype(jnp.bfloat16)
    by_columns = partial_value.reshape(
        partial_value.shape[:3] + (tp_count, partial_value.shape[3] // tp_count)
    )
    exchanged = lax.all_to_all(by_columns, TP, split_axis=3, concat_axis=3, tiled=True)
    summed_up = jnp.sum(exchanged, axis=3, dtype=jnp.float32)
    handed = lax.all_to_all(
        summed_up.astype(jnp.bfloat16), "fs", split_axis=0, concat_axis=0, tiled=True
    ).astype(summed_up.dtype)
    combined = combine(handed, slots, route_weights, experts, copies)
    return (gate_new, up_new, down_new, combined.astype(jnp.bfloat16))


def solution(mesh):
    split = Mesh(
        mesh.devices.reshape(mesh.shape["grp"], mesh.shape["fs"], 4, 2),
        ("grp", "fs", "tp_0", "tp_1"),
    )
    placed = (
        P(("grp", "fs"), TP),
        P(("grp", "fs"), None),
        P(("grp", "fs"), None),
        P("fs"),
        P(None, "fs", TP),
        P(None, "fs", TP),
        P(None, "fs", TP),
    )
    return jax.shard_map(
        on_device,
        mesh=split,
        in_specs=placed,
        out_specs=(
            P("fs", "grp", TP),
            P("fs", "grp", TP),
            P("fs", "grp", TP),
            P(("grp", "fs"), TP),
        ),
        check_vma=False,
    )
```

profile of v0, /device:TPU:33, one launch (start us, length us, event | category | flops | bytes accessed | tf_op | source)
XLA Modules:
  0.0 489.8 jit_solution(7211711055712730180)
XLA Ops:
  8.7 44.7 %all-to-all-start.1 = ((f32[8,1,128]{2,1,0:T(1,128)}), f32[8,1,128]{2,1,0:T(1,128)S(1)}, u32[]{:S(2)}, u32[]{:S(2)}) async-start(f32[8,1,128]{2,1,0:T(1,128)} %broadcast_in_dim.8), calls=%async_computation.1 | async-start | bytes 8192 | tf_op jit(solution)/shard_map/all_to_all | solution.py:22
  56.4 1.6 all-to-all-done.1
  60.0 6.8 %all-to-all-start.2 = ((bf16[32,1,40,256]{3,2,1,0:T(8,128)(2,1)}), bf16[32,1,40,256]{3,2,1,0:T(8,128)(2,1)S(1)}, u32[]{:S(2)}, u32[]{:S(2)}) async-start(bf16[32,1,40,256]{3,2,1,0:T(8,128)(2,1)} %bitcast.12), calls=%async_computation.2 | async-start | bytes 1310720 | tf_op jit(solution)/shard_map/all_to_all | solution.py:129
  66.8 1.3 convert_element_type.46
  68.1 1.9 multiply_convert_fusion.1
  70.5 1.4 pad_maximum_fusion
  71.9 69.8 %all-to-all-done.2 = bf16[32,1,40,256]{3,2,1,0:T(8,128)(2,1)S(1)} async-done(((bf16[32,1,40,256]{3,2,1,0:T(8,128)(2,1)}), bf16[32,1,40,256]{3,2,1,0:T(8,128)(2,1)S(1)}, u32[]{:S(2)}, u32[]{:S(2)}) %all-to-all-start.2) | async-done | bytes 655392 | tf_op jit(solution)/shard_map/all_to_all | solution.py:129
  141.7 5.5 %all-to-all-start = ((bf16[32,64,384]{2,1,0:T(8,128)(2,1)}), bf16[32,64,384]{2,1,0:T(8,128)(2,1)}, u32[]{:S(2)}, u32[]{:S(2)}) async-start(bf16[32,64,384]{2,1,0:T(8,128)(2,1)} %pad_maximum_fusion), calls=%async_computation | async-start | bytes 3145728 | tf_op jit(solution)/shard_map/all_to_all | solution.py:16
  148.2 45.0 %all-gather.10.cloned.1.call-done = bf16[128,1,24,256]{3,2,1,0:T(8,128)(2,1)} async-done(((bf16[32,1,24,256]{3,2,1,0:T(8,128)(2,1)}), bf16[128,1,24,256]{3,2,1,0:T(8,128)(2,1)}) %all-gather.10.cloned.1.call-update) | async-done | bytes 1572880 | tf_op jit(solution)/shard_map/all_gather | solution.py:39
  193.3 3.2 all-gather
  196.5 33.0 %all-gather.12.cloned.1.call-done = bf16[8,32,1,24,256]{4,3,2,1,0:T(8,128)(2,1)} async-done(((bf16[4,32,1,24,256]{4,3,2,1,0:T(8,128)(2,1)}), bf16[8,32,1,24,256]{4,3,2,1,0:T(8,128)(2,1)}) %all-gather.12.cloned.1.call-update) | async-done | bytes 3145744 | tf_op jit(solution)/shard_map/all_gather | solution.py:39
  229.6 2.1 copy.69
  231.7 45.8 %all-gather.8.cloned.1.call-done = bf16[8,32,1,16,256]{4,3,2,1,0:T(8,128)(2,1)} async-done(((bf16[2,32,1,16,256]{4,3,2,1,0:T(8,128)(2,1)}), bf16[8,32,1,16,256]{4,3,2,1,0:T(8,128)(2,1)}) %all-gather.8.cloned.1.call-update) | async-done | bytes 2097168 | tf_op jit(solution)/shard_map/all_gather | solution.py:39
  277.4 1.9 maximum_bitcast_fusion
  279.4 6.6 %copy.71 = bf16[32,1,40,8,256]{4,3,2,0,1:T(8,128)(2,1)} copy(bf16[32,1,40,8,256]{4,2,0,3,1:T(8,128)(2,1)S(1)} %maximum_bitcast_fusion) | data formatting | bytes 10485760 | tf_op jit(solution)/shard_map/transpose | solution.py:49
  286.0 8.9 %reshape.119 = bf16[32,40,2048]{2,1,0:T(8,128)(2,1)} reshape(bf16[32,1,40,8,256]{4,3,2,0,1:T(8,128)(2,1)} %copy.71) | data formatting | bytes 10485760 | tf_op jit(solution)/shard_map/reshape.7
  294.9 1.5 fusion.22
  296.4 4.6 convolution_bitcast_fusion.1
  301.0 10.2 %convolution_convert_fusion = bf16[2048,32,40]{0,2,1:T(8,128)(2,1)} fusion(bf16[32,40,2048]{2,1,0:T(8,128)(2,1)} %reshape.119, f32[32,1,40,128]{3,2,0,1:T(8,128)S(1)} %convolution_bitcast_fusion.1, bf16[1,2048,128]{2,1,0:T(8,128)(2,1)S(1)} %get-tuple-element.7, bf16[1,2048,128]{2,1,0:T(8,128)(2,1)S(1)} %get-tuple-element.6), kind=kOutput, calls=%fused_computation.3 | convolution fusion | flops 1345781760 | bytes 12189696 | tf_op jit(solution)/shard_map/slcf,ldf->slcd/dot_general | solution.py:136
  311.3 2.8 copy.76
  314.1 71.1 %all_to_all.33 = bf16[32,1,40,8,256]{4,2,0,1,3:T(8,128)(2,1)} all-to-all(bf16[32,1,40,8,256]{4,2,0,1,3:T(8,128)(2,1)S(1)} %bitcast.82), channel_id=1, replica_groups=mesh['grp'=2,'fs'=32,'tp_0'=4,'tp_1'=2] {'tp_0','tp_1'}, dimensions={3} | all-to-all | bytes 10485760 | tf_op jit(solution)/shard_map/all_to_all | solution.py:142
  385.2 4.2 reduce_sum.65
  389.4 16.4 %all-to-all-start.4 = ((bf16[32,1,40,256]{3,2,1,0:T(8,128)(2,1)}), bf16[32,1,40,256]{3,2,1,0:T(8,128)(2,1)S(1)}, u32[]{:S(2)}, u32[]{:S(2)}) async-start(bf16[32,1,40,256]{3,2,1,0:T(8,128)(2,1)} %bitcast.32), calls=%async_computation.4 | async-start | bytes 1310720 | tf_op jit(solution)/shard_map/all_to_all | solution.py:144
  406.2 74.8 %all-to-all-done.4 = bf16[32,1,40,256]{3,2,1,0:T(8,128)(2,1)S(1)} async-done(((bf16[32,1,40,256]{3,2,1,0:T(8,128)(2,1)}), bf16[32,1,40,256]{3,2,1,0:T(8,128)(2,1)S(1)}, u32[]{:S(2)}, u32[]{:S(2)}) %all-to-all-start.4) | async-done | bytes 655392 | tf_op jit(solution)/shard_map/all_to_all | solution.py:144
  (49 shorter events, 10.8 us)
Async XLA Ops:
  8.7 49.2 %all-to-all-start.1 = ((f32[8,1,128]{2,1,0:T(1,128)}), f32[8,1,128]{2,1,0:T(1,128)S(1)}, u32[]{:S(2)}, u32[]{:S(2)}) async-start(f32[8,1,128]{2,1,0:T(1,128)} %broadcast_in_dim.8), calls=%async_computation.1 | async-start | bytes 8192 | tf_op jit(solution)/shard_map/all_to_all | solution.py:22
  60.0 81.7 %all-to-all-start.2 = ((bf16[32,1,40,256]{3,2,1,0:T(8,128)(2,1)}), bf16[32,1,40,256]{3,2,1,0:T(8,128)(2,1)S(1)}, u32[]{:S(2)}, u32[]{:S(2)}) async-start(bf16[32,1,40,256]{3,2,1,0:T(8,128)(2,1)} %bitcast.12), calls=%async_computation.2 | async-start | bytes 1310720 | tf_op jit(solution)/shard_map/all_to_all | solution.py:129
  141.7 153.3 %all-to-all-start = ((bf16[32,64,384]{2,1,0:T(8,128)(2,1)}), bf16[32,64,384]{2,1,0:T(8,128)(2,1)}, u32[]{:S(2)}, u32[]{:S(2)}) async-start(bf16[32,64,384]{2,1,0:T(8,128)(2,1)} %pad_maximum_fusion), calls=%async_computation | async-start | bytes 3145728 | tf_op jit(solution)/shard_map/all_to_all | solution.py:16
  147.2 46.0 %all-gather.10.cloned.1.call-start = ((), (), s32[]{:S(2)}) async-start(), calls=%async_computation.6 | async-start | bytes 1966080 | tf_op jit(solution)/shard_map/all_gather | solution.py:39
  148.1 81.5 %all-gather.12.cloned.1.call-start = ((), (), s32[]{:S(2)}) async-start(), calls=%async_computation.7 | async-start | bytes 4718592 | tf_op jit(solution)/shard_map/all_gather | solution.py:39
  193.2 84.2 %all-gather.8.cloned.1.call-start = ((), (), s32[]{:S(2)}) async-start(), calls=%async_computation.5 | async-start | bytes 2621440 | tf_op jit(solution)/shard_map/all_gather | solution.py:39
  296.4 14.8 %copy-start = (bf16[1,2048,128]{2,1,0:T(8,128)(2,1)}, bf16[1,2048,128]{2,1,0:T(8,128)(2,1)S(1)}, u32[]{:S(2)}) copy-start(bf16[1,2048,128]{2,1,0:T(8,128)(2,1)S(1)} %get-tuple-element.6) | copy-start | bytes 1572868
  296.4 14.8 %copy-start.1 = (bf16[1,2048,128]{2,1,0:T(8,128)(2,1)}, bf16[1,2048,128]{2,1,0:T(8,128)(2,1)S(1)}, u32[]{:S(2)}) copy-start(bf16[1,2048,128]{2,1,0:T(8,128)(2,1)S(1)} %get-tuple-element.7) | copy-start | bytes 1572868
  296.4 14.8 %copy-start.2 = (bf16[1,2048,128]{2,1,0:T(8,128)(2,1)}, bf16[1,2048,128]{2,1,0:T(8,128)(2,1)S(1)}, u32[]{:S(2)}) copy-start(bf16[1,2048,128]{2,1,0:T(8,128)(2,1)S(1)} %get-tuple-element.8) | copy-start | bytes 1572868
  385.2 20.9 %copy-start.3 = (f32[128,2]{0,1:T(2,128)S(1)}, f32[128,2]{0,1:T(2,128)}, u32[]{:S(2)}) copy-start(f32[128,2]{0,1:T(2,128)} %param.9) | copy-start | bytes 3076
  389.4 91.6 %all-to-all-start.4 = ((bf16[32,1,40,256]{3,2,1,0:T(8,128)(2,1)}), bf16[32,1,40,256]{3,2,1,0:T(8,128)(2,1)S(1)}, u32[]{:S(2)}, u32[]{:S(2)}) async-start(bf16[32,1,40,256]{3,2,1,0:T(8,128)(2,1)} %bitcast.32), calls=%async_computation.4 | async-start | bytes 1310720 | tf_op jit(solution)/shard_map/all_to_all | solution.py:144
Sparse Core Ops, SparseCore 0:
  150.7 42.3 all-gather.9
  195.3 34.2 all-gather.11
  231.7 45.6 all-gather.7
where the time goes:
time: 491 us; the launch traced here: 490 us
  waiting for transfers between devices  270 us (55%)
  blocking collectives  74.3 us (15%)
  starting transfers between devices  73.5 us (15%)
  local copies, waits for them, and re-layouts  27.6 us (6%)
  matrix products  15.9 us (3%)
  other arithmetic  14.4 us (3%)
  between operations  14 us (3%)
    all_gather x3, waiting for transfers between devices, gather_in_order(): pieces = lax.all_gather(pieces, axes[k])  124 us
    all_to_all x1, waiting for transfers between devices, on_device(): lax.all_to_all(summed_up.astype(jnp.bfloat16), 'fs', split_axis=0, concat...  74.8 us
    all_to_all x1, blocking collectives, on_device(): lax.all_to_all(by_columns, TP, split_axis=3, concat_axis=3, tiled=True)  71.1 us
    all_to_all x1, waiting for transfers between devices, on_device(): lax.all_to_all(outgoing, 'fs', split_axis=0, concat_axis=0, tiled=True)  69.8 us
    all_to_all x1, starting transfers between devices, sent_to_all(): return lax.all_to_all(copies, axis, split_axis=0, concat_axis=0, tiled=True)  44.7 us
    all_to_all x1, starting transfers between devices, on_device(): lax.all_to_all(summed_up.astype(jnp.bfloat16), 'fs', split_axis=0, concat...  16.4 us
    dot_general x1, matrix products, on_device(): jnp.einsum('slcf,ldf->slcd', hidden, down_new, preferred_element_type=jnp...  10.2 us
  transfers between devices with their start and end apart: 7, of which 6 were waited for; matrix products, arithmetic and copies ran while one was open for 6% of the time, Pallas kernels for 0%

commit v1 on v0

v1 whole, which is shorter than its diff:
```python
import functools

import jax
import jax.numpy as jnp
from jax import lax
from jax.experimental import pallas as pl
from jax.experimental.pallas import tpu as pltpu
from jax.sharding import Mesh
from jax.sharding import PartitionSpec as P

FS = ("fs_hi", "fs_lo")
TP = ("tp_x", "tp_c")

epsilon = 1e-06


def shifted(value, axis, step):
    count = lax.axis_size(axis)
    return lax.ppermute(value, axis, [(k, (k + step) % count) for k in range(count)])


def exchange(value, axis):
    return lax.all_to_all(value, axis, split_axis=0, concat_axis=0, tiled=True)


def pack_kernel(turn, gain, gate, up, down, out):
    copies, _, width = out.shape
    width = width // 3
    factor = gain[...]
    for k, (source, scaled) in enumerate(((gate, True), (up, True), (down, False))):
        value = source[0]
        value = (factor * value if scaled else value).astype(jnp.bfloat16)
        for s in range(copies):
            out[s, :, k * width : (k + 1) * width] = value[:, s * width : (s + 1) * width]


def packed_weights(norm_gain, gate_weight, up_weight, down_weight, copies):
    experts, rows, columns = gate_weight.shape
    groups = lax.axis_size("grp")
    part = rows // groups
    width = columns // copies
    turn = lax.axis_index("grp").astype(jnp.int32).reshape(1)
    block = pl.BlockSpec((1, part, columns), lambda e, turn: (e, turn[0], 0))
    return pl.pallas_call(
        pack_kernel,
        out_shape=jax.ShapeDtypeStruct((experts * copies, part, 3 * width), jnp.bfloat16),
        grid_spec=pltpu.PrefetchScalarGridSpec(
            num_scalar_prefetch=1,
            grid=(experts,),
            in_specs=[
                pl.BlockSpec((part, 1), lambda e, turn: (turn[0], 0)),
                block,
                block,
                block,
            ],
            out_specs=pl.BlockSpec((copies, part, 3 * width), lambda e, turn: (e, 0, 0)),
        ),
        name="pack",
    )(turn, norm_gain.reshape(rows, 1), gate_weight, up_weight, down_weight)


def expert_kernel(place, own, other, *refs):
    parts, out = refs[:-1], refs[-1]
    count = len(parts)
    halves, tokens, cols = parts[0].shape[1:]
    width = own.shape[1] // 3
    sums = [jnp.zeros((tokens, 2 * width), jnp.float32) for _ in range(2)]
    for k, part in enumerate(parts):
        block = lax.rem(place[0] + (count - k), count) * halves
        for c in range(halves):
            rows = pl.ds(pl.multiple_of((block + c) * cols, cols), cols)
            left = part[0, c]
            sums = [
                total
                + jnp.dot(left, ref[rows, : 2 * width], preferred_element_type=jnp.float32)
                for total, ref in zip(sums, (own, other))
            ]
    hidden = []
    for total in sums:
        gate, up = total[:, :width], total[:, width:]
        hidden.append((gate / (1.0 + jnp.exp(-gate)) * up).astype(jnp.bfloat16))
    for k in range(count):
        for c in range(halves):
            start = (k * halves + c) * cols
            out[k, 0, c] = sum(
                lax.dot_general(
                    left,
                    ref[start : start + cols, 2 * width :],
                    (((1,), (1,)), ((), ())),
                    preferred_element_type=jnp.float32,
                )
                for left, ref in zip(hidden, (own, other))
            ).astype(jnp.bfloat16)


def expert_outputs(own, other, parts):
    copies, halves, tokens, cols = parts[0].shape
    place = lax.axis_index("tp_x").astype(jnp.int32).reshape(1)
    whole = pl.BlockSpec(own.shape, lambda t, place: (0, 0))
    return pl.pallas_call(
        expert_kernel,
        out_shape=jax.ShapeDtypeStruct((len(parts), *parts[0].shape), jnp.bfloat16),
        grid_spec=pltpu.PrefetchScalarGridSpec(
            num_scalar_prefetch=1,
            grid=(copies,),
            in_specs=[whole, whole]
            + [pl.BlockSpec((1, halves, tokens, cols), lambda t, place: (t, 0, 0, 0))]
            * len(parts),
            out_specs=pl.BlockSpec(
                (len(parts), 1, halves, tokens, cols), lambda t, place: (0, t, 0, 0, 0)
            ),
        ),
        compiler_params=pltpu.CompilerParams(vmem_limit_bytes=48 * 1024 * 1024),
        name="experts",
    )(place, own, other, *parts)


def expert_slots(routes, experts, capacity):
    flat_routes = routes.reshape(-1)
    onehot = (flat_routes[:, None] == jnp.arange(experts, dtype=jnp.int32)[None, :]).astype(
        jnp.int32
    )
    earlier = jnp.cumsum(onehot, axis=0) - onehot
    position = jnp.sum(earlier * onehot, axis=1)
    return (flat_routes * capacity + position).reshape(routes.shape)


def on_device(tokens, routes, route_weights, norm_gain, gate_weight, up_weight, down_weight):
    experts, rows, _ = gate_weight.shape
    copies = lax.axis_size("fs_lo")
    groups = lax.axis_size("grp")
    tp_count = lax.axis_size(TP)
    cores = lax.axis_size("tp_c")
    row_count, col_width = tokens.shape
    capacity = row_count * 5 // 16
    part = rows // groups

    packed = packed_weights(norm_gain, gate_weight, up_weight, down_weight, copies)
    mine = exchange(packed, FS)
    sources, _, triple = mine.shape
    weights = jnp.zeros((sources, groups, part, triple), jnp.bfloat16)
    for k in range(groups):
        piece = mine if k == 0 else shifted(mine, "grp", k)
        weights = lax.dynamic_update_slice_in_dim(
            weights, piece[:, None], lax.rem(lax.axis_index("grp") + groups - k, groups), axis=1
        )
    own = weights.reshape(sources * rows, triple)
    other = shifted(own, "tp_c", 1)

    widened = tokens.astype(jnp.float32)
    squares = lax.all_gather(jnp.sum(widened * widened, axis=1)[None], TP, tiled=True)
    row_scale = lax.rsqrt(
        jnp.sum(squares, axis=0)[:, None] / (col_width * tp_count) + epsilon
    )
    normed = (widened * row_scale).astype(jnp.bfloat16)

    slots = expert_slots(routes, experts, capacity)
    slot_ids = jnp.arange(experts * capacity, dtype=jnp.int32)
    select = jnp.any(slot_ids[:, None, None] == slots[None, :, :], axis=2).astype(jnp.bfloat16)
    outgoing = jnp.dot(select, normed, preferred_element_type=jnp.float32).astype(jnp.bfloat16)
    arrived = exchange(outgoing.reshape(experts, capacity, col_width), "fs_hi")
    share = experts * capacity // cores
    halved = exchange(arrived.reshape(cores, share, col_width), "tp_c")
    block = lax.all_gather(halved, "fs_lo")
    parts = [block] + [shifted(block, "tp_x", k) for k in range(1, lax.axis_size("tp_x"))]

    partial_value = expert_outputs(own, other, parts)
    over_x = jnp.sum(exchange(partial_value, "tp_x"), axis=0, dtype=jnp.float32)
    over_s = jnp.sum(
        exchange(over_x.astype(jnp.bfloat16), "fs_lo"), axis=0, dtype=jnp.float32
    )
    back = exchange(over_s.astype(jnp.bfloat16), "tp_c")
    returned = exchange(back.reshape(experts, capacity, col_width), "fs_hi")
    returned = returned.reshape(experts * capacity, col_width)
    combined = jnp.zeros((row_count, col_width), jnp.float32)
    for k in range(routes.shape[1]):
        chosen = (slots[:, k, None] == slot_ids[None, :]).astype(jnp.bfloat16)
        picked = jnp.dot(chosen, returned, preferred_element_type=jnp.float32)
        combined = combined + route_weights[:, k, None] * picked
    width = triple // 3
    outputs = [own[None, :, k * width : (k + 1) * width] for k in range(3)]
    return (*outputs, combined.astype(jnp.bfloat16))


def solution(mesh):
    split = Mesh(
        mesh.devices.reshape(mesh.shape["grp"], mesh.shape["fs"] // 4, 4, 4, 2),
        ("grp", *FS, *TP),
    )
    rows = P(("grp", *FS), None)
    weight = P(None, FS, TP)
    taken = P(FS, "grp", TP)
    return jax.shard_map(
        on_device,
        mesh=split,
        in_specs=(P(("grp", *FS), TP), rows, rows, P(FS), weight, weight, weight),
        out_specs=(taken, taken, taken, P(("grp", *FS), TP)),
        check_vma=False,
    )
```

time: 491 us -> 339 us (0.69)
  waiting for transfers between devices: 270 us -> 143 us
  blocking collectives: 74.3 us -> 99.6 us
  local copies, waits for them, and re-layouts: 27.6 us -> 3.99 us
  matrix products: 15.9 us -> 2.02 us
  between operations: 14 us -> 0.85 us
  Pallas kernels: 0 us -> 11.8 us
  other arithmetic: 14.4 us -> 3.27 us
    all_gather x3 -> x0, waiting for transfers between devices: 124 us -> none  [gather_in_order(): pieces = lax.all_gather(pieces, axes[k])]
    all_to_all x4 -> x3, waiting for transfers between devices: 146 us -> 107 us  [exchange(): return lax.all_to_all(value, axis, split_axis=0, concat_axis=0, tiled=True)]
    ppermute x0 -> x5, waiting for transfers between devices: none -> 36.2 us  [shifted(): lax.ppermute(value, axis, [(k, (k + step) % count) for k in range(count)])]
    all_gather x1 -> x2, blocking collectives: 3.17 us -> 28.6 us  [the longest x1 16.9 us: on_device(): block = lax.all_gather(halved, 'fs_lo')]
    all_to_all x4 -> x3, starting transfers between devices: 73.3 us -> 53.6 us  [exchange(): return lax.all_to_all(value, axis, split_axis=0, concat_axis=0, tiled=True)]
    ppermute x0 -> x5, starting transfers between devices: none -> 18.5 us  [shifted(): lax.ppermute(value, axis, [(k, (k + step) % count) for k in range(count)])]
    dot_general x3, matrix products: 15.9 us -> 2.02 us  [the longest x2 1.09 us: on_device(): picked = jnp.dot(chosen, returned, preferred_element_type=jnp.float32)]
    pallas_call x0 -> x2, Pallas kernels: none -> 11.8 us  [the longest x1 6.44 us: expert_outputs(): pl.pallas_call(expert_kernel, out_shape=jax.ShapeDtypeStruct((len(parts),...]
  transfers between devices with their start and end apart: 7 -> 8, of which waited for: 6 -> 7; matrix products, arithmetic and copies ran while one was open for 6% -> 1% of each run, Pallas kernels for 0% -> 0%
where the time goes in v1:
time: 339 us; the launch traced here: 337 us
  waiting for transfers between devices  143 us (42%)
  blocking collectives  99.6 us (29%)
  starting transfers between devices  72.1 us (21%)
  Pallas kernels  11.8 us (3%)
  local copies, waits for them, and re-layouts  3.99 us (1%)
    all_to_all x3, waiting for transfers between devices, exchange(): return lax.all_to_all(value, axis, split_axis=0, concat_axis=0, tiled=True)  107 us
    all_to_all x4, blocking collectives, exchange(): return lax.all_to_all(value, axis, split_axis=0, concat_axis=0, tiled=True)  70.9 us
    all_to_all x3, starting transfers between devices, exchange(): return lax.all_to_all(value, axis, split_axis=0, concat_axis=0, tiled=True)  53.6 us
    ppermute x5, waiting for transfers between devices, shifted(): lax.ppermute(value, axis, [(k, (k + step) % count) for k in range(count)])  36.2 us
    ppermute x5, starting transfers between devices, shifted(): lax.ppermute(value, axis, [(k, (k + step) % count) for k in range(count)])  18.5 us
    all_gather x1, blocking collectives, on_device(): block = lax.all_gather(halved, 'fs_lo')  16.9 us
    all_gather x1, blocking collectives, on_device(): lax.all_gather(jnp.sum(widened * widened, axis=1)[None], TP, tiled=True)  11.7 us
  transfers between devices with their start and end apart: 8, of which 7 were waited for; matrix products, arithmetic and copies ran while one was open for 1% of the time, Pallas kernels for 0%

profile of v1, /device:TPU:33, one launch (start us, length us, event | category | flops | bytes accessed | tf_op | source)
XLA Modules:
  0.0 336.6 jit_solution(3989514820260871163)
XLA Ops:
  2.0 5.4 %pack.1 = bf16[32,32,384]{2,1,0:T(8,128)(2,1)} custom-call(s32[1]{0:T(128)} %bitcast.turn, f32[64,1]{1,0:T(8,128)} %copy.44.gain, f32[8,64,512]{2,1,0:T(8,128)} %gate.1, f32[8,64,512]{2,1,0:T(8,128)} %up.1, f32[8,64,512]{2,1,0:T(8,128)} %down.1), custom_call_target="tpu_custom_call" | custom-call | tf_op jit(solution)/shard_map/pack/pallas_call | solution.py:44
  7.4 46.4 %all-to-all-start = ((bf16[32,32,384]{2,1,0:T(8,128)(2,1)}), bf16[32,32,384]{2,1,0:T(8,128)(2,1)S(1)}, u32[]{:S(2)}, u32[]{:S(2)}) async-start(bf16[32,32,384]{2,1,0:T(8,128)(2,1)} %pack.1), calls=%async_computation | async-start | bytes 1572864 | tf_op jit(solution)/shard_map/all_to_all | solution.py:23
  55.5 11.7 %all-gather.2 = f32[8,1,128]{2,1,0:T(1,128)S(1)} all-gather(f32[1,1,128]{2,1,0:T(1,128)S(1)} %bitcast.53), channel_id=2, replica_groups=mesh['grp'=2,'fs_hi'=8,'fs_lo'=4,'tp_x'=4,'tp_c'=2] {'tp_x','tp_c'}, dimensions={0}, use_global_device_ids=true | all-gather | bytes 4608 | tf_op jit(solution)/shard_map/all_gather | solution.py:151
  67.3 72.5 %all-to-all-done = bf16[32,32,384]{2,1,0:T(8,128)(2,1)S(1)} async-done(((bf16[32,32,384]{2,1,0:T(8,128)(2,1)}), bf16[32,32,384]{2,1,0:T(8,128)(2,1)S(1)}, u32[]{:S(2)}, u32[]{:S(2)}) %all-to-all-start) | async-done | bytes 786464 | tf_op jit(solution)/shard_map/all_to_all | solution.py:23
  139.8 3.8 %collective-permute-start = (bf16[32,32,384]{2,1,0:T(8,128)(2,1)S(1)}, bf16[32,32,384]{2,1,0:T(8,128)(2,1)S(1)}, u32[]{:S(2)}, u32[]{:S(2)}) collective-permute-start(bf16[32,32,384]{2,1,0:T(8,128)(2,1)S(1)} %all-to-all-done), channel_id=1, source_target_pairs={{0,256},{256,0},{1,257},{257,1},{2,258},{258,2},{3,259},{259,3},{4... | collective-permute-start | bytes 2359304 | tf_op jit(solution)/shard_map/ppermute | solution.py:19
  144.5 3.6 %all-to-all-start.1 = ((bf16[8,40,256]{2,1,0:T(8,128)(2,1)}), bf16[8,40,256]{2,1,0:T(8,128)(2,1)S(1)}, u32[]{:S(2)}, u32[]{:S(2)}) async-start(bf16[8,40,256]{2,1,0:T(8,128)(2,1)} %bitcast.16), calls=%async_computation.1 | async-start | bytes 327680 | tf_op jit(solution)/shard_map/all_to_all | solution.py:23
  148.5 11.6 %collective-permute-done = bf16[32,32,384]{2,1,0:T(8,128)(2,1)S(1)} collective-permute-done((bf16[32,32,384]{2,1,0:T(8,128)(2,1)S(1)}, bf16[32,32,384]{2,1,0:T(8,128)(2,1)S(1)}, u32[]{:S(2)}, u32[]{:S(2)}) %collective-permute-start) | collective-permute-done | bytes 786464 | tf_op jit(solution)/shard_map/ppermute | solution.py:19
  160.3 3.8 %collective-permute-start.1 = (bf16[2048,384]{1,0:T(8,128)(2,1)S(1)}, bf16[2048,384]{1,0:T(8,128)(2,1)}, u32[]{:S(2)}, u32[]{:S(2)}) collective-permute-start(bf16[2048,384]{1,0:T(8,128)(2,1)S(1)} %bitcast.43), channel_id=1, source_target_pairs={{0,1},{1,0},{2,3},{3,2},{4,5},{5,4},{6,7},{7,6},{8,9},{9,8},{10,11... | collective-permute-start | bytes 4718600 | tf_op jit(solution)/shard_map/ppermute | solution.py:19
  164.1 7.3 %all-to-all-done.1 = bf16[8,40,256]{2,1,0:T(8,128)(2,1)S(1)} async-done(((bf16[8,40,256]{2,1,0:T(8,128)(2,1)}), bf16[8,40,256]{2,1,0:T(8,128)(2,1)S(1)}, u32[]{:S(2)}, u32[]{:S(2)}) %all-to-all-start.1) | async-done | bytes 163872 | tf_op jit(solution)/shard_map/all_to_all | solution.py:23
  171.5 8.9 %all_to_all.35 = bf16[2,160,256]{2,1,0:T(8,128)(2,1)S(1)} all-to-all(bf16[2,160,256]{2,1,0:T(8,128)(2,1)S(1)} %bitcast.52), channel_id=1, replica_groups=mesh['grp'=2,'fs_hi'=8,'fs_lo'=4,'tp_x'=4,'tp_c'=2] {'tp_c'}, dimensions={0} | all-to-all | bytes 327680 | tf_op jit(solution)/shard_map/all_to_all | solution.py:23
  180.4 16.9 %all-gather.1 = bf16[8,160,256]{2,1,0:T(8,128)(2,1)S(1)} all-gather(bf16[2,160,256]{2,1,0:T(8,128)(2,1)S(1)} %all_to_all.35), channel_id=3, replica_groups=mesh['grp'=2,'fs_hi'=8,'fs_lo'=4,'tp_x'=4,'tp_c'=2] {'fs_lo'}, dimensions={0}, use_global_device_ids=true | all-gather | bytes 819200 | tf_op jit(solution)/shard_map/all_gather | solution.py:164
  197.2 3.3 collective-permute-start.2
  200.5 4.7 %collective-permute-start.3 = (bf16[4,2,160,256]{3,2,1,0:T(8,128)(2,1)S(1)}, bf16[4,2,160,256]{3,2,1,0:T(8,128)(2,1)S(1)}, u32[]{:S(2)}, u32[]{:S(2)}) collective-permute-start(bf16[4,2,160,256]{3,2,1,0:T(8,128)(2,1)S(1)} %bitcast.47), channel_id=1, source_target_pairs={{0,4},{2,6},{4,0},{6,2},{1,5},{3,7},{5,1},{7,3},{8,12},{10,14},{12... | collective-permute-start | bytes 1966088 | tf_op jit(solution)/shard_map/ppermute | solution.py:19
  205.2 3.0 collective-permute-start.4
  208.2 5.2 %collective-permute-done.2.refs_1_ = bf16[4,2,160,256]{3,2,1,0:T(8,128)(2,1)S(1)} collective-permute-done((bf16[4,2,160,256]{3,2,1,0:T(8,128)(2,1)S(1)}, bf16[4,2,160,256]{3,2,1,0:T(8,128)(2,1)S(1)}, u32[]{:S(2)}, u32[]{:S(2)}) %collective-permute-start.2) | collective-permute-done | bytes 655392 | tf_op jit(solution)/shard_map/ppermute | solution.py:19
  213.4 15.0 %collective-permute-done.3.refs_2_ = bf16[4,2,160,256]{3,2,1,0:T(8,128)(2,1)S(1)} collective-permute-done((bf16[4,2,160,256]{3,2,1,0:T(8,128)(2,1)S(1)}, bf16[4,2,160,256]{3,2,1,0:T(8,128)(2,1)S(1)}, u32[]{:S(2)}, u32[]{:S(2)}) %collective-permute-start.3) | collective-permute-done | bytes 655392 | tf_op jit(solution)/shard_map/ppermute | solution.py:19
  228.4 4.4 %collective-permute-done.4.refs_3_ = bf16[4,2,160,256]{3,2,1,0:T(8,128)(2,1)} collective-permute-done((bf16[4,2,160,256]{3,2,1,0:T(8,128)(2,1)S(1)}, bf16[4,2,160,256]{3,2,1,0:T(8,128)(2,1)}, u32[]{:S(2)}, u32[]{:S(2)}) %collective-permute-start.4) | collective-permute-done | bytes 655392 | tf_op jit(solution)/shard_map/ppermute | solution.py:19
  232.8 6.4 %experts.1 = bf16[4,4,2,160,256]{4,3,2,1,0:T(8,128)(2,1)} custom-call(s32[1]{0:T(128)} %bitcast.14.place, bf16[2048,384]{1,0:T(8,128)(2,1)S(1)} %bitcast.44, bf16[2048,384]{1,0:T(8,128)(2,1)} %collective-permute-done.1.other, bf16[4,2,160,256]{3,2,1,0:T(8,128)(2,1)S(1)} %bitcast.49, bf16[4,2,160,256]{3,2,1,0:T(8,128)(2,1)S(1)} %collective-permute-done.2.refs_1_, ...), custom_call_target="tpu_custom_call" | custom-call | tf_op jit(solution)/shard_map/experts/pallas_call | solution.py:100
  239.2 36.3 %all_to_all.36 = bf16[4,4,2,160,256]{4,3,2,1,0:T(8,128)(2,1)} all-to-all(bf16[4,4,2,160,256]{4,3,2,1,0:T(8,128)(2,1)} %experts.1), channel_id=1, replica_groups=mesh['grp'=2,'fs_hi'=8,'fs_lo'=4,'tp_x'=4,'tp_c'=2] {'tp_x'}, dimensions={0} | all-to-all | bytes 5242880 | tf_op jit(solution)/shard_map/all_to_all | solution.py:23
  275.5 2.2 reduce_sum.57
  277.8 19.7 %all_to_all.37 = bf16[4,2,160,256]{3,2,1,0:T(8,128)(2,1)S(1)} all-to-all(bf16[4,2,160,256]{3,2,1,0:T(8,128)(2,1)S(1)} %reduce_sum.57), channel_id=1, replica_groups=mesh['grp'=2,'fs_hi'=8,'fs_lo'=4,'tp_x'=4,'tp_c'=2] {'fs_lo'}, dimensions={0} | all-to-all | bytes 1310720 | tf_op jit(solution)/shard_map/all_to_all | solution.py:23
  297.6 6.1 %all_to_all.38 = bf16[2,160,256]{2,1,0:T(8,128)(2,1)} all-to-all(bf16[2,160,256]{2,1,0:T(8,128)(2,1)S(1)} %reduce_sum.58), channel_id=1, replica_groups=mesh['grp'=2,'fs_hi'=8,'fs_lo'=4,'tp_x'=4,'tp_c'=2] {'tp_c'}, dimensions={0} | all-to-all | bytes 327680 | tf_op jit(solution)/shard_map/all_to_all | solution.py:23
  303.6 3.6 %all-to-all-start.6 = ((bf16[8,40,256]{2,1,0:T(8,128)(2,1)}), bf16[8,40,256]{2,1,0:T(8,128)(2,1)S(1)}, u32[]{:S(2)}, u32[]{:S(2)}) async-start(bf16[8,40,256]{2,1,0:T(8,128)(2,1)} %bitcast.19), calls=%async_computation.6 | async-start | bytes 327680 | tf_op jit(solution)/shard_map/all_to_all | solution.py:23
  308.5 27.0 %all-to-all-done.6 = bf16[8,40,256]{2,1,0:T(8,128)(2,1)S(1)} async-done(((bf16[8,40,256]{2,1,0:T(8,128)(2,1)}), bf16[8,40,256]{2,1,0:T(8,128)(2,1)S(1)}, u32[]{:S(2)}, u32[]{:S(2)}) %all-to-all-start.6) | async-done | bytes 163872 | tf_op jit(solution)/shard_map/all_to_all | solution.py:23
  (34 shorter events, 7.1 us)
Async XLA Ops:
  7.4 46.4 %copy-start.1 = (s32[128,2]{0,1:T(2,128)S(1)}, s32[128,2]{0,1:T(2,128)}, u32[]{:S(2)}) copy-start(s32[128,2]{0,1:T(2,128)} %param.8) | copy-start | bytes 3076
  7.4 48.0 %copy-start = (bf16[128,256]{1,0:T(8,128)(2,1)S(1)}, bf16[128,256]{1,0:T(8,128)(2,1)}, u32[]{:S(2)}) copy-start(bf16[128,256]{1,0:T(8,128)(2,1)} %param.7) | copy-start | bytes 196612
  7.4 132.4 %all-to-all-start = ((bf16[32,32,384]{2,1,0:T(8,128)(2,1)}), bf16[32,32,384]{2,1,0:T(8,128)(2,1)S(1)}, u32[]{:S(2)}, u32[]{:S(2)}) async-start(bf16[32,32,384]{2,1,0:T(8,128)(2,1)} %pack.1), calls=%async_computation | async-start | bytes 1572864 | tf_op jit(solution)/shard_map/all_to_all | solution.py:23
  139.8 20.4 %collective-permute-start = (bf16[32,32,384]{2,1,0:T(8,128)(2,1)S(1)}, bf16[32,32,384]{2,1,0:T(8,128)(2,1)S(1)}, u32[]{:S(2)}, u32[]{:S(2)}) collective-permute-start(bf16[32,32,384]{2,1,0:T(8,128)(2,1)S(1)} %all-to-all-done), channel_id=1, source_target_pairs={{0,256},{256,0},{1,257},{257,1},{2,258},{258,2},{3,259},{259,3},{4... | collective-permute-start | bytes 2359304 | tf_op jit(solution)/shard_map/ppermute | solution.py:19
  144.5 26.9 %all-to-all-start.1 = ((bf16[8,40,256]{2,1,0:T(8,128)(2,1)}), bf16[8,40,256]{2,1,0:T(8,128)(2,1)S(1)}, u32[]{:S(2)}, u32[]{:S(2)}) async-start(bf16[8,40,256]{2,1,0:T(8,128)(2,1)} %bitcast.16), calls=%async_computation.1 | async-start | bytes 327680 | tf_op jit(solution)/shard_map/all_to_all | solution.py:23
  160.3 72.5 %collective-permute-start.1 = (bf16[2048,384]{1,0:T(8,128)(2,1)S(1)}, bf16[2048,384]{1,0:T(8,128)(2,1)}, u32[]{:S(2)}, u32[]{:S(2)}) collective-permute-start(bf16[2048,384]{1,0:T(8,128)(2,1)S(1)} %bitcast.43), channel_id=1, source_target_pairs={{0,1},{1,0},{2,3},{3,2},{4,5},{5,4},{6,7},{7,6},{8,9},{9,8},{10,11... | collective-permute-start | bytes 4718600 | tf_op jit(solution)/shard_map/ppermute | solution.py:19
  197.2 16.2 %collective-permute-start.2 = (bf16[4,2,160,256]{3,2,1,0:T(8,128)(2,1)S(1)}, bf16[4,2,160,256]{3,2,1,0:T(8,128)(2,1)S(1)}, u32[]{:S(2)}, u32[]{:S(2)}) collective-permute-start(bf16[4,2,160,256]{3,2,1,0:T(8,128)(2,1)S(1)} %bitcast.46), channel_id=1, source_target_pairs={{0,2},{2,4},{4,6},{6,0},{1,3},{3,5},{5,7},{7,1},{8,10},{10,12},{12... | collective-permute-start | bytes 1966088 | tf_op jit(solution)/shard_map/ppermute | solution.py:19
  200.5 27.9 %collective-permute-start.3 = (bf16[4,2,160,256]{3,2,1,0:T(8,128)(2,1)S(1)}, bf16[4,2,160,256]{3,2,1,0:T(8,128)(2,1)S(1)}, u32[]{:S(2)}, u32[]{:S(2)}) collective-permute-start(bf16[4,2,160,256]{3,2,1,0:T(8,128)(2,1)S(1)} %bitcast.47), channel_id=1, source_target_pairs={{0,4},{2,6},{4,0},{6,2},{1,5},{3,7},{5,1},{7,3},{8,12},{10,14},{12... | collective-permute-start | bytes 1966088 | tf_op jit(solution)/shard_map/ppermute | solution.py:19
  205.2 27.6 %collective-permute-start.4 = (bf16[4,2,160,256]{3,2,1,0:T(8,128)(2,1)S(1)}, bf16[4,2,160,256]{3,2,1,0:T(8,128)(2,1)}, u32[]{:S(2)}, u32[]{:S(2)}) collective-permute-start(bf16[4,2,160,256]{3,2,1,0:T(8,128)(2,1)S(1)} %bitcast.48), channel_id=1, source_target_pairs={{0,6},{2,0},{4,2},{6,4},{1,7},{3,1},{5,3},{7,5},{8,14},{10,8},{12,... | collective-permute-start | bytes 1966088 | tf_op jit(solution)/shard_map/ppermute | solution.py:19
  277.8 29.5 %copy-start.2 = (f32[128,2]{0,1:T(2,128)S(1)}, f32[128,2]{0,1:T(2,128)}, u32[]{:S(2)}) copy-start(f32[128,2]{0,1:T(2,128)} %param.9) | copy-start | bytes 3076
  303.6 31.9 %all-to-all-start.6 = ((bf16[8,40,256]{2,1,0:T(8,128)(2,1)}), bf16[8,40,256]{2,1,0:T(8,128)(2,1)S(1)}, u32[]{:S(2)}, u32[]{:S(2)}) async-start(bf16[8,40,256]{2,1,0:T(8,128)(2,1)} %bitcast.19), calls=%async_computation.6 | async-start | bytes 327680 | tf_op jit(solution)/shard_map/all_to_all | solution.py:23

commit v2 on v1

--- a/solution.py
+++ b/solution.py
@@ -1,5 +1,3 @@
-import functools
-
 import jax
 import jax.numpy as jnp
 from jax import lax
@@ -65,18 +63,25 @@
     halves, tokens, cols = parts[0].shape[1:]
     width = own.shape[1] // 3
     sums = [jnp.zeros((tokens, 2 * width), jnp.float32) for _ in range(2)]
+    squares = jnp.zeros((tokens, cols), jnp.float32)
     for k, part in enumerate(parts):
         block = lax.rem(place[0] + (count - k), count) * halves
         for c in range(halves):
-            rows = pl.ds(pl.multiple_of((block + c) * cols, cols), cols)
+            start = (block + lax.rem(place[1] + (halves - c), halves)) * cols
+            rows = pl.ds(pl.multiple_of(start, cols), cols)
             left = part[0, c]
+            wide = left.astype(jnp.float32)
+            squares = squares + wide * wide
             sums = [
                 total
                 + jnp.dot(left, ref[rows, : 2 * width], preferred_element_type=jnp.float32)
                 for total, ref in zip(sums, (own, other))
             ]
+    features = count * halves * cols
+    row_scale = lax.rsqrt(jnp.sum(squares, axis=1, keepdims=True) / features + epsilon)
     hidden = []
     for total in sums:
+        total = total * row_scale
         gate, up = total[:, :width], total[:, width:]
         hidden.append((gate / (1.0 + jnp.exp(-gate)) * up).astype(jnp.bfloat16))
     for k in range(count):
@@ -95,7 +100,7 @@
 
 def expert_outputs(own, other, parts):
     copies, halves, tokens, cols = parts[0].shape
-    place = lax.axis_index("tp_x").astype(jnp.int32).reshape(1)
+    place = jnp.stack([lax.axis_index("tp_x"), lax.axis_index("tp_c")]).astype(jnp.int32)
     whole = pl.BlockSpec(own.shape, lambda t, place: (0, 0))
     return pl.pallas_call(
         expert_kernel,
@@ -115,69 +120,90 @@
     )(place, own, other, *parts)
 
 
-def expert_slots(routes, experts, capacity):
-    flat_routes = routes.reshape(-1)
-    onehot = (flat_routes[:, None] == jnp.arange(experts, dtype=jnp.int32)[None, :]).astype(
-        jnp.int32
-    )
-    earlier = jnp.cumsum(onehot, axis=0) - onehot
-    position = jnp.sum(earlier * onehot, axis=1)
-    return (flat_routes * capacity + position).reshape(routes.shape)
-
-
-def on_device(tokens, routes, route_weights, norm_gain, gate_weight, up_weight, down_weight):
-    experts, rows, _ = gate_weight.shape
-    copies = lax.axis_size("fs_lo")
+def earlier_rows(named):
+    count = named.shape[-1]
+    before = jnp.arange(count)[:, None] < jnp.arange(count)[None, :]
+    return jnp.dot(
+        named.astype(jnp.bfloat16),
+        before.astype(jnp.bfloat16),
+        preferred_element_type=jnp.float32,
+    ).astype(jnp.int32)
+
+
+def assembled_weights(mine, rows):
+    sources, part, triple = mine.shape
     groups = lax.axis_size("grp")
-    tp_count = lax.axis_size(TP)
-    cores = lax.axis_size("tp_c")
-    row_count, col_width = tokens.shape
-    capacity = row_count * 5 // 16
-    part = rows // groups
-
-    packed = packed_weights(norm_gain, gate_weight, up_weight, down_weight, copies)
-    mine = exchange(packed, FS)
-    sources, _, triple = mine.shape
     weights = jnp.zeros((sources, groups, part, triple), jnp.bfloat16)
     for k in range(groups):
         piece = mine if k == 0 else shifted(mine, "grp", k)
         weights = lax.dynamic_update_slice_in_dim(
             weights, piece[:, None], lax.rem(lax.axis_index("grp") + groups - k, groups), axis=1
         )
-    own = weights.reshape(sources * rows, triple)
+    return weights.reshape(sources * rows, triple)
+
+
+def dispatched(tokens, routes, capacity):
+    row_count, col_width = tokens.shape
+    cores = lax.axis_size("tp_c")
+    table = routes.T.astype(jnp.bfloat16).reshape(-1, col_width)
+    table = jnp.pad(table, ((0, 16 - table.shape[0]), (0, 0)))
+    gathered = lax.all_gather(jnp.concatenate([tokens, table]), "fs_hi")
+    sources = gathered.shape[0]
+    named = gathered[:, row_count:].reshape(sources, -1, row_count)[:, : routes.shape[1]]
+    expert = lax.axis_index("fs_hi").astype(jnp.bfloat16)
+    match = jnp.any(named == expert, axis=1)
+    position = earlier_rows(match)
+    slot = jnp.arange(capacity, dtype=jnp.int32)[None, :, None]
+    select = ((position[:, None, :] == slot) & match[:, None, :]).astype(jnp.bfloat16)
+    packed = jnp.einsum(
+        "jpt,jtc->jpc", select, gathered[:, :row_count], preferred_element_type=jnp.float32
+    ).astype(jnp.bfloat16)
+    packed = packed.reshape(cores, sources * capacity // cores, col_width)
+    core = lax.axis_index("tp_c")
+    halves = []
+    for j in range(cores):
+        half = lax.dynamic_index_in_dim(
+            packed, lax.rem(core + j, cores), axis=0, keepdims=False
+        )
+        halves.append(half if j == 0 else shifted(half, "tp_c", j))
+    block = lax.all_gather(jnp.stack(halves), "fs_lo")
+    return [block] + [
+        shifted(block, "tp_x", k) for k in range(1, lax.axis_size("tp_x"))
+    ]
+
+
+def on_device(tokens, routes, route_weights, norm_gain, gate_weight, up_weight, down_weight):
+    experts, rows, _ = gate_weight.shape
+    copies = lax.axis_size("fs_lo")
+    row_count, col_width = tokens.shape
+    capacity = row_count * 5 // 16
+
+    packed = packed_weights(norm_gain, gate_weight, up_weight, down_weight, copies)
+    mine = exchange(packed, FS)
+    parts = dispatched(tokens, routes, capacity)
+    own = assembled_weights(mine, rows)
     other = shifted(own, "tp_c", 1)
-
-    widened = tokens.astype(jnp.float32)
-    squares = lax.all_gather(jnp.sum(widened * widened, axis=1)[None], TP, tiled=True)
-    row_scale = lax.rsqrt(
-        jnp.sum(squares, axis=0)[:, None] / (col_width * tp_count) + epsilon
-    )
-    normed = (widened * row_scale).astype(jnp.bfloat16)
-
-    slots = expert_slots(routes, experts, capacity)
-    slot_ids = jnp.arange(experts * capacity, dtype=jnp.int32)
-    select = jnp.any(slot_ids[:, None, None] == slots[None, :, :], axis=2).astype(jnp.bfloat16)
-    outgoing = jnp.dot(select, normed, preferred_element_type=jnp.float32).astype(jnp.bfloat16)
-    arrived = exchange(outgoing.reshape(experts, capacity, col_width), "fs_hi")
-    share = experts * capacity // cores
-    halved = exchange(arrived.reshape(cores, share, col_width), "tp_c")
-    block = lax.all_gather(halved, "fs_lo")
-    parts = [block] + [shifted(block, "tp_x", k) for k in range(1, lax.axis_size("tp_x"))]
 
     partial_value = expert_outputs(own, other, parts)
     over_x = jnp.sum(exchange(partial_value, "tp_x"), axis=0, dtype=jnp.float32)
-    over_s = jnp.sum(
-        exchange(over_x.astype(jnp.bfloat16), "fs_lo"), axis=0, dtype=jnp.float32
-    )
-    back = exchange(over_s.astype(jnp.bfloat16), "tp_c")
-    returned = exchange(back.reshape(experts, capacity, col_width), "fs_hi")
-    returned = returned.reshape(experts * capacity, col_width)
+    over_x = over_x.astype(jnp.bfloat16)
+    sent = exchange(over_x.reshape(-1, *over_x.shape[2:]), ("fs_lo", "tp_c"))
+    over_s = jnp.sum(sent.reshape(over_x.shape), axis=0, dtype=jnp.float32)
+    returned = exchange(
+        over_s.astype(jnp.bfloat16).reshape(experts, capacity, col_width), "fs_hi"
+    ).reshape(experts * capacity, col_width)
+
+    expert_ids = jnp.arange(experts, dtype=jnp.int32)
+    onehot = [expert_ids[:, None] == routes[None, :, k] for k in range(routes.shape[1])]
+    position = earlier_rows(sum(hot.astype(jnp.int32) for hot in onehot))
+    slot_ids = jnp.arange(experts * capacity, dtype=jnp.int32)
     combined = jnp.zeros((row_count, col_width), jnp.float32)
-    for k in range(routes.shape[1]):
-        chosen = (slots[:, k, None] == slot_ids[None, :]).astype(jnp.bfloat16)
+    for k, hot in enumerate(onehot):
+        slot = jnp.sum(jnp.where(hot, expert_ids[:, None] * capacity + position, 0), axis=0)
+        chosen = (slot[:, None] == slot_ids[None, :]).astype(jnp.bfloat16)
         picked = jnp.dot(chosen, returned, preferred_element_type=jnp.float32)
         combined = combined + route_weights[:, k, None] * picked
-    width = triple // 3
+    width = own.shape[1] // 3
     outputs = [own[None, :, k * width : (k + 1) * width] for k in range(3)]
     return (*outputs, combined.astype(jnp.bfloat16))
 

time: 339 us -> 356 us (1.050)
  blocking collectives: 99.6 us -> 241 us
  waiting for transfers between devices: 143 us -> 51.1 us
  starting transfers between devices: 72.1 us -> 36.1 us
    all_to_all x4 -> x3, blocking collectives: 70.9 us -> 191 us  [exchange(): return lax.all_to_all(value, axis, split_axis=0, concat_axis=0, tiled=True)]
    all_to_all x3 -> x1, waiting for transfers between devices: 107 us -> 25.3 us  [exchange(): return lax.all_to_all(value, axis, split_axis=0, concat_axis=0, tiled=True)]
    all_to_all x3 -> x1, starting transfers between devices: 53.6 us -> 11.2 us  [exchange(): return lax.all_to_all(value, axis, split_axis=0, concat_axis=0, tiled=True)]
    all_gather x2, blocking collectives: 28.6 us -> 50.3 us  [the longest x1 35.9 us: dispatched(): gathered = lax.all_gather(jnp.concatenate([tokens, table]), 'fs_hi')]
    ppermute x5 -> x6, waiting for transfers between devices: 36.2 us -> 25.8 us  [shifted(): lax.ppermute(value, axis, [(k, (k + step) % count) for k in range(count)])]
    ppermute x5 -> x6, starting transfers between devices: 18.5 us -> 25 us  [shifted(): lax.ppermute(value, axis, [(k, (k + step) % count) for k in range(count)])]
  transfers between devices with their start and end apart: 8 -> 7, of which waited for: 7 -> 5; matrix products, arithmetic and copies ran while one was open for 1% -> 1% of each run, Pallas kernels for 0% -> 0%
where the time goes in v2:
time: 356 us; the launch traced here: 351 us
  blocking collectives  241 us (68%)
  waiting for transfers between devices  51.1 us (14%)
  starting transfers between devices  36.1 us (10%)
  Pallas kernels  12.4 us (3%)
  local copies, waits for them, and re-layouts  4.41 us (1%)
    all_to_all x3, blocking collectives, exchange(): return lax.all_to_all(value, axis, split_axis=0, concat_axis=0, tiled=True)  191 us
    all_gather x1, blocking collectives, dispatched(): gathered = lax.all_gather(jnp.concatenate([tokens, table]), 'fs_hi')  35.9 us
    ppermute x6, waiting for transfers between devices, shifted(): lax.ppermute(value, axis, [(k, (k + step) % count) for k in range(count)])  25.8 us
    all_to_all x1, waiting for transfers between devices, exchange(): return lax.all_to_all(value, axis, split_axis=0, concat_axis=0, tiled=True)  25.3 us
    ppermute x6, starting transfers between devices, shifted(): lax.ppermute(value, axis, [(k, (k + step) % count) for k in range(count)])  25 us
    all_gather x1, blocking collectives, dispatched(): block = lax.all_gather(jnp.stack(halves), 'fs_lo')  14.4 us
    all_to_all x1, starting transfers between devices, exchange(): return lax.all_to_all(value, axis, split_axis=0, concat_axis=0, tiled=True)  11.2 us
  transfers between devices with their start and end apart: 7, of which 5 were waited for; matrix products, arithmetic and copies ran while one was open for 1% of the time, Pallas kernels for 0%

profile of v2, /device:TPU:33, one launch (start us, length us, event | category | flops | bytes accessed | tf_op | source)
XLA Modules:
  0.0 351.0 jit_solution(7451290088789808411)
XLA Ops:
  0.6 1.4 copy.17.gain
  2.0 5.4 %pack.1 = bf16[32,32,384]{2,1,0:T(8,128)(2,1)} custom-call(s32[1]{0:T(128)} %bitcast.turn, f32[64,1]{1,0:T(8,128)} %copy.17.gain, f32[8,64,512]{2,1,0:T(8,128)} %gate.1, f32[8,64,512]{2,1,0:T(8,128)} %up.1, f32[8,64,512]{2,1,0:T(8,128)} %down.1), custom_call_target="tpu_custom_call" | custom-call | tf_op jit(solution)/shard_map/pack/pallas_call | solution.py:42
  7.4 132.4 %all_to_all.20 = bf16[32,32,384]{2,1,0:T(8,128)(2,1)S(1)} all-to-all(bf16[32,32,384]{2,1,0:T(8,128)(2,1)} %pack.1), channel_id=1, replica_groups=mesh['grp'=2,'fs_hi'=8,'fs_lo'=4,'tp_x'=4,'tp_c'=2] {'fs_hi','fs_lo'}, dimensions={0} | all-to-all | bytes 1572864 | tf_op jit(solution)/shard_map/all_to_all | solution.py:21
  139.7 3.8 %collective-permute-start = (bf16[32,32,384]{2,1,0:T(8,128)(2,1)S(1)}, bf16[32,32,384]{2,1,0:T(8,128)(2,1)}, u32[]{:S(2)}, u32[]{:S(2)}) collective-permute-start(bf16[32,32,384]{2,1,0:T(8,128)(2,1)S(1)} %all_to_all.20), channel_id=1, source_target_pairs={{0,256},{256,0},{1,257},{257,1},{2,258},{258,2},{3,259},{259,3},{4... | collective-permute-start | bytes 2359304 | tf_op jit(solution)/shard_map/ppermute | solution.py:17
  143.6 35.9 %all-gather = bf16[1152,256]{1,0:T(8,128)(2,1)S(1)} all-gather(bf16[144,256]{1,0:T(8,128)(2,1)S(1)} %fusion.11), channel_id=2, replica_groups=mesh['grp'=2,'fs_hi'=8,'fs_lo'=4,'tp_x'=4,'tp_c'=2] {'fs_hi'}, dimensions={0}, use_global_device_ids=true | all-gather | bytes 663552 | tf_op jit(solution)/shard_map/all_gather | solution.py:150
  180.0 1.3 bitcast_dynamic-update-slice_fusion
  181.3 8.3 %collective-permute-start.1 = (bf16[2048,384]{1,0:T(8,128)(2,1)S(1)}, bf16[2048,384]{1,0:T(8,128)(2,1)}, u32[]{:S(2)}, u32[]{:S(2)}) collective-permute-start(bf16[2048,384]{1,0:T(8,128)(2,1)S(1)} %bitcast.47), channel_id=1, source_target_pairs={{0,1},{1,0},{2,3},{3,2},{4,5},{5,4},{6,7},{7,6},{8,9},{9,8},{10,11... | collective-permute-start | bytes 4718600 | tf_op jit(solution)/shard_map/ppermute | solution.py:17
  190.0 2.0 collective-permute-start.2
  192.0 1.2 collective-permute-done.2
  193.3 14.4 %all-gather.1 = bf16[8,160,256]{2,1,0:T(8,128)(2,1)S(1)} all-gather(bf16[2,160,256]{2,1,0:T(8,128)(2,1)S(1)} %pad_maximum_fusion), channel_id=3, replica_groups=mesh['grp'=2,'fs_hi'=8,'fs_lo'=4,'tp_x'=4,'tp_c'=2] {'fs_lo'}, dimensions={0}, use_global_device_ids=true | all-gather | bytes 819200 | tf_op jit(solution)/shard_map/all_gather | solution.py:169
  207.6 3.3 collective-permute-start.3
  210.9 4.7 %collective-permute-start.4 = (bf16[4,2,160,256]{3,2,1,0:T(8,128)(2,1)S(1)}, bf16[4,2,160,256]{3,2,1,0:T(8,128)(2,1)S(1)}, u32[]{:S(2)}, u32[]{:S(2)}) collective-permute-start(bf16[4,2,160,256]{3,2,1,0:T(8,128)(2,1)S(1)} %bitcast.51), channel_id=1, source_target_pairs={{0,4},{2,6},{4,0},{6,2},{1,5},{3,7},{5,1},{7,3},{8,12},{10,14},{12... | collective-permute-start | bytes 1966088 | tf_op jit(solution)/shard_map/ppermute | solution.py:17
  215.6 3.0 collective-permute-start.5
  218.6 6.0 %collective-permute-done.3.refs_1_ = bf16[4,2,160,256]{3,2,1,0:T(8,128)(2,1)S(1)} collective-permute-done((bf16[4,2,160,256]{3,2,1,0:T(8,128)(2,1)S(1)}, bf16[4,2,160,256]{3,2,1,0:T(8,128)(2,1)S(1)}, u32[]{:S(2)}, u32[]{:S(2)}) %collective-permute-start.3) | collective-permute-done | bytes 655392 | tf_op jit(solution)/shard_map/ppermute | solution.py:17
  224.7 15.0 %collective-permute-done.4.refs_2_ = bf16[4,2,160,256]{3,2,1,0:T(8,128)(2,1)S(1)} collective-permute-done((bf16[4,2,160,256]{3,2,1,0:T(8,128)(2,1)S(1)}, bf16[4,2,160,256]{3,2,1,0:T(8,128)(2,1)S(1)}, u32[]{:S(2)}, u32[]{:S(2)}) %collective-permute-start.4) | collective-permute-done | bytes 655392 | tf_op jit(solution)/shard_map/ppermute | solution.py:17
  239.6 3.6 %collective-permute-done.5.refs_3_ = bf16[4,2,160,256]{3,2,1,0:T(8,128)(2,1)} collective-permute-done((bf16[4,2,160,256]{3,2,1,0:T(8,128)(2,1)S(1)}, bf16[4,2,160,256]{3,2,1,0:T(8,128)(2,1)}, u32[]{:S(2)}, u32[]{:S(2)}) %collective-permute-start.5) | collective-permute-done | bytes 655392 | tf_op jit(solution)/shard_map/ppermute | solution.py:17
  243.2 7.1 %experts.1 = bf16[4,4,2,160,256]{4,3,2,1,0:T(8,128)(2,1)} custom-call(s32[2]{0:T(128)S(1)} %pad_add_fusion.place, bf16[2048,384]{1,0:T(8,128)(2,1)S(1)} %bitcast.48, bf16[2048,384]{1,0:T(8,128)(2,1)} %collective-permute-done.1.other, bf16[4,2,160,256]{3,2,1,0:T(8,128)(2,1)S(1)} %bitcast.53, bf16[4,2,160,256]{3,2,1,0:T(8,128)(2,1)S(1)} %collective-permute-done.3.refs_1_, ...), custom_call_target="tpu_custom_call" | custom-call | tf_op jit(solution)/shard_map/experts/pallas_call | solution.py:105
  250.3 36.3 %all_to_all.21 = bf16[4,4,2,160,256]{4,3,2,1,0:T(8,128)(2,1)} all-to-all(bf16[4,4,2,160,256]{4,3,2,1,0:T(8,128)(2,1)} %experts.1), channel_id=1, replica_groups=mesh['grp'=2,'fs_hi'=8,'fs_lo'=4,'tp_x'=4,'tp_c'=2] {'tp_x'}, dimensions={0} | all-to-all | bytes 5242880 | tf_op jit(solution)/shard_map/all_to_all | solution.py:21
  286.6 2.2 reduce_sum.43
  288.8 22.5 %all_to_all.22 = bf16[8,160,256]{2,1,0:T(8,128)(2,1)S(1)} all-to-all(bf16[8,160,256]{2,1,0:T(8,128)(2,1)S(1)} %bitcast.55), channel_id=1, replica_groups=mesh['grp'=2,'fs_hi'=8,'fs_lo'=4,'tp_x'=4,'tp_c'=2] {'fs_lo','tp_c'}, dimensions={0} | all-to-all | bytes 1310720 | tf_op jit(solution)/shard_map/all_to_all | solution.py:21
  312.0 11.2 %all-to-all-start.3 = ((bf16[8,40,256]{2,1,0:T(8,128)(2,1)}), bf16[8,40,256]{2,1,0:T(8,128)(2,1)S(1)}, u32[]{:S(2)}, u32[]{:S(2)}) async-start(bf16[8,40,256]{2,1,0:T(8,128)(2,1)} %bitcast.23), calls=%async_computation.3 | async-start | bytes 327680 | tf_op jit(solution)/shard_map/all_to_all | solution.py:21
  323.4 1.2 slice_bitcast_fusion
  324.6 25.3 %all-to-all-done.3 = bf16[8,40,256]{2,1,0:T(8,128)(2,1)S(1)} async-done(((bf16[8,40,256]{2,1,0:T(8,128)(2,1)}), bf16[8,40,256]{2,1,0:T(8,128)(2,1)S(1)}, u32[]{:S(2)}, u32[]{:S(2)}) %all-to-all-start.3) | async-done | bytes 163872 | tf_op jit(solution)/shard_map/all_to_all | solution.py:21
  350.2 0.9 fusion.1
  (27 shorter events, 2.1 us)
Async XLA Ops:
  7.4 136.2 %copy-start.1 = (s32[128,2]{0,1:T(2,128)S(1)}, s32[128,2]{0,1:T(2,128)}, u32[]{:S(2)}) copy-start(s32[128,2]{0,1:T(2,128)} %param.8) | copy-start | bytes 3076
  7.4 136.2 %copy-start = (bf16[128,256]{1,0:T(8,128)(2,1)S(1)}, bf16[128,256]{1,0:T(8,128)(2,1)}, u32[]{:S(2)}) copy-start(bf16[128,256]{1,0:T(8,128)(2,1)} %param.7) | copy-start | bytes 196612
  139.7 40.3 %collective-permute-start = (bf16[32,32,384]{2,1,0:T(8,128)(2,1)S(1)}, bf16[32,32,384]{2,1,0:T(8,128)(2,1)}, u32[]{:S(2)}, u32[]{:S(2)}) collective-permute-start(bf16[32,32,384]{2,1,0:T(8,128)(2,1)S(1)} %all_to_all.20), channel_id=1, source_target_pairs={{0,256},{256,0},{1,257},{257,1},{2,258},{258,2},{3,259},{259,3},{4... | collective-permute-start | bytes 2359304 | tf_op jit(solution)/shard_map/ppermute | solution.py:17
  181.3 61.9 %collective-permute-start.1 = (bf16[2048,384]{1,0:T(8,128)(2,1)S(1)}, bf16[2048,384]{1,0:T(8,128)(2,1)}, u32[]{:S(2)}, u32[]{:S(2)}) collective-permute-start(bf16[2048,384]{1,0:T(8,128)(2,1)S(1)} %bitcast.47), channel_id=1, source_target_pairs={{0,1},{1,0},{2,3},{3,2},{4,5},{5,4},{6,7},{7,6},{8,9},{9,8},{10,11... | collective-permute-start | bytes 4718600 | tf_op jit(solution)/shard_map/ppermute | solution.py:17
  190.0 3.2 collective-permute-start.2
  207.6 17.0 %collective-permute-start.3 = (bf16[4,2,160,256]{3,2,1,0:T(8,128)(2,1)S(1)}, bf16[4,2,160,256]{3,2,1,0:T(8,128)(2,1)S(1)}, u32[]{:S(2)}, u32[]{:S(2)}) collective-permute-start(bf16[4,2,160,256]{3,2,1,0:T(8,128)(2,1)S(1)} %bitcast.50), channel_id=1, source_target_pairs={{0,2},{2,4},{4,6},{6,0},{1,3},{3,5},{5,7},{7,1},{8,10},{10,12},{12... | collective-permute-start | bytes 1966088 | tf_op jit(solution)/shard_map/ppermute | solution.py:17
  210.9 28.7 %collective-permute-start.4 = (bf16[4,2,160,256]{3,2,1,0:T(8,128)(2,1)S(1)}, bf16[4,2,160,256]{3,2,1,0:T(8,128)(2,1)S(1)}, u32[]{:S(2)}, u32[]{:S(2)}) collective-permute-start(bf16[4,2,160,256]{3,2,1,0:T(8,128)(2,1)S(1)} %bitcast.51), channel_id=1, source_target_pairs={{0,4},{2,6},{4,0},{6,2},{1,5},{3,7},{5,1},{7,3},{8,12},{10,14},{12... | collective-permute-start | bytes 1966088 | tf_op jit(solution)/shard_map/ppermute | solution.py:17
  215.6 27.6 %collective-permute-start.5 = (bf16[4,2,160,256]{3,2,1,0:T(8,128)(2,1)S(1)}, bf16[4,2,160,256]{3,2,1,0:T(8,128)(2,1)}, u32[]{:S(2)}, u32[]{:S(2)}) collective-permute-start(bf16[4,2,160,256]{3,2,1,0:T(8,128)(2,1)S(1)} %bitcast.52), channel_id=1, source_target_pairs={{0,6},{2,0},{4,2},{6,4},{1,7},{3,1},{5,3},{7,5},{8,14},{10,8},{12,... | collective-permute-start | bytes 1966088 | tf_op jit(solution)/shard_map/ppermute | solution.py:17
  288.8 34.6 %copy-start.2 = (f32[128,2]{0,1:T(2,128)S(1)}, f32[128,2]{0,1:T(2,128)}, u32[]{:S(2)}) copy-start(f32[128,2]{0,1:T(2,128)} %param.9) | copy-start | bytes 3076
  312.0 37.9 %all-to-all-start.3 = ((bf16[8,40,256]{2,1,0:T(8,128)(2,1)}), bf16[8,40,256]{2,1,0:T(8,128)(2,1)S(1)}, u32[]{:S(2)}, u32[]{:S(2)}) async-start(bf16[8,40,256]{2,1,0:T(8,128)(2,1)} %bitcast.23), calls=%async_computation.3 | async-start | bytes 327680 | tf_op jit(solution)/shard_map/all_to_all | solution.py:21

commit v3 on v2

v3 whole, which is shorter than its diff:
```python
import functools

import jax
import jax.numpy as jnp
from jax import lax
from jax.experimental import pallas as pl
from jax.experimental.pallas import tpu as pltpu
from jax.sharding import Mesh
from jax.sharding import PartitionSpec as P

FS = ("fs_hi", "fs_lo")
TP = ("tp_x", "tp_c")

epsilon = 1e-06
chunks = 2


def shifted(value, axis, step):
    count = lax.axis_size(axis)
    return lax.ppermute(value, axis, [(k, (k + step) % count) for k in range(count)])


def exchange(value, axis):
    return lax.all_to_all(value, axis, split_axis=0, concat_axis=0, tiled=True)


def position_of(*axes):
    return jnp.stack([lax.axis_index(axis) for axis in axes]).astype(jnp.int32)


def pack_kernel(turn, gain, gate, up, down, out):
    copies, part, width = out.shape
    width = width // 3
    rows = gain.shape[1]
    row = lax.broadcasted_iota(jnp.int32, (part, rows), 0) + turn[0] * part
    column = lax.broadcasted_iota(jnp.int32, (part, rows), 1)
    factor = jnp.sum(jnp.where(row == column, gain[...], 0.0), axis=1, keepdims=True)
    for k, (source, scaled) in enumerate(((gate, True), (up, True), (down, False))):
        value = source[0]
        value = (factor * value if scaled else value).astype(jnp.bfloat16)
        for s in range(copies):
            out[s, :, k * width : (k + 1) * width] = value[:, s * width : (s + 1) * width]


def packed_weights(norm_gain, gate_weight, up_weight, down_weight, copies):
    experts, rows, columns = gate_weight.shape
    part = rows // lax.axis_size("grp")
    width = columns // copies
    block = pl.BlockSpec((1, part, columns), lambda e, turn: (e, turn[0], 0))
    return pl.pallas_call(
        pack_kernel,
        out_shape=jax.ShapeDtypeStruct((experts * copies, part, 3 * width), jnp.bfloat16),
        grid_spec=pltpu.PrefetchScalarGridSpec(
            num_scalar_prefetch=1,
            grid=(experts,),
            in_specs=[pl.BlockSpec((1, rows), lambda e, turn: (0, 0)), block, block, block],
            out_specs=pl.BlockSpec((copies, part, 3 * width), lambda e, turn: (e, 0, 0)),
        ),
        name="pack",
    )(position_of("grp"), norm_gain.reshape(1, rows), gate_weight, up_weight, down_weight)


def before_matrix(count):
    row = lax.broadcasted_iota(jnp.int32, (count, count), 0)
    column = lax.broadcasted_iota(jnp.int32, (count, count), 1)
    return jnp.where(row < column, 1.0, 0.0).astype(jnp.bfloat16)


def dispatch_kernel(routes, tokens, out):
    experts, capacity, _ = out.shape
    top, count = routes.shape
    expert = lax.broadcasted_iota(jnp.int32, (experts, count), 0)
    named = routes[0:1, :] == expert
    for k in range(1, top):
        named = named | (routes[k : k + 1, :] == expert)
    position = jnp.dot(
        jnp.where(named, 1.0, 0.0).astype(jnp.bfloat16),
        before_matrix(count),
        preferred_element_type=jnp.float32,
    )
    position = jnp.where(named, position.astype(jnp.int32), capacity)
    slot = lax.broadcasted_iota(jnp.int32, (capacity, count), 0)
    for e in range(experts):
        select = jnp.where(position[e : e + 1, :] == slot, 1.0, 0.0).astype(jnp.bfloat16)
        out[e] = jnp.dot(
            select, tokens[...], preferred_element_type=jnp.float32
        ).astype(jnp.bfloat16)


def dispatched(tokens, routes, experts, capacity):
    return pl.pallas_call(
        dispatch_kernel,
        out_shape=jax.ShapeDtypeStruct((experts, capacity, tokens.shape[1]), jnp.bfloat16),
        name="dispatch",
    )(routes.T, tokens)


def expert_kernel(place, own, other, *refs):
    count = len(refs) // 2
    parts, outs = refs[:count], refs[count:]
    copies, halves, tokens, cols = parts[0].shape
    width = own.shape[1] // 3
    rows = copies * tokens
    sums = [jnp.zeros((rows, 2 * width), jnp.float32) for _ in range(2)]
    squares = jnp.zeros((rows, cols), jnp.float32)

    def block(k, c):
        start = lax.rem(place[0] + k, count) * halves + c
        return pl.ds(pl.multiple_of(start * cols, cols), cols)

    for k, part in enumerate(parts):
        for c in range(halves):
            core = lax.rem(place[1] + (halves - c), halves)
            left = part[:, c].reshape(rows, cols)
            wide = left.astype(jnp.float32)
            squares = squares + wide * wide
            where = block(count - k, core)
            sums = [
                total
                + jnp.dot(left, ref[where, : 2 * width], preferred_element_type=jnp.float32)
                for total, ref in zip(sums, (own, other))
            ]
    features = count * halves * cols
    row_scale = lax.rsqrt(jnp.sum(squares, axis=1, keepdims=True) / features + epsilon)
    hidden = []
    for total in sums:
        total = total * row_scale
        gate, up = total[:, :width], total[:, width:]
        hidden.append((gate / (1.0 + jnp.exp(-gate)) * up).astype(jnp.bfloat16))
    hidden = jnp.concatenate(hidden, axis=1)
    for k, out in enumerate(outs):
        for c in range(halves):
            where = block(k, c)
            down = jnp.concatenate([ref[where, 2 * width :] for ref in (own, other)], axis=1)
            value = lax.dot_general(
                hidden, down, (((1,), (1,)), ((), ())), preferred_element_type=jnp.float32
            ).astype(jnp.bfloat16)
            for r in range(copies):
                target = lax.rem(place[2] + (copies - r), copies)
                out[pl.ds(target, 1), c] = value[r * tokens : (r + 1) * tokens][None]


def expert_outputs(own, other, parts, chunk):
    copies, halves, tokens, cols = parts[0].shape
    share = tokens // chunks
    whole = pl.BlockSpec(own.shape, lambda t, place: (0, 0))
    piece = (copies, halves, share, cols)
    return pl.pallas_call(
        expert_kernel,
        out_shape=[jax.ShapeDtypeStruct(piece, jnp.bfloat16)] * len(parts),
        grid_spec=pltpu.PrefetchScalarGridSpec(
            num_scalar_prefetch=1,
            grid=(1,),
            in_specs=[whole, whole]
            + [pl.BlockSpec(piece, lambda t, place: (0, 0, chunk, 0))] * len(parts),
            out_specs=[pl.BlockSpec(piece, lambda t, place: (0, 0, 0, 0))] * len(parts),
        ),
        compiler_params=pltpu.CompilerParams(vmem_limit_bytes=48 * 1024 * 1024),
        name="experts",
    )(position_of("tp_x", "tp_c", "fs_lo"), own, other, *parts)


def combine_kernel(routes, route_weights, returned, out):
    experts, capacity, cols = returned.shape
    top, count = routes.shape
    expert = lax.broadcasted_iota(jnp.int32, (experts, count), 0)
    named = [routes[k : k + 1, :] == expert for k in range(top)]
    either = functools.reduce(jnp.logical_or, named)
    position = jnp.dot(
        jnp.where(either, 1.0, 0.0).astype(jnp.bfloat16),
        before_matrix(count),
        preferred_element_type=jnp.float32,
    ).astype(jnp.int32)
    values = returned[...].reshape(experts * capacity, cols)
    slot = lax.broadcasted_iota(jnp.int32, (experts * capacity, count), 0)
    total = jnp.zeros((count, cols), jnp.float32)
    for k in range(top):
        mine = jnp.sum(
            jnp.where(named[k], expert * capacity + position, 0), axis=0, keepdims=True
        )
        chosen = jnp.where(mine == slot, 1.0, 0.0).astype(jnp.bfloat16)
        picked = lax.dot_general(
            chosen, values, (((0,), (0,)), ((), ())), preferred_element_type=jnp.float32
        )
        total = total + route_weights[:, k : k + 1] * picked
    out[...] = total.astype(jnp.bfloat16)


def combined(routes, route_weights, returned):
    return pl.pallas_call(
        combine_kernel,
        out_shape=jax.ShapeDtypeStruct((routes.shape[0], returned.shape[2]), jnp.bfloat16),
        name="combine",
    )(routes.T, route_weights, returned)


def assembled_weights(mine, rows):
    sources, part, triple = mine.shape
    groups = lax.axis_size("grp")
    weights = jnp.zeros((sources, groups, part, triple), jnp.bfloat16)
    for k in range(groups):
        piece = mine if k == 0 else shifted(mine, "grp", k)
        weights = lax.dynamic_update_slice_in_dim(
            weights, piece[:, None], lax.rem(lax.axis_index("grp") + groups - k, groups), axis=1
        )
    return weights.reshape(sources * rows, triple)


def halved(arrived):
    experts, capacity, cols = arrived.shape
    cores = lax.axis_size("tp_c")
    arrived = arrived.reshape(cores, experts * capacity // cores, cols)
    halves = []
    for j in range(cores):
        half = lax.dynamic_index_in_dim(
            arrived, lax.rem(lax.axis_index("tp_c") + j, cores), axis=0, keepdims=False
        )
        halves.append(half if j == 0 else shifted(half, "tp_c", j))
    return jnp.stack(halves)


def on_device(tokens, routes, route_weights, norm_gain, gate_weight, up_weight, down_weight):
    experts, rows, _ = gate_weight.shape
    copies = lax.axis_size("fs_lo")
    row_count, col_width = tokens.shape
    capacity = row_count * 5 // 16

    outgoing = dispatched(tokens, routes, experts, capacity)
    arrived = exchange(outgoing, "fs_hi")
    block = lax.optimization_barrier(halved(arrived))
    blocks = [block] + [shifted(block, "fs_lo", k) for k in range(1, copies)]
    blocks = jnp.stack(blocks)
    parts = [blocks] + [
        shifted(blocks, "tp_x", k) for k in range(1, lax.axis_size("tp_x"))
    ]

    packed = packed_weights(norm_gain, gate_weight, up_weight, down_weight, copies)
    mine = exchange(packed, FS)
    own = assembled_weights(mine, rows)
    other = shifted(own, "tp_c", 1)

    sums = []
    for t in range(chunks):
        outs = expert_outputs(own, other, parts, t)
        got = [outs[0]] + [shifted(outs[k], "tp_x", k) for k in range(1, len(outs))]
        over_x = sum(value.astype(jnp.float32) for value in got).astype(jnp.bfloat16)
        sent = exchange(over_x.reshape(-1, *over_x.shape[2:]), ("fs_lo", "tp_c"))
        over_s = jnp.sum(sent.reshape(over_x.shape), axis=0, dtype=jnp.float32)
        sums.append(over_s.astype(jnp.bfloat16))
    back = jnp.concatenate(sums, axis=1).reshape(experts, capacity, col_width)
    returned = exchange(back, "fs_hi")
    width = own.shape[1] // 3
    outputs = [own[None, :, k * width : (k + 1) * width] for k in range(3)]
    return (*outputs, combined(routes, route_weights, returned))


def solution(mesh):
    split = Mesh(
        mesh.devices.reshape(mesh.shape["grp"], mesh.shape["fs"] // 4, 4, 4, 2),
        ("grp", *FS, *TP),
    )
    rows = P(("grp", *FS), None)
    weight = P(None, FS, TP)
    taken = P(FS, "grp", TP)

    return jax.shard_map(
        on_device,
        mesh=split,
        in_specs=(P(("grp", *FS), TP), rows, rows, P(FS), weight, weight, weight),
        out_specs=(taken, taken, taken, P(("grp", *FS), TP)),
        check_vma=False,
    )
```

time: 356 us -> 348 us (0.978)
  blocking collectives: 241 us -> 132 us
  waiting for transfers between devices: 51.1 us -> 103 us
  starting transfers between devices: 36.1 us -> 84.5 us
  Pallas kernels: 12.4 us -> 16 us
    all_to_all x3 -> x1, blocking collectives: 191 us -> 132 us  [exchange(): return lax.all_to_all(value, axis, split_axis=0, concat_axis=0, tiled=True)]
    all_gather x2 -> x0, blocking collectives: 50.3 us -> none  [the longest x1 35.9 us: dispatched(): gathered = lax.all_gather(jnp.concatenate([tokens, table]), 'fs_hi')]
    ppermute x6 -> x15, starting transfers between devices: 25 us -> 60.7 us  [shifted(): lax.ppermute(value, axis, [(k, (k + step) % count) for k in range(count)])]
    ppermute x6 -> x15, waiting for transfers between devices: 25.8 us -> 60.8 us  [shifted(): lax.ppermute(value, axis, [(k, (k + step) % count) for k in range(count)])]
    all_to_all x1 -> x4, waiting for transfers between devices: 25.3 us -> 42.5 us  [exchange(): return lax.all_to_all(value, axis, split_axis=0, concat_axis=0, tiled=True)]
    all_to_all x1 -> x4, starting transfers between devices: 11.2 us -> 23.9 us  [exchange(): return lax.all_to_all(value, axis, split_axis=0, concat_axis=0, tiled=True)]
    pallas_call x1 -> x4, Pallas kernels: 7.07 us -> 10.6 us  [the longest x2 6.69 us: expert_outputs(): pl.pallas_call(expert_kernel, out_shape=[jax.ShapeDtypeStruct(piece, jnp....]
  transfers between devices with their start and end apart: 7 -> 19, of which waited for: 5 -> 15; matrix products, arithmetic and copies ran while one was open for 1% -> 1% of each run, Pallas kernels for 0% -> 2%
where the time goes in v3:
time: 348 us; the launch traced here: 344 us
  blocking collectives  132 us (38%)
  waiting for transfers between devices  103 us (30%)
  starting transfers between devices  84.5 us (24%)
  Pallas kernels  16 us (5%)
  other arithmetic  3.68 us (1%)
    all_to_all x1, blocking collectives, exchange(): return lax.all_to_all(value, axis, split_axis=0, concat_axis=0, tiled=True)  132 us
    ppermute x15, waiting for transfers between devices, shifted(): lax.ppermute(value, axis, [(k, (k + step) % count) for k in range(count)])  60.8 us
    ppermute x15, starting transfers between devices, shifted(): lax.ppermute(value, axis, [(k, (k + step) % count) for k in range(count)])  60.7 us
    all_to_all x4, waiting for transfers between devices, exchange(): return lax.all_to_all(value, axis, split_axis=0, concat_axis=0, tiled=True)  42.5 us
    all_to_all x4, starting transfers between devices, exchange(): return lax.all_to_all(value, axis, split_axis=0, concat_axis=0, tiled=True)  23.9 us
  transfers between devices with their start and end apart: 19, of which 15 were waited for; matrix products, arithmetic and copies ran while one was open for 1% of the time, Pallas kernels for 2%

profile of v3, /device:TPU:33, one launch (start us, length us, event | category | flops | bytes accessed | tf_op | source)
XLA Modules:
  0.0 343.9 jit_solution(15073002275744559269)
XLA Ops:
  0.6 5.4 %pack.1 = bf16[32,32,384]{2,1,0:T(8,128)(2,1)} custom-call(s32[1]{0:T(128)} %bitcast.turn, f32[1,64]{1,0:T(1,128)} %bitcast.48, f32[8,64,512]{2,1,0:T(8,128)} %gate.1, f32[8,64,512]{2,1,0:T(8,128)} %up.1, f32[8,64,512]{2,1,0:T(8,128)} %down.1), custom_call_target="tpu_custom_call" | custom-call | tf_op jit(solution)/shard_map/pack/pallas_call | solution.py:50
  6.1 132.2 %all_to_all.25 = bf16[32,32,384]{2,1,0:T(8,128)(2,1)S(1)} all-to-all(bf16[32,32,384]{2,1,0:T(8,128)(2,1)} %pack.1), channel_id=1, replica_groups=mesh['grp'=2,'fs_hi'=8,'fs_lo'=4,'tp_x'=4,'tp_c'=2] {'fs_hi','fs_lo'}, dimensions={0} | all-to-all | bytes 1572864 | tf_op jit(solution)/shard_map/all_to_all | solution.py:24
  138.3 3.8 %collective-permute-start = (bf16[32,32,384]{2,1,0:T(8,128)(2,1)S(1)}, bf16[32,32,384]{2,1,0:T(8,128)(2,1)S(1)}, u32[]{:S(2)}, u32[]{:S(2)}) collective-permute-start(bf16[32,32,384]{2,1,0:T(8,128)(2,1)S(1)} %all_to_all.25), channel_id=1, source_target_pairs={{0,256},{256,0},{1,257},{257,1},{2,258},{258,2},{3,259},{259,3},{4... | collective-permute-start | bytes 2359304 | tf_op jit(solution)/shard_map/ppermute | solution.py:20
  144.0 3.6 %all-to-all-start.1 = ((bf16[8,40,256]{2,1,0:T(8,128)(2,1)}), bf16[8,40,256]{2,1,0:T(8,128)(2,1)S(1)}, u32[]{:S(2)}, u32[]{:S(2)}) async-start(bf16[8,40,256]{2,1,0:T(8,128)(2,1)} %dispatch.1), calls=%async_computation.1 | async-start | bytes 327680 | tf_op jit(solution)/shard_map/all_to_all | solution.py:24
  148.0 10.7 %collective-permute-done = bf16[32,32,384]{2,1,0:T(8,128)(2,1)S(1)} collective-permute-done((bf16[32,32,384]{2,1,0:T(8,128)(2,1)S(1)}, bf16[32,32,384]{2,1,0:T(8,128)(2,1)S(1)}, u32[]{:S(2)}, u32[]{:S(2)}) %collective-permute-start) | collective-permute-done | bytes 786464 | tf_op jit(solution)/shard_map/ppermute | solution.py:20
  158.9 3.8 %collective-permute-start.1 = (bf16[2048,384]{1,0:T(8,128)(2,1)S(1)}, bf16[2048,384]{1,0:T(8,128)(2,1)}, u32[]{:S(2)}, u32[]{:S(2)}) collective-permute-start(bf16[2048,384]{1,0:T(8,128)(2,1)S(1)} %bitcast.34), channel_id=1, source_target_pairs={{0,1},{1,0},{2,3},{3,2},{4,5},{5,4},{6,7},{7,6},{8,9},{9,8},{10,11... | collective-permute-start | bytes 4718600 | tf_op jit(solution)/shard_map/ppermute | solution.py:20
  162.7 8.2 %all-to-all-done.1 = bf16[8,40,256]{2,1,0:T(8,128)(2,1)S(1)} async-done(((bf16[8,40,256]{2,1,0:T(8,128)(2,1)}), bf16[8,40,256]{2,1,0:T(8,128)(2,1)S(1)}, u32[]{:S(2)}, u32[]{:S(2)}) %all-to-all-start.1) | async-done | bytes 163872 | tf_op jit(solution)/shard_map/all_to_all | solution.py:24
  170.9 7.4 %collective-permute-start.2 = (bf16[160,256]{1,0:T(8,128)(2,1)S(1)}, bf16[160,256]{1,0:T(8,128)(2,1)S(1)}, u32[]{:S(2)}, u32[]{:S(2)}) collective-permute-start(bf16[160,256]{1,0:T(8,128)(2,1)S(1)} %get-tuple-element.24), channel_id=1, source_target_pairs={{0,1},{1,0},{2,3},{3,2},{4,5},{5,4},{6,7},{7,6},{8,9},{9,8},{10,11... | collective-permute-start | bytes 245768 | tf_op jit(solution)/shard_map/ppermute | solution.py:20
  179.2 4.9 %collective-permute-start.3 = (bf16[2,160,256]{2,1,0:T(8,128)(2,1)S(1)}, bf16[2,160,256]{2,1,0:T(8,128)(2,1)S(1)}, u32[]{:S(2)}, u32[]{:S(2)}) collective-permute-start(bf16[2,160,256]{2,1,0:T(8,128)(2,1)S(1)} %pad_maximum_fusion.1), channel_id=1, source_target_pairs={{0,8},{8,16},{16,24},{24,0},{1,9},{9,17},{17,25},{25,1},{2,10},{10... | collective-permute-start | bytes 491528 | tf_op jit(solution)/shard_map/ppermute | solution.py:20
  184.1 4.6 %collective-permute-start.4 = (bf16[2,160,256]{2,1,0:T(8,128)(2,1)S(1)}, bf16[2,160,256]{2,1,0:T(8,128)(2,1)S(1)}, u32[]{:S(2)}, u32[]{:S(2)}) collective-permute-start(bf16[2,160,256]{2,1,0:T(8,128)(2,1)S(1)} %pad_maximum_fusion.1), channel_id=1, source_target_pairs={{0,16},{8,24},{16,0},{24,8},{1,17},{9,25},{17,1},{25,9},{2,18},{10... | collective-permute-start | bytes 491528 | tf_op jit(solution)/shard_map/ppermute | solution.py:20
  188.7 4.3 %collective-permute-start.5 = (bf16[2,160,256]{2,1,0:T(8,128)(2,1)S(1)}, bf16[2,160,256]{2,1,0:T(8,128)(2,1)S(1)}, u32[]{:S(2)}, u32[]{:S(2)}) collective-permute-start(bf16[2,160,256]{2,1,0:T(8,128)(2,1)S(1)} %pad_maximum_fusion.1), channel_id=1, source_target_pairs={{0,24},{8,0},{16,8},{24,16},{1,25},{9,1},{17,9},{25,17},{2,26},{10... | collective-permute-start | bytes 491528 | tf_op jit(solution)/shard_map/ppermute | solution.py:20
  199.5 4.7 %collective-permute-start.7 = (bf16[4,2,160,256]{3,2,1,0:T(8,128)(2,1)S(1)}, bf16[4,2,160,256]{3,2,1,0:T(8,128)(2,1)S(1)}, u32[]{:S(2)}, u32[]{:S(2)}) collective-permute-start(bf16[4,2,160,256]{3,2,1,0:T(8,128)(2,1)S(1)} %pad_maximum_fusion.refs_0_), channel_id=1, source_target_pairs={{0,4},{2,6},{4,0},{6,2},{1,5},{3,7},{5,1},{7,3},{8,12},{10,14},{12... | collective-permute-start | bytes 1966088 | tf_op jit(solution)/shard_map/ppermute | solution.py:20
  207.2 6.7 %collective-permute-done.6.refs_1_ = bf16[4,2,160,256]{3,2,1,0:T(8,128)(2,1)S(1)} collective-permute-done((bf16[4,2,160,256]{3,2,1,0:T(8,128)(2,1)S(1)}, bf16[4,2,160,256]{3,2,1,0:T(8,128)(2,1)S(1)}, u32[]{:S(2)}, u32[]{:S(2)}) %collective-permute-start.6) | collective-permute-done | bytes 655392 | tf_op jit(solution)/shard_map/ppermute | solution.py:20
  214.0 15.0 %collective-permute-done.7.refs_2_ = bf16[4,2,160,256]{3,2,1,0:T(8,128)(2,1)S(1)} collective-permute-done((bf16[4,2,160,256]{3,2,1,0:T(8,128)(2,1)S(1)}, bf16[4,2,160,256]{3,2,1,0:T(8,128)(2,1)S(1)}, u32[]{:S(2)}, u32[]{:S(2)}) %collective-permute-start.7) | collective-permute-done | bytes 655392 | tf_op jit(solution)/shard_map/ppermute | solution.py:20
  231.8 3.3 experts.2
  235.1 4.7 %collective-permute-start.10 = (bf16[4,2,80,256]{3,2,1,0:T(8,128)(2,1)S(1)}, bf16[4,2,80,256]{3,2,1,0:T(8,128)(2,1)S(1)}, u32[]{:S(2)}, u32[]{:S(2)}) collective-permute-start(bf16[4,2,80,256]{3,2,1,0:T(8,128)(2,1)S(1)} %get-tuple-element.14), channel_id=1, source_target_pairs={{0,4},{2,6},{4,0},{6,2},{1,5},{3,7},{5,1},{7,3},{8,12},{10,14},{12... | collective-permute-start | bytes 983048 | tf_op jit(solution)/shard_map/ppermute | solution.py:20
  239.9 4.9 %collective-permute-start.11 = (bf16[4,2,80,256]{3,2,1,0:T(8,128)(2,1)S(1)}, bf16[4,2,80,256]{3,2,1,0:T(8,128)(2,1)S(1)}, u32[]{:S(2)}, u32[]{:S(2)}) collective-permute-start(bf16[4,2,80,256]{3,2,1,0:T(8,128)(2,1)S(1)} %get-tuple-element.15), channel_id=1, source_target_pairs={{0,6},{2,0},{4,2},{6,4},{1,7},{3,1},{5,3},{7,5},{8,14},{10,8},{12,... | collective-permute-start | bytes 983048 | tf_op jit(solution)/shard_map/ppermute | solution.py:20
  246.7 8.8 %collective-permute-done.11 = bf16[4,2,80,256]{3,2,1,0:T(8,128)(2,1)S(1)} collective-permute-done((bf16[4,2,80,256]{3,2,1,0:T(8,128)(2,1)S(1)}, bf16[4,2,80,256]{3,2,1,0:T(8,128)(2,1)S(1)}, u32[]{:S(2)}, u32[]{:S(2)}) %collective-permute-start.11) | collective-permute-done | bytes 327712 | tf_op jit(solution)/shard_map/ppermute | solution.py:20
  257.0 10.9 %all-to-all-start.2 = ((bf16[8,80,256]{2,1,0:T(8,128)(2,1)}), bf16[8,80,256]{2,1,0:T(8,128)(2,1)}, u32[]{:S(2)}, u32[]{:S(2)}) async-start(bf16[8,80,256]{2,1,0:T(8,128)(2,1)} %bitcast.39), calls=%async_computation.2 | async-start | bytes 655360 | tf_op jit(solution)/shard_map/all_to_all | solution.py:24
  283.8 6.6 %collective-permute-done.13 = bf16[4,2,80,256]{3,2,1,0:T(8,128)(2,1)S(1)} collective-permute-done((bf16[4,2,80,256]{3,2,1,0:T(8,128)(2,1)S(1)}, bf16[4,2,80,256]{3,2,1,0:T(8,128)(2,1)S(1)}, u32[]{:S(2)}, u32[]{:S(2)}) %collective-permute-start.13) | collective-permute-done | bytes 327712 | tf_op jit(solution)/shard_map/ppermute | solution.py:20
  293.8 5.9 %all-to-all-start.3 = ((bf16[8,80,256]{2,1,0:T(8,128)(2,1)}), bf16[8,80,256]{2,1,0:T(8,128)(2,1)S(1)}, u32[]{:S(2)}, u32[]{:S(2)}) async-start(bf16[8,80,256]{2,1,0:T(8,128)(2,1)} %bitcast.23), calls=%async_computation.3 | async-start | bytes 655360 | tf_op jit(solution)/shard_map/all_to_all | solution.py:24
  300.6 9.0 %all-to-all-done.3 = bf16[8,80,256]{2,1,0:T(8,128)(2,1)S(1)} async-done(((bf16[8,80,256]{2,1,0:T(8,128)(2,1)}), bf16[8,80,256]{2,1,0:T(8,128)(2,1)S(1)}, u32[]{:S(2)}, u32[]{:S(2)}) %all-to-all-start.3) | async-done | bytes 327712 | tf_op jit(solution)/shard_map/all_to_all | solution.py:24
  310.3 3.6 %all-to-all-start.4 = ((bf16[8,40,256]{2,1,0:T(8,128)(2,1)}), bf16[8,40,256]{2,1,0:T(8,128)(2,1)S(1)}, u32[]{:S(2)}, u32[]{:S(2)}) async-start(bf16[8,40,256]{2,1,0:T(8,128)(2,1)} %bitcast.25), calls=%async_computation.4 | async-start | bytes 327680 | tf_op jit(solution)/shard_map/all_to_all | solution.py:24
  315.9 25.3 %all-to-all-done.4.returned = bf16[8,40,256]{2,1,0:T(8,128)(2,1)S(1)} async-done(((bf16[8,40,256]{2,1,0:T(8,128)(2,1)}), bf16[8,40,256]{2,1,0:T(8,128)(2,1)S(1)}, u32[]{:S(2)}, u32[]{:S(2)}) %all-to-all-start.4) | async-done | bytes 163872 | tf_op jit(solution)/shard_map/all_to_all | solution.py:24
  (38 shorter events, 44.9 us)
Async XLA Ops:
  138.3 20.4 %collective-permute-start = (bf16[32,32,384]{2,1,0:T(8,128)(2,1)S(1)}, bf16[32,32,384]{2,1,0:T(8,128)(2,1)S(1)}, u32[]{:S(2)}, u32[]{:S(2)}) collective-permute-start(bf16[32,32,384]{2,1,0:T(8,128)(2,1)S(1)} %all_to_all.25), channel_id=1, source_target_pairs={{0,256},{256,0},{1,257},{257,1},{2,258},{258,2},{3,259},{259,3},{4... | collective-permute-start | bytes 2359304 | tf_op jit(solution)/shard_map/ppermute | solution.py:20
  144.0 26.9 %all-to-all-start.1 = ((bf16[8,40,256]{2,1,0:T(8,128)(2,1)}), bf16[8,40,256]{2,1,0:T(8,128)(2,1)S(1)}, u32[]{:S(2)}, u32[]{:S(2)}) async-start(bf16[8,40,256]{2,1,0:T(8,128)(2,1)} %dispatch.1), calls=%async_computation.1 | async-start | bytes 327680 | tf_op jit(solution)/shard_map/all_to_all | solution.py:24
  158.9 72.9 %collective-permute-start.1 = (bf16[2048,384]{1,0:T(8,128)(2,1)S(1)}, bf16[2048,384]{1,0:T(8,128)(2,1)}, u32[]{:S(2)}, u32[]{:S(2)}) collective-permute-start(bf16[2048,384]{1,0:T(8,128)(2,1)S(1)} %bitcast.34), channel_id=1, source_target_pairs={{0,1},{1,0},{2,3},{3,2},{4,5},{5,4},{6,7},{7,6},{8,9},{9,8},{10,11... | collective-permute-start | bytes 4718600 | tf_op jit(solution)/shard_map/ppermute | solution.py:20
  170.9 8.3 %collective-permute-start.2 = (bf16[160,256]{1,0:T(8,128)(2,1)S(1)}, bf16[160,256]{1,0:T(8,128)(2,1)S(1)}, u32[]{:S(2)}, u32[]{:S(2)}) collective-permute-start(bf16[160,256]{1,0:T(8,128)(2,1)S(1)} %get-tuple-element.24), channel_id=1, source_target_pairs={{0,1},{1,0},{2,3},{3,2},{4,5},{5,4},{6,7},{7,6},{8,9},{9,8},{10,11... | collective-permute-start | bytes 245768 | tf_op jit(solution)/shard_map/ppermute | solution.py:20
  179.2 13.7 %collective-permute-start.3 = (bf16[2,160,256]{2,1,0:T(8,128)(2,1)S(1)}, bf16[2,160,256]{2,1,0:T(8,128)(2,1)S(1)}, u32[]{:S(2)}, u32[]{:S(2)}) collective-permute-start(bf16[2,160,256]{2,1,0:T(8,128)(2,1)S(1)} %pad_maximum_fusion.1), channel_id=1, source_target_pairs={{0,8},{8,16},{16,24},{24,0},{1,9},{9,17},{17,25},{25,1},{2,10},{10... | collective-permute-start | bytes 491528 | tf_op jit(solution)/shard_map/ppermute | solution.py:20
  184.1 11.2 %collective-permute-start.4 = (bf16[2,160,256]{2,1,0:T(8,128)(2,1)S(1)}, bf16[2,160,256]{2,1,0:T(8,128)(2,1)S(1)}, u32[]{:S(2)}, u32[]{:S(2)}) collective-permute-start(bf16[2,160,256]{2,1,0:T(8,128)(2,1)S(1)} %pad_maximum_fusion.1), channel_id=1, source_target_pairs={{0,16},{8,24},{16,0},{24,8},{1,17},{9,25},{17,1},{25,9},{2,18},{10... | collective-permute-start | bytes 491528 | tf_op jit(solution)/shard_map/ppermute | solution.py:20
  188.7 7.5 %collective-permute-start.5 = (bf16[2,160,256]{2,1,0:T(8,128)(2,1)S(1)}, bf16[2,160,256]{2,1,0:T(8,128)(2,1)S(1)}, u32[]{:S(2)}, u32[]{:S(2)}) collective-permute-start(bf16[2,160,256]{2,1,0:T(8,128)(2,1)S(1)} %pad_maximum_fusion.1), channel_id=1, source_target_pairs={{0,24},{8,0},{16,8},{24,16},{1,25},{9,1},{17,9},{25,17},{2,26},{10... | collective-permute-start | bytes 491528 | tf_op jit(solution)/shard_map/ppermute | solution.py:20
  196.2 17.7 %collective-permute-start.6 = (bf16[4,2,160,256]{3,2,1,0:T(8,128)(2,1)S(1)}, bf16[4,2,160,256]{3,2,1,0:T(8,128)(2,1)S(1)}, u32[]{:S(2)}, u32[]{:S(2)}) collective-permute-start(bf16[4,2,160,256]{3,2,1,0:T(8,128)(2,1)S(1)} %pad_maximum_fusion.refs_0_), channel_id=1, source_target_pairs={{0,2},{2,4},{4,6},{6,0},{1,3},{3,5},{5,7},{7,1},{8,10},{10,12},{12... | collective-permute-start | bytes 1966088 | tf_op jit(solution)/shard_map/ppermute | solution.py:20
  199.5 29.4 %collective-permute-start.7 = (bf16[4,2,160,256]{3,2,1,0:T(8,128)(2,1)S(1)}, bf16[4,2,160,256]{3,2,1,0:T(8,128)(2,1)S(1)}, u32[]{:S(2)}, u32[]{:S(2)}) collective-permute-start(bf16[4,2,160,256]{3,2,1,0:T(8,128)(2,1)S(1)} %pad_maximum_fusion.refs_0_), channel_id=1, source_target_pairs={{0,4},{2,6},{4,0},{6,2},{1,5},{3,7},{5,1},{7,3},{8,12},{10,14},{12... | collective-permute-start | bytes 1966088 | tf_op jit(solution)/shard_map/ppermute | solution.py:20
  204.2 27.6 %collective-permute-start.8 = (bf16[4,2,160,256]{3,2,1,0:T(8,128)(2,1)S(1)}, bf16[4,2,160,256]{3,2,1,0:T(8,128)(2,1)}, u32[]{:S(2)}, u32[]{:S(2)}) collective-permute-start(bf16[4,2,160,256]{3,2,1,0:T(8,128)(2,1)S(1)} %pad_maximum_fusion.refs_0_), channel_id=1, source_target_pairs={{0,6},{2,0},{4,2},{6,4},{1,7},{3,1},{5,3},{7,5},{8,14},{10,8},{12,... | collective-permute-start | bytes 1966088 | tf_op jit(solution)/shard_map/ppermute | solution.py:20
  235.1 11.6 %collective-permute-start.10 = (bf16[4,2,80,256]{3,2,1,0:T(8,128)(2,1)S(1)}, bf16[4,2,80,256]{3,2,1,0:T(8,128)(2,1)S(1)}, u32[]{:S(2)}, u32[]{:S(2)}) collective-permute-start(bf16[4,2,80,256]{3,2,1,0:T(8,128)(2,1)S(1)} %get-tuple-element.14), channel_id=1, source_target_pairs={{0,4},{2,6},{4,0},{6,2},{1,5},{3,7},{5,1},{7,3},{8,12},{10,14},{12... | collective-permute-start | bytes 983048 | tf_op jit(solution)/shard_map/ppermute | solution.py:20
  239.9 15.7 %collective-permute-start.11 = (bf16[4,2,80,256]{3,2,1,0:T(8,128)(2,1)S(1)}, bf16[4,2,80,256]{3,2,1,0:T(8,128)(2,1)S(1)}, u32[]{:S(2)}, u32[]{:S(2)}) collective-permute-start(bf16[4,2,80,256]{3,2,1,0:T(8,128)(2,1)S(1)} %get-tuple-element.15), channel_id=1, source_target_pairs={{0,6},{2,0},{4,2},{6,4},{1,7},{3,1},{5,3},{7,5},{8,14},{10,8},{12,... | collective-permute-start | bytes 983048 | tf_op jit(solution)/shard_map/ppermute | solution.py:20
  244.7 11.4 %collective-permute-start.9 = (bf16[4,2,80,256]{3,2,1,0:T(8,128)(2,1)S(1)}, bf16[4,2,80,256]{3,2,1,0:T(8,128)(2,1)S(1)}, u32[]{:S(2)}, u32[]{:S(2)}) collective-permute-start(bf16[4,2,80,256]{3,2,1,0:T(8,128)(2,1)S(1)} %get-tuple-element.13), channel_id=1, source_target_pairs={{0,2},{2,4},{4,6},{6,0},{1,3},{3,5},{5,7},{7,1},{8,10},{10,12},{12... | collective-permute-start | bytes 983048 | tf_op jit(solution)/shard_map/ppermute | solution.py:20
  257.0 36.8 %all-to-all-start.2 = ((bf16[8,80,256]{2,1,0:T(8,128)(2,1)}), bf16[8,80,256]{2,1,0:T(8,128)(2,1)}, u32[]{:S(2)}, u32[]{:S(2)}) async-start(bf16[8,80,256]{2,1,0:T(8,128)(2,1)} %bitcast.39), calls=%async_computation.2 | async-start | bytes 655360 | tf_op jit(solution)/shard_map/all_to_all | solution.py:24
  271.2 12.6 %collective-permute-start.12 = (bf16[4,2,80,256]{3,2,1,0:T(8,128)(2,1)S(1)}, bf16[4,2,80,256]{3,2,1,0:T(8,128)(2,1)S(1)}, u32[]{:S(2)}, u32[]{:S(2)}) collective-permute-start(bf16[4,2,80,256]{3,2,1,0:T(8,128)(2,1)S(1)} %get-tuple-element.17), channel_id=1, source_target_pairs={{0,2},{2,4},{4,6},{6,0},{1,3},{3,5},{5,7},{7,1},{8,10},{10,12},{12... | collective-permute-start | bytes 983048 | tf_op jit(solution)/shard_map/ppermute | solution.py:20
  274.1 16.2 %collective-permute-start.13 = (bf16[4,2,80,256]{3,2,1,0:T(8,128)(2,1)S(1)}, bf16[4,2,80,256]{3,2,1,0:T(8,128)(2,1)S(1)}, u32[]{:S(2)}, u32[]{:S(2)}) collective-permute-start(bf16[4,2,80,256]{3,2,1,0:T(8,128)(2,1)S(1)} %get-tuple-element.18), channel_id=1, source_target_pairs={{0,4},{2,6},{4,0},{6,2},{1,5},{3,7},{5,1},{7,3},{8,12},{10,14},{12... | collective-permute-start | bytes 983048 | tf_op jit(solution)/shard_map/ppermute | solution.py:20
  277.5 15.4 %collective-permute-start.14 = (bf16[4,2,80,256]{3,2,1,0:T(8,128)(2,1)S(1)}, bf16[4,2,80,256]{3,2,1,0:T(8,128)(2,1)S(1)}, u32[]{:S(2)}, u32[]{:S(2)}) collective-permute-start(bf16[4,2,80,256]{3,2,1,0:T(8,128)(2,1)S(1)} %get-tuple-element.19), channel_id=1, source_target_pairs={{0,6},{2,0},{4,2},{6,4},{1,7},{3,1},{5,3},{7,5},{8,14},{10,8},{12,... | collective-permute-start | bytes 983048 | tf_op jit(solution)/shard_map/ppermute | solution.py:20
  292.9 21.1 %copy-start.1 = (f32[128,2]{0,1:T(2,128)S(1)}, f32[128,2]{0,1:T(2,128)}, u32[]{:S(2)}) copy-start(f32[128,2]{0,1:T(2,128)} %param.9) | copy-start | bytes 3076
  293.8 15.8 %all-to-all-start.3 = ((bf16[8,80,256]{2,1,0:T(8,128)(2,1)}), bf16[8,80,256]{2,1,0:T(8,128)(2,1)S(1)}, u32[]{:S(2)}, u32[]{:S(2)}) async-start(bf16[8,80,256]{2,1,0:T(8,128)(2,1)} %bitcast.23), calls=%async_computation.3 | async-start | bytes 655360 | tf_op jit(solution)/shard_map/all_to_all | solution.py:24
  310.3 30.9 %all-to-all-start.4 = ((bf16[8,40,256]{2,1,0:T(8,128)(2,1)}), bf16[8,40,256]{2,1,0:T(8,128)(2,1)S(1)}, u32[]{:S(2)}, u32[]{:S(2)}) async-start(bf16[8,40,256]{2,1,0:T(8,128)(2,1)} %bitcast.25), calls=%async_computation.4 | async-start | bytes 327680 | tf_op jit(solution)/shard_map/all_to_all | solution.py:24
  341.2 0.7 copy-start

commit v4 on v3

--- a/solution.py
+++ b/solution.py
@@ -12,12 +12,15 @@
 TP = ("tp_x", "tp_c")
 
 epsilon = 1e-06
-chunks = 2
 
 
 def shifted(value, axis, step):
     count = lax.axis_size(axis)
     return lax.ppermute(value, axis, [(k, (k + step) % count) for k in range(count)])
+
+
+def vmem(mebibytes):
+    return pltpu.CompilerParams(vmem_limit_bytes=mebibytes * 1024 * 1024)
 
 
 def exchange(value, axis):
@@ -56,6 +59,7 @@
             in_specs=[pl.BlockSpec((1, rows), lambda e, turn: (0, 0)), block, block, block],
             out_specs=pl.BlockSpec((copies, part, 3 * width), lambda e, turn: (e, 0, 0)),
         ),
+        compiler_params=vmem(12),
         name="pack",
     )(position_of("grp"), norm_gain.reshape(1, rows), gate_weight, up_weight, down_weight)
 
@@ -91,79 +95,97 @@
     return pl.pallas_call(
         dispatch_kernel,
         out_shape=jax.ShapeDtypeStruct((experts, capacity, tokens.shape[1]), jnp.bfloat16),
+        compiler_params=vmem(12),
         name="dispatch",
     )(routes.T, tokens)
 
 
-def expert_kernel(place, own, other, *refs):
-    count = len(refs) // 2
-    parts, outs = refs[:count], refs[count:]
-    copies, halves, tokens, cols = parts[0].shape
-    width = own.shape[1] // 3
-    rows = copies * tokens
+def expert_kernel(span, count, place, *refs):
+    first, share = span
+    total, assembled = len(refs), refs[-2:]
+    parts, outs = refs[total - 2 - 2 * count : total - 2 - count], refs[total - 2 - count : -2]
+    pieces = refs[: total - 2 - 2 * count]
+    groups = len(pieces) // 2
+    copies, halves, _, cols = parts[0].shape
+    part, width = pieces[0].shape[1], pieces[0].shape[2] // 3
+    rows = copies * share
+    for k in range(groups):
+        index = lax.rem(place[3] + (groups - k), groups)
+        for held, piece in zip(assembled, (pieces[k], pieces[groups + k])):
+            held[:, pl.ds(index, 1)] = piece[...][:, None]
+
+    def block(held, k, c, start, end):
+        sources = cols // (groups * part)
+        at = (lax.rem(place[0] + k, count) * halves + c) * sources
+        return held[pl.ds(at, sources), :, :, start:end].reshape(cols, end - start)
+
     sums = [jnp.zeros((rows, 2 * width), jnp.float32) for _ in range(2)]
     squares = jnp.zeros((rows, cols), jnp.float32)
-
-    def block(k, c):
-        start = lax.rem(place[0] + k, count) * halves + c
-        return pl.ds(pl.multiple_of(start * cols, cols), cols)
-
-    for k, part in enumerate(parts):
+    for k in range(count):
         for c in range(halves):
             core = lax.rem(place[1] + (halves - c), halves)
-            left = part[:, c].reshape(rows, cols)
+            left = parts[k][:, c, first : first + share].reshape(rows, cols)
             wide = left.astype(jnp.float32)
             squares = squares + wide * wide
-            where = block(count - k, core)
             sums = [
-                total
-                + jnp.dot(left, ref[where, : 2 * width], preferred_element_type=jnp.float32)
-                for total, ref in zip(sums, (own, other))
+                value
+                + jnp.dot(
+                    left,
+                    block(held, count - k, core, 0, 2 * width),
+                    preferred_element_type=jnp.float32,
+                )
+                for value, held in zip(sums, assembled)
             ]
     features = count * halves * cols
     row_scale = lax.rsqrt(jnp.sum(squares, axis=1, keepdims=True) / features + epsilon)
     hidden = []
-    for total in sums:
-        total = total * row_scale
-        gate, up = total[:, :width], total[:, width:]
+    for value in sums:
+        value = value * row_scale
+        gate, up = value[:, :width], value[:, width:]
         hidden.append((gate / (1.0 + jnp.exp(-gate)) * up).astype(jnp.bfloat16))
     hidden = jnp.concatenate(hidden, axis=1)
     for k, out in enumerate(outs):
         for c in range(halves):
-            where = block(k, c)
-            down = jnp.concatenate([ref[where, 2 * width :] for ref in (own, other)], axis=1)
+            down = jnp.concatenate(
+                [block(held, k, c, 2 * width, 3 * width) for held in assembled], axis=1
+            )
             value = lax.dot_general(
                 hidden, down, (((1,), (1,)), ((), ())), preferred_element_type=jnp.float32
             ).astype(jnp.bfloat16)
             for r in range(copies):
                 target = lax.rem(place[2] + (copies - r), copies)
-                out[pl.ds(target, 1), c] = value[r * tokens : (r + 1) * tokens][None]
-
-
-def expert_outputs(own, other, parts, chunk):
-    copies, halves, tokens, cols = parts[0].shape
-    share = tokens // chunks
-    whole = pl.BlockSpec(own.shape, lambda t, place: (0, 0))
-    piece = (copies, halves, share, cols)
-    return pl.pallas_call(
-        expert_kernel,
-        out_shape=[jax.ShapeDtypeStruct(piece, jnp.bfloat16)] * len(parts),
+                out[pl.ds(target, 1), c] = value[r * share : (r + 1) * share][None]
+
+
+def whole_block(value):
+    return pl.BlockSpec(value.shape, lambda t, place, rank=len(value.shape): (0,) * rank)
+
+
+def expert_outputs(pieces, parts, span):
+    copies, halves, _, cols = parts[0].shape
+    sources, part, triple = pieces[0].shape
+    out = jax.ShapeDtypeStruct((copies, halves, span[1], cols), jnp.bfloat16)
+    inputs = (*pieces, *parts)
+    held = pltpu.VMEM((sources, len(pieces) // 2, part, triple), jnp.bfloat16)
+    return pl.pallas_call(
+        functools.partial(expert_kernel, span, len(parts)),
+        out_shape=[out] * len(parts),
         grid_spec=pltpu.PrefetchScalarGridSpec(
             num_scalar_prefetch=1,
             grid=(1,),
-            in_specs=[whole, whole]
-            + [pl.BlockSpec(piece, lambda t, place: (0, 0, chunk, 0))] * len(parts),
-            out_specs=[pl.BlockSpec(piece, lambda t, place: (0, 0, 0, 0))] * len(parts),
+            in_specs=[whole_block(value) for value in inputs],
+            out_specs=[whole_block(out)] * len(parts),
+            scratch_shapes=[held, held],
         ),
-        compiler_params=pltpu.CompilerParams(vmem_limit_bytes=48 * 1024 * 1024),
+        compiler_params=vmem(32),
         name="experts",
-    )(position_of("tp_x", "tp_c", "fs_lo"), own, other, *parts)
-
-
-def combine_kernel(routes, route_weights, returned, out):
-    experts, capacity, cols = returned.shape
-    top, count = routes.shape
-    expert = lax.broadcasted_iota(jnp.int32, (experts, count), 0)
+    )(position_of("tp_x", "tp_c", "fs_lo", "grp"), *inputs)
+
+
+def choose_kernel(routes, out):
+    top, slots, count = out.shape
+    capacity = count * 5 // 16
+    expert = lax.broadcasted_iota(jnp.int32, (slots // capacity, count), 0)
     named = [routes[k : k + 1, :] == expert for k in range(top)]
     either = functools.reduce(jnp.logical_or, named)
     position = jnp.dot(
@@ -171,35 +193,58 @@
         before_matrix(count),
         preferred_element_type=jnp.float32,
     ).astype(jnp.int32)
-    values = returned[...].reshape(experts * capacity, cols)
-    slot = lax.broadcasted_iota(jnp.int32, (experts * capacity, count), 0)
-    total = jnp.zeros((count, cols), jnp.float32)
+    slot = lax.broadcasted_iota(jnp.int32, (slots, count), 0)
     for k in range(top):
         mine = jnp.sum(
             jnp.where(named[k], expert * capacity + position, 0), axis=0, keepdims=True
         )
-        chosen = jnp.where(mine == slot, 1.0, 0.0).astype(jnp.bfloat16)
+        out[k] = jnp.where(mine == slot, 1.0, 0.0).astype(jnp.bfloat16)
+
+
+def chosen_slots(routes, slots):
+    count, top = routes.shape
+    return pl.pallas_call(
+        choose_kernel,
+        out_shape=jax.ShapeDtypeStruct((top, slots, count), jnp.bfloat16),
+        compiler_params=vmem(12),
+        name="choose",
+    )(routes.T)
+
+
+def combine_kernel(place, chosen, route_weights, returned, out):
+    top, slots, _ = chosen.shape
+    values = returned[...].reshape(slots, returned.shape[2])
+    total = jnp.zeros(out.shape, jnp.float32)
+    for k in range(top):
         picked = lax.dot_general(
-            chosen, values, (((0,), (0,)), ((), ())), preferred_element_type=jnp.float32
+            chosen[k], values, (((0,), (0,)), ((), ())), preferred_element_type=jnp.float32
         )
         total = total + route_weights[:, k : k + 1] * picked
     out[...] = total.astype(jnp.bfloat16)
 
 
-def combined(routes, route_weights, returned):
+def combined(chosen, route_weights, returned):
+    out = jax.ShapeDtypeStruct((route_weights.shape[0], returned.shape[2]), jnp.bfloat16)
+    inputs = (chosen, route_weights, returned)
     return pl.pallas_call(
         combine_kernel,
-        out_shape=jax.ShapeDtypeStruct((routes.shape[0], returned.shape[2]), jnp.bfloat16),
+        out_shape=out,
+        grid_spec=pltpu.PrefetchScalarGridSpec(
+            num_scalar_prefetch=1,
+            grid=(1,),
+            in_specs=[whole_block(value) for value in inputs],
+            out_specs=whole_block(out),
+        ),
+        compiler_params=vmem(12),
         name="combine",
-    )(routes.T, route_weights, returned)
-
-
-def assembled_weights(mine, rows):
-    sources, part, triple = mine.shape
-    groups = lax.axis_size("grp")
+    )(position_of("grp"), *inputs)
+
+
+def assembled_weights(pieces, rows):
+    groups = len(pieces)
+    sources, part, triple = pieces[0].shape
     weights = jnp.zeros((sources, groups, part, triple), jnp.bfloat16)
-    for k in range(groups):
-        piece = mine if k == 0 else shifted(mine, "grp", k)
+    for k, piece in enumerate(pieces):
         weights = lax.dynamic_update_slice_in_dim(
             weights, piece[:, None], lax.rem(lax.axis_index("grp") + groups - k, groups), axis=1
         )
@@ -224,6 +269,9 @@
     copies = lax.axis_size("fs_lo")
     row_count, col_width = tokens.shape
     capacity = row_count * 5 // 16
+    share = experts * capacity // lax.axis_size("tp_c")
+    cut = share * 5 // 8 // 32 * 32
+    spans = ((0, cut), (cut, share - cut))
 
     outgoing = dispatched(tokens, routes, experts, capacity)
     arrived = exchange(outgoing, "fs_hi")
@@ -236,22 +284,24 @@
 
     packed = packed_weights(norm_gain, gate_weight, up_weight, down_weight, copies)
     mine = exchange(packed, FS)
-    own = assembled_weights(mine, rows)
-    other = shifted(own, "tp_c", 1)
+    own = [mine] + [shifted(mine, "grp", k) for k in range(1, lax.axis_size("grp"))]
+    other = [shifted(piece, "tp_c", 1) for piece in own]
+    chosen = chosen_slots(routes, experts * capacity)
 
     sums = []
-    for t in range(chunks):
-        outs = expert_outputs(own, other, parts, t)
+    for span in spans:
+        outs = expert_outputs(own + other, parts, span)
         got = [outs[0]] + [shifted(outs[k], "tp_x", k) for k in range(1, len(outs))]
         over_x = sum(value.astype(jnp.float32) for value in got).astype(jnp.bfloat16)
         sent = exchange(over_x.reshape(-1, *over_x.shape[2:]), ("fs_lo", "tp_c"))
         over_s = jnp.sum(sent.reshape(over_x.shape), axis=0, dtype=jnp.float32)
         sums.append(over_s.astype(jnp.bfloat16))
+    own = assembled_weights(own, rows)
     back = jnp.concatenate(sums, axis=1).reshape(experts, capacity, col_width)
     returned = exchange(back, "fs_hi")
     width = own.shape[1] // 3
     outputs = [own[None, :, k * width : (k + 1) * width] for k in range(3)]
-    return (*outputs, combined(routes, route_weights, returned))
+    return (*outputs, combined(chosen, route_weights, returned))
 
 
 def solution(mesh):

time: 348 us -> 347 us (level)
  blocking collectives: 132 us -> 0 us
  waiting for transfers between devices: 103 us -> 190 us
  starting transfers between devices: 84.5 us -> 128 us
    all_to_all x1 -> x0, blocking collectives: 132 us -> none  [exchange(): return lax.all_to_all(value, axis, split_axis=0, concat_axis=0, tiled=True)]
    all_to_all x4 -> x5, waiting for transfers between devices: 42.5 us -> 143 us  [exchange(): return lax.all_to_all(value, axis, split_axis=0, concat_axis=0, tiled=True)]
    all_to_all x4 -> x5, starting transfers between devices: 23.9 us -> 68.5 us  [exchange(): return lax.all_to_all(value, axis, split_axis=0, concat_axis=0, tiled=True)]
    ppermute x15 -> x16, waiting for transfers between devices: 60.8 us -> 46.7 us  [shifted(): lax.ppermute(value, axis, [(k, (k + step) % count) for k in range(count)])]
    ppermute x15 -> x16, starting transfers between devices: 60.7 us -> 59.9 us  [shifted(): lax.ppermute(value, axis, [(k, (k + step) % count) for k in range(count)])]
    pallas_call x3 -> x4, Pallas kernels: 8.7 us -> 8.73 us  [the longest x2 7.63 us: expert_outputs(): pl.pallas_call(functools.partial(expert_kernel, span, len(parts)), out_sh...]
  transfers between devices with their start and end apart: 19 -> 21, of which waited for: 15 -> 13; matrix products, arithmetic and copies ran while one was open for 1% -> 1% of each run, Pallas kernels for 2% -> 2%
where the time goes in v4:
time: 347 us; the launch traced here: 341 us
  waiting for transfers between devices  190 us (55%)
  starting transfers between devices  128 us (37%)
  Pallas kernels  12.7 us (4%)
  local copies, waits for them, and re-layouts  6.44 us (2%)
    all_to_all x5, waiting for transfers between devices, exchange(): return lax.all_to_all(value, axis, split_axis=0, concat_axis=0, tiled=True)  143 us
    all_to_all x5, starting transfers between devices, exchange(): return lax.all_to_all(value, axis, split_axis=0, concat_axis=0, tiled=True)  68.5 us
    ppermute x16, starting transfers between devices, shifted(): lax.ppermute(value, axis, [(k, (k + step) % count) for k in range(count)])  59.9 us
    ppermute x16, waiting for transfers between devices, shifted(): lax.ppermute(value, axis, [(k, (k + step) % count) for k in range(count)])  46.7 us
    pallas_call x2, Pallas kernels, expert_outputs(): pl.pallas_call(functools.partial(expert_kernel, span, len(parts)), out_sh...  7.63 us
  transfers between devices with their start and end apart: 21, of which 13 were waited for; matrix products, arithmetic and copies ran while one was open for 1% of the time, Pallas kernels for 2%

profile of v4, /device:TPU:33, one launch (start us, length us, event | category | flops | bytes accessed | tf_op | source)
XLA Modules:
  0.0 340.9 jit_solution(16116036283991569057)
XLA Ops:
  8.0 46.4 %all-to-all-start = ((bf16[32,32,384]{2,1,0:T(8,128)(2,1)}), bf16[32,32,384]{2,1,0:T(8,128)(2,1)S(1)}, u32[]{:S(2)}, u32[]{:S(2)}) async-start(bf16[32,32,384]{2,1,0:T(8,128)(2,1)} %pack.1), calls=%async_computation | async-start | bytes 1572864 | tf_op jit(solution)/shard_map/all_to_all | solution.py:27
  55.5 84.9 %all-to-all-done.refs_0_ = bf16[32,32,384]{2,1,0:T(8,128)(2,1)S(1)} async-done(((bf16[32,32,384]{2,1,0:T(8,128)(2,1)}), bf16[32,32,384]{2,1,0:T(8,128)(2,1)S(1)}, u32[]{:S(2)}, u32[]{:S(2)}) %all-to-all-start) | async-done | bytes 786464 | tf_op jit(solution)/shard_map/all_to_all | solution.py:27
  140.4 3.6 %all-to-all-start.1 = ((bf16[8,40,256]{2,1,0:T(8,128)(2,1)}), bf16[8,40,256]{2,1,0:T(8,128)(2,1)S(1)}, u32[]{:S(2)}, u32[]{:S(2)}) async-start(bf16[8,40,256]{2,1,0:T(8,128)(2,1)} %dispatch.1), calls=%async_computation.1 | async-start | bytes 327680 | tf_op jit(solution)/shard_map/all_to_all | solution.py:27
  144.0 3.8 %collective-permute-start = (bf16[32,32,384]{2,1,0:T(8,128)(2,1)S(1)}, bf16[32,32,384]{2,1,0:T(8,128)(2,1)S(1)}, u32[]{:S(2)}, u32[]{:S(2)}) collective-permute-start(bf16[32,32,384]{2,1,0:T(8,128)(2,1)S(1)} %all-to-all-done.refs_0_), channel_id=1, source_target_pairs={{0,256},{256,0},{1,257},{257,1},{2,258},{258,2},{3,259},{259,3},{4... | collective-permute-start | bytes 2359304 | tf_op jit(solution)/shard_map/ppermute | solution.py:19
  147.8 22.4 %all-to-all-done.1 = bf16[8,40,256]{2,1,0:T(8,128)(2,1)S(1)} async-done(((bf16[8,40,256]{2,1,0:T(8,128)(2,1)}), bf16[8,40,256]{2,1,0:T(8,128)(2,1)S(1)}, u32[]{:S(2)}, u32[]{:S(2)}) %all-to-all-start.1) | async-done | bytes 163872 | tf_op jit(solution)/shard_map/all_to_all | solution.py:27
  170.1 4.1 %collective-permute-start.3 = (bf16[160,256]{1,0:T(8,128)(2,1)S(1)}, bf16[160,256]{1,0:T(8,128)(2,1)S(1)}, u32[]{:S(2)}, u32[]{:S(2)}) collective-permute-start(bf16[160,256]{1,0:T(8,128)(2,1)S(1)} %get-tuple-element.24), channel_id=1, source_target_pairs={{0,1},{1,0},{2,3},{3,2},{4,5},{5,4},{6,7},{7,6},{8,9},{9,8},{10,11... | collective-permute-start | bytes 245768 | tf_op jit(solution)/shard_map/ppermute | solution.py:19
  175.2 5.6 %collective-permute-start.4 = (bf16[2,160,256]{2,1,0:T(8,128)(2,1)S(1)}, bf16[2,160,256]{2,1,0:T(8,128)(2,1)S(1)}, u32[]{:S(2)}, u32[]{:S(2)}) collective-permute-start(bf16[2,160,256]{2,1,0:T(8,128)(2,1)S(1)} %pad_maximum_fusion.1), channel_id=1, source_target_pairs={{0,8},{8,16},{16,24},{24,0},{1,9},{9,17},{17,25},{25,1},{2,10},{10... | collective-permute-start | bytes 491528 | tf_op jit(solution)/shard_map/ppermute | solution.py:19
  180.8 3.9 %collective-permute-start.5 = (bf16[2,160,256]{2,1,0:T(8,128)(2,1)S(1)}, bf16[2,160,256]{2,1,0:T(8,128)(2,1)S(1)}, u32[]{:S(2)}, u32[]{:S(2)}) collective-permute-start(bf16[2,160,256]{2,1,0:T(8,128)(2,1)S(1)} %pad_maximum_fusion.1), channel_id=1, source_target_pairs={{0,16},{8,24},{16,0},{24,8},{1,17},{9,25},{17,1},{25,9},{2,18},{10... | collective-permute-start | bytes 491528 | tf_op jit(solution)/shard_map/ppermute | solution.py:19
  184.8 4.3 %collective-permute-start.6 = (bf16[2,160,256]{2,1,0:T(8,128)(2,1)S(1)}, bf16[2,160,256]{2,1,0:T(8,128)(2,1)S(1)}, u32[]{:S(2)}, u32[]{:S(2)}) collective-permute-start(bf16[2,160,256]{2,1,0:T(8,128)(2,1)S(1)} %pad_maximum_fusion.1), channel_id=1, source_target_pairs={{0,24},{8,0},{16,8},{24,16},{1,25},{9,1},{17,9},{25,17},{2,26},{10... | collective-permute-start | bytes 491528 | tf_op jit(solution)/shard_map/ppermute | solution.py:19
  197.6 4.7 %collective-permute-start.8 = (bf16[4,2,160,256]{3,2,1,0:T(8,128)(2,1)S(1)}, bf16[4,2,160,256]{3,2,1,0:T(8,128)(2,1)}, u32[]{:S(2)}, u32[]{:S(2)}) collective-permute-start(bf16[4,2,160,256]{3,2,1,0:T(8,128)(2,1)S(1)} %pad_maximum_fusion.refs_4_), channel_id=1, source_target_pairs={{0,4},{2,6},{4,0},{6,2},{1,5},{3,7},{5,1},{7,3},{8,12},{10,14},{12... | collective-permute-start | bytes 1966088 | tf_op jit(solution)/shard_map/ppermute | solution.py:19
  205.3 8.3 %collective-permute-done.7.refs_5_ = bf16[4,2,160,256]{3,2,1,0:T(8,128)(2,1)} collective-permute-done((bf16[4,2,160,256]{3,2,1,0:T(8,128)(2,1)S(1)}, bf16[4,2,160,256]{3,2,1,0:T(8,128)(2,1)}, u32[]{:S(2)}, u32[]{:S(2)}) %collective-permute-start.7) | collective-permute-done | bytes 655392 | tf_op jit(solution)/shard_map/ppermute | solution.py:19
  213.6 15.0 %collective-permute-done.8.refs_6_ = bf16[4,2,160,256]{3,2,1,0:T(8,128)(2,1)} collective-permute-done((bf16[4,2,160,256]{3,2,1,0:T(8,128)(2,1)S(1)}, bf16[4,2,160,256]{3,2,1,0:T(8,128)(2,1)}, u32[]{:S(2)}, u32[]{:S(2)}) %collective-permute-start.8) | collective-permute-done | bytes 655392 | tf_op jit(solution)/shard_map/ppermute | solution.py:19
  230.0 3.6 %experts.3 = (bf16[4,2,64,256]{3,2,1,0:T(8,128)(2,1)S(1)}, bf16[4,2,64,256]{3,2,1,0:T(8,128)(2,1)S(1)}, bf16[4,2,64,256]{3,2,1,0:T(8,128)(2,1)S(1)}, bf16[4,2,64,256]{3,2,1,0:T(8,128)(2,1)S(1)}) custom-call(s32[4]{0:T(128)S(1)} %pad_add_fusion.place, bf16[32,32,384]{2,1,0:T(8,128)(2,1)S(1)} %all-to-all-done.refs_0_, ...), custom_call_target="tpu_custom_call" | custom-call | tf_op jit(solution)/shard_map/experts/pallas_call | solution.py:170
  233.6 5.1 %collective-permute-start.13 = (bf16[4,2,64,256]{3,2,1,0:T(8,128)(2,1)S(1)}, bf16[4,2,64,256]{3,2,1,0:T(8,128)(2,1)S(1)}, u32[]{:S(2)}, u32[]{:S(2)}) collective-permute-start(bf16[4,2,64,256]{3,2,1,0:T(8,128)(2,1)S(1)} %get-tuple-element.17), channel_id=1, source_target_pairs={{0,2},{2,4},{4,6},{6,0},{1,3},{3,5},{5,7},{7,1},{8,10},{10,12},{12... | collective-permute-start | bytes 786440 | tf_op jit(solution)/shard_map/ppermute | solution.py:19
  238.7 3.3 collective-permute-start.14
  245.0 6.6 %collective-permute-done.14 = bf16[4,2,64,256]{3,2,1,0:T(8,128)(2,1)S(1)} collective-permute-done((bf16[4,2,64,256]{3,2,1,0:T(8,128)(2,1)S(1)}, bf16[4,2,64,256]{3,2,1,0:T(8,128)(2,1)S(1)}, u32[]{:S(2)}, u32[]{:S(2)}) %collective-permute-start.14) | collective-permute-done | bytes 262176 | tf_op jit(solution)/shard_map/ppermute | solution.py:19
  253.2 8.9 %all-to-all-start.3 = ((bf16[8,64,256]{2,1,0:T(8,128)(2,1)}), bf16[8,64,256]{2,1,0:T(8,128)(2,1)S(1)}, u32[]{:S(2)}, u32[]{:S(2)}) async-start(bf16[8,64,256]{2,1,0:T(8,128)(2,1)} %bitcast.22), calls=%async_computation.3 | async-start | bytes 524288 | tf_op jit(solution)/shard_map/all_to_all | solution.py:27
  262.1 4.0 %experts.2 = (bf16[4,2,96,256]{3,2,1,0:T(8,128)(2,1)S(1)}, bf16[4,2,96,256]{3,2,1,0:T(8,128)(2,1)S(1)}, bf16[4,2,96,256]{3,2,1,0:T(8,128)(2,1)S(1)}, bf16[4,2,96,256]{3,2,1,0:T(8,128)(2,1)S(1)}) custom-call(s32[4]{0:T(128)S(1)} %pad_add_fusion.place, bf16[32,32,384]{2,1,0:T(8,128)(2,1)S(1)} %all-to-all-done.refs_0_, ...), custom_call_target="tpu_custom_call" | custom-call | tf_op jit(solution)/shard_map/experts/pallas_call | solution.py:170
  266.2 4.1 %collective-permute-start.10 = (bf16[4,2,96,256]{3,2,1,0:T(8,128)(2,1)S(1)}, bf16[4,2,96,256]{3,2,1,0:T(8,128)(2,1)S(1)}, u32[]{:S(2)}, u32[]{:S(2)}) collective-permute-start(bf16[4,2,96,256]{3,2,1,0:T(8,128)(2,1)S(1)} %get-tuple-element.13), channel_id=1, source_target_pairs={{0,2},{2,4},{4,6},{6,0},{1,3},{3,5},{5,7},{7,1},{8,10},{10,12},{12... | collective-permute-start | bytes 1179656 | tf_op jit(solution)/shard_map/ppermute | solution.py:19
  280.0 9.3 %collective-permute-done.11 = bf16[4,2,96,256]{3,2,1,0:T(8,128)(2,1)S(1)} collective-permute-done((bf16[4,2,96,256]{3,2,1,0:T(8,128)(2,1)S(1)}, bf16[4,2,96,256]{3,2,1,0:T(8,128)(2,1)S(1)}, u32[]{:S(2)}, u32[]{:S(2)}) %collective-permute-start.11) | collective-permute-done | bytes 393248 | tf_op jit(solution)/shard_map/ppermute | solution.py:19
  291.7 6.0 %all-to-all-start.2 = ((bf16[8,96,256]{2,1,0:T(8,128)(2,1)}), bf16[8,96,256]{2,1,0:T(8,128)(2,1)S(1)}, u32[]{:S(2)}, u32[]{:S(2)}) async-start(bf16[8,96,256]{2,1,0:T(8,128)(2,1)} %bitcast.20), calls=%async_computation.2 | async-start | bytes 786432 | tf_op jit(solution)/shard_map/all_to_all | solution.py:27
  297.7 11.3 %all-to-all-done.2 = bf16[8,96,256]{2,1,0:T(8,128)(2,1)S(1)} async-done(((bf16[8,96,256]{2,1,0:T(8,128)(2,1)}), bf16[8,96,256]{2,1,0:T(8,128)(2,1)S(1)}, u32[]{:S(2)}, u32[]{:S(2)}) %all-to-all-start.2) | async-done | bytes 393248 | tf_op jit(solution)/shard_map/all_to_all | solution.py:27
  309.7 3.6 %all-to-all-start.4 = ((bf16[8,40,256]{2,1,0:T(8,128)(2,1)}), bf16[8,40,256]{2,1,0:T(8,128)(2,1)S(1)}, u32[]{:S(2)}, u32[]{:S(2)}) async-start(bf16[8,40,256]{2,1,0:T(8,128)(2,1)} %bitcast.24), calls=%async_computation.4 | async-start | bytes 327680 | tf_op jit(solution)/shard_map/all_to_all | solution.py:27
  315.7 24.4 %all-to-all-done.4.returned = bf16[8,40,256]{2,1,0:T(8,128)(2,1)S(1)} async-done(((bf16[8,40,256]{2,1,0:T(8,128)(2,1)}), bf16[8,40,256]{2,1,0:T(8,128)(2,1)S(1)}, u32[]{:S(2)}, u32[]{:S(2)}) %all-to-all-start.4) | async-done | bytes 163872 | tf_op jit(solution)/shard_map/all_to_all | solution.py:27
  (53 shorter events, 42.7 us)
Async XLA Ops:
  8.0 46.4 %copy-start.3 = (bf16[128,256]{1,0:T(8,128)(2,1)S(1)}, bf16[128,256]{1,0:T(8,128)(2,1)}, u32[]{:S(2)}) copy-start(bf16[128,256]{1,0:T(8,128)(2,1)} %tokens.1) | copy-start | bytes 196612
  8.0 46.5 %copy-start.4 = (s32[128,2]{0,1:T(2,128)S(1)}, s32[128,2]{0,1:T(2,128)}, u32[]{:S(2)}) copy-start(s32[128,2]{0,1:T(2,128)} %param.8) | copy-start | bytes 3076
  8.0 132.4 %all-to-all-start = ((bf16[32,32,384]{2,1,0:T(8,128)(2,1)}), bf16[32,32,384]{2,1,0:T(8,128)(2,1)S(1)}, u32[]{:S(2)}, u32[]{:S(2)}) async-start(bf16[32,32,384]{2,1,0:T(8,128)(2,1)} %pack.1), calls=%async_computation | async-start | bytes 1572864 | tf_op jit(solution)/shard_map/all_to_all | solution.py:27
  140.4 29.8 %all-to-all-start.1 = ((bf16[8,40,256]{2,1,0:T(8,128)(2,1)}), bf16[8,40,256]{2,1,0:T(8,128)(2,1)S(1)}, u32[]{:S(2)}, u32[]{:S(2)}) async-start(bf16[8,40,256]{2,1,0:T(8,128)(2,1)} %dispatch.1), calls=%async_computation.1 | async-start | bytes 327680 | tf_op jit(solution)/shard_map/all_to_all | solution.py:27
  144.0 48.2 %collective-permute-start = (bf16[32,32,384]{2,1,0:T(8,128)(2,1)S(1)}, bf16[32,32,384]{2,1,0:T(8,128)(2,1)S(1)}, u32[]{:S(2)}, u32[]{:S(2)}) collective-permute-start(bf16[32,32,384]{2,1,0:T(8,128)(2,1)S(1)} %all-to-all-done.refs_0_), channel_id=1, source_target_pairs={{0,256},{256,0},{1,257},{257,1},{2,258},{258,2},{3,259},{259,3},{4... | collective-permute-start | bytes 2359304 | tf_op jit(solution)/shard_map/ppermute | solution.py:19
  170.1 5.0 %collective-permute-start.3 = (bf16[160,256]{1,0:T(8,128)(2,1)S(1)}, bf16[160,256]{1,0:T(8,128)(2,1)S(1)}, u32[]{:S(2)}, u32[]{:S(2)}) collective-permute-start(bf16[160,256]{1,0:T(8,128)(2,1)S(1)} %get-tuple-element.24), channel_id=1, source_target_pairs={{0,1},{1,0},{2,3},{3,2},{4,5},{5,4},{6,7},{7,6},{8,9},{9,8},{10,11... | collective-permute-start | bytes 245768 | tf_op jit(solution)/shard_map/ppermute | solution.py:19
  175.2 19.0 %collective-permute-start.4 = (bf16[2,160,256]{2,1,0:T(8,128)(2,1)S(1)}, bf16[2,160,256]{2,1,0:T(8,128)(2,1)S(1)}, u32[]{:S(2)}, u32[]{:S(2)}) collective-permute-start(bf16[2,160,256]{2,1,0:T(8,128)(2,1)S(1)} %pad_maximum_fusion.1), channel_id=1, source_target_pairs={{0,8},{8,16},{16,24},{24,0},{1,9},{9,17},{17,25},{25,1},{2,10},{10... | collective-permute-start | bytes 491528 | tf_op jit(solution)/shard_map/ppermute | solution.py:19
  180.8 13.4 %collective-permute-start.5 = (bf16[2,160,256]{2,1,0:T(8,128)(2,1)S(1)}, bf16[2,160,256]{2,1,0:T(8,128)(2,1)S(1)}, u32[]{:S(2)}, u32[]{:S(2)}) collective-permute-start(bf16[2,160,256]{2,1,0:T(8,128)(2,1)S(1)} %pad_maximum_fusion.1), channel_id=1, source_target_pairs={{0,16},{8,24},{16,0},{24,8},{1,17},{9,25},{17,1},{25,9},{2,18},{10... | collective-permute-start | bytes 491528 | tf_op jit(solution)/shard_map/ppermute | solution.py:19
  184.8 9.4 %collective-permute-start.6 = (bf16[2,160,256]{2,1,0:T(8,128)(2,1)S(1)}, bf16[2,160,256]{2,1,0:T(8,128)(2,1)S(1)}, u32[]{:S(2)}, u32[]{:S(2)}) collective-permute-start(bf16[2,160,256]{2,1,0:T(8,128)(2,1)S(1)} %pad_maximum_fusion.1), channel_id=1, source_target_pairs={{0,24},{8,0},{16,8},{24,16},{1,25},{9,1},{17,9},{25,17},{2,26},{10... | collective-permute-start | bytes 491528 | tf_op jit(solution)/shard_map/ppermute | solution.py:19
  189.1 40.9 %collective-permute-start.1 = (bf16[32,32,384]{2,1,0:T(8,128)(2,1)S(1)}, bf16[32,32,384]{2,1,0:T(8,128)(2,1)S(1)}, u32[]{:S(2)}, u32[]{:S(2)}) collective-permute-start(bf16[32,32,384]{2,1,0:T(8,128)(2,1)S(1)} %all-to-all-done.refs_0_), channel_id=1, source_target_pairs={{0,1},{1,0},{2,3},{3,2},{4,5},{5,4},{6,7},{7,6},{8,9},{9,8},{10,11... | collective-permute-start | bytes 2359304 | tf_op jit(solution)/shard_map/ppermute | solution.py:19
  192.2 37.8 %collective-permute-start.2 = (bf16[32,32,384]{2,1,0:T(8,128)(2,1)S(1)}, bf16[32,32,384]{2,1,0:T(8,128)(2,1)}, u32[]{:S(2)}, u32[]{:S(2)}) collective-permute-start(bf16[32,32,384]{2,1,0:T(8,128)(2,1)S(1)} %collective-permute-done.refs_1_), channel_id=1, source_target_pairs={{0,1},{1,0},{2,3},{3,2},{4,5},{5,4},{6,7},{7,6},{8,9},{9,8},{10,11... | collective-permute-start | bytes 2359304 | tf_op jit(solution)/shard_map/ppermute | solution.py:19
  194.3 19.3 %collective-permute-start.7 = (bf16[4,2,160,256]{3,2,1,0:T(8,128)(2,1)S(1)}, bf16[4,2,160,256]{3,2,1,0:T(8,128)(2,1)}, u32[]{:S(2)}, u32[]{:S(2)}) collective-permute-start(bf16[4,2,160,256]{3,2,1,0:T(8,128)(2,1)S(1)} %pad_maximum_fusion.refs_4_), channel_id=1, source_target_pairs={{0,2},{2,4},{4,6},{6,0},{1,3},{3,5},{5,7},{7,1},{8,10},{10,12},{12... | collective-permute-start | bytes 1966088 | tf_op jit(solution)/shard_map/ppermute | solution.py:19
  197.6 31.0 %collective-permute-start.8 = (bf16[4,2,160,256]{3,2,1,0:T(8,128)(2,1)S(1)}, bf16[4,2,160,256]{3,2,1,0:T(8,128)(2,1)}, u32[]{:S(2)}, u32[]{:S(2)}) collective-permute-start(bf16[4,2,160,256]{3,2,1,0:T(8,128)(2,1)S(1)} %pad_maximum_fusion.refs_4_), channel_id=1, source_target_pairs={{0,4},{2,6},{4,0},{6,2},{1,5},{3,7},{5,1},{7,3},{8,12},{10,14},{12... | collective-permute-start | bytes 1966088 | tf_op jit(solution)/shard_map/ppermute | solution.py:19
  202.3 27.7 %collective-permute-start.9 = (bf16[4,2,160,256]{3,2,1,0:T(8,128)(2,1)S(1)}, bf16[4,2,160,256]{3,2,1,0:T(8,128)(2,1)}, u32[]{:S(2)}, u32[]{:S(2)}) collective-permute-start(bf16[4,2,160,256]{3,2,1,0:T(8,128)(2,1)S(1)} %pad_maximum_fusion.refs_4_), channel_id=1, source_target_pairs={{0,6},{2,0},{4,2},{6,4},{1,7},{3,1},{5,3},{7,5},{8,14},{10,8},{12,... | collective-permute-start | bytes 1966088 | tf_op jit(solution)/shard_map/ppermute | solution.py:19
  233.6 11.5 %collective-permute-start.13 = (bf16[4,2,64,256]{3,2,1,0:T(8,128)(2,1)S(1)}, bf16[4,2,64,256]{3,2,1,0:T(8,128)(2,1)S(1)}, u32[]{:S(2)}, u32[]{:S(2)}) collective-permute-start(bf16[4,2,64,256]{3,2,1,0:T(8,128)(2,1)S(1)} %get-tuple-element.17), channel_id=1, source_target_pairs={{0,2},{2,4},{4,6},{6,0},{1,3},{3,5},{5,7},{7,1},{8,10},{10,12},{12... | collective-permute-start | bytes 786440 | tf_op jit(solution)/shard_map/ppermute | solution.py:19
  238.7 12.9 %collective-permute-start.14 = (bf16[4,2,64,256]{3,2,1,0:T(8,128)(2,1)S(1)}, bf16[4,2,64,256]{3,2,1,0:T(8,128)(2,1)S(1)}, u32[]{:S(2)}, u32[]{:S(2)}) collective-permute-start(bf16[4,2,64,256]{3,2,1,0:T(8,128)(2,1)S(1)} %get-tuple-element.18), channel_id=1, source_target_pairs={{0,4},{2,6},{4,0},{6,2},{1,5},{3,7},{5,1},{7,3},{8,12},{10,14},{12... | collective-permute-start | bytes 786440 | tf_op jit(solution)/shard_map/ppermute | solution.py:19
  242.1 10.3 %collective-permute-start.15 = (bf16[4,2,64,256]{3,2,1,0:T(8,128)(2,1)S(1)}, bf16[4,2,64,256]{3,2,1,0:T(8,128)(2,1)S(1)}, u32[]{:S(2)}, u32[]{:S(2)}) collective-permute-start(bf16[4,2,64,256]{3,2,1,0:T(8,128)(2,1)S(1)} %get-tuple-element.19), channel_id=1, source_target_pairs={{0,6},{2,0},{4,2},{6,4},{1,7},{3,1},{5,3},{7,5},{8,14},{10,8},{12,... | collective-permute-start | bytes 786440 | tf_op jit(solution)/shard_map/ppermute | solution.py:19
  253.2 38.4 %all-to-all-start.3 = ((bf16[8,64,256]{2,1,0:T(8,128)(2,1)}), bf16[8,64,256]{2,1,0:T(8,128)(2,1)S(1)}, u32[]{:S(2)}, u32[]{:S(2)}) async-start(bf16[8,64,256]{2,1,0:T(8,128)(2,1)} %bitcast.22), calls=%async_computation.3 | async-start | bytes 524288 | tf_op jit(solution)/shard_map/all_to_all | solution.py:27
  266.2 13.8 %collective-permute-start.10 = (bf16[4,2,96,256]{3,2,1,0:T(8,128)(2,1)S(1)}, bf16[4,2,96,256]{3,2,1,0:T(8,128)(2,1)S(1)}, u32[]{:S(2)}, u32[]{:S(2)}) collective-permute-start(bf16[4,2,96,256]{3,2,1,0:T(8,128)(2,1)S(1)} %get-tuple-element.13), channel_id=1, source_target_pairs={{0,2},{2,4},{4,6},{6,0},{1,3},{3,5},{5,7},{7,1},{8,10},{10,12},{12... | collective-permute-start | bytes 1179656 | tf_op jit(solution)/shard_map/ppermute | solution.py:19
  270.3 19.0 %collective-permute-start.11 = (bf16[4,2,96,256]{3,2,1,0:T(8,128)(2,1)S(1)}, bf16[4,2,96,256]{3,2,1,0:T(8,128)(2,1)S(1)}, u32[]{:S(2)}, u32[]{:S(2)}) collective-permute-start(bf16[4,2,96,256]{3,2,1,0:T(8,128)(2,1)S(1)} %get-tuple-element.14), channel_id=1, source_target_pairs={{0,4},{2,6},{4,0},{6,2},{1,5},{3,7},{5,1},{7,3},{8,12},{10,14},{12... | collective-permute-start | bytes 1179656 | tf_op jit(solution)/shard_map/ppermute | solution.py:19
  273.6 17.0 %collective-permute-start.12 = (bf16[4,2,96,256]{3,2,1,0:T(8,128)(2,1)S(1)}, bf16[4,2,96,256]{3,2,1,0:T(8,128)(2,1)S(1)}, u32[]{:S(2)}, u32[]{:S(2)}) collective-permute-start(bf16[4,2,96,256]{3,2,1,0:T(8,128)(2,1)S(1)} %get-tuple-element.15), channel_id=1, source_target_pairs={{0,6},{2,0},{4,2},{6,4},{1,7},{3,1},{5,3},{7,5},{8,14},{10,8},{12,... | collective-permute-start | bytes 1179656 | tf_op jit(solution)/shard_map/ppermute | solution.py:19
  291.7 21.9 %copy-start.6 = (f32[128,2]{0,1:T(2,128)S(1)}, f32[128,2]{0,1:T(2,128)}, u32[]{:S(2)}) copy-start(f32[128,2]{0,1:T(2,128)} %param.9) | copy-start | bytes 3076
  291.7 17.3 %all-to-all-start.2 = ((bf16[8,96,256]{2,1,0:T(8,128)(2,1)}), bf16[8,96,256]{2,1,0:T(8,128)(2,1)S(1)}, u32[]{:S(2)}, u32[]{:S(2)}) async-start(bf16[8,96,256]{2,1,0:T(8,128)(2,1)} %bitcast.20), calls=%async_computation.2 | async-start | bytes 786432 | tf_op jit(solution)/shard_map/all_to_all | solution.py:27
  309.7 30.3 %all-to-all-start.4 = ((bf16[8,40,256]{2,1,0:T(8,128)(2,1)}), bf16[8,40,256]{2,1,0:T(8,128)(2,1)S(1)}, u32[]{:S(2)}, u32[]{:S(2)}) async-start(bf16[8,40,256]{2,1,0:T(8,128)(2,1)} %bitcast.24), calls=%async_computation.4 | async-start | bytes 327680 | tf_op jit(solution)/shard_map/all_to_all | solution.py:27
  (4 other events, 4.3 us)

commit v5 on v4

--- a/solution.py
+++ b/solution.py
@@ -59,7 +59,6 @@
             in_specs=[pl.BlockSpec((1, rows), lambda e, turn: (0, 0)), block, block, block],
             out_specs=pl.BlockSpec((copies, part, 3 * width), lambda e, turn: (e, 0, 0)),
         ),
-        compiler_params=vmem(12),
         name="pack",
     )(position_of("grp"), norm_gain.reshape(1, rows), gate_weight, up_weight, down_weight)
 
@@ -95,17 +94,16 @@
     return pl.pallas_call(
         dispatch_kernel,
         out_shape=jax.ShapeDtypeStruct((experts, capacity, tokens.shape[1]), jnp.bfloat16),
-        compiler_params=vmem(12),
         name="dispatch",
     )(routes.T, tokens)
 
 
-def expert_kernel(span, count, place, *refs):
+def expert_kernel(span, count, groups, whole, place, *refs):
     first, share = span
-    total, assembled = len(refs), refs[-2:]
-    parts, outs = refs[total - 2 - 2 * count : total - 2 - count], refs[total - 2 - count : -2]
-    pieces = refs[: total - 2 - 2 * count]
-    groups = len(pieces) // 2
+    pieces, parts = refs[: 2 * groups], refs[2 * groups : 2 * groups + count]
+    outs, assembled = refs[2 * groups + count : -2], refs[-2:]
+    if whole:
+        outs = [outs[0].at[k] for k in range(count)]
     copies, halves, _, cols = parts[0].shape
     part, width = pieces[0].shape[1], pieces[0].shape[2] // 3
     rows = copies * share
@@ -114,9 +112,9 @@
         for held, piece in zip(assembled, (pieces[k], pieces[groups + k])):
             held[:, pl.ds(index, 1)] = piece[...][:, None]
 
-    def block(held, k, c, start, end):
+    def block(held, k, c, start, end, origin=place[0]):
         sources = cols // (groups * part)
-        at = (lax.rem(place[0] + k, count) * halves + c) * sources
+        at = (lax.rem(origin + k, count) * halves + c) * sources
         return held[pl.ds(at, sources), :, :, start:end].reshape(cols, end - start)
 
     sums = [jnp.zeros((rows, 2 * width), jnp.float32) for _ in range(2)]
@@ -147,7 +145,11 @@
     for k, out in enumerate(outs):
         for c in range(halves):
             down = jnp.concatenate(
-                [block(held, k, c, 2 * width, 3 * width) for held in assembled], axis=1
+                [
+                    block(held, k, c, 2 * width, 3 * width, 0 if whole else place[0])
+                    for held in assembled
+                ],
+                axis=1,
             )
             value = lax.dot_general(
                 hidden, down, (((1,), (1,)), ((), ())), preferred_element_type=jnp.float32
@@ -161,20 +163,22 @@
     return pl.BlockSpec(value.shape, lambda t, place, rank=len(value.shape): (0,) * rank)
 
 
-def expert_outputs(pieces, parts, span):
+def expert_outputs(pieces, parts, span, whole):
     copies, halves, _, cols = parts[0].shape
     sources, part, triple = pieces[0].shape
-    out = jax.ShapeDtypeStruct((copies, halves, span[1], cols), jnp.bfloat16)
+    size = (copies, halves, span[1], cols)
+    size = (len(parts), *size) if whole else size
+    outs = [jax.ShapeDtypeStruct(size, jnp.bfloat16)] * (1 if whole else len(parts))
     inputs = (*pieces, *parts)
     held = pltpu.VMEM((sources, len(pieces) // 2, part, triple), jnp.bfloat16)
     return pl.pallas_call(
-        functools.partial(expert_kernel, span, len(parts)),
-        out_shape=[out] * len(parts),
+        functools.partial(expert_kernel, span, len(parts), len(pieces) // 2, whole),
+        out_shape=outs,
         grid_spec=pltpu.PrefetchScalarGridSpec(
             num_scalar_prefetch=1,
             grid=(1,),
             in_specs=[whole_block(value) for value in inputs],
-            out_specs=[whole_block(out)] * len(parts),
+            out_specs=[whole_block(out) for out in outs],
             scratch_shapes=[held, held],
         ),
         compiler_params=vmem(32),
@@ -251,17 +255,17 @@
     return weights.reshape(sources * rows, triple)
 
 
-def halved(arrived):
-    experts, capacity, cols = arrived.shape
+def halved(blocks):
+    copies, slots, cols = blocks.shape
     cores = lax.axis_size("tp_c")
-    arrived = arrived.reshape(cores, experts * capacity // cores, cols)
+    blocks = blocks.reshape(copies, cores, slots // cores, cols)
     halves = []
     for j in range(cores):
         half = lax.dynamic_index_in_dim(
-            arrived, lax.rem(lax.axis_index("tp_c") + j, cores), axis=0, keepdims=False
+            blocks, lax.rem(lax.axis_index("tp_c") + j, cores), axis=1, keepdims=False
         )
         halves.append(half if j == 0 else shifted(half, "tp_c", j))
-    return jnp.stack(halves)
+    return jnp.stack(halves, axis=1)
 
 
 def on_device(tokens, routes, route_weights, norm_gain, gate_weight, up_weight, down_weight):
@@ -270,14 +274,14 @@
     row_count, col_width = tokens.shape
     capacity = row_count * 5 // 16
     share = experts * capacity // lax.axis_size("tp_c")
-    cut = share * 5 // 8 // 32 * 32
+    cut = share // 2
     spans = ((0, cut), (cut, share - cut))
 
     outgoing = dispatched(tokens, routes, experts, capacity)
     arrived = exchange(outgoing, "fs_hi")
-    block = lax.optimization_barrier(halved(arrived))
+    block = arrived.reshape(experts * capacity, col_width)
     blocks = [block] + [shifted(block, "fs_lo", k) for k in range(1, copies)]
-    blocks = jnp.stack(blocks)
+    blocks = halved(jnp.stack(blocks))
     parts = [blocks] + [
         shifted(blocks, "tp_x", k) for k in range(1, lax.axis_size("tp_x"))
     ]
@@ -289,9 +293,13 @@
     chosen = chosen_slots(routes, experts * capacity)
 
     sums = []
-    for span in spans:
-        outs = expert_outputs(own + other, parts, span)
-        got = [outs[0]] + [shifted(outs[k], "tp_x", k) for k in range(1, len(outs))]
+    for t, span in enumerate(spans):
+        outs = expert_outputs(own + other, parts, span, t == 0)
+        if t == 0:
+            arrived = exchange(outs[0], "tp_x")
+            got = [arrived[k] for k in range(len(parts))]
+        else:
+            got = [outs[0]] + [shifted(outs[k], "tp_x", k) for k in range(1, len(outs))]
         over_x = sum(value.astype(jnp.float32) for value in got).astype(jnp.bfloat16)
         sent = exchange(over_x.reshape(-1, *over_x.shape[2:]), ("fs_lo", "tp_c"))
         over_s = jnp.sum(sent.reshape(over_x.shape), axis=0, dtype=jnp.float32)

time: 347 us -> 343 us (0.988)
  starting transfers between devices: 128 us -> 122 us
  Pallas kernels: 12.7 us -> 17.1 us
  local copies, waits for them, and re-layouts: 6.44 us -> 2.16 us
  waiting for transfers between devices: 190 us -> 194 us
    ppermute x16 -> x13, starting transfers between devices: 59.9 us -> 49.9 us  [shifted(): lax.ppermute(value, axis, [(k, (k + step) % count) for k in range(count)])]
    all_to_all x5 -> x6, waiting for transfers between devices: 143 us -> 150 us  [exchange(): return lax.all_to_all(value, axis, split_axis=0, concat_axis=0, tiled=True)]
    unnamed x15 -> x5, local copies, waits for them, and re-layouts: 4.45 us -> 0.12 us
    all_to_all x5 -> x6, starting transfers between devices: 68.5 us -> 71.6 us  [exchange(): return lax.all_to_all(value, axis, split_axis=0, concat_axis=0, tiled=True)]
    ppermute x16 -> x13, waiting for transfers between devices: 46.7 us -> 44.9 us  [shifted(): lax.ppermute(value, axis, [(k, (k + step) % count) for k in range(count)])]
  transfers between devices with their start and end apart: 21 -> 19, of which waited for: 13 -> 12; matrix products, arithmetic and copies ran while one was open for 1% -> 2% of each run, Pallas kernels for 2% -> 2%
where the time goes in v5:
time: 343 us; the launch traced here: 340 us
  waiting for transfers between devices  194 us (57%)
  starting transfers between devices  122 us (36%)
  Pallas kernels  17.1 us (5%)
  other arithmetic  4.05 us (1%)
    all_to_all x6, waiting for transfers between devices, exchange(): return lax.all_to_all(value, axis, split_axis=0, concat_axis=0, tiled=True)  150 us
    all_to_all x6, starting transfers between devices, exchange(): return lax.all_to_all(value, axis, split_axis=0, concat_axis=0, tiled=True)  71.6 us
    ppermute x13, starting transfers between devices, shifted(): lax.ppermute(value, axis, [(k, (k + step) % count) for k in range(count)])  49.9 us
    ppermute x13, waiting for transfers between devices, shifted(): lax.ppermute(value, axis, [(k, (k + step) % count) for k in range(count)])  44.9 us
    pallas_call x2, Pallas kernels, expert_outputs(): pl.pallas_call(functools.partial(expert_kernel, span, len(parts), len(pie...  8.69 us
  transfers between devices with their start and end apart: 19, of which 12 were waited for; matrix products, arithmetic and copies ran while one was open for 2% of the time, Pallas kernels for 2%

profile of v5, /device:TPU:33, one launch (start us, length us, event | category | flops | bytes accessed | tf_op | source)
XLA Modules:
  0.0 340.2 jit_solution(16488237355133198122)
XLA Ops:
  0.6 5.5 %pack.1 = bf16[32,32,384]{2,1,0:T(8,128)(2,1)} custom-call(s32[1]{0:T(128)} %bitcast.turn.place, f32[1,64]{1,0:T(1,128)} %bitcast.45, f32[8,64,512]{2,1,0:T(8,128)} %gate.1, f32[8,64,512]{2,1,0:T(8,128)} %up.1, f32[8,64,512]{2,1,0:T(8,128)} %down.1), custom_call_target="tpu_custom_call" | custom-call | tf_op jit(solution)/shard_map/pack/pallas_call | solution.py:53
  6.1 46.3 %all-to-all-start = ((bf16[32,32,384]{2,1,0:T(8,128)(2,1)}), bf16[32,32,384]{2,1,0:T(8,128)(2,1)S(1)}, u32[]{:S(2)}, u32[]{:S(2)}) async-start(bf16[32,32,384]{2,1,0:T(8,128)(2,1)} %pack.1), calls=%async_computation | async-start | bytes 1572864 | tf_op jit(solution)/shard_map/all_to_all | solution.py:27
  54.3 84.1 %all-to-all-done.refs_0_ = bf16[32,32,384]{2,1,0:T(8,128)(2,1)S(1)} async-done(((bf16[32,32,384]{2,1,0:T(8,128)(2,1)}), bf16[32,32,384]{2,1,0:T(8,128)(2,1)S(1)}, u32[]{:S(2)}, u32[]{:S(2)}) %all-to-all-start) | async-done | bytes 786464 | tf_op jit(solution)/shard_map/all_to_all | solution.py:27
  138.3 3.6 %all-to-all-start.1 = ((bf16[8,40,256]{2,1,0:T(8,128)(2,1)}), bf16[8,40,256]{2,1,0:T(8,128)(2,1)S(1)}, u32[]{:S(2)}, u32[]{:S(2)}) async-start(bf16[8,40,256]{2,1,0:T(8,128)(2,1)} %dispatch.1), calls=%async_computation.1 | async-start | bytes 327680 | tf_op jit(solution)/shard_map/all_to_all | solution.py:27
  141.9 3.8 %collective-permute-start = (bf16[32,32,384]{2,1,0:T(8,128)(2,1)S(1)}, bf16[32,32,384]{2,1,0:T(8,128)(2,1)S(1)}, u32[]{:S(2)}, u32[]{:S(2)}) collective-permute-start(bf16[32,32,384]{2,1,0:T(8,128)(2,1)S(1)} %all-to-all-done.refs_0_), channel_id=1, source_target_pairs={{0,256},{256,0},{1,257},{257,1},{2,258},{258,2},{3,259},{259,3},{4... | collective-permute-start | bytes 2359304 | tf_op jit(solution)/shard_map/ppermute | solution.py:19
  145.7 22.4 %all-to-all-done.1 = bf16[8,40,256]{2,1,0:T(8,128)(2,1)S(1)} async-done(((bf16[8,40,256]{2,1,0:T(8,128)(2,1)}), bf16[8,40,256]{2,1,0:T(8,128)(2,1)S(1)}, u32[]{:S(2)}, u32[]{:S(2)}) %all-to-all-start.1) | async-done | bytes 163872 | tf_op jit(solution)/shard_map/all_to_all | solution.py:27
  170.0 9.2 %collective-permute-start.4 = (bf16[320,256]{1,0:T(8,128)(2,1)S(1)}, bf16[320,256]{1,0:T(8,128)(2,1)S(1)}, u32[]{:S(2)}, u32[]{:S(2)}) collective-permute-start(bf16[320,256]{1,0:T(8,128)(2,1)S(1)} %bitcast.38), channel_id=1, source_target_pairs={{0,16},{8,24},{16,0},{24,8},{1,17},{9,25},{17,1},{25,9},{2,18},{10... | collective-permute-start | bytes 491528 | tf_op jit(solution)/shard_map/ppermute | solution.py:19
  179.3 4.3 %collective-permute-start.5 = (bf16[320,256]{1,0:T(8,128)(2,1)S(1)}, bf16[320,256]{1,0:T(8,128)(2,1)S(1)}, u32[]{:S(2)}, u32[]{:S(2)}) collective-permute-start(bf16[320,256]{1,0:T(8,128)(2,1)S(1)} %bitcast.39), channel_id=1, source_target_pairs={{0,24},{8,0},{16,8},{24,16},{1,25},{9,1},{17,9},{25,17},{2,26},{10... | collective-permute-start | bytes 491528 | tf_op jit(solution)/shard_map/ppermute | solution.py:19
  186.5 4.6 %collective-permute-start.6 = (bf16[4,160,256]{2,1,0:T(8,128)(2,1)S(1)}, bf16[4,160,256]{2,1,0:T(8,128)(2,1)S(1)}, u32[]{:S(2)}, u32[]{:S(2)}) collective-permute-start(bf16[4,160,256]{2,1,0:T(8,128)(2,1)S(1)} %get-tuple-element.16), channel_id=1, source_target_pairs={{0,1},{1,0},{2,3},{3,2},{4,5},{5,4},{6,7},{7,6},{8,9},{9,8},{10,11... | collective-permute-start | bytes 983048 | tf_op jit(solution)/shard_map/ppermute | solution.py:19
  198.9 4.7 %collective-permute-start.8 = (bf16[4,2,160,256]{3,2,1,0:T(8,128)(2,1)S(1)}, bf16[4,2,160,256]{3,2,1,0:T(8,128)(2,1)}, u32[]{:S(2)}, u32[]{:S(2)}) collective-permute-start(bf16[4,2,160,256]{3,2,1,0:T(8,128)(2,1)S(1)} %pad_maximum_fusion.1.refs_4_), channel_id=1, source_target_pairs={{0,4},{2,6},{4,0},{6,2},{1,5},{3,7},{5,1},{7,3},{8,12},{10,14},{12... | collective-permute-start | bytes 1966088 | tf_op jit(solution)/shard_map/ppermute | solution.py:19
  206.6 8.9 %collective-permute-done.7.refs_5_ = bf16[4,2,160,256]{3,2,1,0:T(8,128)(2,1)} collective-permute-done((bf16[4,2,160,256]{3,2,1,0:T(8,128)(2,1)S(1)}, bf16[4,2,160,256]{3,2,1,0:T(8,128)(2,1)}, u32[]{:S(2)}, u32[]{:S(2)}) %collective-permute-start.7) | collective-permute-done | bytes 655392 | tf_op jit(solution)/shard_map/ppermute | solution.py:19
  215.6 15.0 %collective-permute-done.8.refs_6_ = bf16[4,2,160,256]{3,2,1,0:T(8,128)(2,1)} collective-permute-done((bf16[4,2,160,256]{3,2,1,0:T(8,128)(2,1)S(1)}, bf16[4,2,160,256]{3,2,1,0:T(8,128)(2,1)}, u32[]{:S(2)}, u32[]{:S(2)}) %collective-permute-start.8) | collective-permute-done | bytes 655392 | tf_op jit(solution)/shard_map/ppermute | solution.py:19
  231.9 4.9 %experts.2 = bf16[4,4,2,80,256]{4,3,2,1,0:T(8,128)(2,1)} custom-call(s32[4]{0:T(128)S(1)} %pad_add_fusion.place, bf16[32,32,384]{2,1,0:T(8,128)(2,1)S(1)} %all-to-all-done.refs_0_, bf16[32,32,384]{2,1,0:T(8,128)(2,1)S(1)} %collective-permute-done.refs_1_, bf16[32,32,384]{2,1,0:T(8,128)(2,1)S(1)} %collective-permute-done.1.refs_2_, ...), custom_call_target="tpu_custom_call" | custom-call | tf_op jit(solution)/shard_map/experts/pallas_call | solution.py:174
  236.8 4.4 %all-to-all-start.2 = ((bf16[4,4,2,80,256]{4,3,2,1,0:T(8,128)(2,1)}), bf16[4,4,2,80,256]{4,3,2,1,0:T(8,128)(2,1)}, u32[]{:S(2)}, u32[]{:S(2)}) async-start(bf16[4,4,2,80,256]{4,3,2,1,0:T(8,128)(2,1)} %experts.2), calls=%async_computation.2 | async-start | bytes 2621440 | tf_op jit(solution)/shard_map/all_to_all | solution.py:27
  241.2 3.8 %experts.3 = (bf16[4,2,80,256]{3,2,1,0:T(8,128)(2,1)S(1)}, bf16[4,2,80,256]{3,2,1,0:T(8,128)(2,1)S(1)}, bf16[4,2,80,256]{3,2,1,0:T(8,128)(2,1)S(1)}, bf16[4,2,80,256]{3,2,1,0:T(8,128)(2,1)S(1)}) custom-call(s32[4]{0:T(128)S(1)} %pad_add_fusion.place, bf16[32,32,384]{2,1,0:T(8,128)(2,1)S(1)} %all-to-all-done.refs_0_, ...), custom_call_target="tpu_custom_call" | custom-call | tf_op jit(solution)/shard_map/experts/pallas_call | solution.py:174
  245.0 4.5 %collective-permute-start.10 = (bf16[4,2,80,256]{3,2,1,0:T(8,128)(2,1)S(1)}, bf16[4,2,80,256]{3,2,1,0:T(8,128)(2,1)S(1)}, u32[]{:S(2)}, u32[]{:S(2)}) collective-permute-start(bf16[4,2,80,256]{3,2,1,0:T(8,128)(2,1)S(1)} %get-tuple-element.9), channel_id=1, source_target_pairs={{0,2},{2,4},{4,6},{6,0},{1,3},{3,5},{5,7},{7,1},{8,10},{10,12},{12... | collective-permute-start | bytes 983048 | tf_op jit(solution)/shard_map/ppermute | solution.py:19
  255.8 9.2 %collective-permute-done.10 = bf16[4,2,80,256]{3,2,1,0:T(8,128)(2,1)S(1)} collective-permute-done((bf16[4,2,80,256]{3,2,1,0:T(8,128)(2,1)S(1)}, bf16[4,2,80,256]{3,2,1,0:T(8,128)(2,1)S(1)}, u32[]{:S(2)}, u32[]{:S(2)}) %collective-permute-start.10) | collective-permute-done | bytes 327712 | tf_op jit(solution)/shard_map/ppermute | solution.py:19
  265.0 7.1 %collective-permute-done.11 = bf16[4,2,80,256]{3,2,1,0:T(8,128)(2,1)S(1)} collective-permute-done((bf16[4,2,80,256]{3,2,1,0:T(8,128)(2,1)S(1)}, bf16[4,2,80,256]{3,2,1,0:T(8,128)(2,1)S(1)}, u32[]{:S(2)}, u32[]{:S(2)}) %collective-permute-start.11) | collective-permute-done | bytes 327712 | tf_op jit(solution)/shard_map/ppermute | solution.py:19
  273.5 9.3 %all-to-all-start.4 = ((bf16[8,80,256]{2,1,0:T(8,128)(2,1)}), bf16[8,80,256]{2,1,0:T(8,128)(2,1)S(1)}, u32[]{:S(2)}, u32[]{:S(2)}) async-start(bf16[8,80,256]{2,1,0:T(8,128)(2,1)} %bitcast.22), calls=%async_computation.4 | async-start | bytes 655360 | tf_op jit(solution)/shard_map/all_to_all | solution.py:27
  285.0 7.8 %all-to-all-done.4 = bf16[8,80,256]{2,1,0:T(8,128)(2,1)S(1)} async-done(((bf16[8,80,256]{2,1,0:T(8,128)(2,1)}), bf16[8,80,256]{2,1,0:T(8,128)(2,1)S(1)}, u32[]{:S(2)}, u32[]{:S(2)}) %all-to-all-start.4) | async-done | bytes 327712 | tf_op jit(solution)/shard_map/all_to_all | solution.py:27
  292.8 4.5 %all-to-all-start.3 = ((bf16[8,80,256]{2,1,0:T(8,128)(2,1)}), bf16[8,80,256]{2,1,0:T(8,128)(2,1)S(1)}, u32[]{:S(2)}, u32[]{:S(2)}) async-start(bf16[8,80,256]{2,1,0:T(8,128)(2,1)} %bitcast.20), calls=%async_computation.3 | async-start | bytes 655360 | tf_op jit(solution)/shard_map/all_to_all | solution.py:27
  297.4 10.0 %all-to-all-done.3 = bf16[8,80,256]{2,1,0:T(8,128)(2,1)S(1)} async-done(((bf16[8,80,256]{2,1,0:T(8,128)(2,1)}), bf16[8,80,256]{2,1,0:T(8,128)(2,1)S(1)}, u32[]{:S(2)}, u32[]{:S(2)}) %all-to-all-start.3) | async-done | bytes 327712 | tf_op jit(solution)/shard_map/all_to_all | solution.py:27
  308.1 3.6 %all-to-all-start.5 = ((bf16[8,40,256]{2,1,0:T(8,128)(2,1)}), bf16[8,40,256]{2,1,0:T(8,128)(2,1)S(1)}, u32[]{:S(2)}, u32[]{:S(2)}) async-start(bf16[8,40,256]{2,1,0:T(8,128)(2,1)} %bitcast.24), calls=%async_computation.5 | async-start | bytes 327680 | tf_op jit(solution)/shard_map/all_to_all | solution.py:27
  314.1 25.3 %all-to-all-done.5.returned = bf16[8,40,256]{2,1,0:T(8,128)(2,1)S(1)} async-done(((bf16[8,40,256]{2,1,0:T(8,128)(2,1)}), bf16[8,40,256]{2,1,0:T(8,128)(2,1)S(1)}, u32[]{:S(2)}, u32[]{:S(2)}) %all-to-all-start.5) | async-done | bytes 163872 | tf_op jit(solution)/shard_map/all_to_all | solution.py:27
  (39 shorter events, 32.6 us)
Async XLA Ops:
  6.1 132.2 %all-to-all-start = ((bf16[32,32,384]{2,1,0:T(8,128)(2,1)}), bf16[32,32,384]{2,1,0:T(8,128)(2,1)S(1)}, u32[]{:S(2)}, u32[]{:S(2)}) async-start(bf16[32,32,384]{2,1,0:T(8,128)(2,1)} %pack.1), calls=%async_computation | async-start | bytes 1572864 | tf_op jit(solution)/shard_map/all_to_all | solution.py:27
  138.3 29.8 %all-to-all-start.1 = ((bf16[8,40,256]{2,1,0:T(8,128)(2,1)}), bf16[8,40,256]{2,1,0:T(8,128)(2,1)S(1)}, u32[]{:S(2)}, u32[]{:S(2)}) async-start(bf16[8,40,256]{2,1,0:T(8,128)(2,1)} %dispatch.1), calls=%async_computation.1 | async-start | bytes 327680 | tf_op jit(solution)/shard_map/all_to_all | solution.py:27
  141.9 51.1 %collective-permute-start = (bf16[32,32,384]{2,1,0:T(8,128)(2,1)S(1)}, bf16[32,32,384]{2,1,0:T(8,128)(2,1)S(1)}, u32[]{:S(2)}, u32[]{:S(2)}) collective-permute-start(bf16[32,32,384]{2,1,0:T(8,128)(2,1)S(1)} %all-to-all-done.refs_0_), channel_id=1, source_target_pairs={{0,256},{256,0},{1,257},{257,1},{2,258},{258,2},{3,259},{259,3},{4... | collective-permute-start | bytes 2359304 | tf_op jit(solution)/shard_map/ppermute | solution.py:19
  168.1 15.5 %collective-permute-start.3 = (bf16[320,256]{1,0:T(8,128)(2,1)S(1)}, bf16[320,256]{1,0:T(8,128)(2,1)S(1)}, u32[]{:S(2)}, u32[]{:S(2)}) collective-permute-start(bf16[320,256]{1,0:T(8,128)(2,1)S(1)} %bitcast.37), channel_id=1, source_target_pairs={{0,8},{8,16},{16,24},{24,0},{1,9},{9,17},{17,25},{25,1},{2,10},{10... | collective-permute-start | bytes 491528 | tf_op jit(solution)/shard_map/ppermute | solution.py:19
  170.0 13.6 %collective-permute-start.4 = (bf16[320,256]{1,0:T(8,128)(2,1)S(1)}, bf16[320,256]{1,0:T(8,128)(2,1)S(1)}, u32[]{:S(2)}, u32[]{:S(2)}) collective-permute-start(bf16[320,256]{1,0:T(8,128)(2,1)S(1)} %bitcast.38), channel_id=1, source_target_pairs={{0,16},{8,24},{16,0},{24,8},{1,17},{9,25},{17,1},{25,9},{2,18},{10... | collective-permute-start | bytes 491528 | tf_op jit(solution)/shard_map/ppermute | solution.py:19
  179.3 7.1 %collective-permute-start.5 = (bf16[320,256]{1,0:T(8,128)(2,1)S(1)}, bf16[320,256]{1,0:T(8,128)(2,1)S(1)}, u32[]{:S(2)}, u32[]{:S(2)}) collective-permute-start(bf16[320,256]{1,0:T(8,128)(2,1)S(1)} %bitcast.39), channel_id=1, source_target_pairs={{0,24},{8,0},{16,8},{24,16},{1,25},{9,1},{17,9},{25,17},{2,26},{10... | collective-permute-start | bytes 491528 | tf_op jit(solution)/shard_map/ppermute | solution.py:19
  186.5 9.0 %collective-permute-start.6 = (bf16[4,160,256]{2,1,0:T(8,128)(2,1)S(1)}, bf16[4,160,256]{2,1,0:T(8,128)(2,1)S(1)}, u32[]{:S(2)}, u32[]{:S(2)}) collective-permute-start(bf16[4,160,256]{2,1,0:T(8,128)(2,1)S(1)} %get-tuple-element.16), channel_id=1, source_target_pairs={{0,1},{1,0},{2,3},{3,2},{4,5},{5,4},{6,7},{7,6},{8,9},{9,8},{10,11... | collective-permute-start | bytes 983048 | tf_op jit(solution)/shard_map/ppermute | solution.py:19
  191.1 40.8 %collective-permute-start.1 = (bf16[32,32,384]{2,1,0:T(8,128)(2,1)S(1)}, bf16[32,32,384]{2,1,0:T(8,128)(2,1)S(1)}, u32[]{:S(2)}, u32[]{:S(2)}) collective-permute-start(bf16[32,32,384]{2,1,0:T(8,128)(2,1)S(1)} %all-to-all-done.refs_0_), channel_id=1, source_target_pairs={{0,1},{1,0},{2,3},{3,2},{4,5},{5,4},{6,7},{7,6},{8,9},{9,8},{10,11... | collective-permute-start | bytes 2359304 | tf_op jit(solution)/shard_map/ppermute | solution.py:19
  193.1 38.8 %collective-permute-start.2 = (bf16[32,32,384]{2,1,0:T(8,128)(2,1)S(1)}, bf16[32,32,384]{2,1,0:T(8,128)(2,1)}, u32[]{:S(2)}, u32[]{:S(2)}) collective-permute-start(bf16[32,32,384]{2,1,0:T(8,128)(2,1)S(1)} %collective-permute-done.refs_1_), channel_id=1, source_target_pairs={{0,1},{1,0},{2,3},{3,2},{4,5},{5,4},{6,7},{7,6},{8,9},{9,8},{10,11... | collective-permute-start | bytes 2359304 | tf_op jit(solution)/shard_map/ppermute | solution.py:19
  195.6 20.0 %collective-permute-start.7 = (bf16[4,2,160,256]{3,2,1,0:T(8,128)(2,1)S(1)}, bf16[4,2,160,256]{3,2,1,0:T(8,128)(2,1)}, u32[]{:S(2)}, u32[]{:S(2)}) collective-permute-start(bf16[4,2,160,256]{3,2,1,0:T(8,128)(2,1)S(1)} %pad_maximum_fusion.1.refs_4_), channel_id=1, source_target_pairs={{0,2},{2,4},{4,6},{6,0},{1,3},{3,5},{5,7},{7,1},{8,10},{10,12},{12... | collective-permute-start | bytes 1966088 | tf_op jit(solution)/shard_map/ppermute | solution.py:19
  198.9 31.7 %collective-permute-start.8 = (bf16[4,2,160,256]{3,2,1,0:T(8,128)(2,1)S(1)}, bf16[4,2,160,256]{3,2,1,0:T(8,128)(2,1)}, u32[]{:S(2)}, u32[]{:S(2)}) collective-permute-start(bf16[4,2,160,256]{3,2,1,0:T(8,128)(2,1)S(1)} %pad_maximum_fusion.1.refs_4_), channel_id=1, source_target_pairs={{0,4},{2,6},{4,0},{6,2},{1,5},{3,7},{5,1},{7,3},{8,12},{10,14},{12... | collective-permute-start | bytes 1966088 | tf_op jit(solution)/shard_map/ppermute | solution.py:19
  203.6 28.3 %collective-permute-start.9 = (bf16[4,2,160,256]{3,2,1,0:T(8,128)(2,1)S(1)}, bf16[4,2,160,256]{3,2,1,0:T(8,128)(2,1)}, u32[]{:S(2)}, u32[]{:S(2)}) collective-permute-start(bf16[4,2,160,256]{3,2,1,0:T(8,128)(2,1)S(1)} %pad_maximum_fusion.1.refs_4_), channel_id=1, source_target_pairs={{0,6},{2,0},{4,2},{6,4},{1,7},{3,1},{5,3},{7,5},{8,14},{10,8},{12,... | collective-permute-start | bytes 1966088 | tf_op jit(solution)/shard_map/ppermute | solution.py:19
  236.8 36.7 %all-to-all-start.2 = ((bf16[4,4,2,80,256]{4,3,2,1,0:T(8,128)(2,1)}), bf16[4,4,2,80,256]{4,3,2,1,0:T(8,128)(2,1)}, u32[]{:S(2)}, u32[]{:S(2)}) async-start(bf16[4,4,2,80,256]{4,3,2,1,0:T(8,128)(2,1)} %experts.2), calls=%async_computation.2 | async-start | bytes 2621440 | tf_op jit(solution)/shard_map/all_to_all | solution.py:27
  245.0 20.0 %collective-permute-start.10 = (bf16[4,2,80,256]{3,2,1,0:T(8,128)(2,1)S(1)}, bf16[4,2,80,256]{3,2,1,0:T(8,128)(2,1)S(1)}, u32[]{:S(2)}, u32[]{:S(2)}) collective-permute-start(bf16[4,2,80,256]{3,2,1,0:T(8,128)(2,1)S(1)} %get-tuple-element.9), channel_id=1, source_target_pairs={{0,2},{2,4},{4,6},{6,0},{1,3},{3,5},{5,7},{7,1},{8,10},{10,12},{12... | collective-permute-start | bytes 983048 | tf_op jit(solution)/shard_map/ppermute | solution.py:19
  249.5 22.7 %collective-permute-start.11 = (bf16[4,2,80,256]{3,2,1,0:T(8,128)(2,1)S(1)}, bf16[4,2,80,256]{3,2,1,0:T(8,128)(2,1)S(1)}, u32[]{:S(2)}, u32[]{:S(2)}) collective-permute-start(bf16[4,2,80,256]{3,2,1,0:T(8,128)(2,1)S(1)} %get-tuple-element.10), channel_id=1, source_target_pairs={{0,4},{2,6},{4,0},{6,2},{1,5},{3,7},{5,1},{7,3},{8,12},{10,14},{12... | collective-permute-start | bytes 983048 | tf_op jit(solution)/shard_map/ppermute | solution.py:19
  252.8 19.8 %collective-permute-start.12 = (bf16[4,2,80,256]{3,2,1,0:T(8,128)(2,1)S(1)}, bf16[4,2,80,256]{3,2,1,0:T(8,128)(2,1)S(1)}, u32[]{:S(2)}, u32[]{:S(2)}) collective-permute-start(bf16[4,2,80,256]{3,2,1,0:T(8,128)(2,1)S(1)} %get-tuple-element.11), channel_id=1, source_target_pairs={{0,6},{2,0},{4,2},{6,4},{1,7},{3,1},{5,3},{7,5},{8,14},{10,8},{12,... | collective-permute-start | bytes 983048 | tf_op jit(solution)/shard_map/ppermute | solution.py:19
  273.5 19.3 %all-to-all-start.4 = ((bf16[8,80,256]{2,1,0:T(8,128)(2,1)}), bf16[8,80,256]{2,1,0:T(8,128)(2,1)S(1)}, u32[]{:S(2)}, u32[]{:S(2)}) async-start(bf16[8,80,256]{2,1,0:T(8,128)(2,1)} %bitcast.22), calls=%async_computation.4 | async-start | bytes 655360 | tf_op jit(solution)/shard_map/all_to_all | solution.py:27
  282.8 28.9 %copy-start = (s32[128,2]{0,1:T(2,128)S(1)}, s32[128,2]{0,1:T(2,128)}, u32[]{:S(2)}) copy-start(s32[128,2]{0,1:T(2,128)} %param.8) | copy-start | bytes 3076
  285.0 26.9 %copy-start.1 = (f32[128,2]{0,1:T(2,128)S(1)}, f32[128,2]{0,1:T(2,128)}, u32[]{:S(2)}) copy-start(f32[128,2]{0,1:T(2,128)} %param.9) | copy-start | bytes 3076
  292.8 14.5 %all-to-all-start.3 = ((bf16[8,80,256]{2,1,0:T(8,128)(2,1)}), bf16[8,80,256]{2,1,0:T(8,128)(2,1)S(1)}, u32[]{:S(2)}, u32[]{:S(2)}) async-start(bf16[8,80,256]{2,1,0:T(8,128)(2,1)} %bitcast.20), calls=%async_computation.3 | async-start | bytes 655360 | tf_op jit(solution)/shard_map/all_to_all | solution.py:27
  308.1 31.2 %all-to-all-start.5 = ((bf16[8,40,256]{2,1,0:T(8,128)(2,1)}), bf16[8,40,256]{2,1,0:T(8,128)(2,1)S(1)}, u32[]{:S(2)}, u32[]{:S(2)}) async-start(bf16[8,40,256]{2,1,0:T(8,128)(2,1)} %bitcast.24), calls=%async_computation.5 | async-start | bytes 327680 | tf_op jit(solution)/shard_map/all_to_all | solution.py:27

commit v6 on v5

--- a/solution.py
+++ b/solution.py
@@ -98,92 +98,131 @@
     )(routes.T, tokens)
 
 
-def expert_kernel(span, count, groups, whole, place, *refs):
-    first, share = span
-    pieces, parts = refs[: 2 * groups], refs[2 * groups : 2 * groups + count]
-    outs, assembled = refs[2 * groups + count : -2], refs[-2:]
-    if whole:
-        outs = [outs[0].at[k] for k in range(count)]
-    copies, halves, _, cols = parts[0].shape
-    part, width = pieces[0].shape[1], pieces[0].shape[2] // 3
-    rows = copies * share
-    for k in range(groups):
-        index = lax.rem(place[3] + (groups - k), groups)
-        for held, piece in zip(assembled, (pieces[k], pieces[groups + k])):
-            held[:, pl.ds(index, 1)] = piece[...][:, None]
-
-    def block(held, k, c, start, end, origin=place[0]):
+def hidden_kernel(bundles, place, *refs):
+    parts, out, assembled = refs[2 * bundles : -3], refs[-3], refs[-2:]
+    count, groups = len(parts), assembled[0].shape[1]
+    copies, halves, tokens, cols = parts[0].shape
+    part, width = assembled[0].shape[2], assembled[0].shape[3] // 2
+    rows = copies * tokens
+    for held, pieces in zip(assembled, (refs[:bundles], refs[bundles : 2 * bundles])):
+        step = 0
+        for piece in pieces:
+            for k in range(piece.shape[0]):
+                index = lax.rem(place[3] + (groups - step), groups)
+                held[:, pl.ds(index, 1)] = piece[k, :, :, : 2 * width][:, None]
+                step += 1
+
+    def block(held, x, c):
         sources = cols // (groups * part)
-        at = (lax.rem(origin + k, count) * halves + c) * sources
-        return held[pl.ds(at, sources), :, :, start:end].reshape(cols, end - start)
+        at = (lax.rem(x, count) * halves + c) * sources
+        return held[pl.ds(at, sources)].reshape(cols, 2 * width)
 
     sums = [jnp.zeros((rows, 2 * width), jnp.float32) for _ in range(2)]
     squares = jnp.zeros((rows, cols), jnp.float32)
     for k in range(count):
         for c in range(halves):
             core = lax.rem(place[1] + (halves - c), halves)
-            left = parts[k][:, c, first : first + share].reshape(rows, cols)
+            left = parts[k][:, c].reshape(rows, cols)
             wide = left.astype(jnp.float32)
             squares = squares + wide * wide
             sums = [
                 value
                 + jnp.dot(
                     left,
-                    block(held, count - k, core, 0, 2 * width),
+                    block(held, place[0] + (count - k), core),
                     preferred_element_type=jnp.float32,
                 )
                 for value, held in zip(sums, assembled)
             ]
     features = count * halves * cols
     row_scale = lax.rsqrt(jnp.sum(squares, axis=1, keepdims=True) / features + epsilon)
-    hidden = []
-    for value in sums:
+    for j, value in enumerate(sums):
         value = value * row_scale
         gate, up = value[:, :width], value[:, width:]
-        hidden.append((gate / (1.0 + jnp.exp(-gate)) * up).astype(jnp.bfloat16))
-    hidden = jnp.concatenate(hidden, axis=1)
-    for k, out in enumerate(outs):
-        for c in range(halves):
-            down = jnp.concatenate(
-                [
-                    block(held, k, c, 2 * width, 3 * width, 0 if whole else place[0])
-                    for held in assembled
-                ],
-                axis=1,
-            )
-            value = lax.dot_general(
-                hidden, down, (((1,), (1,)), ((), ())), preferred_element_type=jnp.float32
-            ).astype(jnp.bfloat16)
-            for r in range(copies):
-                target = lax.rem(place[2] + (copies - r), copies)
-                out[pl.ds(target, 1), c] = value[r * share : (r + 1) * share][None]
-
-
-def whole_block(value):
-    return pl.BlockSpec(value.shape, lambda t, place, rank=len(value.shape): (0,) * rank)
-
-
-def expert_outputs(pieces, parts, span, whole):
-    copies, halves, _, cols = parts[0].shape
-    sources, part, triple = pieces[0].shape
-    size = (copies, halves, span[1], cols)
-    size = (len(parts), *size) if whole else size
-    outs = [jax.ShapeDtypeStruct(size, jnp.bfloat16)] * (1 if whole else len(parts))
-    inputs = (*pieces, *parts)
-    held = pltpu.VMEM((sources, len(pieces) // 2, part, triple), jnp.bfloat16)
-    return pl.pallas_call(
-        functools.partial(expert_kernel, span, len(parts), len(pieces) // 2, whole),
-        out_shape=outs,
+        hidden = (gate / (1.0 + jnp.exp(-gate)) * up).astype(jnp.bfloat16)
+        out[:, :, j * width : (j + 1) * width] = hidden.reshape(copies, tokens, width)
+
+
+def hidden_units(own, other, parts):
+    copies, _, tokens, _ = parts[0].shape
+    _, sources, part, triple = own[0].shape
+    groups = sum(piece.shape[0] for piece in own)
+    width = triple // 3
+    out = jax.ShapeDtypeStruct((copies, tokens, 2 * width), jnp.bfloat16)
+    inputs = (*own, *other, *parts)
+    held = pltpu.VMEM((sources, groups, part, 2 * width), jnp.bfloat16)
+    return pl.pallas_call(
+        functools.partial(hidden_kernel, len(own)),
+        out_shape=out,
         grid_spec=pltpu.PrefetchScalarGridSpec(
             num_scalar_prefetch=1,
             grid=(1,),
             in_specs=[whole_block(value) for value in inputs],
-            out_specs=[whole_block(out) for out in outs],
+            out_specs=whole_block(out),
             scratch_shapes=[held, held],
         ),
         compiler_params=vmem(32),
-        name="experts",
+        name="hidden",
     )(position_of("tp_x", "tp_c", "fs_lo", "grp"), *inputs)
+
+
+def project_kernel(bundles, place, *refs):
+    hidden, out, held = refs[2 * bundles : -2], refs[-2], refs[-1]
+    count, groups = len(hidden), held.shape[2]
+    copies, tokens, depth = hidden[0].shape
+    halves, cols = out.shape[1], out.shape[3]
+    width = depth // 2
+    for j, pieces in enumerate((refs[:bundles], refs[bundles : 2 * bundles])):
+        step = 0
+        for piece in pieces:
+            for k in range(piece.shape[1]):
+                index = lax.rem(place[3] + (groups - step), groups)
+                held[:, :, pl.ds(index, 1), :, j * width : (j + 1) * width] = piece[:, k][
+                    :, :, None
+                ]
+                step += 1
+    share = held.shape[1] // halves
+    for c in range(halves):
+        value = jnp.zeros((copies * tokens, cols), jnp.float32)
+        for k in range(count):
+            source = lax.rem(place[0] + (count - k), count)
+            down = held[pl.ds(source, 1), c * share : (c + 1) * share].reshape(cols, depth)
+            value = value + lax.dot_general(
+                hidden[k][...].reshape(copies * tokens, depth),
+                down,
+                (((1,), (1,)), ((), ())),
+                preferred_element_type=jnp.float32,
+            )
+        value = value.astype(jnp.bfloat16)
+        for r in range(copies):
+            target = lax.rem(place[2] + (copies - r), copies)
+            out[pl.ds(target, 1), c] = value[r * tokens : (r + 1) * tokens][None]
+
+
+def projected(own, other, hidden, halves):
+    copies, tokens, depth = hidden[0].shape
+    count, _, sources, part, _ = own[0].shape
+    groups = sum(piece.shape[1] for piece in own)
+    cols = sources * groups * part // halves
+    out = jax.ShapeDtypeStruct((copies, halves, tokens, cols), jnp.bfloat16)
+    inputs = (*own, *other, *hidden)
+    return pl.pallas_call(
+        functools.partial(project_kernel, len(own)),
+        out_shape=out,
+        grid_spec=pltpu.PrefetchScalarGridSpec(
+            num_scalar_prefetch=1,
+            grid=(1,),
+            in_specs=[whole_block(value) for value in inputs],
+            out_specs=whole_block(out),
+            scratch_shapes=[pltpu.VMEM((count, sources, groups, part, depth), jnp.bfloat16)],
+        ),
+        compiler_params=vmem(32),
+        name="project",
+    )(position_of("tp_x", "tp_c", "fs_lo", "grp"), *inputs)
+
+
+def whole_block(value):
+    return pl.BlockSpec(value.shape, lambda t, place, rank=len(value.shape): (0,) * rank)
 
 
 def choose_kernel(routes, out):
@@ -273,9 +312,6 @@
     copies = lax.axis_size("fs_lo")
     row_count, col_width = tokens.shape
     capacity = row_count * 5 // 16
-    share = experts * capacity // lax.axis_size("tp_c")
-    cut = share // 2
-    spans = ((0, cut), (cut, share - cut))
 
     outgoing = dispatched(tokens, routes, experts, capacity)
     arrived = exchange(outgoing, "fs_hi")
@@ -288,25 +324,27 @@
 
     packed = packed_weights(norm_gain, gate_weight, up_weight, down_weight, copies)
     mine = exchange(packed, FS)
-    own = [mine] + [shifted(mine, "grp", k) for k in range(1, lax.axis_size("grp"))]
-    other = [shifted(piece, "tp_c", 1) for piece in own]
+    passed = [shifted(mine, "grp", k) for k in range(1, lax.axis_size("grp"))]
+    own = [mine[None]] + ([jnp.stack(passed)] if passed else [])
+    other = []
+    for piece in own:
+        other.append(shifted(piece, "tp_c", 1))
     chosen = chosen_slots(routes, experts * capacity)
-
-    sums = []
-    for t, span in enumerate(spans):
-        outs = expert_outputs(own + other, parts, span, t == 0)
-        if t == 0:
-            arrived = exchange(outs[0], "tp_x")
-            got = [arrived[k] for k in range(len(parts))]
-        else:
-            got = [outs[0]] + [shifted(outs[k], "tp_x", k) for k in range(1, len(outs))]
-        over_x = sum(value.astype(jnp.float32) for value in got).astype(jnp.bfloat16)
-        sent = exchange(over_x.reshape(-1, *over_x.shape[2:]), ("fs_lo", "tp_c"))
-        over_s = jnp.sum(sent.reshape(over_x.shape), axis=0, dtype=jnp.float32)
-        sums.append(over_s.astype(jnp.bfloat16))
-    own = assembled_weights(own, rows)
-    back = jnp.concatenate(sums, axis=1).reshape(experts, capacity, col_width)
+    turned, paired = [], []
+    for t, piece in enumerate(own):
+        down = piece[..., 2 * piece.shape[3] // 3 :]
+        down = down.reshape(down.shape[0], lax.axis_size("tp_x"), -1, *down.shape[2:])
+        turned.append(exchange(jnp.swapaxes(down, 0, 1), "tp_x"))
+        paired.append(shifted(turned[t], "tp_c", 1))
+
+    units = hidden_units(own, other, parts)
+    units = [units] + [shifted(units, "tp_x", k) for k in range(1, len(parts))]
+    over_x = projected(turned, paired, units, lax.axis_size("tp_c"))
+    sent = exchange(over_x.reshape(-1, *over_x.shape[2:]), ("fs_lo", "tp_c"))
+    over_s = jnp.sum(sent.reshape(over_x.shape), axis=0, dtype=jnp.float32)
+    back = over_s.astype(jnp.bfloat16).reshape(experts, capacity, col_width)
     returned = exchange(back, "fs_hi")
+    own = assembled_weights([mine, *passed], rows)
     width = own.shape[1] // 3
     outputs = [own[None, :, k * width : (k + 1) * width] for k in range(3)]
     return (*outputs, combined(chosen, route_weights, returned))

time: 343 us -> 329 us (0.959)
  waiting for transfers between devices: 194 us -> 159 us
  blocking collectives: 0 us -> 27.1 us
  starting transfers between devices: 122 us -> 117 us
    ppermute x13 -> x15, waiting for transfers between devices: 44.9 us -> 6.42 us  [shifted(): lax.ppermute(value, axis, [(k, (k + step) % count) for k in range(count)])]
    all_to_all x0 -> x1, blocking collectives: none -> 27.1 us  [exchange(): return lax.all_to_all(value, axis, split_axis=0, concat_axis=0, tiled=True)]
    all_to_all x6 -> x5, starting transfers between devices: 71.6 us -> 61.2 us  [exchange(): return lax.all_to_all(value, axis, split_axis=0, concat_axis=0, tiled=True)]
    ppermute x13 -> x15, starting transfers between devices: 49.9 us -> 55.6 us  [shifted(): lax.ppermute(value, axis, [(k, (k + step) % count) for k in range(count)])]
    all_to_all x6 -> x5, waiting for transfers between devices: 150 us -> 152 us  [exchange(): return lax.all_to_all(value, axis, split_axis=0, concat_axis=0, tiled=True)]
  transfers between devices with their start and end apart: 19 -> 20, of which waited for: 12 -> 8; matrix products, arithmetic and copies ran while one was open for 2% -> 1% of each run, Pallas kernels for 2% -> 2%
where the time goes in v6:
time: 329 us; the launch traced here: 324 us
  waiting for transfers between devices  159 us (48%)
  starting transfers between devices  117 us (36%)
  blocking collectives  27.1 us (8%)
  Pallas kernels  15.3 us (5%)
  local copies, waits for them, and re-layouts  3.67 us (1%)
    all_to_all x5, waiting for transfers between devices, exchange(): return lax.all_to_all(value, axis, split_axis=0, concat_axis=0, tiled=True)  152 us
    all_to_all x5, starting transfers between devices, exchange(): return lax.all_to_all(value, axis, split_axis=0, concat_axis=0, tiled=True)  61.2 us
    ppermute x15, starting transfers between devices, shifted(): lax.ppermute(value, axis, [(k, (k + step) % count) for k in range(count)])  55.6 us
    all_to_all x1, blocking collectives, exchange(): return lax.all_to_all(value, axis, split_axis=0, concat_axis=0, tiled=True)  27.1 us
  transfers between devices with their start and end apart: 20, of which 8 were waited for; matrix products, arithmetic and copies ran while one was open for 1% of the time, Pallas kernels for 2%

profile of v6, /device:TPU:33, one launch (start us, length us, event | category | flops | bytes accessed | tf_op | source)
XLA Modules:
  0.0 323.7 jit_solution(17240681861732438691)
XLA Ops:
  0.6 5.4 %pack.1 = bf16[32,32,384]{2,1,0:T(8,128)(2,1)} custom-call(s32[1]{0:T(128)} %bitcast.turn.place, f32[1,64]{1,0:T(1,128)} %bitcast.53, f32[8,64,512]{2,1,0:T(8,128)} %gate.1, f32[8,64,512]{2,1,0:T(8,128)} %up.1, f32[8,64,512]{2,1,0:T(8,128)} %down.1), custom_call_target="tpu_custom_call" | custom-call | tf_op jit(solution)/shard_map/pack/pallas_call | solution.py:53
  6.1 46.3 %all-to-all-start = ((bf16[32,32,384]{2,1,0:T(8,128)(2,1)}), bf16[32,32,384]{2,1,0:T(8,128)(2,1)S(1)}, u32[]{:S(2)}, u32[]{:S(2)}) async-start(bf16[32,32,384]{2,1,0:T(8,128)(2,1)} %pack.1), calls=%async_computation | async-start | bytes 1572864 | tf_op jit(solution)/shard_map/all_to_all | solution.py:27
  54.3 84.1 %all-to-all-done = bf16[32,32,384]{2,1,0:T(8,128)(2,1)S(1)} async-done(((bf16[32,32,384]{2,1,0:T(8,128)(2,1)}), bf16[32,32,384]{2,1,0:T(8,128)(2,1)S(1)}, u32[]{:S(2)}, u32[]{:S(2)}) %all-to-all-start) | async-done | bytes 786464 | tf_op jit(solution)/shard_map/all_to_all | solution.py:27
  138.3 3.6 %all-to-all-start.3 = ((bf16[8,40,256]{2,1,0:T(8,128)(2,1)}), bf16[8,40,256]{2,1,0:T(8,128)(2,1)S(1)}, u32[]{:S(2)}, u32[]{:S(2)}) async-start(bf16[8,40,256]{2,1,0:T(8,128)(2,1)} %dispatch.1), calls=%async_computation.3 | async-start | bytes 327680 | tf_op jit(solution)/shard_map/all_to_all | solution.py:27
  141.9 3.8 %collective-permute-start = (bf16[32,32,384]{2,1,0:T(8,128)(2,1)S(1)}, bf16[32,32,384]{2,1,0:T(8,128)(2,1)S(1)}, u32[]{:S(2)}, u32[]{:S(2)}) collective-permute-start(bf16[32,32,384]{2,1,0:T(8,128)(2,1)S(1)} %all-to-all-done), channel_id=1, source_target_pairs={{0,256},{256,0},{1,257},{257,1},{2,258},{258,2},{3,259},{259,3},{4... | collective-permute-start | bytes 2359304 | tf_op jit(solution)/shard_map/ppermute | solution.py:19
  145.7 22.4 %all-to-all-done.3 = bf16[8,40,256]{2,1,0:T(8,128)(2,1)S(1)} async-done(((bf16[8,40,256]{2,1,0:T(8,128)(2,1)}), bf16[8,40,256]{2,1,0:T(8,128)(2,1)S(1)}, u32[]{:S(2)}, u32[]{:S(2)}) %all-to-all-start.3) | async-done | bytes 163872 | tf_op jit(solution)/shard_map/all_to_all | solution.py:27
  170.0 9.2 %collective-permute-start.6 = (bf16[320,256]{1,0:T(8,128)(2,1)S(1)}, bf16[320,256]{1,0:T(8,128)(2,1)S(1)}, u32[]{:S(2)}, u32[]{:S(2)}) collective-permute-start(bf16[320,256]{1,0:T(8,128)(2,1)S(1)} %bitcast.46), channel_id=1, source_target_pairs={{0,16},{8,24},{16,0},{24,8},{1,17},{9,25},{17,1},{25,9},{2,18},{10... | collective-permute-start | bytes 491528 | tf_op jit(solution)/shard_map/ppermute | solution.py:19
  179.3 4.3 %collective-permute-start.7 = (bf16[320,256]{1,0:T(8,128)(2,1)S(1)}, bf16[320,256]{1,0:T(8,128)(2,1)S(1)}, u32[]{:S(2)}, u32[]{:S(2)}) collective-permute-start(bf16[320,256]{1,0:T(8,128)(2,1)S(1)} %bitcast.47), channel_id=1, source_target_pairs={{0,24},{8,0},{16,8},{24,16},{1,25},{9,1},{17,9},{25,17},{2,26},{10... | collective-permute-start | bytes 491528 | tf_op jit(solution)/shard_map/ppermute | solution.py:19
  183.6 2.7 collective-permute-done.7
  186.5 4.6 %collective-permute-start.8 = (bf16[4,160,256]{2,1,0:T(8,128)(2,1)S(1)}, bf16[4,160,256]{2,1,0:T(8,128)(2,1)S(1)}, u32[]{:S(2)}, u32[]{:S(2)}) collective-permute-start(bf16[4,160,256]{2,1,0:T(8,128)(2,1)S(1)} %get-tuple-element.8), channel_id=1, source_target_pairs={{0,1},{1,0},{2,3},{3,2},{4,5},{5,4},{6,7},{7,6},{8,9},{9,8},{10,11... | collective-permute-start | bytes 983048 | tf_op jit(solution)/shard_map/ppermute | solution.py:19
  195.6 5.0 %collective-permute-start.10 = (bf16[4,2,160,256]{3,2,1,0:T(8,128)(2,1)S(1)}, bf16[4,2,160,256]{3,2,1,0:T(8,128)(2,1)}, u32[]{:S(2)}, u32[]{:S(2)}) collective-permute-start(bf16[4,2,160,256]{3,2,1,0:T(8,128)(2,1)S(1)} %pad_maximum_fusion.1.refs_4_), channel_id=1, source_target_pairs={{0,4},{2,6},{4,0},{6,2},{1,5},{3,7},{5,1},{7,3},{8,12},{10,14},{12... | collective-permute-start | bytes 1966088 | tf_op jit(solution)/shard_map/ppermute | solution.py:19
  200.6 2.7 collective-permute-start.11
  203.2 2.7 collective-permute-start.9
  206.7 3.5 %all-to-all-start.1 = ((bf16[4,1,8,32,128]{4,3,2,1,0:T(8,128)(2,1)}), bf16[4,1,8,32,128]{4,3,2,1,0:T(8,128)(2,1)S(1)}, u32[]{:S(2)}, u32[]{:S(2)}) async-start(bf16[4,1,8,32,128]{4,3,2,1,0:T(8,128)(2,1)} %bitcast.14), calls=%async_computation.1 | async-start | bytes 524288 | tf_op jit(solution)/shard_map/all_to_all | solution.py:27
  210.9 21.4 %all-to-all-done.1.refs_0_ = bf16[4,1,8,32,128]{4,3,2,1,0:T(8,128)(2,1)S(1)} async-done(((bf16[4,1,8,32,128]{4,3,2,1,0:T(8,128)(2,1)}), bf16[4,1,8,32,128]{4,3,2,1,0:T(8,128)(2,1)S(1)}, u32[]{:S(2)}, u32[]{:S(2)}) %all-to-all-start.1) | async-done | bytes 262176 | tf_op jit(solution)/shard_map/all_to_all | solution.py:27
  232.3 4.2 %all-to-all-start.2 = ((bf16[4,1,8,32,128]{4,3,2,1,0:T(8,128)(2,1)}), bf16[4,1,8,32,128]{4,3,2,1,0:T(8,128)(2,1)S(1)}, u32[]{:S(2)}, u32[]{:S(2)}) async-start(bf16[4,1,8,32,128]{4,3,2,1,0:T(8,128)(2,1)} %bitcast.16), calls=%async_computation.2 | async-start | bytes 524288 | tf_op jit(solution)/shard_map/all_to_all | solution.py:27
  236.6 4.4 %hidden.1.refs_4_ = bf16[4,160,256]{2,1,0:T(8,128)(2,1)S(1)} custom-call(s32[4]{0:T(128)S(1)} %pad_add_fusion.place, bf16[1,32,32,384]{3,2,1,0:T(8,128)(2,1)S(1)} %bitcast.36, bf16[1,32,32,384]{3,2,1,0:T(8,128)(2,1)S(1)} %bitcast.39, bf16[1,32,32,384]{3,2,1,0:T(8,128)(2,1)} %collective-permute-done.3.refs_2_, ...), custom_call_target="tpu_custom_call" | custom-call | tf_op jit(solution)/shard_map/hidden/pallas_call | solution.py:154
  241.0 3.4 %collective-permute-start.12 = (bf16[4,160,256]{2,1,0:T(8,128)(2,1)S(1)}, bf16[4,160,256]{2,1,0:T(8,128)(2,1)S(1)}, u32[]{:S(2)}, u32[]{:S(2)}) collective-permute-start(bf16[4,160,256]{2,1,0:T(8,128)(2,1)S(1)} %hidden.1.refs_4_), channel_id=1, source_target_pairs={{0,2},{2,4},{4,6},{6,0},{1,3},{3,5},{5,7},{7,1},{8,10},{10,12},{12... | collective-permute-start | bytes 983048 | tf_op jit(solution)/shard_map/ppermute | solution.py:19
  244.4 4.3 %collective-permute-start.13 = (bf16[4,160,256]{2,1,0:T(8,128)(2,1)S(1)}, bf16[4,160,256]{2,1,0:T(8,128)(2,1)S(1)}, u32[]{:S(2)}, u32[]{:S(2)}) collective-permute-start(bf16[4,160,256]{2,1,0:T(8,128)(2,1)S(1)} %hidden.1.refs_4_), channel_id=1, source_target_pairs={{0,4},{2,6},{4,0},{6,2},{1,5},{3,7},{5,1},{7,3},{8,12},{10,14},{12... | collective-permute-start | bytes 983048 | tf_op jit(solution)/shard_map/ppermute | solution.py:19
  248.8 3.1 collective-permute-start.14
  251.9 4.2 %collective-permute-start.1 = (bf16[4,1,8,32,128]{4,3,2,1,0:T(8,128)(2,1)S(1)}, bf16[4,1,8,32,128]{4,3,2,1,0:T(8,128)(2,1)}, u32[]{:S(2)}, u32[]{:S(2)}) collective-permute-start(bf16[4,1,8,32,128]{4,3,2,1,0:T(8,128)(2,1)S(1)} %all-to-all-done.1.refs_0_), channel_id=1, source_target_pairs={{0,1},{1,0},{2,3},{3,2},{4,5},{5,4},{6,7},{7,6},{8,9},{9,8},{10,11... | collective-permute-start | bytes 786440 | tf_op jit(solution)/shard_map/ppermute | solution.py:19
  264.3 27.1 %all_to_all.30 = bf16[8,160,256]{2,1,0:T(8,128)(2,1)S(1)} all-to-all(bf16[8,160,256]{2,1,0:T(8,128)(2,1)S(1)} %bitcast.40), channel_id=1, replica_groups=mesh['grp'=2,'fs_hi'=8,'fs_lo'=4,'tp_x'=4,'tp_c'=2] {'fs_lo','tp_c'}, dimensions={0} | all-to-all | bytes 1310720 | tf_op jit(solution)/shard_map/all_to_all | solution.py:27
  292.2 3.6 %all-to-all-start.5 = ((bf16[8,40,256]{2,1,0:T(8,128)(2,1)}), bf16[8,40,256]{2,1,0:T(8,128)(2,1)S(1)}, u32[]{:S(2)}, u32[]{:S(2)}) async-start(bf16[8,40,256]{2,1,0:T(8,128)(2,1)} %bitcast.26), calls=%async_computation.5 | async-start | bytes 327680 | tf_op jit(solution)/shard_map/all_to_all | solution.py:27
  298.1 24.6 %all-to-all-done.5.returned = bf16[8,40,256]{2,1,0:T(8,128)(2,1)S(1)} async-done(((bf16[8,40,256]{2,1,0:T(8,128)(2,1)}), bf16[8,40,256]{2,1,0:T(8,128)(2,1)S(1)}, u32[]{:S(2)}, u32[]{:S(2)}) %all-to-all-start.5) | async-done | bytes 163872 | tf_op jit(solution)/shard_map/all_to_all | solution.py:27
  (40 shorter events, 22.2 us)
Async XLA Ops:
  6.1 132.2 %all-to-all-start = ((bf16[32,32,384]{2,1,0:T(8,128)(2,1)}), bf16[32,32,384]{2,1,0:T(8,128)(2,1)S(1)}, u32[]{:S(2)}, u32[]{:S(2)}) async-start(bf16[32,32,384]{2,1,0:T(8,128)(2,1)} %pack.1), calls=%async_computation | async-start | bytes 1572864 | tf_op jit(solution)/shard_map/all_to_all | solution.py:27
  138.3 29.8 %all-to-all-start.3 = ((bf16[8,40,256]{2,1,0:T(8,128)(2,1)}), bf16[8,40,256]{2,1,0:T(8,128)(2,1)S(1)}, u32[]{:S(2)}, u32[]{:S(2)}) async-start(bf16[8,40,256]{2,1,0:T(8,128)(2,1)} %dispatch.1), calls=%async_computation.3 | async-start | bytes 327680 | tf_op jit(solution)/shard_map/all_to_all | solution.py:27
  141.9 51.1 %collective-permute-start = (bf16[32,32,384]{2,1,0:T(8,128)(2,1)S(1)}, bf16[32,32,384]{2,1,0:T(8,128)(2,1)S(1)}, u32[]{:S(2)}, u32[]{:S(2)}) collective-permute-start(bf16[32,32,384]{2,1,0:T(8,128)(2,1)S(1)} %all-to-all-done), channel_id=1, source_target_pairs={{0,256},{256,0},{1,257},{257,1},{2,258},{258,2},{3,259},{259,3},{4... | collective-permute-start | bytes 2359304 | tf_op jit(solution)/shard_map/ppermute | solution.py:19
  168.1 15.5 %collective-permute-start.5 = (bf16[320,256]{1,0:T(8,128)(2,1)S(1)}, bf16[320,256]{1,0:T(8,128)(2,1)S(1)}, u32[]{:S(2)}, u32[]{:S(2)}) collective-permute-start(bf16[320,256]{1,0:T(8,128)(2,1)S(1)} %bitcast.45), channel_id=1, source_target_pairs={{0,8},{8,16},{16,24},{24,0},{1,9},{9,17},{17,25},{25,1},{2,10},{10... | collective-permute-start | bytes 491528 | tf_op jit(solution)/shard_map/ppermute | solution.py:19
  170.0 13.6 %collective-permute-start.6 = (bf16[320,256]{1,0:T(8,128)(2,1)S(1)}, bf16[320,256]{1,0:T(8,128)(2,1)S(1)}, u32[]{:S(2)}, u32[]{:S(2)}) collective-permute-start(bf16[320,256]{1,0:T(8,128)(2,1)S(1)} %bitcast.46), channel_id=1, source_target_pairs={{0,16},{8,24},{16,0},{24,8},{1,17},{9,25},{17,1},{25,9},{2,18},{10... | collective-permute-start | bytes 491528 | tf_op jit(solution)/shard_map/ppermute | solution.py:19
  179.3 7.1 %collective-permute-start.7 = (bf16[320,256]{1,0:T(8,128)(2,1)S(1)}, bf16[320,256]{1,0:T(8,128)(2,1)S(1)}, u32[]{:S(2)}, u32[]{:S(2)}) collective-permute-start(bf16[320,256]{1,0:T(8,128)(2,1)S(1)} %bitcast.47), channel_id=1, source_target_pairs={{0,24},{8,0},{16,8},{24,16},{1,25},{9,1},{17,9},{25,17},{2,26},{10... | collective-permute-start | bytes 491528 | tf_op jit(solution)/shard_map/ppermute | solution.py:19
  186.5 9.0 %collective-permute-start.8 = (bf16[4,160,256]{2,1,0:T(8,128)(2,1)S(1)}, bf16[4,160,256]{2,1,0:T(8,128)(2,1)S(1)}, u32[]{:S(2)}, u32[]{:S(2)}) collective-permute-start(bf16[4,160,256]{2,1,0:T(8,128)(2,1)S(1)} %get-tuple-element.8), channel_id=1, source_target_pairs={{0,1},{1,0},{2,3},{3,2},{4,5},{5,4},{6,7},{7,6},{8,9},{9,8},{10,11... | collective-permute-start | bytes 983048 | tf_op jit(solution)/shard_map/ppermute | solution.py:19
  191.1 45.5 %collective-permute-start.3 = (bf16[1,32,32,384]{3,2,1,0:T(8,128)(2,1)S(1)}, bf16[1,32,32,384]{3,2,1,0:T(8,128)(2,1)}, u32[]{:S(2)}, u32[]{:S(2)}) collective-permute-start(bf16[1,32,32,384]{3,2,1,0:T(8,128)(2,1)S(1)} %bitcast.34), channel_id=1, source_target_pairs={{0,1},{1,0},{2,3},{3,2},{4,5},{5,4},{6,7},{7,6},{8,9},{9,8},{10,11... | collective-permute-start | bytes 2359304 | tf_op jit(solution)/shard_map/ppermute | solution.py:19
  193.1 43.5 %collective-permute-start.4 = (bf16[1,32,32,384]{3,2,1,0:T(8,128)(2,1)S(1)}, bf16[1,32,32,384]{3,2,1,0:T(8,128)(2,1)}, u32[]{:S(2)}, u32[]{:S(2)}) collective-permute-start(bf16[1,32,32,384]{3,2,1,0:T(8,128)(2,1)S(1)} %bitcast.37), channel_id=1, source_target_pairs={{0,1},{1,0},{2,3},{3,2},{4,5},{5,4},{6,7},{7,6},{8,9},{9,8},{10,11... | collective-permute-start | bytes 2359304 | tf_op jit(solution)/shard_map/ppermute | solution.py:19
  195.6 41.0 %collective-permute-start.10 = (bf16[4,2,160,256]{3,2,1,0:T(8,128)(2,1)S(1)}, bf16[4,2,160,256]{3,2,1,0:T(8,128)(2,1)}, u32[]{:S(2)}, u32[]{:S(2)}) collective-permute-start(bf16[4,2,160,256]{3,2,1,0:T(8,128)(2,1)S(1)} %pad_maximum_fusion.1.refs_4_), channel_id=1, source_target_pairs={{0,4},{2,6},{4,0},{6,2},{1,5},{3,7},{5,1},{7,3},{8,12},{10,14},{12... | collective-permute-start | bytes 1966088 | tf_op jit(solution)/shard_map/ppermute | solution.py:19
  200.6 36.0 %collective-permute-start.11 = (bf16[4,2,160,256]{3,2,1,0:T(8,128)(2,1)S(1)}, bf16[4,2,160,256]{3,2,1,0:T(8,128)(2,1)}, u32[]{:S(2)}, u32[]{:S(2)}) collective-permute-start(bf16[4,2,160,256]{3,2,1,0:T(8,128)(2,1)S(1)} %pad_maximum_fusion.1.refs_4_), channel_id=1, source_target_pairs={{0,6},{2,0},{4,2},{6,4},{1,7},{3,1},{5,3},{7,5},{8,14},{10,8},{12,... | collective-permute-start | bytes 1966088 | tf_op jit(solution)/shard_map/ppermute | solution.py:19
  203.2 33.4 %collective-permute-start.9 = (bf16[4,2,160,256]{3,2,1,0:T(8,128)(2,1)S(1)}, bf16[4,2,160,256]{3,2,1,0:T(8,128)(2,1)}, u32[]{:S(2)}, u32[]{:S(2)}) collective-permute-start(bf16[4,2,160,256]{3,2,1,0:T(8,128)(2,1)S(1)} %pad_maximum_fusion.1.refs_4_), channel_id=1, source_target_pairs={{0,2},{2,4},{4,6},{6,0},{1,3},{3,5},{5,7},{7,1},{8,10},{10,12},{12... | collective-permute-start | bytes 1966088 | tf_op jit(solution)/shard_map/ppermute | solution.py:19
  206.7 25.6 %all-to-all-start.1 = ((bf16[4,1,8,32,128]{4,3,2,1,0:T(8,128)(2,1)}), bf16[4,1,8,32,128]{4,3,2,1,0:T(8,128)(2,1)S(1)}, u32[]{:S(2)}, u32[]{:S(2)}) async-start(bf16[4,1,8,32,128]{4,3,2,1,0:T(8,128)(2,1)} %bitcast.14), calls=%async_computation.1 | async-start | bytes 524288 | tf_op jit(solution)/shard_map/all_to_all | solution.py:27
  232.3 23.8 %all-to-all-start.2 = ((bf16[4,1,8,32,128]{4,3,2,1,0:T(8,128)(2,1)}), bf16[4,1,8,32,128]{4,3,2,1,0:T(8,128)(2,1)S(1)}, u32[]{:S(2)}, u32[]{:S(2)}) async-start(bf16[4,1,8,32,128]{4,3,2,1,0:T(8,128)(2,1)} %bitcast.16), calls=%async_computation.2 | async-start | bytes 524288 | tf_op jit(solution)/shard_map/all_to_all | solution.py:27
  241.0 18.6 %collective-permute-start.12 = (bf16[4,160,256]{2,1,0:T(8,128)(2,1)S(1)}, bf16[4,160,256]{2,1,0:T(8,128)(2,1)S(1)}, u32[]{:S(2)}, u32[]{:S(2)}) collective-permute-start(bf16[4,160,256]{2,1,0:T(8,128)(2,1)S(1)} %hidden.1.refs_4_), channel_id=1, source_target_pairs={{0,2},{2,4},{4,6},{6,0},{1,3},{3,5},{5,7},{7,1},{8,10},{10,12},{12... | collective-permute-start | bytes 983048 | tf_op jit(solution)/shard_map/ppermute | solution.py:19
  244.4 15.8 %collective-permute-start.13 = (bf16[4,160,256]{2,1,0:T(8,128)(2,1)S(1)}, bf16[4,160,256]{2,1,0:T(8,128)(2,1)S(1)}, u32[]{:S(2)}, u32[]{:S(2)}) collective-permute-start(bf16[4,160,256]{2,1,0:T(8,128)(2,1)S(1)} %hidden.1.refs_4_), channel_id=1, source_target_pairs={{0,4},{2,6},{4,0},{6,2},{1,5},{3,7},{5,1},{7,3},{8,12},{10,14},{12... | collective-permute-start | bytes 983048 | tf_op jit(solution)/shard_map/ppermute | solution.py:19
  248.8 13.0 %collective-permute-start.14 = (bf16[4,160,256]{2,1,0:T(8,128)(2,1)S(1)}, bf16[4,160,256]{2,1,0:T(8,128)(2,1)S(1)}, u32[]{:S(2)}, u32[]{:S(2)}) collective-permute-start(bf16[4,160,256]{2,1,0:T(8,128)(2,1)S(1)} %hidden.1.refs_4_), channel_id=1, source_target_pairs={{0,6},{2,0},{4,2},{6,4},{1,7},{3,1},{5,3},{7,5},{8,14},{10,8},{12,... | collective-permute-start | bytes 983048 | tf_op jit(solution)/shard_map/ppermute | solution.py:19
  251.9 6.2 %collective-permute-start.1 = (bf16[4,1,8,32,128]{4,3,2,1,0:T(8,128)(2,1)S(1)}, bf16[4,1,8,32,128]{4,3,2,1,0:T(8,128)(2,1)}, u32[]{:S(2)}, u32[]{:S(2)}) collective-permute-start(bf16[4,1,8,32,128]{4,3,2,1,0:T(8,128)(2,1)S(1)} %all-to-all-done.1.refs_0_), channel_id=1, source_target_pairs={{0,1},{1,0},{2,3},{3,2},{4,5},{5,4},{6,7},{7,6},{8,9},{9,8},{10,11... | collective-permute-start | bytes 786440 | tf_op jit(solution)/shard_map/ppermute | solution.py:19
  256.1 3.5 %collective-permute-start.2 = (bf16[4,1,8,32,128]{4,3,2,1,0:T(8,128)(2,1)S(1)}, bf16[4,1,8,32,128]{4,3,2,1,0:T(8,128)(2,1)S(1)}, u32[]{:S(2)}, u32[]{:S(2)}) collective-permute-start(bf16[4,1,8,32,128]{4,3,2,1,0:T(8,128)(2,1)S(1)} %all-to-all-done.2.refs_1_), channel_id=1, source_target_pairs={{0,1},{1,0},{2,3},{3,2},{4,5},{5,4},{6,7},{7,6},{8,9},{9,8},{10,11... | collective-permute-start | bytes 786440 | tf_op jit(solution)/shard_map/ppermute | solution.py:19
  264.3 31.5 %copy-start = (s32[128,2]{0,1:T(2,128)S(1)}, s32[128,2]{0,1:T(2,128)}, u32[]{:S(2)}) copy-start(s32[128,2]{0,1:T(2,128)} %param.8) | copy-start | bytes 3076
  264.3 31.7 %copy-start.1 = (f32[128,2]{0,1:T(2,128)S(1)}, f32[128,2]{0,1:T(2,128)}, u32[]{:S(2)}) copy-start(f32[128,2]{0,1:T(2,128)} %param.9) | copy-start | bytes 3076
  292.2 30.6 %all-to-all-start.5 = ((bf16[8,40,256]{2,1,0:T(8,128)(2,1)}), bf16[8,40,256]{2,1,0:T(8,128)(2,1)S(1)}, u32[]{:S(2)}, u32[]{:S(2)}) async-start(bf16[8,40,256]{2,1,0:T(8,128)(2,1)} %bitcast.26), calls=%async_computation.5 | async-start | bytes 327680 | tf_op jit(solution)/shard_map/all_to_all | solution.py:27

commit v7 on v6

--- a/solution.py
+++ b/solution.py
@@ -109,7 +109,7 @@
         for piece in pieces:
             for k in range(piece.shape[0]):
                 index = lax.rem(place[3] + (groups - step), groups)
-                held[:, pl.ds(index, 1)] = piece[k, :, :, : 2 * width][:, None]
+                held[:, pl.ds(index, 1)] = piece[k][:, None]
                 step += 1
 
     def block(held, x, c):
@@ -145,9 +145,9 @@
 
 def hidden_units(own, other, parts):
     copies, _, tokens, _ = parts[0].shape
-    _, sources, part, triple = own[0].shape
+    _, sources, part, double = own[0].shape
     groups = sum(piece.shape[0] for piece in own)
-    width = triple // 3
+    width = double // 2
     out = jax.ShapeDtypeStruct((copies, tokens, 2 * width), jnp.bfloat16)
     inputs = (*own, *other, *parts)
     held = pltpu.VMEM((sources, groups, part, 2 * width), jnp.bfloat16)
@@ -175,9 +175,9 @@
     for j, pieces in enumerate((refs[:bundles], refs[bundles : 2 * bundles])):
         step = 0
         for piece in pieces:
-            for k in range(piece.shape[1]):
+            for k in range(piece.shape[0]):
                 index = lax.rem(place[3] + (groups - step), groups)
-                held[:, :, pl.ds(index, 1), :, j * width : (j + 1) * width] = piece[:, k][
+                held[:, :, pl.ds(index, 1), :, j * width : (j + 1) * width] = piece[k][
                     :, :, None
                 ]
                 step += 1
@@ -201,8 +201,8 @@
 
 def projected(own, other, hidden, halves):
     copies, tokens, depth = hidden[0].shape
-    count, _, sources, part, _ = own[0].shape
-    groups = sum(piece.shape[1] for piece in own)
+    _, count, sources, part, _ = own[0].shape
+    groups = sum(piece.shape[0] for piece in own)
     cols = sources * groups * part // halves
     out = jax.ShapeDtypeStruct((copies, halves, tokens, cols), jnp.bfloat16)
     inputs = (*own, *other, *hidden)
@@ -294,6 +294,15 @@
     return weights.reshape(sources * rows, triple)
 
 
+def passed_on(value):
+    passed = [shifted(value, "grp", k) for k in range(1, lax.axis_size("grp"))]
+    pieces = [value[None]] + ([jnp.stack(passed)] if passed else [])
+    pairs = []
+    for piece in pieces:
+        pairs.append(shifted(piece, "tp_c", 1))
+    return pieces, pairs
+
+
 def halved(blocks):
     copies, slots, cols = blocks.shape
     cores = lax.axis_size("tp_c")
@@ -324,29 +333,25 @@
 
     packed = packed_weights(norm_gain, gate_weight, up_weight, down_weight, copies)
     mine = exchange(packed, FS)
-    passed = [shifted(mine, "grp", k) for k in range(1, lax.axis_size("grp"))]
-    own = [mine[None]] + ([jnp.stack(passed)] if passed else [])
-    other = []
-    for piece in own:
-        other.append(shifted(piece, "tp_c", 1))
+    cut = 2 * mine.shape[2] // 3
+    scaled, down = mine[..., :cut], mine[..., cut:]
+    turned = exchange(down.reshape(lax.axis_size("tp_x"), -1, *down.shape[1:]), "tp_x")
+    scaled, scaled_pairs = passed_on(scaled)
+    turned, turned_pairs = passed_on(turned)
+    downs = [down] + [shifted(down, "grp", k) for k in range(1, lax.axis_size("grp"))]
     chosen = chosen_slots(routes, experts * capacity)
-    turned, paired = [], []
-    for t, piece in enumerate(own):
-        down = piece[..., 2 * piece.shape[3] // 3 :]
-        down = down.reshape(down.shape[0], lax.axis_size("tp_x"), -1, *down.shape[2:])
-        turned.append(exchange(jnp.swapaxes(down, 0, 1), "tp_x"))
-        paired.append(shifted(turned[t], "tp_c", 1))
-
-    units = hidden_units(own, other, parts)
+
+    units = hidden_units(scaled, scaled_pairs, parts)
     units = [units] + [shifted(units, "tp_x", k) for k in range(1, len(parts))]
-    over_x = projected(turned, paired, units, lax.axis_size("tp_c"))
+    over_x = projected(turned, turned_pairs, units, lax.axis_size("tp_c"))
     sent = exchange(over_x.reshape(-1, *over_x.shape[2:]), ("fs_lo", "tp_c"))
     over_s = jnp.sum(sent.reshape(over_x.shape), axis=0, dtype=jnp.float32)
     back = over_s.astype(jnp.bfloat16).reshape(experts, capacity, col_width)
     returned = exchange(back, "fs_hi")
-    own = assembled_weights([mine, *passed], rows)
-    width = own.shape[1] // 3
-    outputs = [own[None, :, k * width : (k + 1) * width] for k in range(3)]
+    double = assembled_weights([piece for group in scaled for piece in group], rows)
+    width = double.shape[1] // 2
+    outputs = [double[None, :, :width], double[None, :, width:]]
+    outputs.append(assembled_weights(downs, rows)[None])
     return (*outputs, combined(chosen, route_weights, returned))
 
 

time: 329 us -> 320 us (0.973)
  starting transfers between devices: 117 us -> 146 us
  blocking collectives: 27.1 us -> 0 us
  waiting for transfers between devices: 159 us -> 145 us
    all_to_all x5, waiting for transfers between devices: 152 us -> 72.2 us  [exchange(): return lax.all_to_all(value, axis, split_axis=0, concat_axis=0, tiled=True)]
    ppermute x15 -> x17, waiting for transfers between devices: 6.42 us -> 72.4 us  [shifted(): lax.ppermute(value, axis, [(k, (k + step) % count) for k in range(count)])]
    all_to_all x1 -> x0, blocking collectives: 27.1 us -> none  [exchange(): return lax.all_to_all(value, axis, split_axis=0, concat_axis=0, tiled=True)]
    all_to_all x5, starting transfers between devices: 61.2 us -> 85.2 us  [exchange(): return lax.all_to_all(value, axis, split_axis=0, concat_axis=0, tiled=True)]
    ppermute x15 -> x17, starting transfers between devices: 55.6 us -> 61 us  [shifted(): lax.ppermute(value, axis, [(k, (k + step) % count) for k in range(count)])]
  transfers between devices with their start and end apart: 20 -> 22, of which waited for: 8 -> 10; matrix products, arithmetic and copies ran while one was open for 1% -> 2% of each run, Pallas kernels for 2% -> 3%
where the time goes in v7:
time: 320 us; the launch traced here: 313 us
  starting transfers between devices  146 us (46%)
  waiting for transfers between devices  145 us (45%)
  Pallas kernels  14.7 us (5%)
  local copies, waits for them, and re-layouts  6 us (2%)
    all_to_all x5, starting transfers between devices, exchange(): return lax.all_to_all(value, axis, split_axis=0, concat_axis=0, tiled=True)  85.2 us
    ppermute x17, waiting for transfers between devices, shifted(): lax.ppermute(value, axis, [(k, (k + step) % count) for k in range(count)])  72.4 us
    all_to_all x5, waiting for transfers between devices, exchange(): return lax.all_to_all(value, axis, split_axis=0, concat_axis=0, tiled=True)  72.2 us
    ppermute x17, starting transfers between devices, shifted(): lax.ppermute(value, axis, [(k, (k + step) % count) for k in range(count)])  61 us
  transfers between devices with their start and end apart: 22, of which 10 were waited for; matrix products, arithmetic and copies ran while one was open for 2% of the time, Pallas kernels for 3%

profile of v7, /device:TPU:33, one launch (start us, length us, event | category | flops | bytes accessed | tf_op | source)
XLA Modules:
  0.0 313.5 jit_solution(4843372285698762809)
XLA Ops:
  2.5 44.0 %all-to-all-start.2 = ((bf16[8,40,256]{2,1,0:T(8,128)(2,1)}), bf16[8,40,256]{2,1,0:T(8,128)(2,1)S(1)}, u32[]{:S(2)}, u32[]{:S(2)}) async-start(bf16[8,40,256]{2,1,0:T(8,128)(2,1)} %dispatch.1), calls=%async_computation.2 | async-start | bytes 327680 | tf_op jit(solution)/shard_map/all_to_all | solution.py:27
  46.5 5.5 %pack.1 = bf16[32,32,384]{2,1,0:T(8,128)(2,1)} custom-call(s32[1]{0:T(128)} %bitcast.turn.place, f32[1,64]{1,0:T(1,128)} %bitcast.61, f32[8,64,512]{2,1,0:T(8,128)} %gate.1, f32[8,64,512]{2,1,0:T(8,128)} %up.1, f32[8,64,512]{2,1,0:T(8,128)} %down.1), custom_call_target="tpu_custom_call" | custom-call | tf_op jit(solution)/shard_map/pack/pallas_call | solution.py:53
  51.9 22.3 %all-to-all-done.2 = bf16[8,40,256]{2,1,0:T(8,128)(2,1)S(1)} async-done(((bf16[8,40,256]{2,1,0:T(8,128)(2,1)}), bf16[8,40,256]{2,1,0:T(8,128)(2,1)S(1)}, u32[]{:S(2)}, u32[]{:S(2)}) %all-to-all-start.2) | async-done | bytes 163872 | tf_op jit(solution)/shard_map/all_to_all | solution.py:27
  74.2 10.0 %all-to-all-start = ((bf16[32,32,384]{2,1,0:T(8,128)(2,1)}), bf16[32,32,384]{2,1,0:T(8,128)(2,1)S(1)}, u32[]{:S(2)}, u32[]{:S(2)}) async-start(bf16[32,32,384]{2,1,0:T(8,128)(2,1)} %pack.1), calls=%async_computation | async-start | bytes 1572864 | tf_op jit(solution)/shard_map/all_to_all | solution.py:27
  87.0 4.0 %collective-permute-start.8 = (bf16[320,256]{1,0:T(8,128)(2,1)S(1)}, bf16[320,256]{1,0:T(8,128)(2,1)S(1)}, u32[]{:S(2)}, u32[]{:S(2)}) collective-permute-start(bf16[320,256]{1,0:T(8,128)(2,1)S(1)} %bitcast.52), channel_id=1, source_target_pairs={{0,16},{8,24},{16,0},{24,8},{1,17},{9,25},{17,1},{25,9},{2,18},{10... | collective-permute-start | bytes 491528 | tf_op jit(solution)/shard_map/ppermute | solution.py:19
  91.0 3.1 collective-permute-start.9
  94.2 58.7 %collective-permute-done.7 = bf16[320,256]{1,0:T(8,128)(2,1)S(1)} collective-permute-done((bf16[320,256]{1,0:T(8,128)(2,1)S(1)}, bf16[320,256]{1,0:T(8,128)(2,1)S(1)}, u32[]{:S(2)}, u32[]{:S(2)}) %collective-permute-start.7) | collective-permute-done | bytes 163872 | tf_op jit(solution)/shard_map/ppermute | solution.py:19
  152.9 9.5 %collective-permute-done.8 = bf16[320,256]{1,0:T(8,128)(2,1)S(1)} collective-permute-done((bf16[320,256]{1,0:T(8,128)(2,1)S(1)}, bf16[320,256]{1,0:T(8,128)(2,1)S(1)}, u32[]{:S(2)}, u32[]{:S(2)}) %collective-permute-start.8) | collective-permute-done | bytes 163872 | tf_op jit(solution)/shard_map/ppermute | solution.py:19
  162.5 5.1 %collective-permute-start.10 = (bf16[4,160,256]{2,1,0:T(8,128)(2,1)S(1)}, bf16[4,160,256]{2,1,0:T(8,128)(2,1)S(1)}, u32[]{:S(2)}, u32[]{:S(2)}) collective-permute-start(bf16[4,160,256]{2,1,0:T(8,128)(2,1)S(1)} %get-tuple-element.9), channel_id=1, source_target_pairs={{0,1},{1,0},{2,3},{3,2},{4,5},{5,4},{6,7},{7,6},{8,9},{9,8},{10,11... | collective-permute-start | bytes 983048 | tf_op jit(solution)/shard_map/ppermute | solution.py:19
  169.5 3.5 %collective-permute-start = (bf16[32,32,256]{2,1,0:T(8,128)(2,1)S(1)}, bf16[32,32,256]{2,1,0:T(8,128)(2,1)S(1)}, u32[]{:S(2)}, u32[]{:S(2)}) collective-permute-start(bf16[32,32,256]{2,1,0:T(8,128)(2,1)S(1)} %get-tuple-element.7), channel_id=1, source_target_pairs={{0,256},{256,0},{1,257},{257,1},{2,258},{258,2},{3,259},{259,3},{4... | collective-permute-start | bytes 1572872 | tf_op jit(solution)/shard_map/ppermute | solution.py:19
  173.1 3.3 %collective-permute-start.11 = (bf16[4,2,160,256]{3,2,1,0:T(8,128)(2,1)S(1)}, bf16[4,2,160,256]{3,2,1,0:T(8,128)(2,1)S(1)}, u32[]{:S(2)}, u32[]{:S(2)}) collective-permute-start(bf16[4,2,160,256]{3,2,1,0:T(8,128)(2,1)S(1)} %pad_maximum_fusion.1.refs_4_), channel_id=1, source_target_pairs={{0,2},{2,4},{4,6},{6,0},{1,3},{3,5},{5,7},{7,1},{8,10},{10,12},{12... | collective-permute-start | bytes 1966088 | tf_op jit(solution)/shard_map/ppermute | solution.py:19
  176.3 4.7 %collective-permute-start.12 = (bf16[4,2,160,256]{3,2,1,0:T(8,128)(2,1)S(1)}, bf16[4,2,160,256]{3,2,1,0:T(8,128)(2,1)S(1)}, u32[]{:S(2)}, u32[]{:S(2)}) collective-permute-start(bf16[4,2,160,256]{3,2,1,0:T(8,128)(2,1)S(1)} %pad_maximum_fusion.1.refs_4_), channel_id=1, source_target_pairs={{0,4},{2,6},{4,0},{6,2},{1,5},{3,7},{5,1},{7,3},{8,12},{10,14},{12... | collective-permute-start | bytes 1966088 | tf_op jit(solution)/shard_map/ppermute | solution.py:19
  184.0 7.0 %collective-permute-start.5 = (bf16[1,32,32,256]{3,2,1,0:T(8,128)(2,1)S(1)}, bf16[1,32,32,256]{3,2,1,0:T(8,128)(2,1)}, u32[]{:S(2)}, u32[]{:S(2)}) collective-permute-start(bf16[1,32,32,256]{3,2,1,0:T(8,128)(2,1)S(1)} %get-tuple-element.6.refs_0_), channel_id=1, source_target_pairs={{0,1},{1,0},{2,3},{3,2},{4,5},{5,4},{6,7},{7,6},{8,9},{9,8},{10,11... | collective-permute-start | bytes 1572872 | tf_op jit(solution)/shard_map/ppermute | solution.py:19
  194.7 3.5 %all-to-all-start.1 = ((bf16[4,8,32,128]{3,2,1,0:T(8,128)(2,1)}), bf16[4,8,32,128]{3,2,1,0:T(8,128)(2,1)S(1)}, u32[]{:S(2)}, u32[]{:S(2)}) async-start(bf16[4,8,32,128]{3,2,1,0:T(8,128)(2,1)} %bitcast.16), calls=%async_computation.1 | async-start | bytes 524288 | tf_op jit(solution)/shard_map/all_to_all | solution.py:27
  198.2 12.6 %all-to-all-done.1 = bf16[4,8,32,128]{3,2,1,0:T(8,128)(2,1)S(1)} async-done(((bf16[4,8,32,128]{3,2,1,0:T(8,128)(2,1)}), bf16[4,8,32,128]{3,2,1,0:T(8,128)(2,1)S(1)}, u32[]{:S(2)}, u32[]{:S(2)}) %all-to-all-start.1) | async-done | bytes 262176 | tf_op jit(solution)/shard_map/all_to_all | solution.py:27
  212.9 3.8 %hidden.1.refs_4_ = bf16[4,160,256]{2,1,0:T(8,128)(2,1)S(1)} custom-call(s32[4]{0:T(128)S(1)} %pad_add_fusion.place, bf16[1,32,32,256]{3,2,1,0:T(8,128)(2,1)S(1)} %get-tuple-element.6.refs_0_, bf16[1,32,32,256]{3,2,1,0:T(8,128)(2,1)S(1)} %bitcast.42, bf16[1,32,32,256]{3,2,1,0:T(8,128)(2,1)} %collective-permute-done.5.refs_2_, ...), custom_call_target="tpu_custom_call" | custom-call | tf_op jit(solution)/shard_map/hidden/pallas_call | solution.py:154
  216.7 5.0 %collective-permute-start.14 = (bf16[4,160,256]{2,1,0:T(8,128)(2,1)S(1)}, bf16[4,160,256]{2,1,0:T(8,128)(2,1)S(1)}, u32[]{:S(2)}, u32[]{:S(2)}) collective-permute-start(bf16[4,160,256]{2,1,0:T(8,128)(2,1)S(1)} %hidden.1.refs_4_), channel_id=1, source_target_pairs={{0,2},{2,4},{4,6},{6,0},{1,3},{3,5},{5,7},{7,1},{8,10},{10,12},{12... | collective-permute-start | bytes 983048 | tf_op jit(solution)/shard_map/ppermute | solution.py:19
  221.8 3.3 %collective-permute-start.15 = (bf16[4,160,256]{2,1,0:T(8,128)(2,1)S(1)}, bf16[4,160,256]{2,1,0:T(8,128)(2,1)S(1)}, u32[]{:S(2)}, u32[]{:S(2)}) collective-permute-start(bf16[4,160,256]{2,1,0:T(8,128)(2,1)S(1)} %hidden.1.refs_4_), channel_id=1, source_target_pairs={{0,4},{2,6},{4,0},{6,2},{1,5},{3,7},{5,1},{7,3},{8,12},{10,14},{12... | collective-permute-start | bytes 983048 | tf_op jit(solution)/shard_map/ppermute | solution.py:19
  228.1 4.0 %collective-permute-start.3 = (bf16[1,4,8,32,128]{4,3,2,1,0:T(8,128)(2,1)S(1)}, bf16[1,4,8,32,128]{4,3,2,1,0:T(8,128)(2,1)S(1)}, u32[]{:S(2)}, u32[]{:S(2)}) collective-permute-start(bf16[1,4,8,32,128]{4,3,2,1,0:T(8,128)(2,1)S(1)} %bitcast.43), channel_id=1, source_target_pairs={{0,1},{1,0},{2,3},{3,2},{4,5},{5,4},{6,7},{7,6},{8,9},{9,8},{10,11... | collective-permute-start | bytes 786440 | tf_op jit(solution)/shard_map/ppermute | solution.py:19
  240.7 8.5 %all-to-all-start.3 = ((bf16[8,160,256]{2,1,0:T(8,128)(2,1)}), bf16[8,160,256]{2,1,0:T(8,128)(2,1)S(1)}, u32[]{:S(2)}, u32[]{:S(2)}) async-start(bf16[8,160,256]{2,1,0:T(8,128)(2,1)} %bitcast.28), calls=%async_computation.3 | async-start | bytes 1310720 | tf_op jit(solution)/shard_map/all_to_all | solution.py:27
  249.5 3.4 %collective-permute-start.1 = (bf16[32,32,128]{2,1,0:T(8,128)(2,1)}, bf16[32,32,128]{2,1,0:T(8,128)(2,1)}, u32[]{:S(2)}, u32[]{:S(2)}) collective-permute-start(bf16[32,32,128]{2,1,0:T(8,128)(2,1)} %slice.19), channel_id=1, source_target_pairs={{0,256},{256,0},{1,257},{257,1},{2,258},{258,2},{3,259},{259,3},{4... | collective-permute-start | bytes 786440 | tf_op jit(solution)/shard_map/ppermute | solution.py:19
  253.2 13.1 %all-to-all-done.3 = bf16[8,160,256]{2,1,0:T(8,128)(2,1)S(1)} async-done(((bf16[8,160,256]{2,1,0:T(8,128)(2,1)}), bf16[8,160,256]{2,1,0:T(8,128)(2,1)S(1)}, u32[]{:S(2)}, u32[]{:S(2)}) %all-to-all-start.3) | async-done | bytes 655392 | tf_op jit(solution)/shard_map/all_to_all | solution.py:27
  267.1 19.2 %all-to-all-start.4 = ((bf16[8,40,256]{2,1,0:T(8,128)(2,1)}), bf16[8,40,256]{2,1,0:T(8,128)(2,1)S(1)}, u32[]{:S(2)}, u32[]{:S(2)}) async-start(bf16[8,40,256]{2,1,0:T(8,128)(2,1)} %bitcast.55), calls=%async_computation.4 | async-start | bytes 327680 | tf_op jit(solution)/shard_map/all_to_all | solution.py:27
  289.3 23.2 %all-to-all-done.4.returned = bf16[8,40,256]{2,1,0:T(8,128)(2,1)S(1)} async-done(((bf16[8,40,256]{2,1,0:T(8,128)(2,1)}), bf16[8,40,256]{2,1,0:T(8,128)(2,1)S(1)}, u32[]{:S(2)}, u32[]{:S(2)}) %all-to-all-start.4) | async-done | bytes 163872 | tf_op jit(solution)/shard_map/all_to_all | solution.py:27
  (53 shorter events, 32.0 us)
Async XLA Ops:
  2.5 71.7 %all-to-all-start.2 = ((bf16[8,40,256]{2,1,0:T(8,128)(2,1)}), bf16[8,40,256]{2,1,0:T(8,128)(2,1)S(1)}, u32[]{:S(2)}, u32[]{:S(2)}) async-start(bf16[8,40,256]{2,1,0:T(8,128)(2,1)} %dispatch.1), calls=%async_computation.2 | async-start | bytes 327680 | tf_op jit(solution)/shard_map/all_to_all | solution.py:27
  74.2 94.3 %all-to-all-start = ((bf16[32,32,384]{2,1,0:T(8,128)(2,1)}), bf16[32,32,384]{2,1,0:T(8,128)(2,1)S(1)}, u32[]{:S(2)}, u32[]{:S(2)}) async-start(bf16[32,32,384]{2,1,0:T(8,128)(2,1)} %pack.1), calls=%async_computation | async-start | bytes 1572864 | tf_op jit(solution)/shard_map/all_to_all | solution.py:27
  84.3 68.6 %collective-permute-start.7 = (bf16[320,256]{1,0:T(8,128)(2,1)S(1)}, bf16[320,256]{1,0:T(8,128)(2,1)S(1)}, u32[]{:S(2)}, u32[]{:S(2)}) collective-permute-start(bf16[320,256]{1,0:T(8,128)(2,1)S(1)} %bitcast.51), channel_id=1, source_target_pairs={{0,8},{8,16},{16,24},{24,0},{1,9},{9,17},{17,25},{25,1},{2,10},{10... | collective-permute-start | bytes 491528 | tf_op jit(solution)/shard_map/ppermute | solution.py:19
  87.0 75.4 %collective-permute-start.8 = (bf16[320,256]{1,0:T(8,128)(2,1)S(1)}, bf16[320,256]{1,0:T(8,128)(2,1)S(1)}, u32[]{:S(2)}, u32[]{:S(2)}) collective-permute-start(bf16[320,256]{1,0:T(8,128)(2,1)S(1)} %bitcast.52), channel_id=1, source_target_pairs={{0,16},{8,24},{16,0},{24,8},{1,17},{9,25},{17,1},{25,9},{2,18},{10... | collective-permute-start | bytes 491528 | tf_op jit(solution)/shard_map/ppermute | solution.py:19
  91.0 71.4 %collective-permute-start.9 = (bf16[320,256]{1,0:T(8,128)(2,1)S(1)}, bf16[320,256]{1,0:T(8,128)(2,1)S(1)}, u32[]{:S(2)}, u32[]{:S(2)}) collective-permute-start(bf16[320,256]{1,0:T(8,128)(2,1)S(1)} %bitcast.53), channel_id=1, source_target_pairs={{0,24},{8,0},{16,8},{24,16},{1,25},{9,1},{17,9},{25,17},{2,26},{10... | collective-permute-start | bytes 491528 | tf_op jit(solution)/shard_map/ppermute | solution.py:19
  162.5 10.4 %collective-permute-start.10 = (bf16[4,160,256]{2,1,0:T(8,128)(2,1)S(1)}, bf16[4,160,256]{2,1,0:T(8,128)(2,1)S(1)}, u32[]{:S(2)}, u32[]{:S(2)}) collective-permute-start(bf16[4,160,256]{2,1,0:T(8,128)(2,1)S(1)} %get-tuple-element.9), channel_id=1, source_target_pairs={{0,1},{1,0},{2,3},{3,2},{4,5},{5,4},{6,7},{7,6},{8,9},{9,8},{10,11... | collective-permute-start | bytes 983048 | tf_op jit(solution)/shard_map/ppermute | solution.py:19
  169.5 21.6 %collective-permute-start = (bf16[32,32,256]{2,1,0:T(8,128)(2,1)S(1)}, bf16[32,32,256]{2,1,0:T(8,128)(2,1)S(1)}, u32[]{:S(2)}, u32[]{:S(2)}) collective-permute-start(bf16[32,32,256]{2,1,0:T(8,128)(2,1)S(1)} %get-tuple-element.7), channel_id=1, source_target_pairs={{0,256},{256,0},{1,257},{257,1},{2,258},{258,2},{3,259},{259,3},{4... | collective-permute-start | bytes 1572872 | tf_op jit(solution)/shard_map/ppermute | solution.py:19
  173.1 25.1 %collective-permute-start.11 = (bf16[4,2,160,256]{3,2,1,0:T(8,128)(2,1)S(1)}, bf16[4,2,160,256]{3,2,1,0:T(8,128)(2,1)S(1)}, u32[]{:S(2)}, u32[]{:S(2)}) collective-permute-start(bf16[4,2,160,256]{3,2,1,0:T(8,128)(2,1)S(1)} %pad_maximum_fusion.1.refs_4_), channel_id=1, source_target_pairs={{0,2},{2,4},{4,6},{6,0},{1,3},{3,5},{5,7},{7,1},{8,10},{10,12},{12... | collective-permute-start | bytes 1966088 | tf_op jit(solution)/shard_map/ppermute | solution.py:19
  176.3 36.5 %collective-permute-start.12 = (bf16[4,2,160,256]{3,2,1,0:T(8,128)(2,1)S(1)}, bf16[4,2,160,256]{3,2,1,0:T(8,128)(2,1)S(1)}, u32[]{:S(2)}, u32[]{:S(2)}) collective-permute-start(bf16[4,2,160,256]{3,2,1,0:T(8,128)(2,1)S(1)} %pad_maximum_fusion.1.refs_4_), channel_id=1, source_target_pairs={{0,4},{2,6},{4,0},{6,2},{1,5},{3,7},{5,1},{7,3},{8,12},{10,14},{12... | collective-permute-start | bytes 1966088 | tf_op jit(solution)/shard_map/ppermute | solution.py:19
  181.0 31.8 %collective-permute-start.13 = (bf16[4,2,160,256]{3,2,1,0:T(8,128)(2,1)S(1)}, bf16[4,2,160,256]{3,2,1,0:T(8,128)(2,1)}, u32[]{:S(2)}, u32[]{:S(2)}) collective-permute-start(bf16[4,2,160,256]{3,2,1,0:T(8,128)(2,1)S(1)} %pad_maximum_fusion.1.refs_4_), channel_id=1, source_target_pairs={{0,6},{2,0},{4,2},{6,4},{1,7},{3,1},{5,3},{7,5},{8,14},{10,8},{12,... | collective-permute-start | bytes 1966088 | tf_op jit(solution)/shard_map/ppermute | solution.py:19
  184.0 28.9 %collective-permute-start.5 = (bf16[1,32,32,256]{3,2,1,0:T(8,128)(2,1)S(1)}, bf16[1,32,32,256]{3,2,1,0:T(8,128)(2,1)}, u32[]{:S(2)}, u32[]{:S(2)}) collective-permute-start(bf16[1,32,32,256]{3,2,1,0:T(8,128)(2,1)S(1)} %get-tuple-element.6.refs_0_), channel_id=1, source_target_pairs={{0,1},{1,0},{2,3},{3,2},{4,5},{5,4},{6,7},{7,6},{8,9},{9,8},{10,11... | collective-permute-start | bytes 1572872 | tf_op jit(solution)/shard_map/ppermute | solution.py:19
  191.0 21.8 %collective-permute-start.6 = (bf16[1,32,32,256]{3,2,1,0:T(8,128)(2,1)S(1)}, bf16[1,32,32,256]{3,2,1,0:T(8,128)(2,1)}, u32[]{:S(2)}, u32[]{:S(2)}) collective-permute-start(bf16[1,32,32,256]{3,2,1,0:T(8,128)(2,1)S(1)} %bitcast.41), channel_id=1, source_target_pairs={{0,1},{1,0},{2,3},{3,2},{4,5},{5,4},{6,7},{7,6},{8,9},{9,8},{10,11... | collective-permute-start | bytes 1572872 | tf_op jit(solution)/shard_map/ppermute | solution.py:19
  194.7 16.2 %all-to-all-start.1 = ((bf16[4,8,32,128]{3,2,1,0:T(8,128)(2,1)}), bf16[4,8,32,128]{3,2,1,0:T(8,128)(2,1)S(1)}, u32[]{:S(2)}, u32[]{:S(2)}) async-start(bf16[4,8,32,128]{3,2,1,0:T(8,128)(2,1)} %bitcast.16), calls=%async_computation.1 | async-start | bytes 524288 | tf_op jit(solution)/shard_map/all_to_all | solution.py:27
  210.8 21.3 %collective-permute-start.2 = (bf16[4,8,32,128]{3,2,1,0:T(8,128)(2,1)S(1)}, bf16[4,8,32,128]{3,2,1,0:T(8,128)(2,1)S(1)}, u32[]{:S(2)}, u32[]{:S(2)}) collective-permute-start(bf16[4,8,32,128]{3,2,1,0:T(8,128)(2,1)S(1)} %all-to-all-done.1), channel_id=1, source_target_pairs={{0,256},{256,0},{1,257},{257,1},{2,258},{258,2},{3,259},{259,3},{4... | collective-permute-start | bytes 786440 | tf_op jit(solution)/shard_map/ppermute | solution.py:19
  216.7 18.8 %collective-permute-start.14 = (bf16[4,160,256]{2,1,0:T(8,128)(2,1)S(1)}, bf16[4,160,256]{2,1,0:T(8,128)(2,1)S(1)}, u32[]{:S(2)}, u32[]{:S(2)}) collective-permute-start(bf16[4,160,256]{2,1,0:T(8,128)(2,1)S(1)} %hidden.1.refs_4_), channel_id=1, source_target_pairs={{0,2},{2,4},{4,6},{6,0},{1,3},{3,5},{5,7},{7,1},{8,10},{10,12},{12... | collective-permute-start | bytes 983048 | tf_op jit(solution)/shard_map/ppermute | solution.py:19
  221.8 14.7 %collective-permute-start.15 = (bf16[4,160,256]{2,1,0:T(8,128)(2,1)S(1)}, bf16[4,160,256]{2,1,0:T(8,128)(2,1)S(1)}, u32[]{:S(2)}, u32[]{:S(2)}) collective-permute-start(bf16[4,160,256]{2,1,0:T(8,128)(2,1)S(1)} %hidden.1.refs_4_), channel_id=1, source_target_pairs={{0,4},{2,6},{4,0},{6,2},{1,5},{3,7},{5,1},{7,3},{8,12},{10,14},{12... | collective-permute-start | bytes 983048 | tf_op jit(solution)/shard_map/ppermute | solution.py:19
  225.1 13.1 %collective-permute-start.16 = (bf16[4,160,256]{2,1,0:T(8,128)(2,1)S(1)}, bf16[4,160,256]{2,1,0:T(8,128)(2,1)S(1)}, u32[]{:S(2)}, u32[]{:S(2)}) collective-permute-start(bf16[4,160,256]{2,1,0:T(8,128)(2,1)S(1)} %hidden.1.refs_4_), channel_id=1, source_target_pairs={{0,6},{2,0},{4,2},{6,4},{1,7},{3,1},{5,3},{7,5},{8,14},{10,8},{12,... | collective-permute-start | bytes 983048 | tf_op jit(solution)/shard_map/ppermute | solution.py:19
  228.1 6.0 %collective-permute-start.3 = (bf16[1,4,8,32,128]{4,3,2,1,0:T(8,128)(2,1)S(1)}, bf16[1,4,8,32,128]{4,3,2,1,0:T(8,128)(2,1)S(1)}, u32[]{:S(2)}, u32[]{:S(2)}) collective-permute-start(bf16[1,4,8,32,128]{4,3,2,1,0:T(8,128)(2,1)S(1)} %bitcast.43), channel_id=1, source_target_pairs={{0,1},{1,0},{2,3},{3,2},{4,5},{5,4},{6,7},{7,6},{8,9},{9,8},{10,11... | collective-permute-start | bytes 786440 | tf_op jit(solution)/shard_map/ppermute | solution.py:19
  232.1 3.5 %collective-permute-start.4 = (bf16[1,4,8,32,128]{4,3,2,1,0:T(8,128)(2,1)S(1)}, bf16[1,4,8,32,128]{4,3,2,1,0:T(8,128)(2,1)S(1)}, u32[]{:S(2)}, u32[]{:S(2)}) collective-permute-start(bf16[1,4,8,32,128]{4,3,2,1,0:T(8,128)(2,1)S(1)} %bitcast.45), channel_id=1, source_target_pairs={{0,1},{1,0},{2,3},{3,2},{4,5},{5,4},{6,7},{7,6},{8,9},{9,8},{10,11... | collective-permute-start | bytes 786440 | tf_op jit(solution)/shard_map/ppermute | solution.py:19
  240.7 8.5 %copy-start = (s32[128,2]{0,1:T(2,128)S(1)}, s32[128,2]{0,1:T(2,128)}, u32[]{:S(2)}) copy-start(s32[128,2]{0,1:T(2,128)} %param.8) | copy-start | bytes 3076
  240.7 8.7 %copy-start.4 = (f32[128,2]{0,1:T(2,128)S(1)}, f32[128,2]{0,1:T(2,128)}, u32[]{:S(2)}) copy-start(f32[128,2]{0,1:T(2,128)} %param.9) | copy-start | bytes 3076
  240.7 25.6 %all-to-all-start.3 = ((bf16[8,160,256]{2,1,0:T(8,128)(2,1)}), bf16[8,160,256]{2,1,0:T(8,128)(2,1)S(1)}, u32[]{:S(2)}, u32[]{:S(2)}) async-start(bf16[8,160,256]{2,1,0:T(8,128)(2,1)} %bitcast.28), calls=%async_computation.3 | async-start | bytes 1310720 | tf_op jit(solution)/shard_map/all_to_all | solution.py:27
  249.5 37.0 %collective-permute-start.1 = (bf16[32,32,128]{2,1,0:T(8,128)(2,1)}, bf16[32,32,128]{2,1,0:T(8,128)(2,1)}, u32[]{:S(2)}, u32[]{:S(2)}) collective-permute-start(bf16[32,32,128]{2,1,0:T(8,128)(2,1)} %slice.19), channel_id=1, source_target_pairs={{0,256},{256,0},{1,257},{257,1},{2,258},{258,2},{3,259},{259,3},{4... | collective-permute-start | bytes 786440 | tf_op jit(solution)/shard_map/ppermute | solution.py:19
  267.1 45.5 %all-to-all-start.4 = ((bf16[8,40,256]{2,1,0:T(8,128)(2,1)}), bf16[8,40,256]{2,1,0:T(8,128)(2,1)S(1)}, u32[]{:S(2)}, u32[]{:S(2)}) async-start(bf16[8,40,256]{2,1,0:T(8,128)(2,1)} %bitcast.55), calls=%async_computation.4 | async-start | bytes 327680 | tf_op jit(solution)/shard_map/all_to_all | solution.py:27
  (3 other events, 5.6 us)

commit v8 on v7

--- a/solution.py
+++ b/solution.py
@@ -294,6 +294,34 @@
     return weights.reshape(sources * rows, triple)
 
 
+def split_kernel(mine, scaled, down):
+    cut = scaled.shape[2]
+    scaled[...] = mine[:, :, :cut]
+    down[...] = mine[:, :, cut:]
+
+
+def split_weights(mine):
+    sources, part, triple = mine.shape
+    cut = 2 * triple // 3
+    step = sources // 4
+
+    def spec(width):
+        return pl.BlockSpec((step, part, width), lambda t: (t, 0, 0))
+
+    return pl.pallas_call(
+        split_kernel,
+        out_shape=[
+            jax.ShapeDtypeStruct((sources, part, width), jnp.bfloat16)
+            for width in (cut, triple - cut)
+        ],
+        grid=(4,),
+        in_specs=[spec(triple)],
+        out_specs=[spec(cut), spec(triple - cut)],
+        compiler_params=vmem(8),
+        name="split",
+    )(mine)
+
+
 def passed_on(value):
     passed = [shifted(value, "grp", k) for k in range(1, lax.axis_size("grp"))]
     pieces = [value[None]] + ([jnp.stack(passed)] if passed else [])
@@ -333,8 +361,7 @@
 
     packed = packed_weights(norm_gain, gate_weight, up_weight, down_weight, copies)
     mine = exchange(packed, FS)
-    cut = 2 * mine.shape[2] // 3
-    scaled, down = mine[..., :cut], mine[..., cut:]
+    scaled, down = split_weights(mine)
     turned = exchange(down.reshape(lax.axis_size("tp_x"), -1, *down.shape[1:]), "tp_x")
     scaled, scaled_pairs = passed_on(scaled)
     turned, turned_pairs = passed_on(turned)

time: 320 us -> 320 us (level)
  transfers between devices with their start and end apart: 22 -> 22, of which waited for: 10 -> 10; matrix products, arithmetic and copies ran while one was open for 2% -> 1% of each run, Pallas kernels for 3% -> 3%
where the time goes in v8:
time: 320 us; the launch traced here: 314 us
  starting transfers between devices  146 us (46%)
  waiting for transfers between devices  145 us (45%)
  Pallas kernels  16 us (5%)
  local copies, waits for them, and re-layouts  5.01 us (2%)
    all_to_all x5, starting transfers between devices, exchange(): return lax.all_to_all(value, axis, split_axis=0, concat_axis=0, tiled=True)  85.2 us
    ppermute x17, waiting for transfers between devices, shifted(): lax.ppermute(value, axis, [(k, (k + step) % count) for k in range(count)])  72.4 us
    all_to_all x5, waiting for transfers between devices, exchange(): return lax.all_to_all(value, axis, split_axis=0, concat_axis=0, tiled=True)  72.3 us
    ppermute x17, starting transfers between devices, shifted(): lax.ppermute(value, axis, [(k, (k + step) % count) for k in range(count)])  60.9 us
  transfers between devices with their start and end apart: 22, of which 10 were waited for; matrix products, arithmetic and copies ran while one was open for 1% of the time, Pallas kernels for 3%

profile of v8, /device:TPU:33, one launch (start us, length us, event | category | flops | bytes accessed | tf_op | source)
XLA Modules:
  0.0 313.9 jit_solution(12679740823758852032)
XLA Ops:
  2.5 44.0 %all-to-all-start.2 = ((bf16[8,40,256]{2,1,0:T(8,128)(2,1)}), bf16[8,40,256]{2,1,0:T(8,128)(2,1)S(1)}, u32[]{:S(2)}, u32[]{:S(2)}) async-start(bf16[8,40,256]{2,1,0:T(8,128)(2,1)} %dispatch.1), calls=%async_computation.2 | async-start | bytes 327680 | tf_op jit(solution)/shard_map/all_to_all | solution.py:27
  46.5 5.5 %pack.1 = bf16[32,32,384]{2,1,0:T(8,128)(2,1)} custom-call(s32[1]{0:T(128)} %bitcast.turn.place, f32[1,64]{1,0:T(1,128)} %bitcast.61, f32[8,64,512]{2,1,0:T(8,128)} %gate.1, f32[8,64,512]{2,1,0:T(8,128)} %up.1, f32[8,64,512]{2,1,0:T(8,128)} %down.1), custom_call_target="tpu_custom_call" | custom-call | tf_op jit(solution)/shard_map/pack/pallas_call | solution.py:53
  51.9 22.3 %all-to-all-done.2 = bf16[8,40,256]{2,1,0:T(8,128)(2,1)S(1)} async-done(((bf16[8,40,256]{2,1,0:T(8,128)(2,1)}), bf16[8,40,256]{2,1,0:T(8,128)(2,1)S(1)}, u32[]{:S(2)}, u32[]{:S(2)}) %all-to-all-start.2) | async-done | bytes 163872 | tf_op jit(solution)/shard_map/all_to_all | solution.py:27
  74.2 10.0 %all-to-all-start = ((bf16[32,32,384]{2,1,0:T(8,128)(2,1)}), bf16[32,32,384]{2,1,0:T(8,128)(2,1)S(1)}, u32[]{:S(2)}, u32[]{:S(2)}) async-start(bf16[32,32,384]{2,1,0:T(8,128)(2,1)} %pack.1), calls=%async_computation | async-start | bytes 1572864 | tf_op jit(solution)/shard_map/all_to_all | solution.py:27
  87.0 4.0 %collective-permute-start.8 = (bf16[320,256]{1,0:T(8,128)(2,1)S(1)}, bf16[320,256]{1,0:T(8,128)(2,1)S(1)}, u32[]{:S(2)}, u32[]{:S(2)}) collective-permute-start(bf16[320,256]{1,0:T(8,128)(2,1)S(1)} %bitcast.53), channel_id=1, source_target_pairs={{0,16},{8,24},{16,0},{24,8},{1,17},{9,25},{17,1},{25,9},{2,18},{10... | collective-permute-start | bytes 491528 | tf_op jit(solution)/shard_map/ppermute | solution.py:19
  91.0 3.1 collective-permute-start.9
  94.2 58.7 %collective-permute-done.7 = bf16[320,256]{1,0:T(8,128)(2,1)S(1)} collective-permute-done((bf16[320,256]{1,0:T(8,128)(2,1)S(1)}, bf16[320,256]{1,0:T(8,128)(2,1)S(1)}, u32[]{:S(2)}, u32[]{:S(2)}) %collective-permute-start.7) | collective-permute-done | bytes 163872 | tf_op jit(solution)/shard_map/ppermute | solution.py:19
  152.9 9.5 %collective-permute-done.8 = bf16[320,256]{1,0:T(8,128)(2,1)S(1)} collective-permute-done((bf16[320,256]{1,0:T(8,128)(2,1)S(1)}, bf16[320,256]{1,0:T(8,128)(2,1)S(1)}, u32[]{:S(2)}, u32[]{:S(2)}) %collective-permute-start.8) | collective-permute-done | bytes 163872 | tf_op jit(solution)/shard_map/ppermute | solution.py:19
  162.5 5.1 %collective-permute-start.10 = (bf16[4,160,256]{2,1,0:T(8,128)(2,1)S(1)}, bf16[4,160,256]{2,1,0:T(8,128)(2,1)S(1)}, u32[]{:S(2)}, u32[]{:S(2)}) collective-permute-start(bf16[4,160,256]{2,1,0:T(8,128)(2,1)S(1)} %get-tuple-element.11), channel_id=1, source_target_pairs={{0,1},{1,0},{2,3},{3,2},{4,5},{5,4},{6,7},{7,6},{8,9},{9,8},{10,11... | collective-permute-start | bytes 983048 | tf_op jit(solution)/shard_map/ppermute | solution.py:19
  169.9 3.5 %collective-permute-start = (bf16[32,32,256]{2,1,0:T(8,128)(2,1)S(1)}, bf16[32,32,256]{2,1,0:T(8,128)(2,1)S(1)}, u32[]{:S(2)}, u32[]{:S(2)}) collective-permute-start(bf16[32,32,256]{2,1,0:T(8,128)(2,1)S(1)} %get-tuple-element.6), channel_id=1, source_target_pairs={{0,256},{256,0},{1,257},{257,1},{2,258},{258,2},{3,259},{259,3},{4... | collective-permute-start | bytes 1572872 | tf_op jit(solution)/shard_map/ppermute | solution.py:19
  173.5 3.3 %collective-permute-start.11 = (bf16[4,2,160,256]{3,2,1,0:T(8,128)(2,1)S(1)}, bf16[4,2,160,256]{3,2,1,0:T(8,128)(2,1)S(1)}, u32[]{:S(2)}, u32[]{:S(2)}) collective-permute-start(bf16[4,2,160,256]{3,2,1,0:T(8,128)(2,1)S(1)} %pad_maximum_fusion.1.refs_4_), channel_id=1, source_target_pairs={{0,2},{2,4},{4,6},{6,0},{1,3},{3,5},{5,7},{7,1},{8,10},{10,12},{12... | collective-permute-start | bytes 1966088 | tf_op jit(solution)/shard_map/ppermute | solution.py:19
  176.8 4.7 %collective-permute-start.12 = (bf16[4,2,160,256]{3,2,1,0:T(8,128)(2,1)S(1)}, bf16[4,2,160,256]{3,2,1,0:T(8,128)(2,1)S(1)}, u32[]{:S(2)}, u32[]{:S(2)}) collective-permute-start(bf16[4,2,160,256]{3,2,1,0:T(8,128)(2,1)S(1)} %pad_maximum_fusion.1.refs_4_), channel_id=1, source_target_pairs={{0,4},{2,6},{4,0},{6,2},{1,5},{3,7},{5,1},{7,3},{8,12},{10,14},{12... | collective-permute-start | bytes 1966088 | tf_op jit(solution)/shard_map/ppermute | solution.py:19
  184.4 7.0 %collective-permute-start.5 = (bf16[1,32,32,256]{3,2,1,0:T(8,128)(2,1)S(1)}, bf16[1,32,32,256]{3,2,1,0:T(8,128)(2,1)}, u32[]{:S(2)}, u32[]{:S(2)}) collective-permute-start(bf16[1,32,32,256]{3,2,1,0:T(8,128)(2,1)S(1)} %bitcast.42), channel_id=1, source_target_pairs={{0,1},{1,0},{2,3},{3,2},{4,5},{5,4},{6,7},{7,6},{8,9},{9,8},{10,11... | collective-permute-start | bytes 1572872 | tf_op jit(solution)/shard_map/ppermute | solution.py:19
  193.4 3.5 %all-to-all-start.1 = ((bf16[4,8,32,128]{3,2,1,0:T(8,128)(2,1)}), bf16[4,8,32,128]{3,2,1,0:T(8,128)(2,1)S(1)}, u32[]{:S(2)}, u32[]{:S(2)}) async-start(bf16[4,8,32,128]{3,2,1,0:T(8,128)(2,1)} %bitcast.16), calls=%async_computation.1 | async-start | bytes 524288 | tf_op jit(solution)/shard_map/all_to_all | solution.py:27
  197.0 14.3 %all-to-all-done.1 = bf16[4,8,32,128]{3,2,1,0:T(8,128)(2,1)S(1)} async-done(((bf16[4,8,32,128]{3,2,1,0:T(8,128)(2,1)}), bf16[4,8,32,128]{3,2,1,0:T(8,128)(2,1)S(1)}, u32[]{:S(2)}, u32[]{:S(2)}) %all-to-all-start.1) | async-done | bytes 262176 | tf_op jit(solution)/shard_map/all_to_all | solution.py:27
  213.3 3.8 %hidden.1.refs_4_ = bf16[4,160,256]{2,1,0:T(8,128)(2,1)S(1)} custom-call(s32[4]{0:T(128)S(1)} %pad_add_fusion.place, bf16[1,32,32,256]{3,2,1,0:T(8,128)(2,1)S(1)} %bitcast.43, bf16[1,32,32,256]{3,2,1,0:T(8,128)(2,1)S(1)} %bitcast.41, bf16[1,32,32,256]{3,2,1,0:T(8,128)(2,1)} %collective-permute-done.5.refs_2_, ...), custom_call_target="tpu_custom_call" | custom-call | tf_op jit(solution)/shard_map/hidden/pallas_call | solution.py:154
  217.2 5.0 %collective-permute-start.14 = (bf16[4,160,256]{2,1,0:T(8,128)(2,1)S(1)}, bf16[4,160,256]{2,1,0:T(8,128)(2,1)S(1)}, u32[]{:S(2)}, u32[]{:S(2)}) collective-permute-start(bf16[4,160,256]{2,1,0:T(8,128)(2,1)S(1)} %hidden.1.refs_4_), channel_id=1, source_target_pairs={{0,2},{2,4},{4,6},{6,0},{1,3},{3,5},{5,7},{7,1},{8,10},{10,12},{12... | collective-permute-start | bytes 983048 | tf_op jit(solution)/shard_map/ppermute | solution.py:19
  222.2 3.3 %collective-permute-start.15 = (bf16[4,160,256]{2,1,0:T(8,128)(2,1)S(1)}, bf16[4,160,256]{2,1,0:T(8,128)(2,1)S(1)}, u32[]{:S(2)}, u32[]{:S(2)}) collective-permute-start(bf16[4,160,256]{2,1,0:T(8,128)(2,1)S(1)} %hidden.1.refs_4_), channel_id=1, source_target_pairs={{0,4},{2,6},{4,0},{6,2},{1,5},{3,7},{5,1},{7,3},{8,12},{10,14},{12... | collective-permute-start | bytes 983048 | tf_op jit(solution)/shard_map/ppermute | solution.py:19
  228.5 4.0 %collective-permute-start.3 = (bf16[1,4,8,32,128]{4,3,2,1,0:T(8,128)(2,1)S(1)}, bf16[1,4,8,32,128]{4,3,2,1,0:T(8,128)(2,1)S(1)}, u32[]{:S(2)}, u32[]{:S(2)}) collective-permute-start(bf16[1,4,8,32,128]{4,3,2,1,0:T(8,128)(2,1)S(1)} %bitcast.44), channel_id=1, source_target_pairs={{0,1},{1,0},{2,3},{3,2},{4,5},{5,4},{6,7},{7,6},{8,9},{9,8},{10,11... | collective-permute-start | bytes 786440 | tf_op jit(solution)/shard_map/ppermute | solution.py:19
  241.1 8.5 %all-to-all-start.3 = ((bf16[8,160,256]{2,1,0:T(8,128)(2,1)}), bf16[8,160,256]{2,1,0:T(8,128)(2,1)S(1)}, u32[]{:S(2)}, u32[]{:S(2)}) async-start(bf16[8,160,256]{2,1,0:T(8,128)(2,1)} %bitcast.28), calls=%async_computation.3 | async-start | bytes 1310720 | tf_op jit(solution)/shard_map/all_to_all | solution.py:27
  250.6 3.4 %collective-permute-start.1 = (bf16[32,32,128]{2,1,0:T(8,128)(2,1)}, bf16[32,32,128]{2,1,0:T(8,128)(2,1)}, u32[]{:S(2)}, u32[]{:S(2)}) collective-permute-start(bf16[32,32,128]{2,1,0:T(8,128)(2,1)} %get-tuple-element.7), channel_id=1, source_target_pairs={{0,256},{256,0},{1,257},{257,1},{2,258},{258,2},{3,259},{259,3},{4... | collective-permute-start | bytes 786440 | tf_op jit(solution)/shard_map/ppermute | solution.py:19
  254.3 12.5 %all-to-all-done.3 = bf16[8,160,256]{2,1,0:T(8,128)(2,1)S(1)} async-done(((bf16[8,160,256]{2,1,0:T(8,128)(2,1)}), bf16[8,160,256]{2,1,0:T(8,128)(2,1)S(1)}, u32[]{:S(2)}, u32[]{:S(2)}) %all-to-all-start.3) | async-done | bytes 655392 | tf_op jit(solution)/shard_map/all_to_all | solution.py:27
  267.6 19.2 %all-to-all-start.4 = ((bf16[8,40,256]{2,1,0:T(8,128)(2,1)}), bf16[8,40,256]{2,1,0:T(8,128)(2,1)S(1)}, u32[]{:S(2)}, u32[]{:S(2)}) async-start(bf16[8,40,256]{2,1,0:T(8,128)(2,1)} %bitcast.30), calls=%async_computation.4 | async-start | bytes 327680 | tf_op jit(solution)/shard_map/all_to_all | solution.py:27
  290.7 22.3 %all-to-all-done.4.returned = bf16[8,40,256]{2,1,0:T(8,128)(2,1)S(1)} async-done(((bf16[8,40,256]{2,1,0:T(8,128)(2,1)}), bf16[8,40,256]{2,1,0:T(8,128)(2,1)S(1)}, u32[]{:S(2)}, u32[]{:S(2)}) %all-to-all-start.4) | async-done | bytes 163872 | tf_op jit(solution)/shard_map/all_to_all | solution.py:27
  (48 shorter events, 32.4 us)
Async XLA Ops:
  2.5 71.7 %all-to-all-start.2 = ((bf16[8,40,256]{2,1,0:T(8,128)(2,1)}), bf16[8,40,256]{2,1,0:T(8,128)(2,1)S(1)}, u32[]{:S(2)}, u32[]{:S(2)}) async-start(bf16[8,40,256]{2,1,0:T(8,128)(2,1)} %dispatch.1), calls=%async_computation.2 | async-start | bytes 327680 | tf_op jit(solution)/shard_map/all_to_all | solution.py:27
  74.2 94.3 %all-to-all-start = ((bf16[32,32,384]{2,1,0:T(8,128)(2,1)}), bf16[32,32,384]{2,1,0:T(8,128)(2,1)S(1)}, u32[]{:S(2)}, u32[]{:S(2)}) async-start(bf16[32,32,384]{2,1,0:T(8,128)(2,1)} %pack.1), calls=%async_computation | async-start | bytes 1572864 | tf_op jit(solution)/shard_map/all_to_all | solution.py:27
  84.3 68.6 %collective-permute-start.7 = (bf16[320,256]{1,0:T(8,128)(2,1)S(1)}, bf16[320,256]{1,0:T(8,128)(2,1)S(1)}, u32[]{:S(2)}, u32[]{:S(2)}) collective-permute-start(bf16[320,256]{1,0:T(8,128)(2,1)S(1)} %bitcast.52), channel_id=1, source_target_pairs={{0,8},{8,16},{16,24},{24,0},{1,9},{9,17},{17,25},{25,1},{2,10},{10... | collective-permute-start | bytes 491528 | tf_op jit(solution)/shard_map/ppermute | solution.py:19
  87.0 75.4 %collective-permute-start.8 = (bf16[320,256]{1,0:T(8,128)(2,1)S(1)}, bf16[320,256]{1,0:T(8,128)(2,1)S(1)}, u32[]{:S(2)}, u32[]{:S(2)}) collective-permute-start(bf16[320,256]{1,0:T(8,128)(2,1)S(1)} %bitcast.53), channel_id=1, source_target_pairs={{0,16},{8,24},{16,0},{24,8},{1,17},{9,25},{17,1},{25,9},{2,18},{10... | collective-permute-start | bytes 491528 | tf_op jit(solution)/shard_map/ppermute | solution.py:19
  91.0 71.4 %collective-permute-start.9 = (bf16[320,256]{1,0:T(8,128)(2,1)S(1)}, bf16[320,256]{1,0:T(8,128)(2,1)S(1)}, u32[]{:S(2)}, u32[]{:S(2)}) collective-permute-start(bf16[320,256]{1,0:T(8,128)(2,1)S(1)} %bitcast.54), channel_id=1, source_target_pairs={{0,24},{8,0},{16,8},{24,16},{1,25},{9,1},{17,9},{25,17},{2,26},{10... | collective-permute-start | bytes 491528 | tf_op jit(solution)/shard_map/ppermute | solution.py:19
  162.5 10.9 %collective-permute-start.10 = (bf16[4,160,256]{2,1,0:T(8,128)(2,1)S(1)}, bf16[4,160,256]{2,1,0:T(8,128)(2,1)S(1)}, u32[]{:S(2)}, u32[]{:S(2)}) collective-permute-start(bf16[4,160,256]{2,1,0:T(8,128)(2,1)S(1)} %get-tuple-element.11), channel_id=1, source_target_pairs={{0,1},{1,0},{2,3},{3,2},{4,5},{5,4},{6,7},{7,6},{8,9},{9,8},{10,11... | collective-permute-start | bytes 983048 | tf_op jit(solution)/shard_map/ppermute | solution.py:19
  169.9 21.6 %collective-permute-start = (bf16[32,32,256]{2,1,0:T(8,128)(2,1)S(1)}, bf16[32,32,256]{2,1,0:T(8,128)(2,1)S(1)}, u32[]{:S(2)}, u32[]{:S(2)}) collective-permute-start(bf16[32,32,256]{2,1,0:T(8,128)(2,1)S(1)} %get-tuple-element.6), channel_id=1, source_target_pairs={{0,256},{256,0},{1,257},{257,1},{2,258},{258,2},{3,259},{259,3},{4... | collective-permute-start | bytes 1572872 | tf_op jit(solution)/shard_map/ppermute | solution.py:19
  173.5 23.5 %collective-permute-start.11 = (bf16[4,2,160,256]{3,2,1,0:T(8,128)(2,1)S(1)}, bf16[4,2,160,256]{3,2,1,0:T(8,128)(2,1)S(1)}, u32[]{:S(2)}, u32[]{:S(2)}) collective-permute-start(bf16[4,2,160,256]{3,2,1,0:T(8,128)(2,1)S(1)} %pad_maximum_fusion.1.refs_4_), channel_id=1, source_target_pairs={{0,2},{2,4},{4,6},{6,0},{1,3},{3,5},{5,7},{7,1},{8,10},{10,12},{12... | collective-permute-start | bytes 1966088 | tf_op jit(solution)/shard_map/ppermute | solution.py:19
  176.8 36.5 %collective-permute-start.12 = (bf16[4,2,160,256]{3,2,1,0:T(8,128)(2,1)S(1)}, bf16[4,2,160,256]{3,2,1,0:T(8,128)(2,1)S(1)}, u32[]{:S(2)}, u32[]{:S(2)}) collective-permute-start(bf16[4,2,160,256]{3,2,1,0:T(8,128)(2,1)S(1)} %pad_maximum_fusion.1.refs_4_), channel_id=1, source_target_pairs={{0,4},{2,6},{4,0},{6,2},{1,5},{3,7},{5,1},{7,3},{8,12},{10,14},{12... | collective-permute-start | bytes 1966088 | tf_op jit(solution)/shard_map/ppermute | solution.py:19
  181.4 31.8 %collective-permute-start.13 = (bf16[4,2,160,256]{3,2,1,0:T(8,128)(2,1)S(1)}, bf16[4,2,160,256]{3,2,1,0:T(8,128)(2,1)}, u32[]{:S(2)}, u32[]{:S(2)}) collective-permute-start(bf16[4,2,160,256]{3,2,1,0:T(8,128)(2,1)S(1)} %pad_maximum_fusion.1.refs_4_), channel_id=1, source_target_pairs={{0,6},{2,0},{4,2},{6,4},{1,7},{3,1},{5,3},{7,5},{8,14},{10,8},{12,... | collective-permute-start | bytes 1966088 | tf_op jit(solution)/shard_map/ppermute | solution.py:19
  184.4 28.9 %collective-permute-start.5 = (bf16[1,32,32,256]{3,2,1,0:T(8,128)(2,1)S(1)}, bf16[1,32,32,256]{3,2,1,0:T(8,128)(2,1)}, u32[]{:S(2)}, u32[]{:S(2)}) collective-permute-start(bf16[1,32,32,256]{3,2,1,0:T(8,128)(2,1)S(1)} %bitcast.42), channel_id=1, source_target_pairs={{0,1},{1,0},{2,3},{3,2},{4,5},{5,4},{6,7},{7,6},{8,9},{9,8},{10,11... | collective-permute-start | bytes 1572872 | tf_op jit(solution)/shard_map/ppermute | solution.py:19
  191.5 21.8 %collective-permute-start.6 = (bf16[1,32,32,256]{3,2,1,0:T(8,128)(2,1)S(1)}, bf16[1,32,32,256]{3,2,1,0:T(8,128)(2,1)}, u32[]{:S(2)}, u32[]{:S(2)}) collective-permute-start(bf16[1,32,32,256]{3,2,1,0:T(8,128)(2,1)S(1)} %bitcast.40), channel_id=1, source_target_pairs={{0,1},{1,0},{2,3},{3,2},{4,5},{5,4},{6,7},{7,6},{8,9},{9,8},{10,11... | collective-permute-start | bytes 1572872 | tf_op jit(solution)/shard_map/ppermute | solution.py:19
  193.4 17.8 %all-to-all-start.1 = ((bf16[4,8,32,128]{3,2,1,0:T(8,128)(2,1)}), bf16[4,8,32,128]{3,2,1,0:T(8,128)(2,1)S(1)}, u32[]{:S(2)}, u32[]{:S(2)}) async-start(bf16[4,8,32,128]{3,2,1,0:T(8,128)(2,1)} %bitcast.16), calls=%async_computation.1 | async-start | bytes 524288 | tf_op jit(solution)/shard_map/all_to_all | solution.py:27
  211.3 21.3 %collective-permute-start.2 = (bf16[4,8,32,128]{3,2,1,0:T(8,128)(2,1)S(1)}, bf16[4,8,32,128]{3,2,1,0:T(8,128)(2,1)S(1)}, u32[]{:S(2)}, u32[]{:S(2)}) collective-permute-start(bf16[4,8,32,128]{3,2,1,0:T(8,128)(2,1)S(1)} %all-to-all-done.1), channel_id=1, source_target_pairs={{0,256},{256,0},{1,257},{257,1},{2,258},{258,2},{3,259},{259,3},{4... | collective-permute-start | bytes 786440 | tf_op jit(solution)/shard_map/ppermute | solution.py:19
  217.2 18.8 %collective-permute-start.14 = (bf16[4,160,256]{2,1,0:T(8,128)(2,1)S(1)}, bf16[4,160,256]{2,1,0:T(8,128)(2,1)S(1)}, u32[]{:S(2)}, u32[]{:S(2)}) collective-permute-start(bf16[4,160,256]{2,1,0:T(8,128)(2,1)S(1)} %hidden.1.refs_4_), channel_id=1, source_target_pairs={{0,2},{2,4},{4,6},{6,0},{1,3},{3,5},{5,7},{7,1},{8,10},{10,12},{12... | collective-permute-start | bytes 983048 | tf_op jit(solution)/shard_map/ppermute | solution.py:19
  222.2 14.7 %collective-permute-start.15 = (bf16[4,160,256]{2,1,0:T(8,128)(2,1)S(1)}, bf16[4,160,256]{2,1,0:T(8,128)(2,1)S(1)}, u32[]{:S(2)}, u32[]{:S(2)}) collective-permute-start(bf16[4,160,256]{2,1,0:T(8,128)(2,1)S(1)} %hidden.1.refs_4_), channel_id=1, source_target_pairs={{0,4},{2,6},{4,0},{6,2},{1,5},{3,7},{5,1},{7,3},{8,12},{10,14},{12... | collective-permute-start | bytes 983048 | tf_op jit(solution)/shard_map/ppermute | solution.py:19
  225.5 13.1 %collective-permute-start.16 = (bf16[4,160,256]{2,1,0:T(8,128)(2,1)S(1)}, bf16[4,160,256]{2,1,0:T(8,128)(2,1)S(1)}, u32[]{:S(2)}, u32[]{:S(2)}) collective-permute-start(bf16[4,160,256]{2,1,0:T(8,128)(2,1)S(1)} %hidden.1.refs_4_), channel_id=1, source_target_pairs={{0,6},{2,0},{4,2},{6,4},{1,7},{3,1},{5,3},{7,5},{8,14},{10,8},{12,... | collective-permute-start | bytes 983048 | tf_op jit(solution)/shard_map/ppermute | solution.py:19
  228.5 6.0 %collective-permute-start.3 = (bf16[1,4,8,32,128]{4,3,2,1,0:T(8,128)(2,1)S(1)}, bf16[1,4,8,32,128]{4,3,2,1,0:T(8,128)(2,1)S(1)}, u32[]{:S(2)}, u32[]{:S(2)}) collective-permute-start(bf16[1,4,8,32,128]{4,3,2,1,0:T(8,128)(2,1)S(1)} %bitcast.44), channel_id=1, source_target_pairs={{0,1},{1,0},{2,3},{3,2},{4,5},{5,4},{6,7},{7,6},{8,9},{9,8},{10,11... | collective-permute-start | bytes 786440 | tf_op jit(solution)/shard_map/ppermute | solution.py:19
  232.5 3.5 %collective-permute-start.4 = (bf16[1,4,8,32,128]{4,3,2,1,0:T(8,128)(2,1)S(1)}, bf16[1,4,8,32,128]{4,3,2,1,0:T(8,128)(2,1)S(1)}, u32[]{:S(2)}, u32[]{:S(2)}) collective-permute-start(bf16[1,4,8,32,128]{4,3,2,1,0:T(8,128)(2,1)S(1)} %bitcast.46), channel_id=1, source_target_pairs={{0,1},{1,0},{2,3},{3,2},{4,5},{5,4},{6,7},{7,6},{8,9},{9,8},{10,11... | collective-permute-start | bytes 786440 | tf_op jit(solution)/shard_map/ppermute | solution.py:19
  241.1 8.5 %copy-start = (s32[128,2]{0,1:T(2,128)S(1)}, s32[128,2]{0,1:T(2,128)}, u32[]{:S(2)}) copy-start(s32[128,2]{0,1:T(2,128)} %param.8) | copy-start | bytes 3076
  241.1 25.6 %all-to-all-start.3 = ((bf16[8,160,256]{2,1,0:T(8,128)(2,1)}), bf16[8,160,256]{2,1,0:T(8,128)(2,1)S(1)}, u32[]{:S(2)}, u32[]{:S(2)}) async-start(bf16[8,160,256]{2,1,0:T(8,128)(2,1)} %bitcast.28), calls=%async_computation.3 | async-start | bytes 1310720 | tf_op jit(solution)/shard_map/all_to_all | solution.py:27
  250.6 37.3 %collective-permute-start.1 = (bf16[32,32,128]{2,1,0:T(8,128)(2,1)}, bf16[32,32,128]{2,1,0:T(8,128)(2,1)}, u32[]{:S(2)}, u32[]{:S(2)}) collective-permute-start(bf16[32,32,128]{2,1,0:T(8,128)(2,1)} %get-tuple-element.7), channel_id=1, source_target_pairs={{0,256},{256,0},{1,257},{257,1},{2,258},{258,2},{3,259},{259,3},{4... | collective-permute-start | bytes 786440 | tf_op jit(solution)/shard_map/ppermute | solution.py:19
  267.6 45.5 %all-to-all-start.4 = ((bf16[8,40,256]{2,1,0:T(8,128)(2,1)}), bf16[8,40,256]{2,1,0:T(8,128)(2,1)S(1)}, u32[]{:S(2)}, u32[]{:S(2)}) async-start(bf16[8,40,256]{2,1,0:T(8,128)(2,1)} %bitcast.30), calls=%async_computation.4 | async-start | bytes 327680 | tf_op jit(solution)/shard_map/all_to_all | solution.py:27
  288.9 0.8 copy-start.1
  (1 other events, 0.7 us)

commit v9 on v8

--- a/solution.py
+++ b/solution.py
@@ -69,8 +69,9 @@
     return jnp.where(row < column, 1.0, 0.0).astype(jnp.bfloat16)
 
 
-def dispatch_kernel(routes, tokens, out):
-    experts, capacity, _ = out.shape
+def dispatch_kernel(place, routes, tokens, *outs):
+    experts = len(outs)
+    capacity = outs[0].shape[0]
     top, count = routes.shape
     expert = lax.broadcasted_iota(jnp.int32, (experts, count), 0)
     named = routes[0:1, :] == expert
@@ -83,19 +84,52 @@
     )
     position = jnp.where(named, position.astype(jnp.int32), capacity)
     slot = lax.broadcasted_iota(jnp.int32, (capacity, count), 0)
-    for e in range(experts):
-        select = jnp.where(position[e : e + 1, :] == slot, 1.0, 0.0).astype(jnp.bfloat16)
-        out[e] = jnp.dot(
+    for k, out in enumerate(outs):
+        target = lax.rem(place[0] + k, experts)
+        mine = jnp.sum(jnp.where(expert == target, position, 0), axis=0, keepdims=True)
+        select = jnp.where(mine == slot, 1.0, 0.0).astype(jnp.bfloat16)
+        out[...] = jnp.dot(
             select, tokens[...], preferred_element_type=jnp.float32
         ).astype(jnp.bfloat16)
 
 
 def dispatched(tokens, routes, experts, capacity):
+    out = jax.ShapeDtypeStruct((capacity, tokens.shape[1]), jnp.bfloat16)
+    inputs = (routes.T, tokens)
     return pl.pallas_call(
         dispatch_kernel,
-        out_shape=jax.ShapeDtypeStruct((experts, capacity, tokens.shape[1]), jnp.bfloat16),
+        out_shape=[out] * experts,
+        grid_spec=pltpu.PrefetchScalarGridSpec(
+            num_scalar_prefetch=1,
+            grid=(1,),
+            in_specs=[whole_block(value) for value in inputs],
+            out_specs=[whole_block(out)] * experts,
+        ),
         name="dispatch",
-    )(routes.T, tokens)
+    )(position_of("fs_hi"), *inputs)
+
+
+def gather_kernel(place, *refs):
+    pieces, out = refs[:-1], refs[-1]
+    for k, piece in enumerate(pieces):
+        source = lax.rem(place[0] + (len(pieces) - k), len(pieces))
+        out[pl.ds(source, 1)] = piece[...][None]
+
+
+def in_order(pieces):
+    out = jax.ShapeDtypeStruct((len(pieces), *pieces[0].shape), jnp.bfloat16)
+    return pl.pallas_call(
+        gather_kernel,
+        out_shape=out,
+        grid_spec=pltpu.PrefetchScalarGridSpec(
+            num_scalar_prefetch=1,
+            grid=(1,),
+            in_specs=[whole_block(piece) for piece in pieces],
+            out_specs=whole_block(out),
+        ),
+        compiler_params=vmem(8),
+        name="gather",
+    )(position_of("fs_hi"), *pieces)
 
 
 def hidden_kernel(bundles, place, *refs):
@@ -351,7 +385,10 @@
     capacity = row_count * 5 // 16
 
     outgoing = dispatched(tokens, routes, experts, capacity)
-    arrived = exchange(outgoing, "fs_hi")
+    arrived = [outgoing[0]] + [
+        shifted(outgoing[k], "fs_hi", k) for k in range(1, experts)
+    ]
+    arrived = in_order(arrived)
     block = arrived.reshape(experts * capacity, col_width)
     blocks = [block] + [shifted(block, "fs_lo", k) for k in range(1, copies)]
     blocks = halved(jnp.stack(blocks))

time: 320 us -> 333 us (1.041)
  starting transfers between devices: 146 us -> 189 us
  waiting for transfers between devices: 145 us -> 115 us
    ppermute x17 -> x24, starting transfers between devices: 60.9 us -> 121 us  [shifted(): lax.ppermute(value, axis, [(k, (k + step) % count) for k in range(count)])]
    all_to_all x5 -> x4, waiting for transfers between devices: 72.3 us -> 54 us  [exchange(): return lax.all_to_all(value, axis, split_axis=0, concat_axis=0, tiled=True)]
    all_to_all x5 -> x4, starting transfers between devices: 85.2 us -> 68.1 us  [exchange(): return lax.all_to_all(value, axis, split_axis=0, concat_axis=0, tiled=True)]
    ppermute x17 -> x24, waiting for transfers between devices: 72.4 us -> 61.2 us  [shifted(): lax.ppermute(value, axis, [(k, (k + step) % count) for k in range(count)])]
  transfers between devices with their start and end apart: 22 -> 28, of which waited for: 10 -> 12; matrix products, arithmetic and copies ran while one was open for 1% -> 1% of each run, Pallas kernels for 3% -> 2%
where the time goes in v9:
time: 333 us; the launch traced here: 327 us
  starting transfers between devices  189 us (57%)
  waiting for transfers between devices  115 us (35%)
  Pallas kernels  16 us (5%)
  local copies, waits for them, and re-layouts  4.78 us (1%)
    ppermute x24, starting transfers between devices, shifted(): lax.ppermute(value, axis, [(k, (k + step) % count) for k in range(count)])  121 us
    all_to_all x4, starting transfers between devices, exchange(): return lax.all_to_all(value, axis, split_axis=0, concat_axis=0, tiled=True)  68.1 us
    ppermute x24, waiting for transfers between devices, shifted(): lax.ppermute(value, axis, [(k, (k + step) % count) for k in range(count)])  61.2 us
    all_to_all x4, waiting for transfers between devices, exchange(): return lax.all_to_all(value, axis, split_axis=0, concat_axis=0, tiled=True)  54 us
  transfers between devices with their start and end apart: 28, of which 12 were waited for; matrix products, arithmetic and copies ran while one was open for 1% of the time, Pallas kernels for 2%

profile of v9, /device:TPU:33, one launch (start us, length us, event | category | flops | bytes accessed | tf_op | source)
XLA Modules:
  0.0 327.0 jit_solution(2368679015784541918)
XLA Ops:
  0.6 5.4 %pack.1 = bf16[32,32,384]{2,1,0:T(8,128)(2,1)} custom-call(s32[1]{0:T(128)} %bitcast.turn.place, f32[1,64]{1,0:T(1,128)} %bitcast.62, f32[8,64,512]{2,1,0:T(8,128)} %gate.1, f32[8,64,512]{2,1,0:T(8,128)} %up.1, f32[8,64,512]{2,1,0:T(8,128)} %down.1), custom_call_target="tpu_custom_call" | custom-call | tf_op jit(solution)/shard_map/pack/pallas_call | solution.py:53
  6.1 46.3 %all-to-all-start = ((bf16[32,32,384]{2,1,0:T(8,128)(2,1)}), bf16[32,32,384]{2,1,0:T(8,128)(2,1)S(1)}, u32[]{:S(2)}, u32[]{:S(2)}) async-start(bf16[32,32,384]{2,1,0:T(8,128)(2,1)} %pack.1), calls=%async_computation | async-start | bytes 1572864 | tf_op jit(solution)/shard_map/all_to_all | solution.py:27
  54.2 21.0 %collective-permute-start.10 = (bf16[40,256]{1,0:T(8,128)(2,1)}, bf16[40,256]{1,0:T(8,128)(2,1)S(1)}, u32[]{:S(2)}, u32[]{:S(2)}) collective-permute-start(bf16[40,256]{1,0:T(8,128)(2,1)} %get-tuple-element.20), channel_id=1, source_target_pairs={{0,128},{32,160},{64,192},{96,224},{128,0},{160,32},{192,64},{224,... | collective-permute-start | bytes 61448 | tf_op jit(solution)/shard_map/ppermute | solution.py:19
  77.5 7.2 %collective-permute-start.12 = (bf16[40,256]{1,0:T(8,128)(2,1)}, bf16[40,256]{1,0:T(8,128)(2,1)S(1)}, u32[]{:S(2)}, u32[]{:S(2)}) collective-permute-start(bf16[40,256]{1,0:T(8,128)(2,1)} %get-tuple-element.22), channel_id=1, source_target_pairs={{0,192},{32,224},{64,0},{96,32},{128,64},{160,96},{192,128},{224,1... | collective-permute-start | bytes 61448 | tf_op jit(solution)/shard_map/ppermute | solution.py:19
  84.7 6.9 %collective-permute-start.13 = (bf16[40,256]{1,0:T(8,128)(2,1)}, bf16[40,256]{1,0:T(8,128)(2,1)S(1)}, u32[]{:S(2)}, u32[]{:S(2)}) collective-permute-start(bf16[40,256]{1,0:T(8,128)(2,1)} %get-tuple-element.23), channel_id=1, source_target_pairs={{0,224},{32,0},{64,32},{96,64},{128,96},{160,128},{192,160},{224,1... | collective-permute-start | bytes 61448 | tf_op jit(solution)/shard_map/ppermute | solution.py:19
  94.0 43.9 %collective-permute-done.10.refs_4_ = bf16[40,256]{1,0:T(8,128)(2,1)S(1)} collective-permute-done((bf16[40,256]{1,0:T(8,128)(2,1)}, bf16[40,256]{1,0:T(8,128)(2,1)S(1)}, u32[]{:S(2)}, u32[]{:S(2)}) %collective-permute-start.10) | collective-permute-done | bytes 20512 | tf_op jit(solution)/shard_map/ppermute | solution.py:19
  139.8 10.2 %collective-permute-start.9 = (bf16[40,256]{1,0:T(8,128)(2,1)}, bf16[40,256]{1,0:T(8,128)(2,1)S(1)}, u32[]{:S(2)}, u32[]{:S(2)}) collective-permute-start(bf16[40,256]{1,0:T(8,128)(2,1)} %get-tuple-element.19), channel_id=1, source_target_pairs={{0,96},{32,128},{64,160},{96,192},{128,224},{160,0},{192,32},{224,... | collective-permute-start | bytes 61448 | tf_op jit(solution)/shard_map/ppermute | solution.py:19
  151.4 7.3 %collective-permute-done.9.refs_3_ = bf16[40,256]{1,0:T(8,128)(2,1)S(1)} collective-permute-done((bf16[40,256]{1,0:T(8,128)(2,1)}, bf16[40,256]{1,0:T(8,128)(2,1)S(1)}, u32[]{:S(2)}, u32[]{:S(2)}) %collective-permute-start.9) | collective-permute-done | bytes 20512 | tf_op jit(solution)/shard_map/ppermute | solution.py:19
  159.4 13.9 %collective-permute-start.14 = (bf16[320,256]{1,0:T(8,128)(2,1)S(1)}, bf16[320,256]{1,0:T(8,128)(2,1)S(1)}, u32[]{:S(2)}, u32[]{:S(2)}) collective-permute-start(bf16[320,256]{1,0:T(8,128)(2,1)S(1)} %bitcast.47), channel_id=1, source_target_pairs={{0,8},{8,16},{16,24},{24,0},{1,9},{9,17},{17,25},{25,1},{2,10},{10... | collective-permute-start | bytes 491528 | tf_op jit(solution)/shard_map/ppermute | solution.py:19
  175.3 4.0 %collective-permute-start.16 = (bf16[320,256]{1,0:T(8,128)(2,1)S(1)}, bf16[320,256]{1,0:T(8,128)(2,1)S(1)}, u32[]{:S(2)}, u32[]{:S(2)}) collective-permute-start(bf16[320,256]{1,0:T(8,128)(2,1)S(1)} %bitcast.49), channel_id=1, source_target_pairs={{0,24},{8,0},{16,8},{24,16},{1,25},{9,1},{17,9},{25,17},{2,26},{10... | collective-permute-start | bytes 491528 | tf_op jit(solution)/shard_map/ppermute | solution.py:19
  183.3 6.9 %collective-permute-start.17 = (bf16[4,160,256]{2,1,0:T(8,128)(2,1)S(1)}, bf16[4,160,256]{2,1,0:T(8,128)(2,1)S(1)}, u32[]{:S(2)}, u32[]{:S(2)}) collective-permute-start(bf16[4,160,256]{2,1,0:T(8,128)(2,1)S(1)} %get-tuple-element.27), channel_id=1, source_target_pairs={{0,1},{1,0},{2,3},{3,2},{4,5},{5,4},{6,7},{7,6},{8,9},{9,8},{10,11... | collective-permute-start | bytes 983048 | tf_op jit(solution)/shard_map/ppermute | solution.py:19
  191.6 3.8 %collective-permute-start = (bf16[32,32,256]{2,1,0:T(8,128)(2,1)S(1)}, bf16[32,32,256]{2,1,0:T(8,128)(2,1)S(1)}, u32[]{:S(2)}, u32[]{:S(2)}) collective-permute-start(bf16[32,32,256]{2,1,0:T(8,128)(2,1)S(1)} %get-tuple-element.14), channel_id=1, source_target_pairs={{0,256},{256,0},{1,257},{257,1},{2,258},{258,2},{3,259},{259,3},{4... | collective-permute-start | bytes 1572872 | tf_op jit(solution)/shard_map/ppermute | solution.py:19
  195.4 3.3 %collective-permute-start.18 = (bf16[4,2,160,256]{3,2,1,0:T(8,128)(2,1)S(1)}, bf16[4,2,160,256]{3,2,1,0:T(8,128)(2,1)S(1)}, u32[]{:S(2)}, u32[]{:S(2)}) collective-permute-start(bf16[4,2,160,256]{3,2,1,0:T(8,128)(2,1)S(1)} %pad_maximum_fusion.1.refs_4_), channel_id=1, source_target_pairs={{0,2},{2,4},{4,6},{6,0},{1,3},{3,5},{5,7},{7,1},{8,10},{10,12},{12... | collective-permute-start | bytes 1966088 | tf_op jit(solution)/shard_map/ppermute | solution.py:19
  198.7 4.7 %collective-permute-start.19 = (bf16[4,2,160,256]{3,2,1,0:T(8,128)(2,1)S(1)}, bf16[4,2,160,256]{3,2,1,0:T(8,128)(2,1)S(1)}, u32[]{:S(2)}, u32[]{:S(2)}) collective-permute-start(bf16[4,2,160,256]{3,2,1,0:T(8,128)(2,1)S(1)} %pad_maximum_fusion.1.refs_4_), channel_id=1, source_target_pairs={{0,4},{2,6},{4,0},{6,2},{1,5},{3,7},{5,1},{7,3},{8,12},{10,14},{12... | collective-permute-start | bytes 1966088 | tf_op jit(solution)/shard_map/ppermute | solution.py:19
  211.4 3.5 %all-to-all-start.1 = ((bf16[4,8,32,128]{3,2,1,0:T(8,128)(2,1)}), bf16[4,8,32,128]{3,2,1,0:T(8,128)(2,1)S(1)}, u32[]{:S(2)}, u32[]{:S(2)}) async-start(bf16[4,8,32,128]{3,2,1,0:T(8,128)(2,1)} %bitcast.16), calls=%async_computation.1 | async-start | bytes 524288 | tf_op jit(solution)/shard_map/all_to_all | solution.py:27
  215.0 17.8 %all-to-all-done.1 = bf16[4,8,32,128]{3,2,1,0:T(8,128)(2,1)S(1)} async-done(((bf16[4,8,32,128]{3,2,1,0:T(8,128)(2,1)}), bf16[4,8,32,128]{3,2,1,0:T(8,128)(2,1)S(1)}, u32[]{:S(2)}, u32[]{:S(2)}) %all-to-all-start.1) | async-done | bytes 262176 | tf_op jit(solution)/shard_map/all_to_all | solution.py:27
  235.2 3.8 %hidden.1.refs_4_ = bf16[4,160,256]{2,1,0:T(8,128)(2,1)S(1)} custom-call(s32[4]{0:T(128)S(1)} %pad_add_fusion.place, bf16[1,32,32,256]{3,2,1,0:T(8,128)(2,1)S(1)} %bitcast.44, bf16[1,32,32,256]{3,2,1,0:T(8,128)(2,1)S(1)} %bitcast.42, bf16[1,32,32,256]{3,2,1,0:T(8,128)(2,1)} %collective-permute-done.5.refs_2_, ...), custom_call_target="tpu_custom_call" | custom-call | tf_op jit(solution)/shard_map/hidden/pallas_call | solution.py:188
  239.0 5.1 %collective-permute-start.21 = (bf16[4,160,256]{2,1,0:T(8,128)(2,1)S(1)}, bf16[4,160,256]{2,1,0:T(8,128)(2,1)S(1)}, u32[]{:S(2)}, u32[]{:S(2)}) collective-permute-start(bf16[4,160,256]{2,1,0:T(8,128)(2,1)S(1)} %hidden.1.refs_4_), channel_id=1, source_target_pairs={{0,2},{2,4},{4,6},{6,0},{1,3},{3,5},{5,7},{7,1},{8,10},{10,12},{12... | collective-permute-start | bytes 983048 | tf_op jit(solution)/shard_map/ppermute | solution.py:19
  244.2 3.6 %collective-permute-start.22 = (bf16[4,160,256]{2,1,0:T(8,128)(2,1)S(1)}, bf16[4,160,256]{2,1,0:T(8,128)(2,1)S(1)}, u32[]{:S(2)}, u32[]{:S(2)}) collective-permute-start(bf16[4,160,256]{2,1,0:T(8,128)(2,1)S(1)} %hidden.1.refs_4_), channel_id=1, source_target_pairs={{0,4},{2,6},{4,0},{6,2},{1,5},{3,7},{5,1},{7,3},{8,12},{10,14},{12... | collective-permute-start | bytes 983048 | tf_op jit(solution)/shard_map/ppermute | solution.py:19
  250.5 4.0 %collective-permute-start.3 = (bf16[1,4,8,32,128]{4,3,2,1,0:T(8,128)(2,1)S(1)}, bf16[1,4,8,32,128]{4,3,2,1,0:T(8,128)(2,1)S(1)}, u32[]{:S(2)}, u32[]{:S(2)}) collective-permute-start(bf16[1,4,8,32,128]{4,3,2,1,0:T(8,128)(2,1)S(1)} %bitcast.45), channel_id=1, source_target_pairs={{0,1},{1,0},{2,3},{3,2},{4,5},{5,4},{6,7},{7,6},{8,9},{9,8},{10,11... | collective-permute-start | bytes 786440 | tf_op jit(solution)/shard_map/ppermute | solution.py:19
  263.7 6.6 %all-to-all-start.2 = ((bf16[8,160,256]{2,1,0:T(8,128)(2,1)}), bf16[8,160,256]{2,1,0:T(8,128)(2,1)S(1)}, u32[]{:S(2)}, u32[]{:S(2)}) async-start(bf16[8,160,256]{2,1,0:T(8,128)(2,1)} %bitcast.29), calls=%async_computation.2 | async-start | bytes 1310720 | tf_op jit(solution)/shard_map/all_to_all | solution.py:27
  274.6 12.9 %all-to-all-done.2 = bf16[8,160,256]{2,1,0:T(8,128)(2,1)S(1)} async-done(((bf16[8,160,256]{2,1,0:T(8,128)(2,1)}), bf16[8,160,256]{2,1,0:T(8,128)(2,1)S(1)}, u32[]{:S(2)}, u32[]{:S(2)}) %all-to-all-start.2) | async-done | bytes 655392 | tf_op jit(solution)/shard_map/all_to_all | solution.py:27
  288.2 11.6 %all-to-all-start.3 = ((bf16[8,40,256]{2,1,0:T(8,128)(2,1)}), bf16[8,40,256]{2,1,0:T(8,128)(2,1)S(1)}, u32[]{:S(2)}, u32[]{:S(2)}) async-start(bf16[8,40,256]{2,1,0:T(8,128)(2,1)} %bitcast.31), calls=%async_computation.3 | async-start | bytes 327680 | tf_op jit(solution)/shard_map/all_to_all | solution.py:27
  302.9 23.3 %all-to-all-done.3.returned = bf16[8,40,256]{2,1,0:T(8,128)(2,1)S(1)} async-done(((bf16[8,40,256]{2,1,0:T(8,128)(2,1)}), bf16[8,40,256]{2,1,0:T(8,128)(2,1)S(1)}, u32[]{:S(2)}, u32[]{:S(2)}) %all-to-all-start.3) | async-done | bytes 163872 | tf_op jit(solution)/shard_map/all_to_all | solution.py:27
  (63 shorter events, 48.7 us)
Async XLA Ops:
  6.1 184.1 %all-to-all-start = ((bf16[32,32,384]{2,1,0:T(8,128)(2,1)}), bf16[32,32,384]{2,1,0:T(8,128)(2,1)S(1)}, u32[]{:S(2)}, u32[]{:S(2)}) async-start(bf16[32,32,384]{2,1,0:T(8,128)(2,1)} %pack.1), calls=%async_computation | async-start | bytes 1572864 | tf_op jit(solution)/shard_map/all_to_all | solution.py:27
  54.2 83.7 %collective-permute-start.10 = (bf16[40,256]{1,0:T(8,128)(2,1)}, bf16[40,256]{1,0:T(8,128)(2,1)S(1)}, u32[]{:S(2)}, u32[]{:S(2)}) collective-permute-start(bf16[40,256]{1,0:T(8,128)(2,1)} %get-tuple-element.20), channel_id=1, source_target_pairs={{0,128},{32,160},{64,192},{96,224},{128,0},{160,32},{192,64},{224,... | collective-permute-start | bytes 61448 | tf_op jit(solution)/shard_map/ppermute | solution.py:19
  75.2 64.6 %collective-permute-start.11 = (bf16[40,256]{1,0:T(8,128)(2,1)}, bf16[40,256]{1,0:T(8,128)(2,1)S(1)}, u32[]{:S(2)}, u32[]{:S(2)}) collective-permute-start(bf16[40,256]{1,0:T(8,128)(2,1)} %get-tuple-element.21), channel_id=1, source_target_pairs={{0,160},{32,192},{64,224},{96,0},{128,32},{160,64},{192,96},{224,1... | collective-permute-start | bytes 61448 | tf_op jit(solution)/shard_map/ppermute | solution.py:19
  77.5 72.6 %collective-permute-start.12 = (bf16[40,256]{1,0:T(8,128)(2,1)}, bf16[40,256]{1,0:T(8,128)(2,1)S(1)}, u32[]{:S(2)}, u32[]{:S(2)}) collective-permute-start(bf16[40,256]{1,0:T(8,128)(2,1)} %get-tuple-element.22), channel_id=1, source_target_pairs={{0,192},{32,224},{64,0},{96,32},{128,64},{160,96},{192,128},{224,1... | collective-permute-start | bytes 61448 | tf_op jit(solution)/shard_map/ppermute | solution.py:19
  84.7 65.4 %collective-permute-start.13 = (bf16[40,256]{1,0:T(8,128)(2,1)}, bf16[40,256]{1,0:T(8,128)(2,1)S(1)}, u32[]{:S(2)}, u32[]{:S(2)}) collective-permute-start(bf16[40,256]{1,0:T(8,128)(2,1)} %get-tuple-element.23), channel_id=1, source_target_pairs={{0,224},{32,0},{64,32},{96,64},{128,96},{160,128},{192,160},{224,1... | collective-permute-start | bytes 61448 | tf_op jit(solution)/shard_map/ppermute | solution.py:19
  91.6 58.5 %collective-permute-start.7 = (bf16[40,256]{1,0:T(8,128)(2,1)}, bf16[40,256]{1,0:T(8,128)(2,1)S(1)}, u32[]{:S(2)}, u32[]{:S(2)}) collective-permute-start(bf16[40,256]{1,0:T(8,128)(2,1)} %get-tuple-element.17), channel_id=1, source_target_pairs={{0,32},{32,64},{64,96},{96,128},{128,160},{160,192},{192,224},{224... | collective-permute-start | bytes 61448 | tf_op jit(solution)/shard_map/ppermute | solution.py:19
  137.9 13.5 %collective-permute-start.8 = (bf16[40,256]{1,0:T(8,128)(2,1)}, bf16[40,256]{1,0:T(8,128)(2,1)S(1)}, u32[]{:S(2)}, u32[]{:S(2)}) collective-permute-start(bf16[40,256]{1,0:T(8,128)(2,1)} %get-tuple-element.18), channel_id=1, source_target_pairs={{0,64},{32,96},{64,128},{96,160},{128,192},{160,224},{192,0},{224,... | collective-permute-start | bytes 61448 | tf_op jit(solution)/shard_map/ppermute | solution.py:19
  139.8 18.8 %collective-permute-start.9 = (bf16[40,256]{1,0:T(8,128)(2,1)}, bf16[40,256]{1,0:T(8,128)(2,1)S(1)}, u32[]{:S(2)}, u32[]{:S(2)}) collective-permute-start(bf16[40,256]{1,0:T(8,128)(2,1)} %get-tuple-element.19), channel_id=1, source_target_pairs={{0,96},{32,128},{64,160},{96,192},{128,224},{160,0},{192,32},{224,... | collective-permute-start | bytes 61448 | tf_op jit(solution)/shard_map/ppermute | solution.py:19
  159.4 19.9 %collective-permute-start.14 = (bf16[320,256]{1,0:T(8,128)(2,1)S(1)}, bf16[320,256]{1,0:T(8,128)(2,1)S(1)}, u32[]{:S(2)}, u32[]{:S(2)}) collective-permute-start(bf16[320,256]{1,0:T(8,128)(2,1)S(1)} %bitcast.47), channel_id=1, source_target_pairs={{0,8},{8,16},{16,24},{24,0},{1,9},{9,17},{17,25},{25,1},{2,10},{10... | collective-permute-start | bytes 491528 | tf_op jit(solution)/shard_map/ppermute | solution.py:19
  183.3 12.0 %collective-permute-start.17 = (bf16[4,160,256]{2,1,0:T(8,128)(2,1)S(1)}, bf16[4,160,256]{2,1,0:T(8,128)(2,1)S(1)}, u32[]{:S(2)}, u32[]{:S(2)}) collective-permute-start(bf16[4,160,256]{2,1,0:T(8,128)(2,1)S(1)} %get-tuple-element.27), channel_id=1, source_target_pairs={{0,1},{1,0},{2,3},{3,2},{4,5},{5,4},{6,7},{7,6},{8,9},{9,8},{10,11... | collective-permute-start | bytes 983048 | tf_op jit(solution)/shard_map/ppermute | solution.py:19
  191.6 17.9 %collective-permute-start = (bf16[32,32,256]{2,1,0:T(8,128)(2,1)S(1)}, bf16[32,32,256]{2,1,0:T(8,128)(2,1)S(1)}, u32[]{:S(2)}, u32[]{:S(2)}) collective-permute-start(bf16[32,32,256]{2,1,0:T(8,128)(2,1)S(1)} %get-tuple-element.14), channel_id=1, source_target_pairs={{0,256},{256,0},{1,257},{257,1},{2,258},{258,2},{3,259},{259,3},{4... | collective-permute-start | bytes 1572872 | tf_op jit(solution)/shard_map/ppermute | solution.py:19
  195.4 19.6 %collective-permute-start.18 = (bf16[4,2,160,256]{3,2,1,0:T(8,128)(2,1)S(1)}, bf16[4,2,160,256]{3,2,1,0:T(8,128)(2,1)S(1)}, u32[]{:S(2)}, u32[]{:S(2)}) collective-permute-start(bf16[4,2,160,256]{3,2,1,0:T(8,128)(2,1)S(1)} %pad_maximum_fusion.1.refs_4_), channel_id=1, source_target_pairs={{0,2},{2,4},{4,6},{6,0},{1,3},{3,5},{5,7},{7,1},{8,10},{10,12},{12... | collective-permute-start | bytes 1966088 | tf_op jit(solution)/shard_map/ppermute | solution.py:19
  198.7 36.4 %collective-permute-start.19 = (bf16[4,2,160,256]{3,2,1,0:T(8,128)(2,1)S(1)}, bf16[4,2,160,256]{3,2,1,0:T(8,128)(2,1)S(1)}, u32[]{:S(2)}, u32[]{:S(2)}) collective-permute-start(bf16[4,2,160,256]{3,2,1,0:T(8,128)(2,1)S(1)} %pad_maximum_fusion.1.refs_4_), channel_id=1, source_target_pairs={{0,4},{2,6},{4,0},{6,2},{1,5},{3,7},{5,1},{7,3},{8,12},{10,14},{12... | collective-permute-start | bytes 1966088 | tf_op jit(solution)/shard_map/ppermute | solution.py:19
  203.4 31.8 %collective-permute-start.20 = (bf16[4,2,160,256]{3,2,1,0:T(8,128)(2,1)S(1)}, bf16[4,2,160,256]{3,2,1,0:T(8,128)(2,1)}, u32[]{:S(2)}, u32[]{:S(2)}) collective-permute-start(bf16[4,2,160,256]{3,2,1,0:T(8,128)(2,1)S(1)} %pad_maximum_fusion.1.refs_4_), channel_id=1, source_target_pairs={{0,6},{2,0},{4,2},{6,4},{1,7},{3,1},{5,3},{7,5},{8,14},{10,8},{12,... | collective-permute-start | bytes 1966088 | tf_op jit(solution)/shard_map/ppermute | solution.py:19
  206.4 28.8 %collective-permute-start.5 = (bf16[1,32,32,256]{3,2,1,0:T(8,128)(2,1)S(1)}, bf16[1,32,32,256]{3,2,1,0:T(8,128)(2,1)}, u32[]{:S(2)}, u32[]{:S(2)}) collective-permute-start(bf16[1,32,32,256]{3,2,1,0:T(8,128)(2,1)S(1)} %bitcast.43), channel_id=1, source_target_pairs={{0,1},{1,0},{2,3},{3,2},{4,5},{5,4},{6,7},{7,6},{8,9},{9,8},{10,11... | collective-permute-start | bytes 1572872 | tf_op jit(solution)/shard_map/ppermute | solution.py:19
  209.5 25.7 %collective-permute-start.6 = (bf16[1,32,32,256]{3,2,1,0:T(8,128)(2,1)S(1)}, bf16[1,32,32,256]{3,2,1,0:T(8,128)(2,1)}, u32[]{:S(2)}, u32[]{:S(2)}) collective-permute-start(bf16[1,32,32,256]{3,2,1,0:T(8,128)(2,1)S(1)} %bitcast.41), channel_id=1, source_target_pairs={{0,1},{1,0},{2,3},{3,2},{4,5},{5,4},{6,7},{7,6},{8,9},{9,8},{10,11... | collective-permute-start | bytes 1572872 | tf_op jit(solution)/shard_map/ppermute | solution.py:19
  211.4 21.4 %all-to-all-start.1 = ((bf16[4,8,32,128]{3,2,1,0:T(8,128)(2,1)}), bf16[4,8,32,128]{3,2,1,0:T(8,128)(2,1)S(1)}, u32[]{:S(2)}, u32[]{:S(2)}) async-start(bf16[4,8,32,128]{3,2,1,0:T(8,128)(2,1)} %bitcast.16), calls=%async_computation.1 | async-start | bytes 524288 | tf_op jit(solution)/shard_map/all_to_all | solution.py:27
  232.9 21.6 %collective-permute-start.2 = (bf16[4,8,32,128]{3,2,1,0:T(8,128)(2,1)S(1)}, bf16[4,8,32,128]{3,2,1,0:T(8,128)(2,1)S(1)}, u32[]{:S(2)}, u32[]{:S(2)}) collective-permute-start(bf16[4,8,32,128]{3,2,1,0:T(8,128)(2,1)S(1)} %all-to-all-done.1), channel_id=1, source_target_pairs={{0,256},{256,0},{1,257},{257,1},{2,258},{258,2},{3,259},{259,3},{4... | collective-permute-start | bytes 786440 | tf_op jit(solution)/shard_map/ppermute | solution.py:19
  239.0 18.9 %collective-permute-start.21 = (bf16[4,160,256]{2,1,0:T(8,128)(2,1)S(1)}, bf16[4,160,256]{2,1,0:T(8,128)(2,1)S(1)}, u32[]{:S(2)}, u32[]{:S(2)}) collective-permute-start(bf16[4,160,256]{2,1,0:T(8,128)(2,1)S(1)} %hidden.1.refs_4_), channel_id=1, source_target_pairs={{0,2},{2,4},{4,6},{6,0},{1,3},{3,5},{5,7},{7,1},{8,10},{10,12},{12... | collective-permute-start | bytes 983048 | tf_op jit(solution)/shard_map/ppermute | solution.py:19
  244.2 15.3 %collective-permute-start.22 = (bf16[4,160,256]{2,1,0:T(8,128)(2,1)S(1)}, bf16[4,160,256]{2,1,0:T(8,128)(2,1)S(1)}, u32[]{:S(2)}, u32[]{:S(2)}) collective-permute-start(bf16[4,160,256]{2,1,0:T(8,128)(2,1)S(1)} %hidden.1.refs_4_), channel_id=1, source_target_pairs={{0,4},{2,6},{4,0},{6,2},{1,5},{3,7},{5,1},{7,3},{8,12},{10,14},{12... | collective-permute-start | bytes 983048 | tf_op jit(solution)/shard_map/ppermute | solution.py:19
  247.8 13.4 %collective-permute-start.23 = (bf16[4,160,256]{2,1,0:T(8,128)(2,1)S(1)}, bf16[4,160,256]{2,1,0:T(8,128)(2,1)S(1)}, u32[]{:S(2)}, u32[]{:S(2)}) collective-permute-start(bf16[4,160,256]{2,1,0:T(8,128)(2,1)S(1)} %hidden.1.refs_4_), channel_id=1, source_target_pairs={{0,6},{2,0},{4,2},{6,4},{1,7},{3,1},{5,3},{7,5},{8,14},{10,8},{12,... | collective-permute-start | bytes 983048 | tf_op jit(solution)/shard_map/ppermute | solution.py:19
  263.7 23.8 %all-to-all-start.2 = ((bf16[8,160,256]{2,1,0:T(8,128)(2,1)}), bf16[8,160,256]{2,1,0:T(8,128)(2,1)S(1)}, u32[]{:S(2)}, u32[]{:S(2)}) async-start(bf16[8,160,256]{2,1,0:T(8,128)(2,1)} %bitcast.29), calls=%async_computation.2 | async-start | bytes 1310720 | tf_op jit(solution)/shard_map/all_to_all | solution.py:27
  271.3 29.7 %collective-permute-start.1 = (bf16[32,32,128]{2,1,0:T(8,128)(2,1)}, bf16[32,32,128]{2,1,0:T(8,128)(2,1)S(1)}, u32[]{:S(2)}, u32[]{:S(2)}) collective-permute-start(bf16[32,32,128]{2,1,0:T(8,128)(2,1)} %get-tuple-element.15), channel_id=1, source_target_pairs={{0,256},{256,0},{1,257},{257,1},{2,258},{258,2},{3,259},{259,3},{4... | collective-permute-start | bytes 786440 | tf_op jit(solution)/shard_map/ppermute | solution.py:19
  288.2 37.9 %all-to-all-start.3 = ((bf16[8,40,256]{2,1,0:T(8,128)(2,1)}), bf16[8,40,256]{2,1,0:T(8,128)(2,1)S(1)}, u32[]{:S(2)}, u32[]{:S(2)}) async-start(bf16[8,40,256]{2,1,0:T(8,128)(2,1)} %bitcast.31), calls=%async_computation.3 | async-start | bytes 327680 | tf_op jit(solution)/shard_map/all_to_all | solution.py:27
  (8 other events, 34.7 us)

commit v10 on v8

--- a/solution.py
+++ b/solution.py
@@ -140,7 +140,9 @@
         value = value * row_scale
         gate, up = value[:, :width], value[:, width:]
         hidden = (gate / (1.0 + jnp.exp(-gate)) * up).astype(jnp.bfloat16)
-        out[:, :, j * width : (j + 1) * width] = hidden.reshape(copies, tokens, width)
+        hidden = hidden.reshape(copies, tokens, width)
+        for k in range(count):
+            out[k, :, :, j * width : (j + 1) * width] = hidden
 
 
 def hidden_units(own, other, parts):
@@ -148,7 +150,7 @@
     _, sources, part, double = own[0].shape
     groups = sum(piece.shape[0] for piece in own)
     width = double // 2
-    out = jax.ShapeDtypeStruct((copies, tokens, 2 * width), jnp.bfloat16)
+    out = jax.ShapeDtypeStruct((len(parts), copies, tokens, 2 * width), jnp.bfloat16)
     inputs = (*own, *other, *parts)
     held = pltpu.VMEM((sources, groups, part, 2 * width), jnp.bfloat16)
     return pl.pallas_call(
@@ -167,9 +169,9 @@
 
 
 def project_kernel(bundles, place, *refs):
-    hidden, out, held = refs[2 * bundles : -2], refs[-2], refs[-1]
-    count, groups = len(hidden), held.shape[2]
-    copies, tokens, depth = hidden[0].shape
+    hidden, out, held = refs[-3:]
+    groups = held.shape[2]
+    count, copies, tokens, depth = hidden.shape
     halves, cols = out.shape[1], out.shape[3]
     width = depth // 2
     for j, pieces in enumerate((refs[:bundles], refs[bundles : 2 * bundles])):
@@ -185,10 +187,9 @@
     for c in range(halves):
         value = jnp.zeros((copies * tokens, cols), jnp.float32)
         for k in range(count):
-            source = lax.rem(place[0] + (count - k), count)
-            down = held[pl.ds(source, 1), c * share : (c + 1) * share].reshape(cols, depth)
+            down = held[k, c * share : (c + 1) * share].reshape(cols, depth)
             value = value + lax.dot_general(
-                hidden[k][...].reshape(copies * tokens, depth),
+                hidden[k].reshape(copies * tokens, depth),
                 down,
                 (((1,), (1,)), ((), ())),
                 preferred_element_type=jnp.float32,
@@ -200,12 +201,12 @@
 
 
 def projected(own, other, hidden, halves):
-    copies, tokens, depth = hidden[0].shape
+    _, copies, tokens, depth = hidden.shape
     _, count, sources, part, _ = own[0].shape
     groups = sum(piece.shape[0] for piece in own)
     cols = sources * groups * part // halves
     out = jax.ShapeDtypeStruct((copies, halves, tokens, cols), jnp.bfloat16)
-    inputs = (*own, *other, *hidden)
+    inputs = (*own, *other, hidden)
     return pl.pallas_call(
         functools.partial(project_kernel, len(own)),
         out_shape=out,
@@ -369,7 +370,7 @@
     chosen = chosen_slots(routes, experts * capacity)
 
     units = hidden_units(scaled, scaled_pairs, parts)
-    units = [units] + [shifted(units, "tp_x", k) for k in range(1, len(parts))]
+    units = exchange(units, "tp_x")
     over_x = projected(turned, turned_pairs, units, lax.axis_size("tp_c"))
     sent = exchange(over_x.reshape(-1, *over_x.shape[2:]), ("fs_lo", "tp_c"))
     over_s = jnp.sum(sent.reshape(over_x.shape), axis=0, dtype=jnp.float32)

time: 320 us -> 315 us (0.984)
  starting transfers between devices: 146 us -> 141 us
    ppermute x17 -> x14, waiting for transfers between devices: 72.4 us -> 83.8 us  [shifted(): lax.ppermute(value, axis, [(k, (k + step) % count) for k in range(count)])]
    ppermute x17 -> x14, starting transfers between devices: 60.9 us -> 51.1 us  [shifted(): lax.ppermute(value, axis, [(k, (k + step) % count) for k in range(count)])]
    all_to_all x5 -> x6, waiting for transfers between devices: 72.3 us -> 63.2 us  [exchange(): return lax.all_to_all(value, axis, split_axis=0, concat_axis=0, tiled=True)]
    all_to_all x5 -> x6, starting transfers between devices: 85.2 us -> 89.8 us  [exchange(): return lax.all_to_all(value, axis, split_axis=0, concat_axis=0, tiled=True)]
  transfers between devices with their start and end apart: 22 -> 20, of which waited for: 10 -> 11; matrix products, arithmetic and copies ran while one was open for 1% -> 1% of each run, Pallas kernels for 3% -> 4%
where the time goes in v10:
time: 315 us; the launch traced here: 311 us
  waiting for transfers between devices  147 us (47%)
  starting transfers between devices  141 us (45%)
  Pallas kernels  17 us (5%)
  local copies, waits for them, and re-layouts  3.66 us (1%)
    all_to_all x6, starting transfers between devices, exchange(): return lax.all_to_all(value, axis, split_axis=0, concat_axis=0, tiled=True)  89.8 us
    ppermute x14, waiting for transfers between devices, shifted(): lax.ppermute(value, axis, [(k, (k + step) % count) for k in range(count)])  83.8 us
    all_to_all x6, waiting for transfers between devices, exchange(): return lax.all_to_all(value, axis, split_axis=0, concat_axis=0, tiled=True)  63.2 us
    ppermute x14, starting transfers between devices, shifted(): lax.ppermute(value, axis, [(k, (k + step) % count) for k in range(count)])  51.1 us
  transfers between devices with their start and end apart: 20, of which 11 were waited for; matrix products, arithmetic and copies ran while one was open for 1% of the time, Pallas kernels for 4%

profile of v10, /device:TPU:33, one launch (start us, length us, event | category | flops | bytes accessed | tf_op | source)
XLA Modules:
  0.0 310.6 jit_solution(7588737333916539307)
XLA Ops:
  2.5 44.0 %all-to-all-start.2 = ((bf16[8,40,256]{2,1,0:T(8,128)(2,1)}), bf16[8,40,256]{2,1,0:T(8,128)(2,1)S(1)}, u32[]{:S(2)}, u32[]{:S(2)}) async-start(bf16[8,40,256]{2,1,0:T(8,128)(2,1)} %dispatch.1), calls=%async_computation.2 | async-start | bytes 327680 | tf_op jit(solution)/shard_map/all_to_all | solution.py:27
  46.5 5.4 %pack.1 = bf16[32,32,384]{2,1,0:T(8,128)(2,1)} custom-call(s32[1]{0:T(128)} %bitcast.turn.place, f32[1,64]{1,0:T(1,128)} %bitcast.61, f32[8,64,512]{2,1,0:T(8,128)} %gate.1, f32[8,64,512]{2,1,0:T(8,128)} %up.1, f32[8,64,512]{2,1,0:T(8,128)} %down.1), custom_call_target="tpu_custom_call" | custom-call | tf_op jit(solution)/shard_map/pack/pallas_call | solution.py:53
  51.9 22.3 %all-to-all-done.2 = bf16[8,40,256]{2,1,0:T(8,128)(2,1)S(1)} async-done(((bf16[8,40,256]{2,1,0:T(8,128)(2,1)}), bf16[8,40,256]{2,1,0:T(8,128)(2,1)S(1)}, u32[]{:S(2)}, u32[]{:S(2)}) %all-to-all-start.2) | async-done | bytes 163872 | tf_op jit(solution)/shard_map/all_to_all | solution.py:27
  74.2 10.0 %all-to-all-start = ((bf16[32,32,384]{2,1,0:T(8,128)(2,1)}), bf16[32,32,384]{2,1,0:T(8,128)(2,1)S(1)}, u32[]{:S(2)}, u32[]{:S(2)}) async-start(bf16[32,32,384]{2,1,0:T(8,128)(2,1)} %pack.1), calls=%async_computation | async-start | bytes 1572864 | tf_op jit(solution)/shard_map/all_to_all | solution.py:27
  87.0 4.0 %collective-permute-start.8 = (bf16[320,256]{1,0:T(8,128)(2,1)S(1)}, bf16[320,256]{1,0:T(8,128)(2,1)S(1)}, u32[]{:S(2)}, u32[]{:S(2)}) collective-permute-start(bf16[320,256]{1,0:T(8,128)(2,1)S(1)} %bitcast.53), channel_id=1, source_target_pairs={{0,16},{8,24},{16,0},{24,8},{1,17},{9,25},{17,1},{25,9},{2,18},{10... | collective-permute-start | bytes 491528 | tf_op jit(solution)/shard_map/ppermute | solution.py:19
  91.0 3.1 %collective-permute-start.9 = (bf16[320,256]{1,0:T(8,128)(2,1)S(1)}, bf16[320,256]{1,0:T(8,128)(2,1)S(1)}, u32[]{:S(2)}, u32[]{:S(2)}) collective-permute-start(bf16[320,256]{1,0:T(8,128)(2,1)S(1)} %bitcast.54), channel_id=1, source_target_pairs={{0,24},{8,0},{16,8},{24,16},{1,25},{9,1},{17,9},{25,17},{2,26},{10... | collective-permute-start | bytes 491528 | tf_op jit(solution)/shard_map/ppermute | solution.py:19
  94.2 58.7 %collective-permute-done.7 = bf16[320,256]{1,0:T(8,128)(2,1)S(1)} collective-permute-done((bf16[320,256]{1,0:T(8,128)(2,1)S(1)}, bf16[320,256]{1,0:T(8,128)(2,1)S(1)}, u32[]{:S(2)}, u32[]{:S(2)}) %collective-permute-start.7) | collective-permute-done | bytes 163872 | tf_op jit(solution)/shard_map/ppermute | solution.py:19
  152.9 9.5 %collective-permute-done.8 = bf16[320,256]{1,0:T(8,128)(2,1)S(1)} collective-permute-done((bf16[320,256]{1,0:T(8,128)(2,1)S(1)}, bf16[320,256]{1,0:T(8,128)(2,1)S(1)}, u32[]{:S(2)}, u32[]{:S(2)}) %collective-permute-start.8) | collective-permute-done | bytes 163872 | tf_op jit(solution)/shard_map/ppermute | solution.py:19
  162.5 5.1 %collective-permute-start.10 = (bf16[4,160,256]{2,1,0:T(8,128)(2,1)S(1)}, bf16[4,160,256]{2,1,0:T(8,128)(2,1)S(1)}, u32[]{:S(2)}, u32[]{:S(2)}) collective-permute-start(bf16[4,160,256]{2,1,0:T(8,128)(2,1)S(1)} %get-tuple-element.11), channel_id=1, source_target_pairs={{0,1},{1,0},{2,3},{3,2},{4,5},{5,4},{6,7},{7,6},{8,9},{9,8},{10,11... | collective-permute-start | bytes 983048 | tf_op jit(solution)/shard_map/ppermute | solution.py:19
  169.9 3.5 %collective-permute-start = (bf16[32,32,256]{2,1,0:T(8,128)(2,1)S(1)}, bf16[32,32,256]{2,1,0:T(8,128)(2,1)S(1)}, u32[]{:S(2)}, u32[]{:S(2)}) collective-permute-start(bf16[32,32,256]{2,1,0:T(8,128)(2,1)S(1)} %get-tuple-element.6), channel_id=1, source_target_pairs={{0,256},{256,0},{1,257},{257,1},{2,258},{258,2},{3,259},{259,3},{4... | collective-permute-start | bytes 1572872 | tf_op jit(solution)/shard_map/ppermute | solution.py:19
  173.5 3.3 %collective-permute-start.11 = (bf16[4,2,160,256]{3,2,1,0:T(8,128)(2,1)S(1)}, bf16[4,2,160,256]{3,2,1,0:T(8,128)(2,1)S(1)}, u32[]{:S(2)}, u32[]{:S(2)}) collective-permute-start(bf16[4,2,160,256]{3,2,1,0:T(8,128)(2,1)S(1)} %pad_maximum_fusion.1.refs_4_), channel_id=1, source_target_pairs={{0,2},{2,4},{4,6},{6,0},{1,3},{3,5},{5,7},{7,1},{8,10},{10,12},{12... | collective-permute-start | bytes 1966088 | tf_op jit(solution)/shard_map/ppermute | solution.py:19
  176.8 4.7 %collective-permute-start.12 = (bf16[4,2,160,256]{3,2,1,0:T(8,128)(2,1)S(1)}, bf16[4,2,160,256]{3,2,1,0:T(8,128)(2,1)S(1)}, u32[]{:S(2)}, u32[]{:S(2)}) collective-permute-start(bf16[4,2,160,256]{3,2,1,0:T(8,128)(2,1)S(1)} %pad_maximum_fusion.1.refs_4_), channel_id=1, source_target_pairs={{0,4},{2,6},{4,0},{6,2},{1,5},{3,7},{5,1},{7,3},{8,12},{10,14},{12... | collective-permute-start | bytes 1966088 | tf_op jit(solution)/shard_map/ppermute | solution.py:19
  184.4 7.0 %collective-permute-start.5 = (bf16[1,32,32,256]{3,2,1,0:T(8,128)(2,1)S(1)}, bf16[1,32,32,256]{3,2,1,0:T(8,128)(2,1)}, u32[]{:S(2)}, u32[]{:S(2)}) collective-permute-start(bf16[1,32,32,256]{3,2,1,0:T(8,128)(2,1)S(1)} %bitcast.42), channel_id=1, source_target_pairs={{0,1},{1,0},{2,3},{3,2},{4,5},{5,4},{6,7},{7,6},{8,9},{9,8},{10,11... | collective-permute-start | bytes 1572872 | tf_op jit(solution)/shard_map/ppermute | solution.py:19
  193.4 3.5 %all-to-all-start.1 = ((bf16[4,8,32,128]{3,2,1,0:T(8,128)(2,1)}), bf16[4,8,32,128]{3,2,1,0:T(8,128)(2,1)S(1)}, u32[]{:S(2)}, u32[]{:S(2)}) async-start(bf16[4,8,32,128]{3,2,1,0:T(8,128)(2,1)} %bitcast.16), calls=%async_computation.1 | async-start | bytes 524288 | tf_op jit(solution)/shard_map/all_to_all | solution.py:27
  197.0 7.1 %collective-permute-done.12.refs_6_ = bf16[4,2,160,256]{3,2,1,0:T(8,128)(2,1)S(1)} collective-permute-done((bf16[4,2,160,256]{3,2,1,0:T(8,128)(2,1)S(1)}, bf16[4,2,160,256]{3,2,1,0:T(8,128)(2,1)S(1)}, u32[]{:S(2)}, u32[]{:S(2)}) %collective-permute-start.12) | collective-permute-done | bytes 655392 | tf_op jit(solution)/shard_map/ppermute | solution.py:19
  204.1 5.6 %collective-permute-done.13.refs_7_ = bf16[4,2,160,256]{3,2,1,0:T(8,128)(2,1)} collective-permute-done((bf16[4,2,160,256]{3,2,1,0:T(8,128)(2,1)S(1)}, bf16[4,2,160,256]{3,2,1,0:T(8,128)(2,1)}, u32[]{:S(2)}, u32[]{:S(2)}) %collective-permute-start.13) | collective-permute-done | bytes 655392 | tf_op jit(solution)/shard_map/ppermute | solution.py:19
  209.8 4.9 %hidden.1 = bf16[4,4,160,256]{3,2,1,0:T(8,128)(2,1)} custom-call(s32[4]{0:T(128)S(1)} %pad_add_fusion.place, bf16[1,32,32,256]{3,2,1,0:T(8,128)(2,1)S(1)} %bitcast.43, bf16[1,32,32,256]{3,2,1,0:T(8,128)(2,1)S(1)} %bitcast.41, bf16[1,32,32,256]{3,2,1,0:T(8,128)(2,1)} %collective-permute-done.5.refs_2_, ...), custom_call_target="tpu_custom_call" | custom-call | tf_op jit(solution)/shard_map/hidden/pallas_call | solution.py:156
  214.7 4.8 %all-to-all-start.3 = ((bf16[4,4,160,256]{3,2,1,0:T(8,128)(2,1)}), bf16[4,4,160,256]{3,2,1,0:T(8,128)(2,1)S(1)}, u32[]{:S(2)}, u32[]{:S(2)}) async-start(bf16[4,4,160,256]{3,2,1,0:T(8,128)(2,1)} %hidden.1), calls=%async_computation.3 | async-start | bytes 2621440 | tf_op jit(solution)/shard_map/all_to_all | solution.py:27
  221.4 4.1 %collective-permute-start.3 = (bf16[1,4,8,32,128]{4,3,2,1,0:T(8,128)(2,1)S(1)}, bf16[1,4,8,32,128]{4,3,2,1,0:T(8,128)(2,1)S(1)}, u32[]{:S(2)}, u32[]{:S(2)}) collective-permute-start(bf16[1,4,8,32,128]{4,3,2,1,0:T(8,128)(2,1)S(1)} %bitcast.44), channel_id=1, source_target_pairs={{0,1},{1,0},{2,3},{3,2},{4,5},{5,4},{6,7},{7,6},{8,9},{9,8},{10,11... | collective-permute-start | bytes 786440 | tf_op jit(solution)/shard_map/ppermute | solution.py:19
  227.3 4.7 %collective-permute-start.4 = (bf16[1,4,8,32,128]{4,3,2,1,0:T(8,128)(2,1)S(1)}, bf16[1,4,8,32,128]{4,3,2,1,0:T(8,128)(2,1)S(1)}, u32[]{:S(2)}, u32[]{:S(2)}) collective-permute-start(bf16[1,4,8,32,128]{4,3,2,1,0:T(8,128)(2,1)S(1)} %bitcast.46), channel_id=1, source_target_pairs={{0,1},{1,0},{2,3},{3,2},{4,5},{5,4},{6,7},{7,6},{8,9},{9,8},{10,11... | collective-permute-start | bytes 786440 | tf_op jit(solution)/shard_map/ppermute | solution.py:19
  237.9 9.3 %all-to-all-start.4 = ((bf16[8,160,256]{2,1,0:T(8,128)(2,1)}), bf16[8,160,256]{2,1,0:T(8,128)(2,1)S(1)}, u32[]{:S(2)}, u32[]{:S(2)}) async-start(bf16[8,160,256]{2,1,0:T(8,128)(2,1)} %bitcast.28), calls=%async_computation.4 | async-start | bytes 1310720 | tf_op jit(solution)/shard_map/all_to_all | solution.py:27
  249.8 14.6 %all-to-all-done.4 = bf16[8,160,256]{2,1,0:T(8,128)(2,1)S(1)} async-done(((bf16[8,160,256]{2,1,0:T(8,128)(2,1)}), bf16[8,160,256]{2,1,0:T(8,128)(2,1)S(1)}, u32[]{:S(2)}, u32[]{:S(2)}) %all-to-all-start.4) | async-done | bytes 655392 | tf_op jit(solution)/shard_map/all_to_all | solution.py:27
  265.2 18.2 %all-to-all-start.5 = ((bf16[8,40,256]{2,1,0:T(8,128)(2,1)}), bf16[8,40,256]{2,1,0:T(8,128)(2,1)S(1)}, u32[]{:S(2)}, u32[]{:S(2)}) async-start(bf16[8,40,256]{2,1,0:T(8,128)(2,1)} %bitcast.30), calls=%async_computation.5 | async-start | bytes 327680 | tf_op jit(solution)/shard_map/all_to_all | solution.py:27
  286.6 23.0 %all-to-all-done.5.returned = bf16[8,40,256]{2,1,0:T(8,128)(2,1)S(1)} async-done(((bf16[8,40,256]{2,1,0:T(8,128)(2,1)}), bf16[8,40,256]{2,1,0:T(8,128)(2,1)S(1)}, u32[]{:S(2)}, u32[]{:S(2)}) %all-to-all-start.5) | async-done | bytes 163872 | tf_op jit(solution)/shard_map/all_to_all | solution.py:27
  (44 shorter events, 29.1 us)
Async XLA Ops:
  2.5 71.7 %all-to-all-start.2 = ((bf16[8,40,256]{2,1,0:T(8,128)(2,1)}), bf16[8,40,256]{2,1,0:T(8,128)(2,1)S(1)}, u32[]{:S(2)}, u32[]{:S(2)}) async-start(bf16[8,40,256]{2,1,0:T(8,128)(2,1)} %dispatch.1), calls=%async_computation.2 | async-start | bytes 327680 | tf_op jit(solution)/shard_map/all_to_all | solution.py:27
  74.2 94.3 %all-to-all-start = ((bf16[32,32,384]{2,1,0:T(8,128)(2,1)}), bf16[32,32,384]{2,1,0:T(8,128)(2,1)S(1)}, u32[]{:S(2)}, u32[]{:S(2)}) async-start(bf16[32,32,384]{2,1,0:T(8,128)(2,1)} %pack.1), calls=%async_computation | async-start | bytes 1572864 | tf_op jit(solution)/shard_map/all_to_all | solution.py:27
  84.3 68.6 %collective-permute-start.7 = (bf16[320,256]{1,0:T(8,128)(2,1)S(1)}, bf16[320,256]{1,0:T(8,128)(2,1)S(1)}, u32[]{:S(2)}, u32[]{:S(2)}) collective-permute-start(bf16[320,256]{1,0:T(8,128)(2,1)S(1)} %bitcast.52), channel_id=1, source_target_pairs={{0,8},{8,16},{16,24},{24,0},{1,9},{9,17},{17,25},{25,1},{2,10},{10... | collective-permute-start | bytes 491528 | tf_op jit(solution)/shard_map/ppermute | solution.py:19
  87.0 75.4 %collective-permute-start.8 = (bf16[320,256]{1,0:T(8,128)(2,1)S(1)}, bf16[320,256]{1,0:T(8,128)(2,1)S(1)}, u32[]{:S(2)}, u32[]{:S(2)}) collective-permute-start(bf16[320,256]{1,0:T(8,128)(2,1)S(1)} %bitcast.53), channel_id=1, source_target_pairs={{0,16},{8,24},{16,0},{24,8},{1,17},{9,25},{17,1},{25,9},{2,18},{10... | collective-permute-start | bytes 491528 | tf_op jit(solution)/shard_map/ppermute | solution.py:19
  91.0 71.4 %collective-permute-start.9 = (bf16[320,256]{1,0:T(8,128)(2,1)S(1)}, bf16[320,256]{1,0:T(8,128)(2,1)S(1)}, u32[]{:S(2)}, u32[]{:S(2)}) collective-permute-start(bf16[320,256]{1,0:T(8,128)(2,1)S(1)} %bitcast.54), channel_id=1, source_target_pairs={{0,24},{8,0},{16,8},{24,16},{1,25},{9,1},{17,9},{25,17},{2,26},{10... | collective-permute-start | bytes 491528 | tf_op jit(solution)/shard_map/ppermute | solution.py:19
  162.5 10.9 %collective-permute-start.10 = (bf16[4,160,256]{2,1,0:T(8,128)(2,1)S(1)}, bf16[4,160,256]{2,1,0:T(8,128)(2,1)S(1)}, u32[]{:S(2)}, u32[]{:S(2)}) collective-permute-start(bf16[4,160,256]{2,1,0:T(8,128)(2,1)S(1)} %get-tuple-element.11), channel_id=1, source_target_pairs={{0,1},{1,0},{2,3},{3,2},{4,5},{5,4},{6,7},{7,6},{8,9},{9,8},{10,11... | collective-permute-start | bytes 983048 | tf_op jit(solution)/shard_map/ppermute | solution.py:19
  169.9 21.6 %collective-permute-start = (bf16[32,32,256]{2,1,0:T(8,128)(2,1)S(1)}, bf16[32,32,256]{2,1,0:T(8,128)(2,1)S(1)}, u32[]{:S(2)}, u32[]{:S(2)}) collective-permute-start(bf16[32,32,256]{2,1,0:T(8,128)(2,1)S(1)} %get-tuple-element.6), channel_id=1, source_target_pairs={{0,256},{256,0},{1,257},{257,1},{2,258},{258,2},{3,259},{259,3},{4... | collective-permute-start | bytes 1572872 | tf_op jit(solution)/shard_map/ppermute | solution.py:19
  173.5 23.6 %collective-permute-start.11 = (bf16[4,2,160,256]{3,2,1,0:T(8,128)(2,1)S(1)}, bf16[4,2,160,256]{3,2,1,0:T(8,128)(2,1)S(1)}, u32[]{:S(2)}, u32[]{:S(2)}) collective-permute-start(bf16[4,2,160,256]{3,2,1,0:T(8,128)(2,1)S(1)} %pad_maximum_fusion.1.refs_4_), channel_id=1, source_target_pairs={{0,2},{2,4},{4,6},{6,0},{1,3},{3,5},{5,7},{7,1},{8,10},{10,12},{12... | collective-permute-start | bytes 1966088 | tf_op jit(solution)/shard_map/ppermute | solution.py:19
  176.8 27.3 %collective-permute-start.12 = (bf16[4,2,160,256]{3,2,1,0:T(8,128)(2,1)S(1)}, bf16[4,2,160,256]{3,2,1,0:T(8,128)(2,1)S(1)}, u32[]{:S(2)}, u32[]{:S(2)}) collective-permute-start(bf16[4,2,160,256]{3,2,1,0:T(8,128)(2,1)S(1)} %pad_maximum_fusion.1.refs_4_), channel_id=1, source_target_pairs={{0,4},{2,6},{4,0},{6,2},{1,5},{3,7},{5,1},{7,3},{8,12},{10,14},{12... | collective-permute-start | bytes 1966088 | tf_op jit(solution)/shard_map/ppermute | solution.py:19
  181.4 28.3 %collective-permute-start.13 = (bf16[4,2,160,256]{3,2,1,0:T(8,128)(2,1)S(1)}, bf16[4,2,160,256]{3,2,1,0:T(8,128)(2,1)}, u32[]{:S(2)}, u32[]{:S(2)}) collective-permute-start(bf16[4,2,160,256]{3,2,1,0:T(8,128)(2,1)S(1)} %pad_maximum_fusion.1.refs_4_), channel_id=1, source_target_pairs={{0,6},{2,0},{4,2},{6,4},{1,7},{3,1},{5,3},{7,5},{8,14},{10,8},{12,... | collective-permute-start | bytes 1966088 | tf_op jit(solution)/shard_map/ppermute | solution.py:19
  184.4 25.3 %collective-permute-start.5 = (bf16[1,32,32,256]{3,2,1,0:T(8,128)(2,1)S(1)}, bf16[1,32,32,256]{3,2,1,0:T(8,128)(2,1)}, u32[]{:S(2)}, u32[]{:S(2)}) collective-permute-start(bf16[1,32,32,256]{3,2,1,0:T(8,128)(2,1)S(1)} %bitcast.42), channel_id=1, source_target_pairs={{0,1},{1,0},{2,3},{3,2},{4,5},{5,4},{6,7},{7,6},{8,9},{9,8},{10,11... | collective-permute-start | bytes 1572872 | tf_op jit(solution)/shard_map/ppermute | solution.py:19
  191.5 18.3 %collective-permute-start.6 = (bf16[1,32,32,256]{3,2,1,0:T(8,128)(2,1)S(1)}, bf16[1,32,32,256]{3,2,1,0:T(8,128)(2,1)}, u32[]{:S(2)}, u32[]{:S(2)}) collective-permute-start(bf16[1,32,32,256]{3,2,1,0:T(8,128)(2,1)S(1)} %bitcast.40), channel_id=1, source_target_pairs={{0,1},{1,0},{2,3},{3,2},{4,5},{5,4},{6,7},{7,6},{8,9},{9,8},{10,11... | collective-permute-start | bytes 1572872 | tf_op jit(solution)/shard_map/ppermute | solution.py:19
  193.4 21.3 %all-to-all-start.1 = ((bf16[4,8,32,128]{3,2,1,0:T(8,128)(2,1)}), bf16[4,8,32,128]{3,2,1,0:T(8,128)(2,1)S(1)}, u32[]{:S(2)}, u32[]{:S(2)}) async-start(bf16[4,8,32,128]{3,2,1,0:T(8,128)(2,1)} %bitcast.16), calls=%async_computation.1 | async-start | bytes 524288 | tf_op jit(solution)/shard_map/all_to_all | solution.py:27
  214.7 20.9 %all-to-all-start.3 = ((bf16[4,4,160,256]{3,2,1,0:T(8,128)(2,1)}), bf16[4,4,160,256]{3,2,1,0:T(8,128)(2,1)S(1)}, u32[]{:S(2)}, u32[]{:S(2)}) async-start(bf16[4,4,160,256]{3,2,1,0:T(8,128)(2,1)} %hidden.1), calls=%async_computation.3 | async-start | bytes 2621440 | tf_op jit(solution)/shard_map/all_to_all | solution.py:27
  219.5 7.9 %collective-permute-start.2 = (bf16[4,8,32,128]{3,2,1,0:T(8,128)(2,1)S(1)}, bf16[4,8,32,128]{3,2,1,0:T(8,128)(2,1)S(1)}, u32[]{:S(2)}, u32[]{:S(2)}) collective-permute-start(bf16[4,8,32,128]{3,2,1,0:T(8,128)(2,1)S(1)} %all-to-all-done.1), channel_id=1, source_target_pairs={{0,256},{256,0},{1,257},{257,1},{2,258},{258,2},{3,259},{259,3},{4... | collective-permute-start | bytes 786440 | tf_op jit(solution)/shard_map/ppermute | solution.py:19
  221.4 10.6 %collective-permute-start.3 = (bf16[1,4,8,32,128]{4,3,2,1,0:T(8,128)(2,1)S(1)}, bf16[1,4,8,32,128]{4,3,2,1,0:T(8,128)(2,1)S(1)}, u32[]{:S(2)}, u32[]{:S(2)}) collective-permute-start(bf16[1,4,8,32,128]{4,3,2,1,0:T(8,128)(2,1)S(1)} %bitcast.44), channel_id=1, source_target_pairs={{0,1},{1,0},{2,3},{3,2},{4,5},{5,4},{6,7},{7,6},{8,9},{9,8},{10,11... | collective-permute-start | bytes 786440 | tf_op jit(solution)/shard_map/ppermute | solution.py:19
  227.3 5.9 %collective-permute-start.4 = (bf16[1,4,8,32,128]{4,3,2,1,0:T(8,128)(2,1)S(1)}, bf16[1,4,8,32,128]{4,3,2,1,0:T(8,128)(2,1)S(1)}, u32[]{:S(2)}, u32[]{:S(2)}) collective-permute-start(bf16[1,4,8,32,128]{4,3,2,1,0:T(8,128)(2,1)S(1)} %bitcast.46), channel_id=1, source_target_pairs={{0,1},{1,0},{2,3},{3,2},{4,5},{5,4},{6,7},{7,6},{8,9},{9,8},{10,11... | collective-permute-start | bytes 786440 | tf_op jit(solution)/shard_map/ppermute | solution.py:19
  237.9 9.3 %copy-start = (s32[128,2]{0,1:T(2,128)S(1)}, s32[128,2]{0,1:T(2,128)}, u32[]{:S(2)}) copy-start(s32[128,2]{0,1:T(2,128)} %param.8) | copy-start | bytes 3076
  237.9 9.5 %copy-start.2 = (f32[128,2]{0,1:T(2,128)S(1)}, f32[128,2]{0,1:T(2,128)}, u32[]{:S(2)}) copy-start(f32[128,2]{0,1:T(2,128)} %param.9) | copy-start | bytes 3076
  237.9 26.5 %all-to-all-start.4 = ((bf16[8,160,256]{2,1,0:T(8,128)(2,1)}), bf16[8,160,256]{2,1,0:T(8,128)(2,1)S(1)}, u32[]{:S(2)}, u32[]{:S(2)}) async-start(bf16[8,160,256]{2,1,0:T(8,128)(2,1)} %bitcast.28), calls=%async_computation.4 | async-start | bytes 1310720 | tf_op jit(solution)/shard_map/all_to_all | solution.py:27
  247.6 36.9 %collective-permute-start.1 = (bf16[32,32,128]{2,1,0:T(8,128)(2,1)}, bf16[32,32,128]{2,1,0:T(8,128)(2,1)}, u32[]{:S(2)}, u32[]{:S(2)}) collective-permute-start(bf16[32,32,128]{2,1,0:T(8,128)(2,1)} %get-tuple-element.7), channel_id=1, source_target_pairs={{0,256},{256,0},{1,257},{257,1},{2,258},{258,2},{3,259},{259,3},{4... | collective-permute-start | bytes 786440 | tf_op jit(solution)/shard_map/ppermute | solution.py:19
  265.2 44.5 %all-to-all-start.5 = ((bf16[8,40,256]{2,1,0:T(8,128)(2,1)}), bf16[8,40,256]{2,1,0:T(8,128)(2,1)S(1)}, u32[]{:S(2)}, u32[]{:S(2)}) async-start(bf16[8,40,256]{2,1,0:T(8,128)(2,1)} %bitcast.30), calls=%async_computation.5 | async-start | bytes 327680 | tf_op jit(solution)/shard_map/all_to_all | solution.py:27
  285.5 1.1 copy-start.1

commit v11 on v10

--- a/solution.py
+++ b/solution.py
@@ -21,6 +21,11 @@
 
 def vmem(mebibytes):
     return pltpu.CompilerParams(vmem_limit_bytes=mebibytes * 1024 * 1024)
+
+
+def paired(value, axis, flip):
+    count = lax.axis_size(axis)
+    return lax.ppermute(value, axis, [(k, k ^ flip) for k in range(count)])
 
 
 def exchange(value, axis):
@@ -196,7 +201,7 @@
             )
         value = value.astype(jnp.bfloat16)
         for r in range(copies):
-            target = lax.rem(place[2] + (copies - r), copies)
+            target = place[2] ^ r
             out[pl.ds(target, 1), c] = value[r * tokens : (r + 1) * tokens][None]
 
 
@@ -354,7 +359,7 @@
     outgoing = dispatched(tokens, routes, experts, capacity)
     arrived = exchange(outgoing, "fs_hi")
     block = arrived.reshape(experts * capacity, col_width)
-    blocks = [block] + [shifted(block, "fs_lo", k) for k in range(1, copies)]
+    blocks = [block] + [paired(block, "fs_lo", k) for k in range(1, copies)]
     blocks = halved(jnp.stack(blocks))
     parts = [blocks] + [
         shifted(blocks, "tp_x", k) for k in range(1, lax.axis_size("tp_x"))

time: 315 us -> 314 us (level)
  starting transfers between devices: 141 us -> 136 us
  waiting for transfers between devices: 147 us -> 151 us
    ppermute x0 -> x3, waiting for transfers between devices: none -> 70.1 us  [paired(): return lax.ppermute(value, axis, [(k, k ^ flip) for k in range(count)])]
    ppermute x14 -> x11, waiting for transfers between devices: 83.8 us -> 17.7 us  [shifted(): lax.ppermute(value, axis, [(k, (k + step) % count) for k in range(count)])]
    ppermute x14 -> x11, starting transfers between devices: 51.1 us -> 37.8 us  [shifted(): lax.ppermute(value, axis, [(k, (k + step) % count) for k in range(count)])]
    ppermute x0 -> x3, starting transfers between devices: none -> 9.36 us  [paired(): return lax.ppermute(value, axis, [(k, k ^ flip) for k in range(count)])]
  transfers between devices with their start and end apart: 20 -> 20, of which waited for: 11 -> 11; matrix products, arithmetic and copies ran while one was open for 1% -> 2% of each run, Pallas kernels for 4% -> 4%
where the time goes in v11:
time: 314 us; the launch traced here: 310 us
  waiting for transfers between devices  151 us (48%)
  starting transfers between devices  136 us (43%)
  Pallas kernels  17 us (5%)
  local copies, waits for them, and re-layouts  3.66 us (1%)
    all_to_all x6, starting transfers between devices, exchange(): return lax.all_to_all(value, axis, split_axis=0, concat_axis=0, tiled=True)  88.4 us
    ppermute x3, waiting for transfers between devices, paired(): return lax.ppermute(value, axis, [(k, k ^ flip) for k in range(count)])  70.1 us
    all_to_all x6, waiting for transfers between devices, exchange(): return lax.all_to_all(value, axis, split_axis=0, concat_axis=0, tiled=True)  63.7 us
    ppermute x11, starting transfers between devices, shifted(): lax.ppermute(value, axis, [(k, (k + step) % count) for k in range(count)])  37.8 us
    ppermute x11, waiting for transfers between devices, shifted(): lax.ppermute(value, axis, [(k, (k + step) % count) for k in range(count)])  17.7 us
    ppermute x3, starting transfers between devices, paired(): return lax.ppermute(value, axis, [(k, k ^ flip) for k in range(count)])  9.36 us
  transfers between devices with their start and end apart: 20, of which 11 were waited for; matrix products, arithmetic and copies ran while one was open for 2% of the time, Pallas kernels for 4%

profile of v11, /device:TPU:33, one launch (start us, length us, event | category | flops | bytes accessed | tf_op | source)
XLA Modules:
  0.0 309.7 jit_solution(5069902251391669268)
XLA Ops:
  2.5 44.0 %all-to-all-start.2 = ((bf16[8,40,256]{2,1,0:T(8,128)(2,1)}), bf16[8,40,256]{2,1,0:T(8,128)(2,1)S(1)}, u32[]{:S(2)}, u32[]{:S(2)}) async-start(bf16[8,40,256]{2,1,0:T(8,128)(2,1)} %dispatch.1), calls=%async_computation.2 | async-start | bytes 327680 | tf_op jit(solution)/shard_map/all_to_all | solution.py:32
  46.5 5.4 %pack.1 = bf16[32,32,384]{2,1,0:T(8,128)(2,1)} custom-call(s32[1]{0:T(128)} %bitcast.turn.place, f32[1,64]{1,0:T(1,128)} %bitcast.61, f32[8,64,512]{2,1,0:T(8,128)} %gate.1, f32[8,64,512]{2,1,0:T(8,128)} %up.1, f32[8,64,512]{2,1,0:T(8,128)} %down.1), custom_call_target="tpu_custom_call" | custom-call | tf_op jit(solution)/shard_map/pack/pallas_call | solution.py:58
  51.9 22.3 %all-to-all-done.2 = bf16[8,40,256]{2,1,0:T(8,128)(2,1)S(1)} async-done(((bf16[8,40,256]{2,1,0:T(8,128)(2,1)}), bf16[8,40,256]{2,1,0:T(8,128)(2,1)S(1)}, u32[]{:S(2)}, u32[]{:S(2)}) %all-to-all-start.2) | async-done | bytes 163872 | tf_op jit(solution)/shard_map/all_to_all | solution.py:32
  74.2 10.0 %all-to-all-start = ((bf16[32,32,384]{2,1,0:T(8,128)(2,1)}), bf16[32,32,384]{2,1,0:T(8,128)(2,1)S(1)}, u32[]{:S(2)}, u32[]{:S(2)}) async-start(bf16[32,32,384]{2,1,0:T(8,128)(2,1)} %pack.1), calls=%async_computation | async-start | bytes 1572864 | tf_op jit(solution)/shard_map/all_to_all | solution.py:32
  87.0 4.0 %collective-permute-start.8 = (bf16[320,256]{1,0:T(8,128)(2,1)S(1)}, bf16[320,256]{1,0:T(8,128)(2,1)S(1)}, u32[]{:S(2)}, u32[]{:S(2)}) collective-permute-start(bf16[320,256]{1,0:T(8,128)(2,1)S(1)} %bitcast.53), channel_id=1, source_target_pairs={{0,16},{8,24},{16,0},{24,8},{1,17},{9,25},{17,1},{25,9},{2,18},{10... | collective-permute-start | bytes 491528 | tf_op jit(solution)/shard_map/ppermute | solution.py:28
  93.7 64.0 %collective-permute-done.7 = bf16[320,256]{1,0:T(8,128)(2,1)S(1)} collective-permute-done((bf16[320,256]{1,0:T(8,128)(2,1)S(1)}, bf16[320,256]{1,0:T(8,128)(2,1)S(1)}, u32[]{:S(2)}, u32[]{:S(2)}) %collective-permute-start.7) | collective-permute-done | bytes 163872 | tf_op jit(solution)/shard_map/ppermute | solution.py:28
  157.6 6.1 %collective-permute-done.9 = bf16[320,256]{1,0:T(8,128)(2,1)S(1)} collective-permute-done((bf16[320,256]{1,0:T(8,128)(2,1)S(1)}, bf16[320,256]{1,0:T(8,128)(2,1)S(1)}, u32[]{:S(2)}, u32[]{:S(2)}) %collective-permute-start.9) | collective-permute-done | bytes 163872 | tf_op jit(solution)/shard_map/ppermute | solution.py:28
  163.9 3.9 %collective-permute-start.10 = (bf16[4,160,256]{2,1,0:T(8,128)(2,1)S(1)}, bf16[4,160,256]{2,1,0:T(8,128)(2,1)S(1)}, u32[]{:S(2)}, u32[]{:S(2)}) collective-permute-start(bf16[4,160,256]{2,1,0:T(8,128)(2,1)S(1)} %get-tuple-element.11), channel_id=1, source_target_pairs={{0,1},{1,0},{2,3},{3,2},{4,5},{5,4},{6,7},{7,6},{8,9},{9,8},{10,11... | collective-permute-start | bytes 983048 | tf_op jit(solution)/shard_map/ppermute | solution.py:19
  170.6 3.6 %collective-permute-start = (bf16[32,32,256]{2,1,0:T(8,128)(2,1)S(1)}, bf16[32,32,256]{2,1,0:T(8,128)(2,1)S(1)}, u32[]{:S(2)}, u32[]{:S(2)}) collective-permute-start(bf16[32,32,256]{2,1,0:T(8,128)(2,1)S(1)} %get-tuple-element.6), channel_id=1, source_target_pairs={{0,256},{256,0},{1,257},{257,1},{2,258},{258,2},{3,259},{259,3},{4... | collective-permute-start | bytes 1572872 | tf_op jit(solution)/shard_map/ppermute | solution.py:19
  174.3 3.3 %collective-permute-start.11 = (bf16[4,2,160,256]{3,2,1,0:T(8,128)(2,1)S(1)}, bf16[4,2,160,256]{3,2,1,0:T(8,128)(2,1)S(1)}, u32[]{:S(2)}, u32[]{:S(2)}) collective-permute-start(bf16[4,2,160,256]{3,2,1,0:T(8,128)(2,1)S(1)} %pad_maximum_fusion.1.refs_4_), channel_id=1, source_target_pairs={{0,2},{2,4},{4,6},{6,0},{1,3},{3,5},{5,7},{7,1},{8,10},{10,12},{12... | collective-permute-start | bytes 1966088 | tf_op jit(solution)/shard_map/ppermute | solution.py:19
  177.6 4.7 %collective-permute-start.12 = (bf16[4,2,160,256]{3,2,1,0:T(8,128)(2,1)S(1)}, bf16[4,2,160,256]{3,2,1,0:T(8,128)(2,1)S(1)}, u32[]{:S(2)}, u32[]{:S(2)}) collective-permute-start(bf16[4,2,160,256]{3,2,1,0:T(8,128)(2,1)S(1)} %pad_maximum_fusion.1.refs_4_), channel_id=1, source_target_pairs={{0,4},{2,6},{4,0},{6,2},{1,5},{3,7},{5,1},{7,3},{8,12},{10,14},{12... | collective-permute-start | bytes 1966088 | tf_op jit(solution)/shard_map/ppermute | solution.py:19
  182.2 3.0 collective-permute-start.13
  185.2 4.7 %collective-permute-start.5 = (bf16[1,32,32,256]{3,2,1,0:T(8,128)(2,1)S(1)}, bf16[1,32,32,256]{3,2,1,0:T(8,128)(2,1)}, u32[]{:S(2)}, u32[]{:S(2)}) collective-permute-start(bf16[1,32,32,256]{3,2,1,0:T(8,128)(2,1)S(1)} %bitcast.42), channel_id=1, source_target_pairs={{0,1},{1,0},{2,3},{3,2},{4,5},{5,4},{6,7},{7,6},{8,9},{9,8},{10,11... | collective-permute-start | bytes 1572872 | tf_op jit(solution)/shard_map/ppermute | solution.py:19
  191.9 3.5 %all-to-all-start.1 = ((bf16[4,8,32,128]{3,2,1,0:T(8,128)(2,1)}), bf16[4,8,32,128]{3,2,1,0:T(8,128)(2,1)S(1)}, u32[]{:S(2)}, u32[]{:S(2)}) async-start(bf16[4,8,32,128]{3,2,1,0:T(8,128)(2,1)} %bitcast.16), calls=%async_computation.1 | async-start | bytes 524288 | tf_op jit(solution)/shard_map/all_to_all | solution.py:32
  195.5 11.7 %collective-permute-done.12.refs_6_ = bf16[4,2,160,256]{3,2,1,0:T(8,128)(2,1)S(1)} collective-permute-done((bf16[4,2,160,256]{3,2,1,0:T(8,128)(2,1)S(1)}, bf16[4,2,160,256]{3,2,1,0:T(8,128)(2,1)S(1)}, u32[]{:S(2)}, u32[]{:S(2)}) %collective-permute-start.12) | collective-permute-done | bytes 655392 | tf_op jit(solution)/shard_map/ppermute | solution.py:19
  207.2 3.0 collective-permute-done.13.refs_7_
  210.3 4.9 %hidden.1 = bf16[4,4,160,256]{3,2,1,0:T(8,128)(2,1)} custom-call(s32[4]{0:T(128)S(1)} %pad_add_fusion.place, bf16[1,32,32,256]{3,2,1,0:T(8,128)(2,1)S(1)} %bitcast.43, bf16[1,32,32,256]{3,2,1,0:T(8,128)(2,1)S(1)} %bitcast.41, bf16[1,32,32,256]{3,2,1,0:T(8,128)(2,1)} %collective-permute-done.5.refs_2_, ...), custom_call_target="tpu_custom_call" | custom-call | tf_op jit(solution)/shard_map/hidden/pallas_call | solution.py:161
  215.2 5.1 %all-to-all-start.3 = ((bf16[4,4,160,256]{3,2,1,0:T(8,128)(2,1)}), bf16[4,4,160,256]{3,2,1,0:T(8,128)(2,1)S(1)}, u32[]{:S(2)}, u32[]{:S(2)}) async-start(bf16[4,4,160,256]{3,2,1,0:T(8,128)(2,1)} %hidden.1), calls=%async_computation.3 | async-start | bytes 2621440 | tf_op jit(solution)/shard_map/all_to_all | solution.py:32
  222.2 4.1 %collective-permute-start.3 = (bf16[1,4,8,32,128]{4,3,2,1,0:T(8,128)(2,1)S(1)}, bf16[1,4,8,32,128]{4,3,2,1,0:T(8,128)(2,1)S(1)}, u32[]{:S(2)}, u32[]{:S(2)}) collective-permute-start(bf16[1,4,8,32,128]{4,3,2,1,0:T(8,128)(2,1)S(1)} %bitcast.44), channel_id=1, source_target_pairs={{0,1},{1,0},{2,3},{3,2},{4,5},{5,4},{6,7},{7,6},{8,9},{9,8},{10,11... | collective-permute-start | bytes 786440 | tf_op jit(solution)/shard_map/ppermute | solution.py:19
  228.1 4.7 %collective-permute-start.4 = (bf16[1,4,8,32,128]{4,3,2,1,0:T(8,128)(2,1)S(1)}, bf16[1,4,8,32,128]{4,3,2,1,0:T(8,128)(2,1)S(1)}, u32[]{:S(2)}, u32[]{:S(2)}) collective-permute-start(bf16[1,4,8,32,128]{4,3,2,1,0:T(8,128)(2,1)S(1)} %bitcast.46), channel_id=1, source_target_pairs={{0,1},{1,0},{2,3},{3,2},{4,5},{5,4},{6,7},{7,6},{8,9},{9,8},{10,11... | collective-permute-start | bytes 786440 | tf_op jit(solution)/shard_map/ppermute | solution.py:19
  238.7 8.8 %all-to-all-start.4 = ((bf16[8,160,256]{2,1,0:T(8,128)(2,1)}), bf16[8,160,256]{2,1,0:T(8,128)(2,1)S(1)}, u32[]{:S(2)}, u32[]{:S(2)}) async-start(bf16[8,160,256]{2,1,0:T(8,128)(2,1)} %bitcast.28), calls=%async_computation.4 | async-start | bytes 1310720 | tf_op jit(solution)/shard_map/all_to_all | solution.py:32
  250.1 14.6 %all-to-all-done.4 = bf16[8,160,256]{2,1,0:T(8,128)(2,1)S(1)} async-done(((bf16[8,160,256]{2,1,0:T(8,128)(2,1)}), bf16[8,160,256]{2,1,0:T(8,128)(2,1)S(1)}, u32[]{:S(2)}, u32[]{:S(2)}) %all-to-all-start.4) | async-done | bytes 655392 | tf_op jit(solution)/shard_map/all_to_all | solution.py:32
  265.5 17.0 %all-to-all-start.5 = ((bf16[8,40,256]{2,1,0:T(8,128)(2,1)}), bf16[8,40,256]{2,1,0:T(8,128)(2,1)S(1)}, u32[]{:S(2)}, u32[]{:S(2)}) async-start(bf16[8,40,256]{2,1,0:T(8,128)(2,1)} %bitcast.30), calls=%async_computation.5 | async-start | bytes 327680 | tf_op jit(solution)/shard_map/all_to_all | solution.py:32
  285.8 23.0 %all-to-all-done.5.returned = bf16[8,40,256]{2,1,0:T(8,128)(2,1)S(1)} async-done(((bf16[8,40,256]{2,1,0:T(8,128)(2,1)}), bf16[8,40,256]{2,1,0:T(8,128)(2,1)S(1)}, u32[]{:S(2)}, u32[]{:S(2)}) %all-to-all-start.5) | async-done | bytes 163872 | tf_op jit(solution)/shard_map/all_to_all | solution.py:32
  (44 shorter events, 29.3 us)
Async XLA Ops:
  2.5 71.7 %all-to-all-start.2 = ((bf16[8,40,256]{2,1,0:T(8,128)(2,1)}), bf16[8,40,256]{2,1,0:T(8,128)(2,1)S(1)}, u32[]{:S(2)}, u32[]{:S(2)}) async-start(bf16[8,40,256]{2,1,0:T(8,128)(2,1)} %dispatch.1), calls=%async_computation.2 | async-start | bytes 327680 | tf_op jit(solution)/shard_map/all_to_all | solution.py:32
  74.2 95.0 %all-to-all-start = ((bf16[32,32,384]{2,1,0:T(8,128)(2,1)}), bf16[32,32,384]{2,1,0:T(8,128)(2,1)S(1)}, u32[]{:S(2)}, u32[]{:S(2)}) async-start(bf16[32,32,384]{2,1,0:T(8,128)(2,1)} %pack.1), calls=%async_computation | async-start | bytes 1572864 | tf_op jit(solution)/shard_map/all_to_all | solution.py:32
  84.3 73.4 %collective-permute-start.7 = (bf16[320,256]{1,0:T(8,128)(2,1)S(1)}, bf16[320,256]{1,0:T(8,128)(2,1)S(1)}, u32[]{:S(2)}, u32[]{:S(2)}) collective-permute-start(bf16[320,256]{1,0:T(8,128)(2,1)S(1)} %bitcast.52), channel_id=1, source_target_pairs={{0,8},{8,0},{16,24},{24,16},{1,9},{9,1},{17,25},{25,17},{2,10},{10... | collective-permute-start | bytes 491528 | tf_op jit(solution)/shard_map/ppermute | solution.py:28
  87.0 70.7 %collective-permute-start.8 = (bf16[320,256]{1,0:T(8,128)(2,1)S(1)}, bf16[320,256]{1,0:T(8,128)(2,1)S(1)}, u32[]{:S(2)}, u32[]{:S(2)}) collective-permute-start(bf16[320,256]{1,0:T(8,128)(2,1)S(1)} %bitcast.53), channel_id=1, source_target_pairs={{0,16},{8,24},{16,0},{24,8},{1,17},{9,25},{17,1},{25,9},{2,18},{10... | collective-permute-start | bytes 491528 | tf_op jit(solution)/shard_map/ppermute | solution.py:28
  91.0 72.7 %collective-permute-start.9 = (bf16[320,256]{1,0:T(8,128)(2,1)S(1)}, bf16[320,256]{1,0:T(8,128)(2,1)S(1)}, u32[]{:S(2)}, u32[]{:S(2)}) collective-permute-start(bf16[320,256]{1,0:T(8,128)(2,1)S(1)} %bitcast.54), channel_id=1, source_target_pairs={{0,24},{8,16},{16,8},{24,0},{1,25},{9,17},{17,9},{25,1},{2,26},{10... | collective-permute-start | bytes 491528 | tf_op jit(solution)/shard_map/ppermute | solution.py:28
  163.9 10.3 %collective-permute-start.10 = (bf16[4,160,256]{2,1,0:T(8,128)(2,1)S(1)}, bf16[4,160,256]{2,1,0:T(8,128)(2,1)S(1)}, u32[]{:S(2)}, u32[]{:S(2)}) collective-permute-start(bf16[4,160,256]{2,1,0:T(8,128)(2,1)S(1)} %get-tuple-element.11), channel_id=1, source_target_pairs={{0,1},{1,0},{2,3},{3,2},{4,5},{5,4},{6,7},{7,6},{8,9},{9,8},{10,11... | collective-permute-start | bytes 983048 | tf_op jit(solution)/shard_map/ppermute | solution.py:19
  170.6 19.4 %collective-permute-start = (bf16[32,32,256]{2,1,0:T(8,128)(2,1)S(1)}, bf16[32,32,256]{2,1,0:T(8,128)(2,1)S(1)}, u32[]{:S(2)}, u32[]{:S(2)}) collective-permute-start(bf16[32,32,256]{2,1,0:T(8,128)(2,1)S(1)} %get-tuple-element.6), channel_id=1, source_target_pairs={{0,256},{256,0},{1,257},{257,1},{2,258},{258,2},{3,259},{259,3},{4... | collective-permute-start | bytes 1572872 | tf_op jit(solution)/shard_map/ppermute | solution.py:19
  174.3 21.2 %collective-permute-start.11 = (bf16[4,2,160,256]{3,2,1,0:T(8,128)(2,1)S(1)}, bf16[4,2,160,256]{3,2,1,0:T(8,128)(2,1)S(1)}, u32[]{:S(2)}, u32[]{:S(2)}) collective-permute-start(bf16[4,2,160,256]{3,2,1,0:T(8,128)(2,1)S(1)} %pad_maximum_fusion.1.refs_4_), channel_id=1, source_target_pairs={{0,2},{2,4},{4,6},{6,0},{1,3},{3,5},{5,7},{7,1},{8,10},{10,12},{12... | collective-permute-start | bytes 1966088 | tf_op jit(solution)/shard_map/ppermute | solution.py:19
  177.6 29.7 %collective-permute-start.12 = (bf16[4,2,160,256]{3,2,1,0:T(8,128)(2,1)S(1)}, bf16[4,2,160,256]{3,2,1,0:T(8,128)(2,1)S(1)}, u32[]{:S(2)}, u32[]{:S(2)}) collective-permute-start(bf16[4,2,160,256]{3,2,1,0:T(8,128)(2,1)S(1)} %pad_maximum_fusion.1.refs_4_), channel_id=1, source_target_pairs={{0,4},{2,6},{4,0},{6,2},{1,5},{3,7},{5,1},{7,3},{8,12},{10,14},{12... | collective-permute-start | bytes 1966088 | tf_op jit(solution)/shard_map/ppermute | solution.py:19
  182.2 28.0 %collective-permute-start.13 = (bf16[4,2,160,256]{3,2,1,0:T(8,128)(2,1)S(1)}, bf16[4,2,160,256]{3,2,1,0:T(8,128)(2,1)}, u32[]{:S(2)}, u32[]{:S(2)}) collective-permute-start(bf16[4,2,160,256]{3,2,1,0:T(8,128)(2,1)S(1)} %pad_maximum_fusion.1.refs_4_), channel_id=1, source_target_pairs={{0,6},{2,0},{4,2},{6,4},{1,7},{3,1},{5,3},{7,5},{8,14},{10,8},{12,... | collective-permute-start | bytes 1966088 | tf_op jit(solution)/shard_map/ppermute | solution.py:19
  185.2 25.1 %collective-permute-start.5 = (bf16[1,32,32,256]{3,2,1,0:T(8,128)(2,1)S(1)}, bf16[1,32,32,256]{3,2,1,0:T(8,128)(2,1)}, u32[]{:S(2)}, u32[]{:S(2)}) collective-permute-start(bf16[1,32,32,256]{3,2,1,0:T(8,128)(2,1)S(1)} %bitcast.42), channel_id=1, source_target_pairs={{0,1},{1,0},{2,3},{3,2},{4,5},{5,4},{6,7},{7,6},{8,9},{9,8},{10,11... | collective-permute-start | bytes 1572872 | tf_op jit(solution)/shard_map/ppermute | solution.py:19
  189.9 20.3 %collective-permute-start.6 = (bf16[1,32,32,256]{3,2,1,0:T(8,128)(2,1)S(1)}, bf16[1,32,32,256]{3,2,1,0:T(8,128)(2,1)}, u32[]{:S(2)}, u32[]{:S(2)}) collective-permute-start(bf16[1,32,32,256]{3,2,1,0:T(8,128)(2,1)S(1)} %bitcast.40), channel_id=1, source_target_pairs={{0,1},{1,0},{2,3},{3,2},{4,5},{5,4},{6,7},{7,6},{8,9},{9,8},{10,11... | collective-permute-start | bytes 1572872 | tf_op jit(solution)/shard_map/ppermute | solution.py:19
  191.9 23.3 %all-to-all-start.1 = ((bf16[4,8,32,128]{3,2,1,0:T(8,128)(2,1)}), bf16[4,8,32,128]{3,2,1,0:T(8,128)(2,1)S(1)}, u32[]{:S(2)}, u32[]{:S(2)}) async-start(bf16[4,8,32,128]{3,2,1,0:T(8,128)(2,1)} %bitcast.16), calls=%async_computation.1 | async-start | bytes 524288 | tf_op jit(solution)/shard_map/all_to_all | solution.py:32
  215.2 21.2 %all-to-all-start.3 = ((bf16[4,4,160,256]{3,2,1,0:T(8,128)(2,1)}), bf16[4,4,160,256]{3,2,1,0:T(8,128)(2,1)S(1)}, u32[]{:S(2)}, u32[]{:S(2)}) async-start(bf16[4,4,160,256]{3,2,1,0:T(8,128)(2,1)} %hidden.1), calls=%async_computation.3 | async-start | bytes 2621440 | tf_op jit(solution)/shard_map/all_to_all | solution.py:32
  220.3 7.9 %collective-permute-start.2 = (bf16[4,8,32,128]{3,2,1,0:T(8,128)(2,1)S(1)}, bf16[4,8,32,128]{3,2,1,0:T(8,128)(2,1)S(1)}, u32[]{:S(2)}, u32[]{:S(2)}) collective-permute-start(bf16[4,8,32,128]{3,2,1,0:T(8,128)(2,1)S(1)} %all-to-all-done.1), channel_id=1, source_target_pairs={{0,256},{256,0},{1,257},{257,1},{2,258},{258,2},{3,259},{259,3},{4... | collective-permute-start | bytes 786440 | tf_op jit(solution)/shard_map/ppermute | solution.py:19
  222.2 10.6 %collective-permute-start.3 = (bf16[1,4,8,32,128]{4,3,2,1,0:T(8,128)(2,1)S(1)}, bf16[1,4,8,32,128]{4,3,2,1,0:T(8,128)(2,1)S(1)}, u32[]{:S(2)}, u32[]{:S(2)}) collective-permute-start(bf16[1,4,8,32,128]{4,3,2,1,0:T(8,128)(2,1)S(1)} %bitcast.44), channel_id=1, source_target_pairs={{0,1},{1,0},{2,3},{3,2},{4,5},{5,4},{6,7},{7,6},{8,9},{9,8},{10,11... | collective-permute-start | bytes 786440 | tf_op jit(solution)/shard_map/ppermute | solution.py:19
  228.1 5.9 %collective-permute-start.4 = (bf16[1,4,8,32,128]{4,3,2,1,0:T(8,128)(2,1)S(1)}, bf16[1,4,8,32,128]{4,3,2,1,0:T(8,128)(2,1)S(1)}, u32[]{:S(2)}, u32[]{:S(2)}) collective-permute-start(bf16[1,4,8,32,128]{4,3,2,1,0:T(8,128)(2,1)S(1)} %bitcast.46), channel_id=1, source_target_pairs={{0,1},{1,0},{2,3},{3,2},{4,5},{5,4},{6,7},{7,6},{8,9},{9,8},{10,11... | collective-permute-start | bytes 786440 | tf_op jit(solution)/shard_map/ppermute | solution.py:19
  238.7 8.8 %copy-start = (s32[128,2]{0,1:T(2,128)S(1)}, s32[128,2]{0,1:T(2,128)}, u32[]{:S(2)}) copy-start(s32[128,2]{0,1:T(2,128)} %param.8) | copy-start | bytes 3076
  238.7 9.0 %copy-start.2 = (f32[128,2]{0,1:T(2,128)S(1)}, f32[128,2]{0,1:T(2,128)}, u32[]{:S(2)}) copy-start(f32[128,2]{0,1:T(2,128)} %param.9) | copy-start | bytes 3076
  238.7 26.0 %all-to-all-start.4 = ((bf16[8,160,256]{2,1,0:T(8,128)(2,1)}), bf16[8,160,256]{2,1,0:T(8,128)(2,1)S(1)}, u32[]{:S(2)}, u32[]{:S(2)}) async-start(bf16[8,160,256]{2,1,0:T(8,128)(2,1)} %bitcast.28), calls=%async_computation.4 | async-start | bytes 1310720 | tf_op jit(solution)/shard_map/all_to_all | solution.py:32
  247.9 35.7 %collective-permute-start.1 = (bf16[32,32,128]{2,1,0:T(8,128)(2,1)}, bf16[32,32,128]{2,1,0:T(8,128)(2,1)}, u32[]{:S(2)}, u32[]{:S(2)}) collective-permute-start(bf16[32,32,128]{2,1,0:T(8,128)(2,1)} %get-tuple-element.7), channel_id=1, source_target_pairs={{0,256},{256,0},{1,257},{257,1},{2,258},{258,2},{3,259},{259,3},{4... | collective-permute-start | bytes 786440 | tf_op jit(solution)/shard_map/ppermute | solution.py:19
  265.5 43.3 %all-to-all-start.5 = ((bf16[8,40,256]{2,1,0:T(8,128)(2,1)}), bf16[8,40,256]{2,1,0:T(8,128)(2,1)S(1)}, u32[]{:S(2)}, u32[]{:S(2)}) async-start(bf16[8,40,256]{2,1,0:T(8,128)(2,1)} %bitcast.30), calls=%async_computation.5 | async-start | bytes 327680 | tf_op jit(solution)/shard_map/all_to_all | solution.py:32
  284.6 1.1 copy-start.1

commit v12 on v11

--- a/solution.py
+++ b/solution.py
@@ -88,11 +88,12 @@
     )
     position = jnp.where(named, position.astype(jnp.int32), capacity)
     slot = lax.broadcasted_iota(jnp.int32, (capacity, count), 0)
+    select = jnp.concatenate(
+        [jnp.where(position[e : e + 1, :] == slot, 1.0, 0.0) for e in range(experts)], axis=0
+    ).astype(jnp.bfloat16)
+    packed = jnp.dot(select, tokens[...], preferred_element_type=jnp.float32)
     for e in range(experts):
-        select = jnp.where(position[e : e + 1, :] == slot, 1.0, 0.0).astype(jnp.bfloat16)
-        out[e] = jnp.dot(
-            select, tokens[...], preferred_element_type=jnp.float32
-        ).astype(jnp.bfloat16)
+        out[e] = packed[e * capacity : (e + 1) * capacity].astype(jnp.bfloat16)
 
 
 def dispatched(tokens, routes, experts, capacity):

time: 314 us -> 314 us (level)
  no operation moved by 1% of the time
where the time goes in v12:
time: 314 us; the launch traced here: 310 us
  waiting for transfers between devices  151 us (48%)
  starting transfers between devices  136 us (43%)
  Pallas kernels  17 us (5%)
  local copies, waits for them, and re-layouts  3.66 us (1%)
    all_to_all x6, starting transfers between devices, exchange(): return lax.all_to_all(value, axis, split_axis=0, concat_axis=0, tiled=True)  88.4 us
    ppermute x3, waiting for transfers between devices, paired(): return lax.ppermute(value, axis, [(k, k ^ flip) for k in range(count)])  70 us
    all_to_all x6, waiting for transfers between devices, exchange(): return lax.all_to_all(value, axis, split_axis=0, concat_axis=0, tiled=True)  63.7 us
    ppermute x11, starting transfers between devices, shifted(): lax.ppermute(value, axis, [(k, (k + step) % count) for k in range(count)])  37.9 us
    ppermute x11, waiting for transfers between devices, shifted(): lax.ppermute(value, axis, [(k, (k + step) % count) for k in range(count)])  17.6 us
    ppermute x3, starting transfers between devices, paired(): return lax.ppermute(value, axis, [(k, k ^ flip) for k in range(count)])  9.36 us
  transfers between devices with their start and end apart: 20, of which 11 were waited for; matrix products, arithmetic and copies ran while one was open for 2% of the time, Pallas kernels for 4%

profile of v12, /device:TPU:33, one launch (start us, length us, event | category | flops | bytes accessed | tf_op | source)
XLA Modules:
  0.0 309.6 jit_solution(7292825033985785602)
XLA Ops:
  2.5 44.0 %all-to-all-start.2 = ((bf16[8,40,256]{2,1,0:T(8,128)(2,1)}), bf16[8,40,256]{2,1,0:T(8,128)(2,1)S(1)}, u32[]{:S(2)}, u32[]{:S(2)}) async-start(bf16[8,40,256]{2,1,0:T(8,128)(2,1)} %dispatch.1), calls=%async_computation.2 | async-start | bytes 327680 | tf_op jit(solution)/shard_map/all_to_all | solution.py:32
  46.5 5.4 %pack.1 = bf16[32,32,384]{2,1,0:T(8,128)(2,1)} custom-call(s32[1]{0:T(128)} %bitcast.turn.place, f32[1,64]{1,0:T(1,128)} %bitcast.61, f32[8,64,512]{2,1,0:T(8,128)} %gate.1, f32[8,64,512]{2,1,0:T(8,128)} %up.1, f32[8,64,512]{2,1,0:T(8,128)} %down.1), custom_call_target="tpu_custom_call" | custom-call | tf_op jit(solution)/shard_map/pack/pallas_call | solution.py:58
  51.9 22.3 %all-to-all-done.2 = bf16[8,40,256]{2,1,0:T(8,128)(2,1)S(1)} async-done(((bf16[8,40,256]{2,1,0:T(8,128)(2,1)}), bf16[8,40,256]{2,1,0:T(8,128)(2,1)S(1)}, u32[]{:S(2)}, u32[]{:S(2)}) %all-to-all-start.2) | async-done | bytes 163872 | tf_op jit(solution)/shard_map/all_to_all | solution.py:32
  74.2 10.0 %all-to-all-start = ((bf16[32,32,384]{2,1,0:T(8,128)(2,1)}), bf16[32,32,384]{2,1,0:T(8,128)(2,1)S(1)}, u32[]{:S(2)}, u32[]{:S(2)}) async-start(bf16[32,32,384]{2,1,0:T(8,128)(2,1)} %pack.1), calls=%async_computation | async-start | bytes 1572864 | tf_op jit(solution)/shard_map/all_to_all | solution.py:32
  86.9 4.0 %collective-permute-start.8 = (bf16[320,256]{1,0:T(8,128)(2,1)S(1)}, bf16[320,256]{1,0:T(8,128)(2,1)S(1)}, u32[]{:S(2)}, u32[]{:S(2)}) collective-permute-start(bf16[320,256]{1,0:T(8,128)(2,1)S(1)} %bitcast.53), channel_id=1, source_target_pairs={{0,16},{8,24},{16,0},{24,8},{1,17},{9,25},{17,1},{25,9},{2,18},{10... | collective-permute-start | bytes 491528 | tf_op jit(solution)/shard_map/ppermute | solution.py:28
  93.6 64.0 %collective-permute-done.7 = bf16[320,256]{1,0:T(8,128)(2,1)S(1)} collective-permute-done((bf16[320,256]{1,0:T(8,128)(2,1)S(1)}, bf16[320,256]{1,0:T(8,128)(2,1)S(1)}, u32[]{:S(2)}, u32[]{:S(2)}) %collective-permute-start.7) | collective-permute-done | bytes 163872 | tf_op jit(solution)/shard_map/ppermute | solution.py:28
  157.6 6.1 %collective-permute-done.9 = bf16[320,256]{1,0:T(8,128)(2,1)S(1)} collective-permute-done((bf16[320,256]{1,0:T(8,128)(2,1)S(1)}, bf16[320,256]{1,0:T(8,128)(2,1)S(1)}, u32[]{:S(2)}, u32[]{:S(2)}) %collective-permute-start.9) | collective-permute-done | bytes 163872 | tf_op jit(solution)/shard_map/ppermute | solution.py:28
  163.8 3.9 %collective-permute-start.10 = (bf16[4,160,256]{2,1,0:T(8,128)(2,1)S(1)}, bf16[4,160,256]{2,1,0:T(8,128)(2,1)S(1)}, u32[]{:S(2)}, u32[]{:S(2)}) collective-permute-start(bf16[4,160,256]{2,1,0:T(8,128)(2,1)S(1)} %get-tuple-element.11), channel_id=1, source_target_pairs={{0,1},{1,0},{2,3},{3,2},{4,5},{5,4},{6,7},{7,6},{8,9},{9,8},{10,11... | collective-permute-start | bytes 983048 | tf_op jit(solution)/shard_map/ppermute | solution.py:19
  170.5 3.6 %collective-permute-start = (bf16[32,32,256]{2,1,0:T(8,128)(2,1)S(1)}, bf16[32,32,256]{2,1,0:T(8,128)(2,1)S(1)}, u32[]{:S(2)}, u32[]{:S(2)}) collective-permute-start(bf16[32,32,256]{2,1,0:T(8,128)(2,1)S(1)} %get-tuple-element.6), channel_id=1, source_target_pairs={{0,256},{256,0},{1,257},{257,1},{2,258},{258,2},{3,259},{259,3},{4... | collective-permute-start | bytes 1572872 | tf_op jit(solution)/shard_map/ppermute | solution.py:19
  174.2 3.3 %collective-permute-start.11 = (bf16[4,2,160,256]{3,2,1,0:T(8,128)(2,1)S(1)}, bf16[4,2,160,256]{3,2,1,0:T(8,128)(2,1)S(1)}, u32[]{:S(2)}, u32[]{:S(2)}) collective-permute-start(bf16[4,2,160,256]{3,2,1,0:T(8,128)(2,1)S(1)} %pad_maximum_fusion.1.refs_4_), channel_id=1, source_target_pairs={{0,2},{2,4},{4,6},{6,0},{1,3},{3,5},{5,7},{7,1},{8,10},{10,12},{12... | collective-permute-start | bytes 1966088 | tf_op jit(solution)/shard_map/ppermute | solution.py:19
  177.5 4.7 %collective-permute-start.12 = (bf16[4,2,160,256]{3,2,1,0:T(8,128)(2,1)S(1)}, bf16[4,2,160,256]{3,2,1,0:T(8,128)(2,1)S(1)}, u32[]{:S(2)}, u32[]{:S(2)}) collective-permute-start(bf16[4,2,160,256]{3,2,1,0:T(8,128)(2,1)S(1)} %pad_maximum_fusion.1.refs_4_), channel_id=1, source_target_pairs={{0,4},{2,6},{4,0},{6,2},{1,5},{3,7},{5,1},{7,3},{8,12},{10,14},{12... | collective-permute-start | bytes 1966088 | tf_op jit(solution)/shard_map/ppermute | solution.py:19
  182.2 3.0 collective-permute-start.13
  185.2 4.7 %collective-permute-start.5 = (bf16[1,32,32,256]{3,2,1,0:T(8,128)(2,1)S(1)}, bf16[1,32,32,256]{3,2,1,0:T(8,128)(2,1)}, u32[]{:S(2)}, u32[]{:S(2)}) collective-permute-start(bf16[1,32,32,256]{3,2,1,0:T(8,128)(2,1)S(1)} %bitcast.42), channel_id=1, source_target_pairs={{0,1},{1,0},{2,3},{3,2},{4,5},{5,4},{6,7},{7,6},{8,9},{9,8},{10,11... | collective-permute-start | bytes 1572872 | tf_op jit(solution)/shard_map/ppermute | solution.py:19
  191.9 3.5 %all-to-all-start.1 = ((bf16[4,8,32,128]{3,2,1,0:T(8,128)(2,1)}), bf16[4,8,32,128]{3,2,1,0:T(8,128)(2,1)S(1)}, u32[]{:S(2)}, u32[]{:S(2)}) async-start(bf16[4,8,32,128]{3,2,1,0:T(8,128)(2,1)} %bitcast.16), calls=%async_computation.1 | async-start | bytes 524288 | tf_op jit(solution)/shard_map/all_to_all | solution.py:32
  195.5 11.7 %collective-permute-done.12.refs_6_ = bf16[4,2,160,256]{3,2,1,0:T(8,128)(2,1)S(1)} collective-permute-done((bf16[4,2,160,256]{3,2,1,0:T(8,128)(2,1)S(1)}, bf16[4,2,160,256]{3,2,1,0:T(8,128)(2,1)S(1)}, u32[]{:S(2)}, u32[]{:S(2)}) %collective-permute-start.12) | collective-permute-done | bytes 655392 | tf_op jit(solution)/shard_map/ppermute | solution.py:19
  207.2 3.0 collective-permute-done.13.refs_7_
  210.2 4.9 %hidden.1 = bf16[4,4,160,256]{3,2,1,0:T(8,128)(2,1)} custom-call(s32[4]{0:T(128)S(1)} %pad_add_fusion.place, bf16[1,32,32,256]{3,2,1,0:T(8,128)(2,1)S(1)} %bitcast.43, bf16[1,32,32,256]{3,2,1,0:T(8,128)(2,1)S(1)} %bitcast.41, bf16[1,32,32,256]{3,2,1,0:T(8,128)(2,1)} %collective-permute-done.5.refs_2_, ...), custom_call_target="tpu_custom_call" | custom-call | tf_op jit(solution)/shard_map/hidden/pallas_call | solution.py:162
  215.2 5.1 %all-to-all-start.3 = ((bf16[4,4,160,256]{3,2,1,0:T(8,128)(2,1)}), bf16[4,4,160,256]{3,2,1,0:T(8,128)(2,1)S(1)}, u32[]{:S(2)}, u32[]{:S(2)}) async-start(bf16[4,4,160,256]{3,2,1,0:T(8,128)(2,1)} %hidden.1), calls=%async_computation.3 | async-start | bytes 2621440 | tf_op jit(solution)/shard_map/all_to_all | solution.py:32
  222.2 4.1 %collective-permute-start.3 = (bf16[1,4,8,32,128]{4,3,2,1,0:T(8,128)(2,1)S(1)}, bf16[1,4,8,32,128]{4,3,2,1,0:T(8,128)(2,1)S(1)}, u32[]{:S(2)}, u32[]{:S(2)}) collective-permute-start(bf16[1,4,8,32,128]{4,3,2,1,0:T(8,128)(2,1)S(1)} %bitcast.44), channel_id=1, source_target_pairs={{0,1},{1,0},{2,3},{3,2},{4,5},{5,4},{6,7},{7,6},{8,9},{9,8},{10,11... | collective-permute-start | bytes 786440 | tf_op jit(solution)/shard_map/ppermute | solution.py:19
  228.1 4.7 %collective-permute-start.4 = (bf16[1,4,8,32,128]{4,3,2,1,0:T(8,128)(2,1)S(1)}, bf16[1,4,8,32,128]{4,3,2,1,0:T(8,128)(2,1)S(1)}, u32[]{:S(2)}, u32[]{:S(2)}) collective-permute-start(bf16[1,4,8,32,128]{4,3,2,1,0:T(8,128)(2,1)S(1)} %bitcast.46), channel_id=1, source_target_pairs={{0,1},{1,0},{2,3},{3,2},{4,5},{5,4},{6,7},{7,6},{8,9},{9,8},{10,11... | collective-permute-start | bytes 786440 | tf_op jit(solution)/shard_map/ppermute | solution.py:19
  238.7 8.8 %all-to-all-start.4 = ((bf16[8,160,256]{2,1,0:T(8,128)(2,1)}), bf16[8,160,256]{2,1,0:T(8,128)(2,1)S(1)}, u32[]{:S(2)}, u32[]{:S(2)}) async-start(bf16[8,160,256]{2,1,0:T(8,128)(2,1)} %bitcast.28), calls=%async_computation.4 | async-start | bytes 1310720 | tf_op jit(solution)/shard_map/all_to_all | solution.py:32
  250.1 14.6 %all-to-all-done.4 = bf16[8,160,256]{2,1,0:T(8,128)(2,1)S(1)} async-done(((bf16[8,160,256]{2,1,0:T(8,128)(2,1)}), bf16[8,160,256]{2,1,0:T(8,128)(2,1)S(1)}, u32[]{:S(2)}, u32[]{:S(2)}) %all-to-all-start.4) | async-done | bytes 655392 | tf_op jit(solution)/shard_map/all_to_all | solution.py:32
  265.4 17.0 %all-to-all-start.5 = ((bf16[8,40,256]{2,1,0:T(8,128)(2,1)}), bf16[8,40,256]{2,1,0:T(8,128)(2,1)S(1)}, u32[]{:S(2)}, u32[]{:S(2)}) async-start(bf16[8,40,256]{2,1,0:T(8,128)(2,1)} %bitcast.30), calls=%async_computation.5 | async-start | bytes 327680 | tf_op jit(solution)/shard_map/all_to_all | solution.py:32
  285.7 23.0 %all-to-all-done.5.returned = bf16[8,40,256]{2,1,0:T(8,128)(2,1)S(1)} async-done(((bf16[8,40,256]{2,1,0:T(8,128)(2,1)}), bf16[8,40,256]{2,1,0:T(8,128)(2,1)S(1)}, u32[]{:S(2)}, u32[]{:S(2)}) %all-to-all-start.5) | async-done | bytes 163872 | tf_op jit(solution)/shard_map/all_to_all | solution.py:32
  (44 shorter events, 29.2 us)
Async XLA Ops:
  2.5 71.7 %all-to-all-start.2 = ((bf16[8,40,256]{2,1,0:T(8,128)(2,1)}), bf16[8,40,256]{2,1,0:T(8,128)(2,1)S(1)}, u32[]{:S(2)}, u32[]{:S(2)}) async-start(bf16[8,40,256]{2,1,0:T(8,128)(2,1)} %dispatch.1), calls=%async_computation.2 | async-start | bytes 327680 | tf_op jit(solution)/shard_map/all_to_all | solution.py:32
  74.2 95.0 %all-to-all-start = ((bf16[32,32,384]{2,1,0:T(8,128)(2,1)}), bf16[32,32,384]{2,1,0:T(8,128)(2,1)S(1)}, u32[]{:S(2)}, u32[]{:S(2)}) async-start(bf16[32,32,384]{2,1,0:T(8,128)(2,1)} %pack.1), calls=%async_computation | async-start | bytes 1572864 | tf_op jit(solution)/shard_map/all_to_all | solution.py:32
  84.2 73.4 %collective-permute-start.7 = (bf16[320,256]{1,0:T(8,128)(2,1)S(1)}, bf16[320,256]{1,0:T(8,128)(2,1)S(1)}, u32[]{:S(2)}, u32[]{:S(2)}) collective-permute-start(bf16[320,256]{1,0:T(8,128)(2,1)S(1)} %bitcast.52), channel_id=1, source_target_pairs={{0,8},{8,0},{16,24},{24,16},{1,9},{9,1},{17,25},{25,17},{2,10},{10... | collective-permute-start | bytes 491528 | tf_op jit(solution)/shard_map/ppermute | solution.py:28
  86.9 70.7 %collective-permute-start.8 = (bf16[320,256]{1,0:T(8,128)(2,1)S(1)}, bf16[320,256]{1,0:T(8,128)(2,1)S(1)}, u32[]{:S(2)}, u32[]{:S(2)}) collective-permute-start(bf16[320,256]{1,0:T(8,128)(2,1)S(1)} %bitcast.53), channel_id=1, source_target_pairs={{0,16},{8,24},{16,0},{24,8},{1,17},{9,25},{17,1},{25,9},{2,18},{10... | collective-permute-start | bytes 491528 | tf_op jit(solution)/shard_map/ppermute | solution.py:28
  91.0 72.7 %collective-permute-start.9 = (bf16[320,256]{1,0:T(8,128)(2,1)S(1)}, bf16[320,256]{1,0:T(8,128)(2,1)S(1)}, u32[]{:S(2)}, u32[]{:S(2)}) collective-permute-start(bf16[320,256]{1,0:T(8,128)(2,1)S(1)} %bitcast.54), channel_id=1, source_target_pairs={{0,24},{8,16},{16,8},{24,0},{1,25},{9,17},{17,9},{25,1},{2,26},{10... | collective-permute-start | bytes 491528 | tf_op jit(solution)/shard_map/ppermute | solution.py:28
  163.8 10.3 %collective-permute-start.10 = (bf16[4,160,256]{2,1,0:T(8,128)(2,1)S(1)}, bf16[4,160,256]{2,1,0:T(8,128)(2,1)S(1)}, u32[]{:S(2)}, u32[]{:S(2)}) collective-permute-start(bf16[4,160,256]{2,1,0:T(8,128)(2,1)S(1)} %get-tuple-element.11), channel_id=1, source_target_pairs={{0,1},{1,0},{2,3},{3,2},{4,5},{5,4},{6,7},{7,6},{8,9},{9,8},{10,11... | collective-permute-start | bytes 983048 | tf_op jit(solution)/shard_map/ppermute | solution.py:19
  170.5 19.4 %collective-permute-start = (bf16[32,32,256]{2,1,0:T(8,128)(2,1)S(1)}, bf16[32,32,256]{2,1,0:T(8,128)(2,1)S(1)}, u32[]{:S(2)}, u32[]{:S(2)}) collective-permute-start(bf16[32,32,256]{2,1,0:T(8,128)(2,1)S(1)} %get-tuple-element.6), channel_id=1, source_target_pairs={{0,256},{256,0},{1,257},{257,1},{2,258},{258,2},{3,259},{259,3},{4... | collective-permute-start | bytes 1572872 | tf_op jit(solution)/shard_map/ppermute | solution.py:19
  174.2 21.2 %collective-permute-start.11 = (bf16[4,2,160,256]{3,2,1,0:T(8,128)(2,1)S(1)}, bf16[4,2,160,256]{3,2,1,0:T(8,128)(2,1)S(1)}, u32[]{:S(2)}, u32[]{:S(2)}) collective-permute-start(bf16[4,2,160,256]{3,2,1,0:T(8,128)(2,1)S(1)} %pad_maximum_fusion.1.refs_4_), channel_id=1, source_target_pairs={{0,2},{2,4},{4,6},{6,0},{1,3},{3,5},{5,7},{7,1},{8,10},{10,12},{12... | collective-permute-start | bytes 1966088 | tf_op jit(solution)/shard_map/ppermute | solution.py:19
  177.5 29.7 %collective-permute-start.12 = (bf16[4,2,160,256]{3,2,1,0:T(8,128)(2,1)S(1)}, bf16[4,2,160,256]{3,2,1,0:T(8,128)(2,1)S(1)}, u32[]{:S(2)}, u32[]{:S(2)}) collective-permute-start(bf16[4,2,160,256]{3,2,1,0:T(8,128)(2,1)S(1)} %pad_maximum_fusion.1.refs_4_), channel_id=1, source_target_pairs={{0,4},{2,6},{4,0},{6,2},{1,5},{3,7},{5,1},{7,3},{8,12},{10,14},{12... | collective-permute-start | bytes 1966088 | tf_op jit(solution)/shard_map/ppermute | solution.py:19
  182.2 28.0 %collective-permute-start.13 = (bf16[4,2,160,256]{3,2,1,0:T(8,128)(2,1)S(1)}, bf16[4,2,160,256]{3,2,1,0:T(8,128)(2,1)}, u32[]{:S(2)}, u32[]{:S(2)}) collective-permute-start(bf16[4,2,160,256]{3,2,1,0:T(8,128)(2,1)S(1)} %pad_maximum_fusion.1.refs_4_), channel_id=1, source_target_pairs={{0,6},{2,0},{4,2},{6,4},{1,7},{3,1},{5,3},{7,5},{8,14},{10,8},{12,... | collective-permute-start | bytes 1966088 | tf_op jit(solution)/shard_map/ppermute | solution.py:19
  185.2 25.0 %collective-permute-start.5 = (bf16[1,32,32,256]{3,2,1,0:T(8,128)(2,1)S(1)}, bf16[1,32,32,256]{3,2,1,0:T(8,128)(2,1)}, u32[]{:S(2)}, u32[]{:S(2)}) collective-permute-start(bf16[1,32,32,256]{3,2,1,0:T(8,128)(2,1)S(1)} %bitcast.42), channel_id=1, source_target_pairs={{0,1},{1,0},{2,3},{3,2},{4,5},{5,4},{6,7},{7,6},{8,9},{9,8},{10,11... | collective-permute-start | bytes 1572872 | tf_op jit(solution)/shard_map/ppermute | solution.py:19
  189.9 20.3 %collective-permute-start.6 = (bf16[1,32,32,256]{3,2,1,0:T(8,128)(2,1)S(1)}, bf16[1,32,32,256]{3,2,1,0:T(8,128)(2,1)}, u32[]{:S(2)}, u32[]{:S(2)}) collective-permute-start(bf16[1,32,32,256]{3,2,1,0:T(8,128)(2,1)S(1)} %bitcast.40), channel_id=1, source_target_pairs={{0,1},{1,0},{2,3},{3,2},{4,5},{5,4},{6,7},{7,6},{8,9},{9,8},{10,11... | collective-permute-start | bytes 1572872 | tf_op jit(solution)/shard_map/ppermute | solution.py:19
  191.9 23.3 %all-to-all-start.1 = ((bf16[4,8,32,128]{3,2,1,0:T(8,128)(2,1)}), bf16[4,8,32,128]{3,2,1,0:T(8,128)(2,1)S(1)}, u32[]{:S(2)}, u32[]{:S(2)}) async-start(bf16[4,8,32,128]{3,2,1,0:T(8,128)(2,1)} %bitcast.16), calls=%async_computation.1 | async-start | bytes 524288 | tf_op jit(solution)/shard_map/all_to_all | solution.py:32
  215.2 21.2 %all-to-all-start.3 = ((bf16[4,4,160,256]{3,2,1,0:T(8,128)(2,1)}), bf16[4,4,160,256]{3,2,1,0:T(8,128)(2,1)S(1)}, u32[]{:S(2)}, u32[]{:S(2)}) async-start(bf16[4,4,160,256]{3,2,1,0:T(8,128)(2,1)} %hidden.1), calls=%async_computation.3 | async-start | bytes 2621440 | tf_op jit(solution)/shard_map/all_to_all | solution.py:32
  220.2 7.8 %collective-permute-start.2 = (bf16[4,8,32,128]{3,2,1,0:T(8,128)(2,1)S(1)}, bf16[4,8,32,128]{3,2,1,0:T(8,128)(2,1)S(1)}, u32[]{:S(2)}, u32[]{:S(2)}) collective-permute-start(bf16[4,8,32,128]{3,2,1,0:T(8,128)(2,1)S(1)} %all-to-all-done.1), channel_id=1, source_target_pairs={{0,256},{256,0},{1,257},{257,1},{2,258},{258,2},{3,259},{259,3},{4... | collective-permute-start | bytes 786440 | tf_op jit(solution)/shard_map/ppermute | solution.py:19
  222.2 10.6 %collective-permute-start.3 = (bf16[1,4,8,32,128]{4,3,2,1,0:T(8,128)(2,1)S(1)}, bf16[1,4,8,32,128]{4,3,2,1,0:T(8,128)(2,1)S(1)}, u32[]{:S(2)}, u32[]{:S(2)}) collective-permute-start(bf16[1,4,8,32,128]{4,3,2,1,0:T(8,128)(2,1)S(1)} %bitcast.44), channel_id=1, source_target_pairs={{0,1},{1,0},{2,3},{3,2},{4,5},{5,4},{6,7},{7,6},{8,9},{9,8},{10,11... | collective-permute-start | bytes 786440 | tf_op jit(solution)/shard_map/ppermute | solution.py:19
  228.1 5.9 %collective-permute-start.4 = (bf16[1,4,8,32,128]{4,3,2,1,0:T(8,128)(2,1)S(1)}, bf16[1,4,8,32,128]{4,3,2,1,0:T(8,128)(2,1)S(1)}, u32[]{:S(2)}, u32[]{:S(2)}) collective-permute-start(bf16[1,4,8,32,128]{4,3,2,1,0:T(8,128)(2,1)S(1)} %bitcast.46), channel_id=1, source_target_pairs={{0,1},{1,0},{2,3},{3,2},{4,5},{5,4},{6,7},{7,6},{8,9},{9,8},{10,11... | collective-permute-start | bytes 786440 | tf_op jit(solution)/shard_map/ppermute | solution.py:19
  238.7 8.8 %copy-start = (s32[128,2]{0,1:T(2,128)S(1)}, s32[128,2]{0,1:T(2,128)}, u32[]{:S(2)}) copy-start(s32[128,2]{0,1:T(2,128)} %param.8) | copy-start | bytes 3076
  238.7 9.0 %copy-start.2 = (f32[128,2]{0,1:T(2,128)S(1)}, f32[128,2]{0,1:T(2,128)}, u32[]{:S(2)}) copy-start(f32[128,2]{0,1:T(2,128)} %param.9) | copy-start | bytes 3076
  238.7 26.0 %all-to-all-start.4 = ((bf16[8,160,256]{2,1,0:T(8,128)(2,1)}), bf16[8,160,256]{2,1,0:T(8,128)(2,1)S(1)}, u32[]{:S(2)}, u32[]{:S(2)}) async-start(bf16[8,160,256]{2,1,0:T(8,128)(2,1)} %bitcast.28), calls=%async_computation.4 | async-start | bytes 1310720 | tf_op jit(solution)/shard_map/all_to_all | solution.py:32
  247.8 35.8 %collective-permute-start.1 = (bf16[32,32,128]{2,1,0:T(8,128)(2,1)}, bf16[32,32,128]{2,1,0:T(8,128)(2,1)}, u32[]{:S(2)}, u32[]{:S(2)}) collective-permute-start(bf16[32,32,128]{2,1,0:T(8,128)(2,1)} %get-tuple-element.7), channel_id=1, source_target_pairs={{0,256},{256,0},{1,257},{257,1},{2,258},{258,2},{3,259},{259,3},{4... | collective-permute-start | bytes 786440 | tf_op jit(solution)/shard_map/ppermute | solution.py:19
  265.4 43.3 %all-to-all-start.5 = ((bf16[8,40,256]{2,1,0:T(8,128)(2,1)}), bf16[8,40,256]{2,1,0:T(8,128)(2,1)S(1)}, u32[]{:S(2)}, u32[]{:S(2)}) async-start(bf16[8,40,256]{2,1,0:T(8,128)(2,1)} %bitcast.30), calls=%async_computation.5 | async-start | bytes 327680 | tf_op jit(solution)/shard_map/all_to_all | solution.py:32
  284.6 1.1 copy-start.1
